TPU v7x, 128 devices: a whole 4x4x4 slice. The times are simulated.
128 devices in a mesh: sp: 64 (over z, y, x), tp: 2 (over core).
Axes of the slice: x: 4, y: 4, z: 4, core: 2. Of those that a mesh axis runs over, the one named last changes fastest.
Arguments:
- residual: bfloat16 [16384, 2048], P(('sp', 'tp')), may hold values from -6 to 6
- queries: bfloat16 [16384, 512], P('sp', 'tp'), may hold values from -6 to 6
- key_rows: bfloat16 [16384, 512], P('sp', 'tp'), may hold values from -6 to 6
- value_rows: bfloat16 [16384, 1024], P('sp', 'tp'), may hold values from -6 to 6
- out_gate: bfloat16 [16384, 1024], P('sp', 'tp'), may hold values from -6 to 6
- gate_logits: bfloat16 [16384, 512], P('sp', 'tp')
- head_gain: float32 [128], replicated, may hold values from 0.1 to 1.9
- out_weight: bfloat16 [1024, 2048], replicated, may hold values from -0.1875 to 0.1875
- norm_gain: float32 [2048], replicated, may hold values from 0.1 to 1.9
- routes: int32 [16384, 2], P(('sp', 'tp')), may hold values from 0 to 127, as said below
- group_score: float32 [16384], P(('sp', 'tp')), may hold values from 0.25 to 1
- expert_score: float32 [16384, 2], P(('sp', 'tp')), may hold values from 0.1 to 1
- gate_weight: bfloat16 [128, 2048, 512], P(('sp', 'tp')), may hold values from -0.125 to 0.125
- up_weight: bfloat16 [128, 2048, 512], P(('sp', 'tp')), may hold values from -0.125 to 0.125
- down_weight: bfloat16 [128, 512, 2048], P(('sp', 'tp')), may hold values from -0.25 to 0.25
Outputs:
- layer_out: bfloat16 [16384, 2048], P(('sp', 'tp'))
Inputs may be any that keep to these rules, and one draw needn't show every extreme that they name: `routes`: the two experts of a token differ and lie in one group of 8 consecutive expert numbers. In each aligned block of 128 tokens (the tokens of one device) no expert is named more than 3 times, and one expert, the same for all blocks of a draw, is named exactly 3 times in every block.
All inputs are finite; a program needn't handle non-finite values.
Results may differ from a plain program's by a relative error of at most 0.0056.
Values may be sent and summed in bfloat16 or wider, within the bound.
No kernel may reach another device: no remote copies, remote signals or barrier semaphores. Data moves between devices by JAX's collectives and lax.ppermute only.
A program may use at most 64 MiB of HBM per device.

v0:
```python
import jax
import jax.numpy as jnp
from jax import lax
from jax.sharding import Mesh
from jax.sharding import PartitionSpec as P

KEY_DIM = 64
VALUE_DIM = 128
BLOCK = 64
SP = ("sp_0", "sp_1", "sp_2")
SP_TP = ("sp_0", "sp_1", "sp_2", "tp")


def neutral_like(value, identity):
    return jax.tree.map(
        lambda part, zero: jnp.zeros_like(part) + jnp.asarray(zero, part.dtype), value, identity
    )


def entering_2(value, axes, combine, identity):
    before = start = neutral_like(value, identity)
    so_far = value
    for axis in reversed(axes):
        peers, place = (lax.axis_size(axis), lax.axis_index(axis))
        pieces = jax.tree.map(lambda part: lax.all_gather(part, axis), so_far)
        inside, so_far = (start, start)
        for k in range(peers):
            passed = k < place
            so_far = combine(so_far, jax.tree.map(lambda part: part[k], pieces))
            inside = jax.tree.map(lambda new, old: jnp.where(passed, new, old), so_far, inside)
        before = combine(inside, before)
    return before


def block_parts(queries, key_rows, value_rows, gate_logits):
    length = queries.shape[0]
    head_count = queries.shape[1] // KEY_DIM
    blocks = length // BLOCK

    def arrange(source, inner_size):
        return (
            source.astype(jnp.float32)
            .reshape(blocks, BLOCK, head_count, inner_size)
            .transpose(0, 2, 1, 3)
        )

    decay_log = jax.nn.log_sigmoid(gate_logits.astype(jnp.float32)) / 16.0
    running = jnp.cumsum(arrange(decay_log, KEY_DIM), axis=2)
    closing = running[:, :, -1:, :]
    query_scaled = arrange(queries, KEY_DIM) * KEY_DIM ** (-0.5) * jnp.exp(running)
    key_float = arrange(key_rows, KEY_DIM)
    key_inverse = key_float * jnp.exp(-running)
    key_closing = key_float * jnp.exp(closing - running)
    value_float = arrange(value_rows, VALUE_DIM)
    causal = jnp.tril(jnp.ones((BLOCK, BLOCK), dtype=bool))
    scores = jnp.where(
        causal,
        jnp.einsum("nhcd,nhsd->nhcs", query_scaled, key_inverse, precision=lax.Precision.HIGHEST),
        0.0,
    )
    within = jnp.einsum("nhcs,nhsv->nhcv", scores, value_float, precision=lax.Precision.HIGHEST)
    increments = jnp.einsum(
        "nhcd,nhcv->nhdv", key_closing, value_float, precision=lax.Precision.HIGHEST
    )
    return (query_scaled, within, increments, closing[:, :, 0, :])


def advance(carried, inputs):
    increment, block_log = inputs
    return (jnp.exp(block_log)[..., None] * carried + increment, carried)


def finish(attended, head_gain, out_gate):
    blocks = attended.shape[0]
    head_count = attended.shape[1]
    length = blocks * BLOCK
    ordered = attended.transpose(0, 2, 1, 3).reshape(length, head_count, VALUE_DIM)
    normed = (
        ordered * lax.rsqrt(jnp.mean(ordered * ordered, axis=-1, keepdims=True) + 1e-06) * head_gain
    )
    gating = jax.nn.silu(out_gate.astype(jnp.float32)).reshape(length, head_count, VALUE_DIM)
    return (normed * gating).reshape(length, head_count * VALUE_DIM).astype(jnp.bfloat16)


def route_slots(block_routes, experts_total, capacity):
    row_count = block_routes.shape[0]
    flattened = block_routes.reshape(-1)
    onehot = (flattened[:, None] == jnp.arange(experts_total, dtype=jnp.int32)[None, :]).astype(
        jnp.int32
    )
    ranking = jnp.sum((jnp.cumsum(onehot, axis=0) - onehot) * onehot, axis=1)
    slot_index = flattened * capacity + ranking
    route_ids = jnp.arange(2 * row_count, dtype=jnp.int32) // 2
    owners = (
        jnp.full((experts_total * capacity,), row_count, jnp.int32).at[slot_index].set(route_ids)
    )
    return (slot_index, owners)


def expert_apply(rows_in, gate_matrix, up_matrix, down_matrix):
    gated = jnp.dot(rows_in, gate_matrix, preferred_element_type=jnp.float32)
    lifted = jnp.dot(rows_in, up_matrix, preferred_element_type=jnp.float32)
    inner_rows = (jax.nn.silu(gated) * lifted).astype(jnp.bfloat16)
    return jnp.dot(inner_rows, down_matrix, preferred_element_type=jnp.float32).astype(jnp.bfloat16)


def merge_states(earlier, later):
    return (earlier[0] * later[0], later[0][..., None] * earlier[1] + later[1])


def local(
    residual,
    queries,
    key_rows,
    value_rows,
    out_gate,
    gate_logits,
    head_gain,
    out_weight,
    norm_gain,
    routes,
    group_score,
    expert_score,
    gate_weight,
    up_weight,
    down_weight,
):
    query_scaled, within, increments, block_logs = block_parts(
        queries, key_rows, value_rows, gate_logits
    )
    zero_state = jnp.zeros(increments.shape[1:], jnp.float32)
    local_end, local_prefix = lax.scan(advance, zero_state, (increments, block_logs))
    device_decay = jnp.exp(jnp.sum(block_logs, axis=0))
    identity = (jnp.ones_like(device_decay), jnp.zeros_like(local_end))
    entering = entering_2((device_decay, local_end), SP, merge_states, identity)[1]
    leading = jnp.exp(jnp.cumsum(block_logs, axis=0) - block_logs)
    states = leading[..., None] * entering[None] + local_prefix
    attended = within + jnp.einsum(
        "nhcd,nhdv->nhcv", query_scaled, states, precision=lax.Precision.HIGHEST
    )
    mixer_out = finish(attended, head_gain, out_gate)
    row_count = residual.shape[0]
    model_width = residual.shape[1]
    pair_count = lax.axis_size("tp")
    chip_count = lax.axis_size(SP)
    regrouped = lax.all_to_all(mixer_out, "tp", split_axis=0, concat_axis=1, tiled=True)
    projected = jnp.dot(regrouped, out_weight, preferred_element_type=jnp.float32)
    merged = (residual.astype(jnp.float32) + projected).astype(jnp.bfloat16)
    widened = lax.optimization_barrier(merged).astype(jnp.float32)
    normed = (
        widened * lax.rsqrt(jnp.mean(widened * widened, axis=-1, keepdims=True) + 1e-06) * norm_gain
    ).astype(jnp.bfloat16)
    experts_total = chip_count * pair_count
    capacity = 3 * row_count // experts_total
    slot_index, owners = route_slots(routes, experts_total, capacity)
    padded = jnp.concatenate([normed, jnp.zeros((1, model_width), jnp.bfloat16)], axis=0)
    outgoing = padded[owners].reshape(experts_total, capacity, model_width)
    gate_matrix = gate_weight[0]
    up_matrix = up_weight[0]
    down_matrix = down_weight[0]
    arrived = lax.all_to_all(outgoing, SP_TP, split_axis=0, concat_axis=0, tiled=True)
    shape_in = arrived.shape
    served = expert_apply(arrived.reshape(-1, shape_in[-1]), gate_matrix, up_matrix, down_matrix)
    returned = lax.all_to_all(
        served.reshape(shape_in), SP_TP, split_axis=0, concat_axis=0, tiled=True
    )
    picked = returned.reshape(experts_total * capacity, model_width)[slot_index].reshape(
        row_count, 2, model_width
    )
    weights = group_score[:, None] * expert_score / jnp.sum(expert_score, axis=1, keepdims=True)
    combined = weights[:, 0:1] * picked[:, 0].astype(jnp.float32) + weights[:, 1:2] * picked[
        :, 1
    ].astype(jnp.float32)
    return (widened + combined).astype(jnp.bfloat16)


def solution(mesh):
    torus = Mesh(mesh.devices.reshape(4, 4, 4, mesh.shape["tp"]), ("sp_0", "sp_1", "sp_2", "tp"))
    in_specs = (
        P(SP_TP, None),
        P(SP, "tp"),
        P(SP, "tp"),
        P(SP, "tp"),
        P(SP, "tp"),
        P(SP, "tp"),
        P(),
        P(),
        P(),
        P(SP_TP, None),
        P(SP_TP),
        P(SP_TP, None),
        P(SP_TP, None, None),
        P(SP_TP, None, None),
        P(SP_TP, None, None),
    )
    out_specs = P(SP_TP, None)
    return jax.shard_map(local, mesh=torus, in_specs=in_specs, out_specs=out_specs, check_vma=False)
```

profile of v0, /device:TPU:1, one launch (start us, length us, event | category | flops | bytes accessed | tf_op | source)
XLA Modules:
  0.0 230.2 jit_solution(4951498174471461953)
XLA Ops:
  0.0 1.3 fusion.43
  2.1 9.3 %all-gather.2 = f32[4,4,64]{2,1,0:T(4,128)S(1)} all-gather(f32[1,4,64]{2,1,0:T(4,128)S(1)} %exponential_bitcast_fusion.1), channel_id=2, replica_groups=mesh['sp_0'=4,'sp_1'=4,'sp_2'=4,'tp'=2] {'sp_2'}, dimensions={0}, use_global_device_ids=true | all-gather | bytes 5120 | tf_op jit(solution)/shard_map/all_gather | solution.py:25
  12.6 9.0 %all_gather.27 = f32[4,4,64]{2,1,0:T(4,128)} all-gather(f32[1,4,64]{2,1,0:T(4,128)S(1)} %multiply_bitcast_fusion), channel_id=1, replica_groups=mesh['sp_0'=4,'sp_1'=4,'sp_2'=4,'tp'=2] {'sp_1'}, dimensions={0}, use_global_device_ids=true | all-gather | bytes 5120 | tf_op jit(solution)/shard_map/all_gather | solution.py:25
  23.5 1.4 fusion.31
  24.9 6.9 %while.13 = (s32[]{:T(128)}, f32[4,64,128]{2,1,0:T(8,128)S(1)}, f32[4,4,64,128]{3,2,1,0:T(8,128)}, f32[4,4,64]{2,1,0:T(4,128)S(1)}, f32[4,4,64,128]{3,2,1,0:T(8,128)}, /*index=5*/s32[]{:T(128)}, s32[]{:T(128)}) while((s32[]{:T(128)}, f32[4,64,128]{2,1,0:T(8,128)S(1)}, f32[4,4,64,128]{3,2,1,0:T(8,128)}, f32[4,4,64]{2,1,0:T(4,128)S(1)}, ...), condition=%wide.region_4.5_spmd.clone, body=%wide.region_3.4_spmd.clone.sunk | while | flops 131075 | bytes 659040 | solution.py:132
  31.8 10.0 %all-gather.1 = f32[16,64,128]{2,1,0:T(8,128)S(1)} all-gather(f32[4,64,128]{2,1,0:T(8,128)S(1)} %get-tuple-element.33), channel_id=3, replica_groups=mesh['sp_0'=4,'sp_1'=4,'sp_2'=4,'tp'=2] {'sp_2'}, dimensions={0}, use_global_device_ids=true | all-gather | bytes 655360 | tf_op jit(solution)/shard_map/all_gather | solution.py:25
  42.6 1.3 fusion.69
  44.8 10.2 %all_gather.31 = f32[4,4,64,128]{3,2,1,0:T(8,128)S(1)} all-gather(f32[1,4,64,128]{3,2,1,0:T(8,128)S(1)} %fusion.57), channel_id=1, replica_groups=mesh['sp_0'=4,'sp_1'=4,'sp_2'=4,'tp'=2] {'sp_1'}, dimensions={0}, use_global_device_ids=true | all-gather | bytes 655360 | tf_op jit(solution)/shard_map/all_gather | solution.py:25
  56.0 12.0 %all_gather.32 = f32[4,4,64,128]{3,2,1,0:T(8,128)} all-gather(f32[1,4,64,128]{3,2,1,0:T(8,128)S(1)} %slice_add_fusion.4), channel_id=1, replica_groups=mesh['sp_0'=4,'sp_1'=4,'sp_2'=4,'tp'=2] {'sp_0'}, dimensions={0}, use_global_device_ids=true | all-gather | bytes 655360 | tf_op jit(solution)/shard_map/all_gather | solution.py:25
  68.0 8.5 %all_gather.28 = f32[4,4,64]{2,1,0:T(4,128)S(1)} all-gather(f32[1,4,64]{2,1,0:T(4,128)S(1)} %get-tuple-element.73), channel_id=1, replica_groups=mesh['sp_0'=4,'sp_1'=4,'sp_2'=4,'tp'=2] {'sp_0'}, dimensions={0}, use_global_device_ids=true | all-gather | bytes 5120 | tf_op jit(solution)/shard_map/all_gather | solution.py:25
  77.9 2.0 mul.372
  80.0 2.2 convolution_select_fusion
  83.4 1.5 multiply_reduce_fusion
  85.1 1.4 copy.52
  86.9 1.1 fusion.38
  88.9 19.7 %all-to-all-start = ((bf16[2,128,512]{1,2,0:T(8,128)(2,1)}), bf16[2,128,512]{1,2,0:T(8,128)(2,1)S(1)}, u32[]{:S(2)}, u32[]{:S(2)}) async-start(bf16[2,128,512]{1,2,0:T(8,128)(2,1)} %copy.55), calls=%async_computation | async-start | bytes 524288 | tf_op jit(solution)/shard_map/all_to_all | solution.py:146
  109.9 2.9 %fusion = bf16[128,2048]{1,0:T(8,128)(2,1)S(1)} fusion(bf16[128,1024]{0,1:T(8,128)(2,1)S(1)} %bitcast.224, bf16[1024,2048]{1,0:T(8,128)(2,1)} %param.24, bf16[128,2048]{1,0:T(8,128)(2,1)S(1)} %copy-done.10), kind=kOutput, calls=%fused_computation.8 | convolution fusion | flops 537657344 | bytes 5505024 | tf_op jit(solution)/shard_map/dot_general | solution.py:147
  113.9 1.4 scatter_custom_fusion
  115.6 3.1 %gather_fusion = bf16[384,2048]{1,0:T(8,128)(2,1)} fusion(bf16[129,2048]{1,0:T(8,128)(2,1)S(1)} %concatenate.3, s32[1024]{0:T(1024)S(1)} %pad_clamp_fusion.1), kind=kCustom, calls=%fused_computation | custom fusion | bytes 3147264 | tf_op jit(solution)/shard_map/gather | solution.py:157
  118.7 5.1 %reshape.231 = bf16[128,3,2048]{2,1,0:T(4,128)(2,1)} reshape(bf16[384,2048]{1,0:T(8,128)(2,1)} %gather_fusion) | data formatting | bytes 3145728 | tf_op jit(solution)/shard_map/reshape | solution.py:157
  123.8 36.9 %all_to_all.29 = bf16[128,3,2048]{2,1,0:T(4,128)(2,1)} all-to-all(bf16[128,3,2048]{2,1,0:T(4,128)(2,1)} %reshape.231), channel_id=1, replica_groups=mesh['sp_0'=4,'sp_1'=4,'sp_2'=4,'tp'=2] {'sp_0','sp_1','sp_2','tp'}, dimensions={0} | all-to-all | bytes 3145728 | tf_op jit(solution)/shard_map/all_to_all | solution.py:161
  160.8 5.0 %reshape.232 = bf16[384,2048]{1,0:T(8,128)(2,1)} reshape(bf16[128,3,2048]{2,1,0:T(4,128)(2,1)} %all_to_all.29) | data formatting | bytes 3145728 | tf_op jit(solution)/shard_map/reshape | solution.py:163
  165.8 3.0 %fusion.4 = f32[384,512]{1,0:T(8,128)S(1)} fusion(bf16[384,2048]{1,0:T(8,128)(2,1)} %reshape.232, bf16[1,2048,512]{2,1,0:T(8,128)(2,1)} %param.29), kind=kOutput, calls=%fused_computation.12 | convolution fusion | flops 805306368 | bytes 4456448 | tf_op jit(solution)/shard_map/dot_general | solution.py:101
  168.9 5.2 %convolution_convert_fusion = bf16[384,2048]{1,0:T(8,128)(2,1)} fusion(bf16[1,512,2048]{2,1,0:T(8,128)(2,1)S(1)} %copy-done, bf16[384,2048]{1,0:T(8,128)(2,1)} %reshape.232, bf16[1,2048,512]{2,1,0:T(8,128)(2,1)} %param.30, f32[384,512]{1,0:T(8,128)S(1)} %fusion.4), kind=kOutput, calls=%fused_computation.6 | convolution fusion | flops 1612578816 | bytes 8126464 | tf_op jit(solution)/shard_map/dot_general | solution.py:104
  174.1 5.1 %reshape.233 = bf16[128,3,2048]{2,1,0:T(4,128)(2,1)} reshape(bf16[384,2048]{1,0:T(8,128)(2,1)} %convolution_convert_fusion) | data formatting | bytes 3145728 | tf_op jit(solution)/shard_map/reshape | solution.py:165
  179.2 5.6 %all-to-all-start.2 = ((bf16[128,3,2048]{2,1,0:T(4,128)(2,1)}), bf16[128,3,2048]{2,1,0:T(4,128)(2,1)}, u32[]{:S(2)}, u32[]{:S(2)}) async-start(bf16[128,3,2048]{2,1,0:T(4,128)(2,1)} %reshape.233), calls=%async_computation.2 | async-start | bytes 4194304 | tf_op jit(solution)/shard_map/all_to_all | solution.py:164
  184.9 30.2 %all-to-all-done.2 = bf16[128,3,2048]{2,1,0:T(4,128)(2,1)} async-done(((bf16[128,3,2048]{2,1,0:T(4,128)(2,1)}), bf16[128,3,2048]{2,1,0:T(4,128)(2,1)}, u32[]{:S(2)}, u32[]{:S(2)}) %all-to-all-start.2) | async-done | bytes 1572896 | tf_op jit(solution)/shard_map/all_to_all | solution.py:164
  215.1 5.0 %reshape.234 = bf16[384,2048]{1,0:T(8,128)(2,1)} reshape(bf16[128,3,2048]{2,1,0:T(4,128)(2,1)} %all-to-all-done.2) | data formatting | bytes 3145728 | tf_op jit(solution)/shard_map/reshape | solution.py:167
  220.1 5.0 %gather_fusion.1 = bf16[256,2048]{1,0:T(8,128)(2,1)} fusion(bf16[384,2048]{1,0:T(8,128)(2,1)} %reshape.234, s32[1024]{0:T(1024)S(1)} %pad_clamp_fusion), kind=kCustom, calls=%fused_computation.1 | custom fusion | bytes 2098176 | tf_op jit(solution)/shard_map/gather | solution.py:167
  225.1 1.7 reshape.235
  226.8 1.5 fusion.75
  228.3 1.9 fusion.17
  (139 shorter events, 19.5 us)
Async XLA Ops:
  0.0 168.9 %copy-start = (bf16[1,512,2048]{2,1,0:T(8,128)(2,1)S(1)}, bf16[1,512,2048]{2,1,0:T(8,128)(2,1)}, u32[]{:S(2)}) copy-start(bf16[1,512,2048]{2,1,0:T(8,128)(2,1)} %param.31) | copy-start | bytes 6291460
  0.0 21.6 %copy-start.11 = (bf16[256,256]{1,0:T(8,128)(2,1)S(1)}, bf16[256,256]{1,0:T(8,128)(2,1)}, u32[]{:S(2)}) copy-start(bf16[256,256]{1,0:T(8,128)(2,1)} %param.19) | copy-start | bytes 393220
  31.8 45.4 %copy-start.12 = (bf16[256,256]{1,0:T(8,128)(2,1)S(1)}, bf16[256,256]{1,0:T(8,128)(2,1)}, u32[]{:S(2)}) copy-start(bf16[256,256]{1,0:T(8,128)(2,1)} %param.18) | copy-start | bytes 393220
  41.8 38.1 %copy-start.14 = (pred[64,64]{1,0:T(8,128)(4,1)S(1)}, pred[64,64]{1,0:T(8,128)(4,1)}, u32[]{:S(2)}) copy-start(pred[64,64]{1,0:T(8,128)(4,1)} %iota_compare_fusion.1) | copy-start | bytes 12292
  42.5 34.6 %copy-start.22 = (f32[4,64]{1,0:T(4,128)}, f32[4,64]{1,0:T(4,128)S(1)}, u32[]{:S(2)}) copy-start(f32[4,64]{1,0:T(4,128)S(1)} %get-tuple-element.74) | copy-start | bytes 3076
  42.5 34.6 %copy-start.24 = (f32[4,64]{1,0:T(4,128)}, f32[4,64]{1,0:T(4,128)S(1)}, u32[]{:S(2)}) copy-start(f32[4,64]{1,0:T(4,128)S(1)} %get-tuple-element.75) | copy-start | bytes 3076
  42.6 34.6 %copy-start.26 = (f32[4,64]{1,0:T(4,128)}, f32[4,64]{1,0:T(4,128)S(1)}, u32[]{:S(2)}) copy-start(f32[4,64]{1,0:T(4,128)S(1)} %get-tuple-element.76) | copy-start | bytes 3076
  43.9 33.3 %copy-start.15 = (f32[4,64]{1,0:T(4,128)}, f32[4,64]{1,0:T(4,128)S(1)}, u32[]{:S(2)}) copy-start(f32[4,64]{1,0:T(4,128)S(1)} %get-tuple-element.77) | copy-start | bytes 3076
  43.9 33.3 %copy-start.17 = (f32[4,64]{1,0:T(4,128)}, f32[4,64]{1,0:T(4,128)S(1)}, u32[]{:S(2)}) copy-start(f32[4,64]{1,0:T(4,128)S(1)} %get-tuple-element.78) | copy-start | bytes 3076
  79.9 2.8 %copy-start.5 = (f32[16,64,128]{2,1,0:T(8,128)S(1)}, f32[16,64,128]{2,1,0:T(8,128)}, u32[]{:S(2)}) copy-start(f32[16,64,128]{2,1,0:T(8,128)} %copy-done.4) | copy-start | bytes 1572868
  79.9 2.8 %copy-start.7 = (f32[4,4,64,128]{3,2,1,0:T(8,128)S(1)}, f32[4,4,64,128]{3,2,1,0:T(8,128)}, u32[]{:S(2)}) copy-start(f32[4,4,64,128]{3,2,1,0:T(8,128)} %copy-done.6) | copy-start | bytes 1572868
  79.9 2.8 %copy-start.8 = (f32[4,4,64,128]{3,2,1,0:T(8,128)S(1)}, f32[4,4,64,128]{3,2,1,0:T(8,128)}, u32[]{:S(2)}) copy-start(f32[4,4,64,128]{3,2,1,0:T(8,128)} %all_gather.32) | copy-start | bytes 1572868
  79.9 2.8 %copy-start.16 = (f32[4,64]{1,0:T(4,128)S(1)}, f32[4,64]{1,0:T(4,128)}, u32[]{:S(2)}) copy-start(f32[4,64]{1,0:T(4,128)} %copy-done.15) | copy-start | bytes 3076
  79.9 2.8 %copy-start.18 = (f32[4,64]{1,0:T(4,128)S(1)}, f32[4,64]{1,0:T(4,128)}, u32[]{:S(2)}) copy-start(f32[4,64]{1,0:T(4,128)} %copy-done.17) | copy-start | bytes 3076
  79.9 2.8 %copy-start.19 = (f32[4,64]{1,0:T(4,128)S(1)}, f32[4,64]{1,0:T(4,128)}, u32[]{:S(2)}) copy-start(f32[4,64]{1,0:T(4,128)} %get-tuple-element.79) | copy-start | bytes 3076
  79.9 2.8 %copy-start.20 = (f32[4,64]{1,0:T(4,128)S(1)}, f32[4,64]{1,0:T(4,128)}, u32[]{:S(2)}) copy-start(f32[4,64]{1,0:T(4,128)} %get-tuple-element.80) | copy-start | bytes 3076
  79.9 2.8 %copy-start.21 = (f32[4,64]{1,0:T(4,128)S(1)}, f32[4,64]{1,0:T(4,128)}, u32[]{:S(2)}) copy-start(f32[4,64]{1,0:T(4,128)} %get-tuple-element.81) | copy-start | bytes 3076
  79.9 2.8 %copy-start.23 = (f32[4,64]{1,0:T(4,128)S(1)}, f32[4,64]{1,0:T(4,128)}, u32[]{:S(2)}) copy-start(f32[4,64]{1,0:T(4,128)} %copy-done.22) | copy-start | bytes 3076
  79.9 2.8 %copy-start.25 = (f32[4,64]{1,0:T(4,128)S(1)}, f32[4,64]{1,0:T(4,128)}, u32[]{:S(2)}) copy-start(f32[4,64]{1,0:T(4,128)} %copy-done.24) | copy-start | bytes 3076
  80.0 2.8 %copy-start.27 = (f32[4,64]{1,0:T(4,128)S(1)}, f32[4,64]{1,0:T(4,128)}, u32[]{:S(2)}) copy-start(f32[4,64]{1,0:T(4,128)} %copy-done.26) | copy-start | bytes 3076
  80.0 2.8 %copy-start.29 = (f32[4,64]{1,0:T(4,128)S(1)}, f32[4,64]{1,0:T(4,128)}, u32[]{:S(2)}) copy-start(f32[4,64]{1,0:T(4,128)} %get-tuple-element.63) | copy-start | bytes 3076
  80.0 2.8 %copy-start.30 = (f32[4,64]{1,0:T(4,128)S(1)}, f32[4,64]{1,0:T(4,128)}, u32[]{:S(2)}) copy-start(f32[4,64]{1,0:T(4,128)} %get-tuple-element.64) | copy-start | bytes 3076
  80.0 2.8 %copy-start.31 = (f32[4,64]{1,0:T(4,128)S(1)}, f32[4,64]{1,0:T(4,128)}, u32[]{:S(2)}) copy-start(f32[4,64]{1,0:T(4,128)} %get-tuple-element.71) | copy-start | bytes 3076
  80.0 2.8 %copy-start.32 = (f32[4,64]{1,0:T(4,128)S(1)}, f32[4,64]{1,0:T(4,128)}, u32[]{:S(2)}) copy-start(f32[4,64]{1,0:T(4,128)} %get-tuple-element.72) | copy-start | bytes 3076
  83.4 3.2 %copy-start.35 = (f32[128]{0:T(128)S(1)}, f32[128]{0:T(128)}, u32[]{:S(2)}) copy-start(f32[128]{0:T(128)} %param.23) | copy-start | bytes 1540
  85.1 23.6 %copy-start.33 = (s32[128,2]{0,1:T(2,128)S(1)}, s32[128,2]{0,1:T(2,128)}, u32[]{:S(2)}) copy-start(s32[128,2]{0,1:T(2,128)} %param.26) | copy-start | bytes 3076
  85.1 24.7 %copy-start.10 = (bf16[128,2048]{1,0:T(8,128)(2,1)S(1)}, bf16[128,2048]{1,0:T(8,128)(2,1)}, u32[]{:S(2)}) copy-start(bf16[128,2048]{1,0:T(8,128)(2,1)} %param.17) | copy-start | bytes 1572868
  88.9 20.9 %all-to-all-start = ((bf16[2,128,512]{1,2,0:T(8,128)(2,1)}), bf16[2,128,512]{1,2,0:T(8,128)(2,1)S(1)}, u32[]{:S(2)}, u32[]{:S(2)}) async-start(bf16[2,128,512]{1,2,0:T(8,128)(2,1)} %copy.55), calls=%async_computation | async-start | bytes 524288 | tf_op jit(solution)/shard_map/all_to_all | solution.py:146
  109.9 5.5 %copy-start.28 = (f32[2048]{0:T(1024)S(1)}, f32[2048]{0:T(1024)}, u32[]{:S(2)}) copy-start(f32[2048]{0:T(1024)} %param.25) | copy-start | bytes 24580
  179.2 5.6 %copy-start.34 = (f32[128,2]{0,1:T(2,128)S(1)}, f32[128,2]{0,1:T(2,128)}, u32[]{:S(2)}) copy-start(f32[128,2]{0,1:T(2,128)} %param.28) | copy-start | bytes 3076
  179.2 5.7 %copy-start.36 = (f32[128]{0:T(128)S(1)}, f32[128]{0:T(128)}, u32[]{:S(2)}) copy-start(f32[128]{0:T(128)} %param.27) | copy-start | bytes 1540
  179.2 35.9 %all-to-all-start.2 = ((bf16[128,3,2048]{2,1,0:T(4,128)(2,1)}), bf16[128,3,2048]{2,1,0:T(4,128)(2,1)}, u32[]{:S(2)}, u32[]{:S(2)}) async-start(bf16[128,3,2048]{2,1,0:T(4,128)(2,1)} %reshape.233), calls=%async_computation.2 | async-start | bytes 4194304 | tf_op jit(solution)/shard_map/all_to_all | solution.py:164
  (7 other events, 10.5 us)
where the time goes:
time: 231 us; the launch traced here: 230 us
  blocking collectives  96 us (42%)
  local copies, waits for them, and re-layouts  41.8 us (18%)
  waiting for transfers between devices  30.9 us (13%)
  starting transfers between devices  25.3 us (11%)
  other arithmetic  18.6 us (8%)
  matrix products  16.7 us (7%)
    all_gather x6, blocking collectives, entering_2(): pieces = jax.tree.map(lambda part: lax.all_gather(part, axis), so_far)  59.1 us
    all_to_all x1, blocking collectives, local(): lax.all_to_all(outgoing, SP_TP, split_axis=0, concat_axis=0, tiled=True)  36.9 us
    all_to_all x1, waiting for transfers between devices, local(): lax.all_to_all(served.reshape(shape_in), SP_TP, split_axis=0, concat_axis...  30.2 us
    all_to_all x1, starting transfers between devices, local(): lax.all_to_all(mixer_out, 'tp', split_axis=0, concat_axis=1, tiled=True)  19.7 us
    reshape x2, local copies, waits for them, and re-layouts, local(): returned.reshape(experts_total * capacity, model_width)[slot_index]  6.78 us
    all_to_all x1, starting transfers between devices, local(): lax.all_to_all(served.reshape(shape_in), SP_TP, split_axis=0, concat_axis...  5.6 us
    dot_general x1, matrix products, expert_apply(): jnp.dot(inner_rows, down_matrix, preferred_element_type=jnp.float32)  5.2 us
    reshape x1, local copies, waits for them, and re-layouts, local(): outgoing = padded[owners].reshape(experts_total, capacity, model_width)  5.15 us
  transfers between devices with their start and end apart: 2, of which 2 were waited for; matrix products, arithmetic and copies ran while one was open for 0% of the time, Pallas kernels for 0%

commit v1 on v0

--- a/solution.py
+++ b/solution.py
@@ -1,6 +1,8 @@
 import jax
 import jax.numpy as jnp
 from jax import lax
+from jax.experimental import pallas as pl
+from jax.experimental.pallas import tpu as pltpu
 from jax.sharding import Mesh
 from jax.sharding import PartitionSpec as P
 
@@ -82,26 +84,189 @@
     return (normed * gating).reshape(length, head_count * VALUE_DIM).astype(jnp.bfloat16)
 
 
-def route_slots(block_routes, experts_total, capacity):
-    row_count = block_routes.shape[0]
-    flattened = block_routes.reshape(-1)
-    onehot = (flattened[:, None] == jnp.arange(experts_total, dtype=jnp.int32)[None, :]).astype(
-        jnp.int32
-    )
-    ranking = jnp.sum((jnp.cumsum(onehot, axis=0) - onehot) * onehot, axis=1)
-    slot_index = flattened * capacity + ranking
-    route_ids = jnp.arange(2 * row_count, dtype=jnp.int32) // 2
-    owners = (
-        jnp.full((experts_total * capacity,), row_count, jnp.int32).at[slot_index].set(route_ids)
-    )
-    return (slot_index, owners)
-
-
-def expert_apply(rows_in, gate_matrix, up_matrix, down_matrix):
-    gated = jnp.dot(rows_in, gate_matrix, preferred_element_type=jnp.float32)
-    lifted = jnp.dot(rows_in, up_matrix, preferred_element_type=jnp.float32)
-    inner_rows = (jax.nn.silu(gated) * lifted).astype(jnp.bfloat16)
-    return jnp.dot(inner_rows, down_matrix, preferred_element_type=jnp.float32).astype(jnp.bfloat16)
+VMEM_SPEC = pl.BlockSpec(memory_space=pltpu.VMEM)
+SMEM_SPEC = pl.BlockSpec(memory_space=pltpu.SMEM)
+ANY_SPEC = pl.BlockSpec(memory_space=pl.ANY)
+SUB = 16
+LANES = 128
+SWAP = SUB * SUB
+
+
+def swap_matrix():
+    row = lax.broadcasted_iota(jnp.int32, (SWAP, SWAP), 0)
+    column = lax.broadcasted_iota(jnp.int32, (SWAP, SWAP), 1)
+    partner = (row & (SUB - 1)) * SUB + (row >> 4)
+    return (partner == column).astype(jnp.float32).astype(jnp.bfloat16)
+
+
+def exchange(swap, block):
+    return jnp.dot(swap, block, preferred_element_type=jnp.float32)
+
+
+def routing_kernel(routes_ref, slots_ref, owners_ref, counts):
+    experts_total = counts.shape[0]
+    slot_count = owners_ref.shape[0]
+    route_count = routes_ref.shape[0]
+    capacity = slot_count // experts_total
+
+    def clear_counts(i, carry):
+        counts[i] = 0
+        return carry
+
+    def clear_owners(i, carry):
+        owners_ref[i] = 0
+        return carry
+
+    def place(i, carry):
+        expert = routes_ref[i]
+        used = counts[expert]
+        counts[expert] = used + 1
+        slot = expert * capacity + used
+        slots_ref[i] = slot
+        owners_ref[slot] = i // 2
+        return carry
+
+    lax.fori_loop(0, experts_total, clear_counts, 0, unroll=8)
+    lax.fori_loop(0, slot_count, clear_owners, 0, unroll=8)
+    lax.fori_loop(0, route_count, place, 0, unroll=4)
+
+
+def routing(routes, experts_total, capacity):
+    flattened = routes.reshape(-1)
+    return pl.pallas_call(
+        routing_kernel,
+        out_shape=(
+            jax.ShapeDtypeStruct(flattened.shape, jnp.int32),
+            jax.ShapeDtypeStruct((experts_total * capacity,), jnp.int32),
+        ),
+        in_specs=[SMEM_SPEC],
+        out_specs=(SMEM_SPEC, SMEM_SPEC),
+        scratch_shapes=[pltpu.SMEM((experts_total,), jnp.int32)],
+        name="routing",
+    )(flattened)
+
+
+def dispatch_kernel(owners_ref, normed_ref, outgoing_ref, chunked):
+    swap = swap_matrix()
+    rows, width = normed_ref.shape
+    for g in range(rows // SUB):
+        stacked = jnp.concatenate(
+            [normed_ref[g * SUB : (g + 1) * SUB, j * LANES : (j + 1) * LANES] for j in range(width // LANES)],
+            axis=0,
+        )
+        chunked[g * SUB : (g + 1) * SUB] = (
+            exchange(swap, stacked).astype(jnp.bfloat16).reshape(SUB, SUB, LANES)
+        )
+
+    def copy_row(slot, carry):
+        outgoing_ref[slot] = chunked[owners_ref[slot]]
+        return carry
+
+    lax.fori_loop(0, outgoing_ref.shape[0], copy_row, 0, unroll=16)
+
+
+def dispatch(owners, normed):
+    rows, width = normed.shape
+    return pl.pallas_call(
+        dispatch_kernel,
+        out_shape=jax.ShapeDtypeStruct((owners.shape[0], SUB, LANES), jnp.bfloat16),
+        in_specs=[SMEM_SPEC, VMEM_SPEC],
+        out_specs=VMEM_SPEC,
+        scratch_shapes=[pltpu.VMEM((rows, SUB, LANES), jnp.bfloat16)],
+        name="dispatch",
+    )(owners, normed)
+
+
+def experts_kernel(rows_ref, gate_hbm, up_hbm, down_hbm, out_ref, gate, up, down, rows_in, inner, served, sems):
+    copies = [
+        pltpu.make_async_copy(source.at[0], target, sems.at[k])
+        for k, (source, target) in enumerate(((gate_hbm, gate), (up_hbm, up), (down_hbm, down)))
+    ]
+    for copy in copies:
+        copy.start()
+    swap = swap_matrix()
+    count, width = rows_in.shape
+    hidden = inner.shape[1]
+    for g in range(count // SUB):
+        block = rows_ref[g * SUB : (g + 1) * SUB].reshape(SWAP, LANES)
+        turned = exchange(swap, block).astype(jnp.bfloat16)
+        for j in range(width // LANES):
+            rows_in[g * SUB : (g + 1) * SUB, j * LANES : (j + 1) * LANES] = turned[j * SUB : (j + 1) * SUB]
+    copies[0].wait()
+    copies[1].wait()
+    tile = 256
+    for n in range(hidden // tile):
+        part = slice(n * tile, (n + 1) * tile)
+        gated = jnp.dot(rows_in[...], gate[:, part], preferred_element_type=jnp.float32)
+        lifted = jnp.dot(rows_in[...], up[:, part], preferred_element_type=jnp.float32)
+        inner[:, part] = (gated / (1.0 + jnp.exp(-gated)) * lifted).astype(jnp.bfloat16)
+    copies[2].wait()
+    for n in range(width // tile):
+        part = slice(n * tile, (n + 1) * tile)
+        served[:, part] = jnp.dot(inner[...], down[:, part], preferred_element_type=jnp.float32).astype(jnp.bfloat16)
+    for g in range(count // SUB):
+        stacked = jnp.concatenate(
+            [served[g * SUB : (g + 1) * SUB, j * LANES : (j + 1) * LANES] for j in range(width // LANES)], axis=0
+        )
+        out_ref[g * SUB : (g + 1) * SUB] = (
+            exchange(swap, stacked).astype(jnp.bfloat16).reshape(SUB, SUB, LANES)
+        )
+
+
+def experts(arrived, gate_weight, up_weight, down_weight):
+    count = arrived.shape[0]
+    width, hidden = gate_weight.shape[1:]
+    return pl.pallas_call(
+        experts_kernel,
+        out_shape=jax.ShapeDtypeStruct(arrived.shape, jnp.bfloat16),
+        in_specs=[VMEM_SPEC, ANY_SPEC, ANY_SPEC, ANY_SPEC],
+        out_specs=VMEM_SPEC,
+        scratch_shapes=[
+            pltpu.VMEM((width, hidden), jnp.bfloat16),
+            pltpu.VMEM((width, hidden), jnp.bfloat16),
+            pltpu.VMEM((hidden, width), jnp.bfloat16),
+            pltpu.VMEM((count, width), jnp.bfloat16),
+            pltpu.VMEM((count, hidden), jnp.bfloat16),
+            pltpu.VMEM((count, width), jnp.bfloat16),
+            pltpu.SemaphoreType.DMA((3,)),
+        ],
+        name="experts",
+    )(arrived, gate_weight, up_weight, down_weight)
+
+
+def combine_kernel(slots_ref, returned_ref, merged_ref, weights_ref, out_ref, picked):
+    swap = swap_matrix()
+    rows, width = merged_ref.shape
+
+    def copy_row(i, carry):
+        picked[0, i] = returned_ref[slots_ref[2 * i]]
+        picked[1, i] = returned_ref[slots_ref[2 * i + 1]]
+        return carry
+
+    lax.fori_loop(0, rows, copy_row, 0, unroll=8)
+    for g in range(rows // SUB):
+        group = slice(g * SUB, (g + 1) * SUB)
+        first = exchange(swap, picked[0, group].reshape(SWAP, LANES))
+        second = exchange(swap, picked[1, group].reshape(SWAP, LANES))
+        weight_first = jnp.broadcast_to(weights_ref[group, 0:1], (SUB, LANES))
+        weight_second = jnp.broadcast_to(weights_ref[group, 1:2], (SUB, LANES))
+        for j in range(width // LANES):
+            lanes = slice(j * LANES, (j + 1) * LANES)
+            part = slice(j * SUB, (j + 1) * SUB)
+            total = weight_first * first[part] + weight_second * second[part]
+            out_ref[group, lanes] = (merged_ref[group, lanes].astype(jnp.float32) + total).astype(jnp.bfloat16)
+
+
+def combine(slots, returned, merged, weights):
+    rows = merged.shape[0]
+    return pl.pallas_call(
+        combine_kernel,
+        out_shape=jax.ShapeDtypeStruct(merged.shape, jnp.bfloat16),
+        in_specs=[SMEM_SPEC, VMEM_SPEC, VMEM_SPEC, VMEM_SPEC],
+        out_specs=VMEM_SPEC,
+        scratch_shapes=[pltpu.VMEM((2, rows, SUB, LANES), jnp.bfloat16)],
+        name="combine",
+    )(slots, returned, merged, weights)
 
 
 def merge_states(earlier, later):
@@ -152,26 +317,14 @@
     ).astype(jnp.bfloat16)
     experts_total = chip_count * pair_count
     capacity = 3 * row_count // experts_total
-    slot_index, owners = route_slots(routes, experts_total, capacity)
-    padded = jnp.concatenate([normed, jnp.zeros((1, model_width), jnp.bfloat16)], axis=0)
-    outgoing = padded[owners].reshape(experts_total, capacity, model_width)
-    gate_matrix = gate_weight[0]
-    up_matrix = up_weight[0]
-    down_matrix = down_weight[0]
-    arrived = lax.all_to_all(outgoing, SP_TP, split_axis=0, concat_axis=0, tiled=True)
-    shape_in = arrived.shape
-    served = expert_apply(arrived.reshape(-1, shape_in[-1]), gate_matrix, up_matrix, down_matrix)
-    returned = lax.all_to_all(
-        served.reshape(shape_in), SP_TP, split_axis=0, concat_axis=0, tiled=True
-    )
-    picked = returned.reshape(experts_total * capacity, model_width)[slot_index].reshape(
-        row_count, 2, model_width
-    )
+    slots, owners = routing(routes, experts_total, capacity)
+    outgoing = dispatch(owners, normed)
+    block = (experts_total, capacity * SUB, LANES)
+    arrived = lax.all_to_all(outgoing.reshape(block), SP_TP, split_axis=0, concat_axis=0, tiled=True)
+    served = experts(arrived.reshape(outgoing.shape), gate_weight, up_weight, down_weight)
+    returned = lax.all_to_all(served.reshape(block), SP_TP, split_axis=0, concat_axis=0, tiled=True)
     weights = group_score[:, None] * expert_score / jnp.sum(expert_score, axis=1, keepdims=True)
-    combined = weights[:, 0:1] * picked[:, 0].astype(jnp.float32) + weights[:, 1:2] * picked[
-        :, 1
-    ].astype(jnp.float32)
-    return (widened + combined).astype(jnp.bfloat16)
+    return combine(slots, returned.reshape(outgoing.shape), merged, weights)
 
 
 def solution(mesh):

time: 231 us -> 180 us (0.78)
  local copies, waits for them, and re-layouts: 41.8 us -> 5.02 us
  starting transfers between devices: 25.3 us -> 4.42 us
  Pallas kernels: 0 us -> 19.2 us
  blocking collectives: 96 us -> 109 us
  matrix products: 16.7 us -> 6.64 us
  other arithmetic: 18.6 us -> 10.5 us
  waiting for transfers between devices: 30.9 us -> 24.1 us
    reshape x5 -> x1, local copies, waits for them, and re-layouts: 22.1 us -> 0.71 us  [routing(): flattened = routes.reshape(-1)]
    all_to_all x2 -> x1, starting transfers between devices: 25.3 us -> 4.42 us  [local(): lax.all_to_all(served.reshape(block), SP_TP, split_axis=0, concat_axis=0,...]
    pallas_call x0 -> x4, Pallas kernels: none -> 19.2 us  [the longest x1 8.53 us: experts(): pl.pallas_call(experts_kernel, out_shape=jax.ShapeDtypeStruct(arrived.sha...]
    all_to_all x1 -> x2, blocking collectives: 36.9 us -> 50.8 us  [the longest x1 31.3 us: local(): lax.all_to_all(outgoing.reshape(block), SP_TP, split_axis=0, concat_axis=...]
    dot_general x2 -> x0, matrix products: 8.23 us -> none  [the longest x1 5.2 us: expert_apply(): jnp.dot(inner_rows, down_matrix, preferred_element_type=jnp.float32)]
    gather x2 -> x0, local copies, waits for them, and re-layouts: 8.06 us -> none  [the longest x1 4.96 us: local(): returned.reshape(experts_total * capacity, model_width)[slot_index]]
    all_to_all x2 -> x1, waiting for transfers between devices: 30.9 us -> 24.1 us  [local(): lax.all_to_all(served.reshape(block), SP_TP, split_axis=0, concat_axis=0,...]
    add x4, other arithmetic: 4.1 us -> 0.5 us  [advance(): return (jnp.exp(block_log)[..., None] * carried + increment, carried)]
  transfers between devices with their start and end apart: 2 -> 1, of which waited for: 2 -> 1; matrix products, arithmetic and copies ran while one was open for 0% -> 0% of each run, Pallas kernels for 0% -> 0%
where the time goes in v1:
time: 180 us
  blocking collectives  109 us (61%)
  waiting for transfers between devices  24.1 us (13%)
  Pallas kernels  19.2 us (11%)
  other arithmetic  10.5 us (6%)
  matrix products  6.64 us (4%)
  local copies, waits for them, and re-layouts  5.02 us (3%)
  starting transfers between devices  4.42 us (2%)
    all_gather x6, blocking collectives, entering_2(): pieces = jax.tree.map(lambda part: lax.all_gather(part, axis), so_far)  58.2 us
    all_to_all x1, blocking collectives, local(): lax.all_to_all(outgoing.reshape(block), SP_TP, split_axis=0, concat_axis=...  31.3 us
    all_to_all x1, waiting for transfers between devices, local(): lax.all_to_all(served.reshape(block), SP_TP, split_axis=0, concat_axis=0,...  24.1 us
    all_to_all x1, blocking collectives, local(): lax.all_to_all(mixer_out, 'tp', split_axis=0, concat_axis=1, tiled=True)  19.4 us
    pallas_call x1, Pallas kernels, experts(): pl.pallas_call(experts_kernel, out_shape=jax.ShapeDtypeStruct(arrived.sha...  8.53 us
    all_to_all x1, starting transfers between devices, local(): lax.all_to_all(served.reshape(block), SP_TP, split_axis=0, concat_axis=0,...  4.42 us
    pallas_call x1, Pallas kernels, routing(): pl.pallas_call(routing_kernel, out_shape=(jax.ShapeDtypeStruct(flattened....  4.03 us
  transfers between devices with their start and end apart: 1, of which 1 were waited for; matrix products, arithmetic and copies ran while one was open for 0% of the time, Pallas kernels for 0%

profile of v1, /device:TPU:1, one launch (start us, length us, event | category | flops | bytes accessed | tf_op | source)
XLA Modules:
  0.0 179.6 jit_solution(3534338023881719760)
XLA Ops:
  0.0 1.1 fusion.22
  2.0 9.3 %all-gather.2 = f32[4,4,64]{2,1,0:T(4,128)S(1)} all-gather(f32[1,4,64]{2,1,0:T(4,128)S(1)} %exponential_bitcast_fusion.1), channel_id=2, replica_groups=mesh['sp_0'=4,'sp_1'=4,'sp_2'=4,'tp'=2] {'sp_2'}, dimensions={0}, use_global_device_ids=true | all-gather | bytes 5120 | tf_op jit(solution)/shard_map/all_gather | solution.py:27
  11.4 0.6 iota_compare_fusion
  12.0 8.6 %all_gather.27 = f32[4,4,64]{2,1,0:T(4,128)S(1)} all-gather(f32[1,4,64]{2,1,0:T(4,128)S(1)} %multiply_bitcast_fusion), channel_id=1, replica_groups=mesh['sp_0'=4,'sp_1'=4,'sp_2'=4,'tp'=2] {'sp_1'}, dimensions={0}, use_global_device_ids=true | all-gather | bytes 5120 | tf_op jit(solution)/shard_map/all_gather | solution.py:27
  21.6 3.3 %while.13 = (s32[]{:T(128)}, f32[4,64,128]{2,1,0:T(8,128)S(1)}, f32[4,4,64,128]{3,2,1,0:T(8,128)}, f32[4,4,64]{2,1,0:T(4,128)S(1)}, f32[4,4,64,128]{3,2,1,0:T(8,128)S(1)}, /*index=5*/s32[]{:T(128)}, s32[]{:T(128)}) while((s32[]{:T(128)}, f32[4,64,128]{2,1,0:T(8,128)S(1)}, f32[4,4,64,128]{3,2,1,0:T(8,128)}, ...), condition=%wide.region_4.5_spmd.clone, body=%wide.region_3.4_spmd.clone.sunk | while | flops 131075 | bytes 659040 | solution.py:297
  21.6 0.7 bitcast_dynamic-update-slice_fusion.2
  22.4 0.7 bitcast_dynamic-update-slice_fusion.2
  23.3 0.7 bitcast_dynamic-update-slice_fusion.2
  24.1 0.7 bitcast_dynamic-update-slice_fusion.2
  24.9 10.0 %all-gather.1 = f32[16,64,128]{2,1,0:T(8,128)S(1)} all-gather(f32[4,64,128]{2,1,0:T(8,128)S(1)} %get-tuple-element.37), channel_id=3, replica_groups=mesh['sp_0'=4,'sp_1'=4,'sp_2'=4,'tp'=2] {'sp_2'}, dimensions={0}, use_global_device_ids=true | all-gather | bytes 655360 | tf_op jit(solution)/shard_map/all_gather | solution.py:27
  35.0 0.6 fusion.43
  35.8 10.2 %all_gather.31 = f32[4,4,64,128]{3,2,1,0:T(8,128)S(1)} all-gather(f32[1,4,64,128]{3,2,1,0:T(8,128)S(1)} %fusion.35), channel_id=1, replica_groups=mesh['sp_0'=4,'sp_1'=4,'sp_2'=4,'tp'=2] {'sp_1'}, dimensions={0}, use_global_device_ids=true | all-gather | bytes 655360 | tf_op jit(solution)/shard_map/all_gather | solution.py:27
  46.3 11.1 %all_gather.32 = f32[4,4,64,128]{3,2,1,0:T(8,128)S(1)} all-gather(f32[1,4,64,128]{3,2,1,0:T(8,128)S(1)} %slice_add_fusion.4), channel_id=1, replica_groups=mesh['sp_0'=4,'sp_1'=4,'sp_2'=4,'tp'=2] {'sp_0'}, dimensions={0}, use_global_device_ids=true | all-gather | bytes 655360 | tf_op jit(solution)/shard_map/all_gather | solution.py:27
  57.4 8.9 %all_gather.28 = f32[4,4,64]{2,1,0:T(4,128)S(1)} all-gather(f32[1,4,64]{2,1,0:T(4,128)S(1)} %get-tuple-element.75), channel_id=1, replica_groups=mesh['sp_0'=4,'sp_1'=4,'sp_2'=4,'tp'=2] {'sp_0'}, dimensions={0}, use_global_device_ids=true | all-gather | bytes 5120 | tf_op jit(solution)/shard_map/all_gather | solution.py:27
  66.3 0.6 slice_bitcast_fusion.6
  66.9 0.7 convert_multiply_fusion.3
  67.6 1.2 mul.326
  68.9 1.8 convolution_select_fusion
  71.9 0.9 multiply_reduce_fusion
  74.0 19.4 %all_to_all.29 = bf16[2,128,512]{1,2,0:T(8,128)(2,1)S(1)} all-to-all(bf16[2,128,512]{1,2,0:T(8,128)(2,1)S(1)} %copy.62), channel_id=1, replica_groups=mesh['sp_0'=4,'sp_1'=4,'sp_2'=4,'tp'=2] {'tp'}, dimensions={0} | all-to-all | bytes 524288 | tf_op jit(solution)/shard_map/all_to_all | solution.py:311
  93.5 3.0 %fusion.merged_ref = bf16[128,2048]{1,0:T(8,128)(2,1)S(1)} fusion(bf16[128,1024]{0,1:T(8,128)(2,1)S(1)} %bitcast.186, bf16[1024,2048]{1,0:T(8,128)(2,1)} %param.24, bf16[128,2048]{1,0:T(8,128)(2,1)S(1)} %copy-done.4), kind=kOutput, calls=%fused_computation.4 | convolution fusion | flops 537657344 | bytes 5505024 | tf_op jit(solution)/shard_map/dot_general | solution.py:312
  96.7 0.7 reshape.176.routes_ref
  97.5 4.0 %routing.1 = (s32[256]{0:T(256)}, s32[384]{0:T(512)}) custom-call(s32[256]{0:T(256)} %reshape.176.routes_ref), custom_call_target="tpu_custom_call" | custom-call | tf_op jit(solution)/shard_map/routing/pallas_call | solution.py:136
  101.5 1.0 fusion.5.normed_ref
  102.5 3.2 %dispatch.1 = bf16[384,16,128]{2,1,0:T(8,128)(2,1)} custom-call(s32[384]{0:T(512)} %get-tuple-element.36.owners_ref, bf16[128,2048]{1,0:T(8,128)(2,1)} %fusion.5.normed_ref), custom_call_target="tpu_custom_call" | custom-call | tf_op jit(solution)/shard_map/dispatch/pallas_call | solution.py:170
  105.7 31.3 %all_to_all.30 = bf16[128,48,128]{2,1,0:T(8,128)(2,1)} all-to-all(bf16[128,48,128]{2,1,0:T(8,128)(2,1)} %bitcast.180), channel_id=1, replica_groups=mesh['sp_0'=4,'sp_1'=4,'sp_2'=4,'tp'=2] {'sp_0','sp_1','sp_2','tp'}, dimensions={0} | all-to-all | bytes 3145728 | tf_op jit(solution)/shard_map/all_to_all | solution.py:323
  137.0 8.5 %experts.1 = bf16[384,16,128]{2,1,0:T(8,128)(2,1)} custom-call(bf16[384,16,128]{2,1,0:T(8,128)(2,1)} %bitcast.181, bf16[1,2048,512]{2,1,0:T(8,128)(2,1)} %gate_hbm.1, bf16[1,2048,512]{2,1,0:T(8,128)(2,1)} %up_hbm.1, bf16[1,512,2048]{2,1,0:T(8,128)(2,1)} %down_hbm.1), custom_call_target="tpu_custom_call" | custom-call | tf_op jit(solution)/shard_map/experts/pallas_call | solution.py:219
  145.5 4.4 %all-to-all-start.2 = ((bf16[128,48,128]{2,1,0:T(8,128)(2,1)}), bf16[128,48,128]{2,1,0:T(8,128)(2,1)S(1)}, u32[]{:S(2)}, u32[]{:S(2)}) async-start(bf16[128,48,128]{2,1,0:T(8,128)(2,1)} %bitcast.179), calls=%async_computation.2 | async-start | bytes 3145728 | tf_op jit(solution)/shard_map/all_to_all | solution.py:325
  150.1 0.7 broadcast_divide_fusion.weights_ref
  150.8 24.1 %all-to-all-done.2 = bf16[128,48,128]{2,1,0:T(8,128)(2,1)S(1)} async-done(((bf16[128,48,128]{2,1,0:T(8,128)(2,1)}), bf16[128,48,128]{2,1,0:T(8,128)(2,1)S(1)}, u32[]{:S(2)}, u32[]{:S(2)}) %all-to-all-start.2) | async-done | bytes 1572896 | tf_op jit(solution)/shard_map/all_to_all | solution.py:325
  174.9 1.2 copy-done.2
  176.1 3.5 %combine.1 = bf16[128,2048]{1,0:T(8,128)(2,1)} custom-call(s32[256]{0:T(256)} %get-tuple-element.35.slots_ref, bf16[384,16,128]{2,1,0:T(8,128)(2,1)} %bitcast.178, bf16[128,2048]{1,0:T(8,128)(2,1)} %copy-done.1, f32[128,2]{1,0:T(8,128)} %broadcast_divide_fusion.weights_ref), custom_call_target="tpu_custom_call" | custom-call | tf_op jit(solution)/shard_map/combine/pallas_call | solution.py:262
  (103 shorter events, 5.4 us)
Async XLA Ops:
  0.0 73.3 %copy-start = (f32[128]{0:T(128)S(1)}, f32[128]{0:T(128)}, u32[]{:S(2)}) copy-start(f32[128]{0:T(128)} %param.23) | copy-start | bytes 1540
  0.0 20.6 %copy-start.7 = (bf16[256,256]{1,0:T(8,128)(2,1)S(1)}, bf16[256,256]{1,0:T(8,128)(2,1)}, u32[]{:S(2)}) copy-start(bf16[256,256]{1,0:T(8,128)(2,1)} %param.19) | copy-start | bytes 393220
  0.0 20.9 %copy-start.5 = (bf16[256,512]{1,0:T(8,128)(2,1)S(1)}, bf16[256,512]{1,0:T(8,128)(2,1)}, u32[]{:S(2)}) copy-start(bf16[256,512]{1,0:T(8,128)(2,1)} %param.20) | copy-start | bytes 786436
  11.3 24.3 %copy-start.11 = (f32[4,64]{1,0:T(4,128)}, f32[4,64]{1,0:T(4,128)S(1)}, u32[]{:S(2)}) copy-start(f32[4,64]{1,0:T(4,128)S(1)} %get-tuple-element.81) | copy-start | bytes 3076
  11.3 24.3 %copy-start.13 = (f32[4,64]{1,0:T(4,128)}, f32[4,64]{1,0:T(4,128)S(1)}, u32[]{:S(2)}) copy-start(f32[4,64]{1,0:T(4,128)S(1)} %get-tuple-element.82) | copy-start | bytes 3076
  11.4 24.2 %copy-start.15 = (f32[4,64]{1,0:T(4,128)}, f32[4,64]{1,0:T(4,128)S(1)}, u32[]{:S(2)}) copy-start(f32[4,64]{1,0:T(4,128)S(1)} %get-tuple-element.83) | copy-start | bytes 3076
  24.9 42.0 %copy-start.8 = (bf16[256,256]{1,0:T(8,128)(2,1)S(1)}, bf16[256,256]{1,0:T(8,128)(2,1)}, u32[]{:S(2)}) copy-start(bf16[256,256]{1,0:T(8,128)(2,1)} %param.18) | copy-start | bytes 393220
  35.0 11.1 %copy-start.17 = (f32[4,64]{1,0:T(4,128)}, f32[4,64]{1,0:T(4,128)S(1)}, u32[]{:S(2)}) copy-start(f32[4,64]{1,0:T(4,128)S(1)} %get-tuple-element.76) | copy-start | bytes 3076
  35.0 11.1 %copy-start.19 = (f32[4,64]{1,0:T(4,128)}, f32[4,64]{1,0:T(4,128)S(1)}, u32[]{:S(2)}) copy-start(f32[4,64]{1,0:T(4,128)S(1)} %get-tuple-element.77) | copy-start | bytes 3076
  35.0 11.1 %copy-start.21 = (f32[4,64]{1,0:T(4,128)}, f32[4,64]{1,0:T(4,128)S(1)}, u32[]{:S(2)}) copy-start(f32[4,64]{1,0:T(4,128)S(1)} %get-tuple-element.78) | copy-start | bytes 3076
  35.6 10.5 %copy-start.9 = (f32[4,64]{1,0:T(4,128)}, f32[4,64]{1,0:T(4,128)S(1)}, u32[]{:S(2)}) copy-start(f32[4,64]{1,0:T(4,128)S(1)} %get-tuple-element.80) | copy-start | bytes 3076
  68.8 2.3 %copy-start.10 = (f32[4,64]{1,0:T(4,128)S(1)}, f32[4,64]{1,0:T(4,128)}, u32[]{:S(2)}) copy-start(f32[4,64]{1,0:T(4,128)} %copy-done.9) | copy-start | bytes 3076
  68.8 2.3 %copy-start.12 = (f32[4,64]{1,0:T(4,128)S(1)}, f32[4,64]{1,0:T(4,128)}, u32[]{:S(2)}) copy-start(f32[4,64]{1,0:T(4,128)} %copy-done.11) | copy-start | bytes 3076
  68.8 2.3 %copy-start.14 = (f32[4,64]{1,0:T(4,128)S(1)}, f32[4,64]{1,0:T(4,128)}, u32[]{:S(2)}) copy-start(f32[4,64]{1,0:T(4,128)} %copy-done.13) | copy-start | bytes 3076
  68.8 2.3 %copy-start.16 = (f32[4,64]{1,0:T(4,128)S(1)}, f32[4,64]{1,0:T(4,128)}, u32[]{:S(2)}) copy-start(f32[4,64]{1,0:T(4,128)} %copy-done.15) | copy-start | bytes 3076
  68.8 2.3 %copy-start.18 = (f32[4,64]{1,0:T(4,128)S(1)}, f32[4,64]{1,0:T(4,128)}, u32[]{:S(2)}) copy-start(f32[4,64]{1,0:T(4,128)} %copy-done.17) | copy-start | bytes 3076
  68.9 2.3 %copy-start.20 = (f32[4,64]{1,0:T(4,128)S(1)}, f32[4,64]{1,0:T(4,128)}, u32[]{:S(2)}) copy-start(f32[4,64]{1,0:T(4,128)} %copy-done.19) | copy-start | bytes 3076
  68.9 2.3 %copy-start.22 = (f32[4,64]{1,0:T(4,128)S(1)}, f32[4,64]{1,0:T(4,128)}, u32[]{:S(2)}) copy-start(f32[4,64]{1,0:T(4,128)} %copy-done.21) | copy-start | bytes 3076
  68.9 2.3 %copy-start.24 = (f32[4,64]{1,0:T(4,128)S(1)}, f32[4,64]{1,0:T(4,128)}, u32[]{:S(2)}) copy-start(f32[4,64]{1,0:T(4,128)} %get-tuple-element.67) | copy-start | bytes 3076
  68.9 2.3 %copy-start.25 = (f32[4,64]{1,0:T(4,128)S(1)}, f32[4,64]{1,0:T(4,128)}, u32[]{:S(2)}) copy-start(f32[4,64]{1,0:T(4,128)} %get-tuple-element.68) | copy-start | bytes 3076
  68.9 2.3 %copy-start.26 = (f32[4,64]{1,0:T(4,128)S(1)}, f32[4,64]{1,0:T(4,128)}, u32[]{:S(2)}) copy-start(f32[4,64]{1,0:T(4,128)} %get-tuple-element.71) | copy-start | bytes 3076
  68.9 2.3 %copy-start.27 = (f32[4,64]{1,0:T(4,128)S(1)}, f32[4,64]{1,0:T(4,128)}, u32[]{:S(2)}) copy-start(f32[4,64]{1,0:T(4,128)} %get-tuple-element.72) | copy-start | bytes 3076
  68.9 2.3 %copy-start.28 = (f32[4,64]{1,0:T(4,128)S(1)}, f32[4,64]{1,0:T(4,128)}, u32[]{:S(2)}) copy-start(f32[4,64]{1,0:T(4,128)} %get-tuple-element.73) | copy-start | bytes 3076
  68.9 2.3 %copy-start.29 = (f32[4,64]{1,0:T(4,128)S(1)}, f32[4,64]{1,0:T(4,128)}, u32[]{:S(2)}) copy-start(f32[4,64]{1,0:T(4,128)} %get-tuple-element.74) | copy-start | bytes 3076
  71.8 1.8 copy-start.6
  72.9 20.5 %copy-start.4 = (bf16[128,2048]{1,0:T(8,128)(2,1)S(1)}, bf16[128,2048]{1,0:T(8,128)(2,1)}, u32[]{:S(2)}) copy-start(bf16[128,2048]{1,0:T(8,128)(2,1)} %param.17) | copy-start | bytes 1572868
  93.4 3.2 %copy-start.30 = (s32[128,2]{0,1:T(2,128)S(1)}, s32[128,2]{0,1:T(2,128)}, u32[]{:S(2)}) copy-start(s32[128,2]{0,1:T(2,128)} %param.26) | copy-start | bytes 3076
  93.4 8.0 %copy-start.23 = (f32[2048]{0:T(1024)S(1)}, f32[2048]{0:T(1024)}, u32[]{:S(2)}) copy-start(f32[2048]{0:T(1024)} %param.25) | copy-start | bytes 24580
  96.4 40.6 %copy-start.1 = (bf16[128,2048]{1,0:T(8,128)(2,1)}, bf16[128,2048]{1,0:T(8,128)(2,1)S(1)}, u32[]{:S(2)}) copy-start(bf16[128,2048]{1,0:T(8,128)(2,1)S(1)} %fusion.merged_ref) | copy-start | bytes 1572868
  145.5 4.5 %copy-start.31 = (f32[128,2]{0,1:T(2,128)S(1)}, f32[128,2]{0,1:T(2,128)}, u32[]{:S(2)}) copy-start(f32[128,2]{0,1:T(2,128)} %param.28) | copy-start | bytes 3076
  145.5 4.5 %copy-start.32 = (f32[128]{0:T(128)S(1)}, f32[128]{0:T(128)}, u32[]{:S(2)}) copy-start(f32[128]{0:T(128)} %param.27) | copy-start | bytes 1540
  145.5 29.4 %all-to-all-start.2 = ((bf16[128,48,128]{2,1,0:T(8,128)(2,1)}), bf16[128,48,128]{2,1,0:T(8,128)(2,1)S(1)}, u32[]{:S(2)}, u32[]{:S(2)}) async-start(bf16[128,48,128]{2,1,0:T(8,128)(2,1)} %bitcast.179), calls=%async_computation.2 | async-start | bytes 3145728 | tf_op jit(solution)/shard_map/all_to_all | solution.py:325
  (2 other events, 2.3 us)

commit v2 on v1

--- a/solution.py
+++ b/solution.py
@@ -9,79 +9,9 @@
 KEY_DIM = 64
 VALUE_DIM = 128
 BLOCK = 64
+RING = 4
 SP = ("sp_0", "sp_1", "sp_2")
 SP_TP = ("sp_0", "sp_1", "sp_2", "tp")
-
-
-def neutral_like(value, identity):
-    return jax.tree.map(
-        lambda part, zero: jnp.zeros_like(part) + jnp.asarray(zero, part.dtype), value, identity
-    )
-
-
-def entering_2(value, axes, combine, identity):
-    before = start = neutral_like(value, identity)
-    so_far = value
-    for axis in reversed(axes):
-        peers, place = (lax.axis_size(axis), lax.axis_index(axis))
-        pieces = jax.tree.map(lambda part: lax.all_gather(part, axis), so_far)
-        inside, so_far = (start, start)
-        for k in range(peers):
-            passed = k < place
-            so_far = combine(so_far, jax.tree.map(lambda part: part[k], pieces))
-            inside = jax.tree.map(lambda new, old: jnp.where(passed, new, old), so_far, inside)
-        before = combine(inside, before)
-    return before
-
-
-def block_parts(queries, key_rows, value_rows, gate_logits):
-    length = queries.shape[0]
-    head_count = queries.shape[1] // KEY_DIM
-    blocks = length // BLOCK
-
-    def arrange(source, inner_size):
-        return (
-            source.astype(jnp.float32)
-            .reshape(blocks, BLOCK, head_count, inner_size)
-            .transpose(0, 2, 1, 3)
-        )
-
-    decay_log = jax.nn.log_sigmoid(gate_logits.astype(jnp.float32)) / 16.0
-    running = jnp.cumsum(arrange(decay_log, KEY_DIM), axis=2)
-    closing = running[:, :, -1:, :]
-    query_scaled = arrange(queries, KEY_DIM) * KEY_DIM ** (-0.5) * jnp.exp(running)
-    key_float = arrange(key_rows, KEY_DIM)
-    key_inverse = key_float * jnp.exp(-running)
-    key_closing = key_float * jnp.exp(closing - running)
-    value_float = arrange(value_rows, VALUE_DIM)
-    causal = jnp.tril(jnp.ones((BLOCK, BLOCK), dtype=bool))
-    scores = jnp.where(
-        causal,
-        jnp.einsum("nhcd,nhsd->nhcs", query_scaled, key_inverse, precision=lax.Precision.HIGHEST),
-        0.0,
-    )
-    within = jnp.einsum("nhcs,nhsv->nhcv", scores, value_float, precision=lax.Precision.HIGHEST)
-    increments = jnp.einsum(
-        "nhcd,nhcv->nhdv", key_closing, value_float, precision=lax.Precision.HIGHEST
-    )
-    return (query_scaled, within, increments, closing[:, :, 0, :])
-
-
-def advance(carried, inputs):
-    increment, block_log = inputs
-    return (jnp.exp(block_log)[..., None] * carried + increment, carried)
-
-
-def finish(attended, head_gain, out_gate):
-    blocks = attended.shape[0]
-    head_count = attended.shape[1]
-    length = blocks * BLOCK
-    ordered = attended.transpose(0, 2, 1, 3).reshape(length, head_count, VALUE_DIM)
-    normed = (
-        ordered * lax.rsqrt(jnp.mean(ordered * ordered, axis=-1, keepdims=True) + 1e-06) * head_gain
-    )
-    gating = jax.nn.silu(out_gate.astype(jnp.float32)).reshape(length, head_count, VALUE_DIM)
-    return (normed * gating).reshape(length, head_count * VALUE_DIM).astype(jnp.bfloat16)
 
 
 VMEM_SPEC = pl.BlockSpec(memory_space=pltpu.VMEM)
@@ -144,37 +74,6 @@
         scratch_shapes=[pltpu.SMEM((experts_total,), jnp.int32)],
         name="routing",
     )(flattened)
-
-
-def dispatch_kernel(owners_ref, normed_ref, outgoing_ref, chunked):
-    swap = swap_matrix()
-    rows, width = normed_ref.shape
-    for g in range(rows // SUB):
-        stacked = jnp.concatenate(
-            [normed_ref[g * SUB : (g + 1) * SUB, j * LANES : (j + 1) * LANES] for j in range(width // LANES)],
-            axis=0,
-        )
-        chunked[g * SUB : (g + 1) * SUB] = (
-            exchange(swap, stacked).astype(jnp.bfloat16).reshape(SUB, SUB, LANES)
-        )
-
-    def copy_row(slot, carry):
-        outgoing_ref[slot] = chunked[owners_ref[slot]]
-        return carry
-
-    lax.fori_loop(0, outgoing_ref.shape[0], copy_row, 0, unroll=16)
-
-
-def dispatch(owners, normed):
-    rows, width = normed.shape
-    return pl.pallas_call(
-        dispatch_kernel,
-        out_shape=jax.ShapeDtypeStruct((owners.shape[0], SUB, LANES), jnp.bfloat16),
-        in_specs=[SMEM_SPEC, VMEM_SPEC],
-        out_specs=VMEM_SPEC,
-        scratch_shapes=[pltpu.VMEM((rows, SUB, LANES), jnp.bfloat16)],
-        name="dispatch",
-    )(owners, normed)
 
 
 def experts_kernel(rows_ref, gate_hbm, up_hbm, down_hbm, out_ref, gate, up, down, rows_in, inner, served, sems):
@@ -269,8 +168,237 @@
     )(slots, returned, merged, weights)
 
 
-def merge_states(earlier, later):
-    return (earlier[0] * later[0], later[0][..., None] * earlier[1] + later[1])
+def pieces(value, count):
+    parts = []
+    for _ in range(count):
+        part = value.astype(jnp.bfloat16)
+        parts.append(part)
+        value = value - part.astype(jnp.float32)
+    return parts
+
+
+def product(left, right, left_dim=1, right_dim=0):
+    return lax.dot_general(
+        left, right, (((left_dim,), (right_dim,)), ((), ())), preferred_element_type=jnp.float32
+    )
+
+
+def state_kernel(keys_ref, values_ref, logits_ref, running_ref, states_ref, message_ref):
+    length, channels = keys_ref.shape
+    blocks = length // BLOCK
+    pairs = channels // LANES
+    wide = 2 * VALUE_DIM
+    logits = logits_ref[...].astype(jnp.float32)
+    decay_log = (jnp.minimum(logits, 0.0) - jnp.log1p(jnp.exp(-jnp.abs(logits)))) / 16.0
+    parts = pieces(decay_log, 3)
+    row = lax.broadcasted_iota(jnp.int32, (length, length), 0)
+    column = lax.broadcasted_iota(jnp.int32, (length, length), 1)
+    earlier = (row >= column) & (row // BLOCK == column // BLOCK)
+    earlier = earlier.astype(jnp.float32).astype(jnp.bfloat16)
+    running = sum(product(earlier, part) for part in parts)
+    running_ref[...] = running
+    token = lax.broadcasted_iota(jnp.int32, (length, blocks * LANES), 0)
+    lane = lax.broadcasted_iota(jnp.int32, (length, blocks * LANES), 1)
+    member = (token // BLOCK == lane // LANES).astype(jnp.float32).astype(jnp.bfloat16)
+    block_decay = jnp.exp(sum(product(part, member, 0, 0) for part in parts))
+    states = [jnp.zeros((LANES, VALUE_DIM), jnp.float32)] * pairs
+    total = jnp.zeros((1, channels), jnp.float32)
+    for n in range(blocks):
+        rows = slice(n * BLOCK, (n + 1) * BLOCK)
+        closing = running[(n + 1) * BLOCK - 1 : (n + 1) * BLOCK]
+        total = total + closing
+        key_closing = keys_ref[rows].astype(jnp.float32) * jnp.exp(closing - running[rows])
+        key_closing = key_closing.astype(jnp.bfloat16)
+        for p in range(pairs):
+            states_ref[p, n] = states[p].astype(jnp.bfloat16)
+            grown = product(
+                key_closing[:, p * LANES : (p + 1) * LANES], values_ref[rows, p * wide : (p + 1) * wide], 0, 0
+            )
+            grown = jnp.concatenate([grown[:KEY_DIM, :VALUE_DIM], grown[KEY_DIM:, VALUE_DIM:]], axis=0)
+            decay = block_decay[p * LANES : (p + 1) * LANES, n * LANES : (n + 1) * LANES]
+            states[p] = decay * states[p] + grown
+    for p in range(pairs):
+        message_ref[p * LANES : (p + 1) * LANES] = states[p].astype(jnp.bfloat16)
+    message_ref[channels:] = pack_decay(jnp.exp(total))
+
+
+def pack_decay(decay):
+    pairs = decay.shape[1] // LANES
+    place = lax.broadcasted_iota(jnp.int32, (SUB, LANES), 0)
+    high, low = pieces(decay, 2)
+    packed = jnp.zeros((SUB, LANES), jnp.float32)
+    for p in range(pairs):
+        lanes = slice(p * LANES, (p + 1) * LANES)
+        packed = jnp.where(place == p, high[:, lanes].astype(jnp.float32), packed)
+        packed = jnp.where(place == pairs + p, low[:, lanes].astype(jnp.float32), packed)
+    return packed.astype(jnp.bfloat16)
+
+
+def unpack_decay(message_ref):
+    channels = message_ref.shape[0] - SUB
+    pairs = channels // LANES
+    packed = message_ref[channels:].astype(jnp.float32)
+    diagonal = lax.broadcasted_iota(jnp.int32, (LANES, LANES), 0) == lax.broadcasted_iota(
+        jnp.int32, (LANES, LANES), 1
+    )
+    ones = jnp.ones((LANES, VALUE_DIM), jnp.bfloat16)
+    spread = []
+    for p in range(pairs):
+        both = [jnp.where(diagonal, packed[k : k + 1], 0.0).astype(jnp.bfloat16) for k in (p, pairs + p)]
+        spread.append(product(both[0], ones) + product(both[1], ones))
+    line = jnp.concatenate([packed[p : p + 1] + packed[pairs + p : pairs + p + 1] for p in range(pairs)], axis=1)
+    return line, jnp.concatenate(spread, axis=0)
+
+
+def stage_kernel(place_ref, own_ref, back1_ref, back2_ref, back3_ref, before_ref, decay_ref, message_ref):
+    place = place_ref[0]
+    channels = own_ref.shape[0] - SUB
+    received = []
+    for ref in (back1_ref, back2_ref, back3_ref):
+        line, spread = unpack_decay(ref)
+        received.append((line, spread, ref[:channels].astype(jnp.float32)))
+    own_line, own_spread = unpack_decay(own_ref)
+    before = jnp.zeros((channels, VALUE_DIM), jnp.float32)
+    decay = jnp.ones((channels, VALUE_DIM), jnp.float32)
+    for k in (3, 2, 1):
+        valid = place >= k
+        _, spread, state = received[k - 1]
+        before = jnp.where(valid, spread * before + state, before)
+        decay = jnp.where(valid, spread * decay, decay)
+    before_ref[...] = before
+    decay_ref[...] = decay
+    total = own_spread * before + own_ref[:channels].astype(jnp.float32)
+    for k in (3, 2, 1):
+        later = place < k
+        _, spread, state = received[k - 1]
+        total = jnp.where(later, spread * total + state, total)
+    message_ref[:channels] = total.astype(jnp.bfloat16)
+    line = own_line * received[0][0] * received[1][0] * received[2][0]
+    message_ref[channels:] = pack_decay(line)
+
+
+def masked_heads(rows):
+    lane = lax.broadcasted_iota(jnp.int32, rows.shape, 1)
+    return jnp.concatenate(
+        [jnp.where(lane < KEY_DIM, rows, 0.0), jnp.where(lane >= KEY_DIM, rows, 0.0)], axis=0
+    ).astype(jnp.bfloat16)
+
+
+def within_kernel(queries_ref, keys_ref, values_ref, running_ref, states_ref, partial_ref, reach_ref):
+    length, channels = keys_ref.shape
+    blocks = length // BLOCK
+    pairs = channels // LANES
+    lead = jnp.zeros((1, channels), jnp.float32)
+    row = lax.broadcasted_iota(jnp.int32, (2 * BLOCK, BLOCK), 0)
+    column = lax.broadcasted_iota(jnp.int32, (2 * BLOCK, BLOCK), 1)
+    causal = (row & (BLOCK - 1)) >= column
+    for n in range(blocks):
+        rows = slice(n * BLOCK, (n + 1) * BLOCK)
+        running = running_ref[rows]
+        query_scaled = queries_ref[rows].astype(jnp.float32) * KEY_DIM ** (-0.5) * jnp.exp(running)
+        key_inverse = (keys_ref[rows].astype(jnp.float32) * jnp.exp(-running)).astype(jnp.bfloat16)
+        reach_ref[rows] = query_scaled * jnp.exp(lead)
+        lead = lead + running[BLOCK - 1 : BLOCK]
+        for p in range(pairs):
+            lanes = slice(p * LANES, (p + 1) * LANES)
+            masked = masked_heads(query_scaled[:, lanes])
+            scores = jnp.where(causal, product(masked, key_inverse[:, lanes], 1, 1), 0.0).astype(jnp.bfloat16)
+            carried = product(masked, states_ref[p, n])
+            for h in range(2):
+                place = slice((2 * p + h) * VALUE_DIM, (2 * p + h + 1) * VALUE_DIM)
+                part = slice(h * BLOCK, (h + 1) * BLOCK)
+                partial_ref[rows, place] = product(scores[part], values_ref[rows, place]) + carried[part]
+
+
+def finish_kernel(
+    place_ref, back1_ref, back2_ref, back3_ref, before_y_ref, decay_y_ref, before_x_ref, decay_x_ref,
+    partial_ref, reach_ref, head_gain_ref, out_gate_ref, kept_ref, given_ref, whole,
+):
+    core = place_ref[0]
+    length, channels = reach_ref.shape
+    pairs = channels // LANES
+    state = jnp.zeros((channels, VALUE_DIM), jnp.float32)
+    for ref in (back3_ref, back2_ref, back1_ref):
+        state = unpack_decay(ref)[1] * state + ref[:channels].astype(jnp.float32)
+    state = before_y_ref[...] + decay_y_ref[...] * state
+    state = (before_x_ref[...] + decay_x_ref[...] * state).astype(jnp.bfloat16)
+    half = length // 2
+    for p in range(pairs):
+        lanes = slice(p * LANES, (p + 1) * LANES)
+        carried = product(masked_heads(reach_ref[:, lanes]), state[lanes])
+        for h in range(2):
+            place = slice((2 * p + h) * VALUE_DIM, (2 * p + h + 1) * VALUE_DIM)
+            attended = partial_ref[:, place] + carried[h * length : (h + 1) * length]
+            scale = lax.rsqrt(jnp.mean(attended * attended, axis=1, keepdims=True) + 1e-06)
+            gate = out_gate_ref[:, place].astype(jnp.float32)
+            result = attended * scale * head_gain_ref[...] * (gate / (1.0 + jnp.exp(-gate)))
+            result = result.astype(jnp.bfloat16)
+            whole[0, :, place] = result[:half]
+            whole[1, :, place] = result[half:]
+    kept_ref[...] = whole[core]
+    given_ref[...] = whole[1 - core]
+
+
+def project_kernel(
+    place_ref, owners_ref, kept_ref, taken_ref, weight_ref, residual_ref, norm_gain_ref, merged_ref, outgoing_ref,
+    chunked,
+):
+    core = place_ref[0]
+    rows, width = residual_ref.shape
+    depth = kept_ref.shape[1]
+    tile = 256
+    own = pl.ds(pl.multiple_of(core * depth, depth), depth)
+    other = pl.ds(pl.multiple_of((1 - core) * depth, depth), depth)
+    square = jnp.zeros((rows, 1), jnp.float32)
+    for n in range(width // tile):
+        part = slice(n * tile, (n + 1) * tile)
+        projected = product(kept_ref[...], weight_ref[own, part]) + product(taken_ref[...], weight_ref[other, part])
+        merged = (residual_ref[:, part].astype(jnp.float32) + projected).astype(jnp.bfloat16)
+        merged_ref[:, part] = merged
+        widened = merged.astype(jnp.float32)
+        square = square + jnp.sum(widened * widened, axis=1, keepdims=True)
+    scale = lax.rsqrt(square / width + 1e-06)
+    swap = swap_matrix()
+    for g in range(rows // SUB):
+        group = slice(g * SUB, (g + 1) * SUB)
+        stacked = []
+        for j in range(width // LANES):
+            lanes = slice(j * LANES, (j + 1) * LANES)
+            widened = merged_ref[group, lanes].astype(jnp.float32)
+            stacked.append((widened * scale[group] * norm_gain_ref[:, lanes]).astype(jnp.bfloat16))
+        turned = exchange(swap, jnp.concatenate(stacked, axis=0)).astype(jnp.bfloat16)
+        chunked[group] = turned.reshape(SUB, SUB, LANES)
+
+    def copy_row(slot, carry):
+        outgoing_ref[slot] = chunked[owners_ref[slot]]
+        return carry
+
+    lax.fori_loop(0, outgoing_ref.shape[0], copy_row, 0, unroll=16)
+
+
+def shape_of(shape, dtype):
+    return jax.ShapeDtypeStruct(shape, dtype)
+
+
+def call(kernel, name, outs, operands, scalars=0, scratch=(), cost=2000000):
+    return pl.pallas_call(
+        kernel,
+        out_shape=outs,
+        in_specs=[SMEM_SPEC] * scalars + [VMEM_SPEC] * (len(operands) - scalars),
+        out_specs=jax.tree.map(lambda _: VMEM_SPEC, outs),
+        scratch_shapes=list(scratch),
+        cost_estimate=pl.CostEstimate(flops=cost * 400, bytes_accessed=cost, transcendentals=0),
+        name=name,
+    )(*operands)
+
+
+def from_behind(message, axis, wrap):
+    return [
+        lax.ppermute(
+            message, axis, [(i, (i + k) % RING) for i in range(RING) if wrap or i + k < RING]
+        )
+        for k in range(1, RING)
+    ]
 
 
 def local(
@@ -290,35 +418,64 @@
     up_weight,
     down_weight,
 ):
-    query_scaled, within, increments, block_logs = block_parts(
-        queries, key_rows, value_rows, gate_logits
-    )
-    zero_state = jnp.zeros(increments.shape[1:], jnp.float32)
-    local_end, local_prefix = lax.scan(advance, zero_state, (increments, block_logs))
-    device_decay = jnp.exp(jnp.sum(block_logs, axis=0))
-    identity = (jnp.ones_like(device_decay), jnp.zeros_like(local_end))
-    entering = entering_2((device_decay, local_end), SP, merge_states, identity)[1]
-    leading = jnp.exp(jnp.cumsum(block_logs, axis=0) - block_logs)
-    states = leading[..., None] * entering[None] + local_prefix
-    attended = within + jnp.einsum(
-        "nhcd,nhdv->nhcv", query_scaled, states, precision=lax.Precision.HIGHEST
-    )
-    mixer_out = finish(attended, head_gain, out_gate)
-    row_count = residual.shape[0]
-    model_width = residual.shape[1]
-    pair_count = lax.axis_size("tp")
-    chip_count = lax.axis_size(SP)
-    regrouped = lax.all_to_all(mixer_out, "tp", split_axis=0, concat_axis=1, tiled=True)
-    projected = jnp.dot(regrouped, out_weight, preferred_element_type=jnp.float32)
-    merged = (residual.astype(jnp.float32) + projected).astype(jnp.bfloat16)
-    widened = lax.optimization_barrier(merged).astype(jnp.float32)
-    normed = (
-        widened * lax.rsqrt(jnp.mean(widened * widened, axis=-1, keepdims=True) + 1e-06) * norm_gain
-    ).astype(jnp.bfloat16)
-    experts_total = chip_count * pair_count
+    row_count, model_width = residual.shape
+    length, channels = queries.shape
+    values = value_rows.shape[1]
+    blocks = length // BLOCK
+    pairs = channels // LANES
+    f32, bf16 = jnp.float32, jnp.bfloat16
+    z, y, x, core = (lax.axis_index(axis).astype(jnp.int32).reshape(1) for axis in SP_TP)
+    message_shape = shape_of((channels + SUB, VALUE_DIM), bf16)
+    state_shape = shape_of((channels, VALUE_DIM), f32)
+    running, states, message = call(
+        state_kernel,
+        "local_state",
+        (
+            shape_of((length, channels), f32),
+            shape_of((pairs, blocks, LANES, VALUE_DIM), bf16),
+            message_shape,
+        ),
+        (key_rows, value_rows, gate_logits),
+    )
+    behind = from_behind(message, "sp_2", True)
+    before_x, decay_x, message_x = call(
+        stage_kernel, "stage_x", (state_shape, state_shape, message_shape), (x, message, *behind), 1
+    )
+    partial, reach = call(
+        within_kernel,
+        "within",
+        (shape_of((length, values), f32), shape_of((length, channels), f32)),
+        (queries, key_rows, value_rows, running, states),
+    )
+    behind = from_behind(message_x, "sp_1", True)
+    before_y, decay_y, message_y = call(
+        stage_kernel, "stage_y", (state_shape, state_shape, message_shape), (y, message_x, *behind), 1
+    )
+    behind = from_behind(message_y, "sp_0", False)
+    half = shape_of((length // 2, values), bf16)
+    kept, given = call(
+        finish_kernel,
+        "finish",
+        (half, half),
+        (core, *behind, before_y, decay_y, before_x, decay_x, partial, reach, head_gain.reshape(1, -1), out_gate),
+        1,
+        [pltpu.VMEM((2, length // 2, values), bf16)],
+    )
+    taken = lax.ppermute(given, "tp", [(0, 1), (1, 0)])
+    experts_total = lax.axis_size(SP_TP)
     capacity = 3 * row_count // experts_total
     slots, owners = routing(routes, experts_total, capacity)
-    outgoing = dispatch(owners, normed)
+    merged, outgoing = call(
+        project_kernel,
+        "project",
+        (
+            shape_of((row_count, model_width), bf16),
+            shape_of((experts_total * capacity, SUB, LANES), bf16),
+        ),
+        (core, owners, kept, taken, out_weight, residual, norm_gain.reshape(1, -1)),
+        2,
+        [pltpu.VMEM((row_count, SUB, LANES), bf16)],
+    )
     block = (experts_total, capacity * SUB, LANES)
     arrived = lax.all_to_all(outgoing.reshape(block), SP_TP, split_axis=0, concat_axis=0, tiled=True)
     served = experts(arrived.reshape(outgoing.shape), gate_weight, up_weight, down_weight)

time: 180 us -> 131 us (0.73)
  blocking collectives: 109 us -> 32.9 us
  starting transfers between devices: 4.42 us -> 28.9 us
  Pallas kernels: 19.2 us -> 34.1 us
  other arithmetic: 10.5 us -> 0.73 us
  matrix products: 6.64 us -> 0 us
  waiting for transfers between devices: 24.1 us -> 29.4 us
    all_gather x6 -> x0, blocking collectives: 58.2 us -> none  [entering_2(): pieces = jax.tree.map(lambda part: lax.all_gather(part, axis), so_far)]
    ppermute x0 -> x10, starting transfers between devices: none -> 24.5 us  [the longest x9 20.7 us: from_behind(): lax.ppermute(message, axis, [(i, (i + k) % RING) for i in range(RING) if...]
    all_to_all x1 -> x0, blocking collectives: 19.4 us -> none  [local(): lax.all_to_all(mixer_out, 'tp', split_axis=0, concat_axis=1, tiled=True)]
    pallas_call x1 -> x6, Pallas kernels: 3.18 us -> 18 us  [call(): pl.pallas_call(kernel, out_shape=outs, in_specs=[SMEM_SPEC] * scalars + [...]
    dot_general x5 -> x0, matrix products: 6.64 us -> none  [the longest x1 2.96 us: local(): jnp.dot(regrouped, out_weight, preferred_element_type=jnp.float32)]
    ppermute x0 -> x10, waiting for transfers between devices: none -> 5.33 us  [the longest x9 5.33 us: from_behind(): lax.ppermute(message, axis, [(i, (i + k) % RING) for i in range(RING) if...]
    dynamic_update_slice x4 -> x0, other arithmetic: 2.68 us -> none  [local(): lax.scan(advance, zero_state, (increments, block_logs))]
    mul x6 -> x0, other arithmetic: 2.51 us -> none  [the longest x4 1.22 us: merge_states(): return (earlier[0] * later[0], later[0][..., None] * earlier[1] + later[1])]
  transfers between devices with their start and end apart: 1 -> 11, of which waited for: 1 -> 5; matrix products, arithmetic and copies ran while one was open for 0% -> 1% of each run, Pallas kernels for 0% -> 5%
where the time goes in v2:
time: 131 us
  Pallas kernels  34.1 us (26%)
  blocking collectives  32.9 us (25%)
  waiting for transfers between devices  29.4 us (22%)
  starting transfers between devices  28.9 us (22%)
  local copies, waits for them, and re-layouts  4.69 us (4%)
    all_to_all x1, blocking collectives, local(): lax.all_to_all(outgoing.reshape(block), SP_TP, split_axis=0, concat_axis=...  32.9 us
    all_to_all x1, waiting for transfers between devices, local(): lax.all_to_all(served.reshape(block), SP_TP, split_axis=0, concat_axis=0,...  24.1 us
    ppermute x9, starting transfers between devices, from_behind(): lax.ppermute(message, axis, [(i, (i + k) % RING) for i in range(RING) if...  20.7 us
    pallas_call x6, Pallas kernels, call(): pl.pallas_call(kernel, out_shape=outs, in_specs=[SMEM_SPEC] * scalars + [...  18 us
    pallas_call x1, Pallas kernels, experts(): pl.pallas_call(experts_kernel, out_shape=jax.ShapeDtypeStruct(arrived.sha...  8.54 us
    ppermute x9, waiting for transfers between devices, from_behind(): lax.ppermute(message, axis, [(i, (i + k) % RING) for i in range(RING) if...  5.33 us
    all_to_all x1, starting transfers between devices, local(): lax.all_to_all(served.reshape(block), SP_TP, split_axis=0, concat_axis=0,...  4.41 us
    pallas_call x1, Pallas kernels, routing(): pl.pallas_call(routing_kernel, out_shape=(jax.ShapeDtypeStruct(flattened....  4.03 us
  transfers between devices with their start and end apart: 11, of which 5 were waited for; matrix products, arithmetic and copies ran while one was open for 1% of the time, Pallas kernels for 5%

profile of v2, /device:TPU:1, one launch (start us, length us, event | category | flops | bytes accessed | tf_op | source)
XLA Modules:
  0.0 130.9 jit_solution(6803329053210397099)
XLA Ops:
  0.0 2.6 %local_state.1 = (f32[256,256]{1,0:T(8,128)}, bf16[2,4,128,128]{3,2,1,0:T(8,128)(2,1)}, bf16[272,128]{1,0:T(8,128)(2,1)}) custom-call(bf16[256,256]{1,0:T(8,128)(2,1)} %keys_ref.3, bf16[256,512]{1,0:T(8,128)(2,1)} %values_ref.3, bf16[256,256]{1,0:T(8,128)(2,1)} %logits_ref.1), custom_call_target="tpu_custom_call" | custom-call | flops 800000000 | bytes 2000000 | tf_op jit(solution)/shard_map/local_state/pallas_call | solution.py:384
  2.6 2.0 %collective-permute-start = (bf16[272,128]{1,0:T(8,128)(2,1)}, bf16[272,128]{1,0:T(8,128)(2,1)S(1)}, u32[]{:S(2)}, u32[]{:S(2)}) collective-permute-start(bf16[272,128]{1,0:T(8,128)(2,1)} %get-tuple-element.24.own_ref), channel_id=1, source_target_pairs={{0,2},{2,4},{4,6},{6,0},{1,3},{3,5},{5,7},{7,1},{8,10},{10,12},{12... | collective-permute-start | bytes 208904 | tf_op jit(solution)/shard_map/ppermute | solution.py:397
  4.7 2.5 %collective-permute-start.1 = (bf16[272,128]{1,0:T(8,128)(2,1)}, bf16[272,128]{1,0:T(8,128)(2,1)S(1)}, u32[]{:S(2)}, u32[]{:S(2)}) collective-permute-start(bf16[272,128]{1,0:T(8,128)(2,1)} %get-tuple-element.24.own_ref), channel_id=1, source_target_pairs={{0,4},{2,6},{4,0},{6,2},{1,5},{3,7},{5,1},{7,3},{8,12},{10,14},{12... | collective-permute-start | bytes 208904 | tf_op jit(solution)/shard_map/ppermute | solution.py:397
  7.1 1.2 collective-permute-start.2
  8.3 1.8 %collective-permute-done.1.back2_ref = bf16[272,128]{1,0:T(8,128)(2,1)S(1)} collective-permute-done((bf16[272,128]{1,0:T(8,128)(2,1)}, bf16[272,128]{1,0:T(8,128)(2,1)S(1)}, u32[]{:S(2)}, u32[]{:S(2)}) %collective-permute-start.1) | collective-permute-done | bytes 69664 | tf_op jit(solution)/shard_map/ppermute | solution.py:397
  10.1 0.8 collective-permute-done.2.back3_ref
  11.0 0.6 copy-done.13
  11.6 2.0 %stage_x.1 = (f32[256,128]{1,0:T(8,128)}, f32[256,128]{1,0:T(8,128)}, bf16[272,128]{1,0:T(8,128)(2,1)}) custom-call(s32[1]{0:T(128)} %bitcast.2.place_ref, bf16[272,128]{1,0:T(8,128)(2,1)} %get-tuple-element.24.own_ref, bf16[272,128]{1,0:T(8,128)(2,1)} %copy-done.9, bf16[272,128]{1,0:T(8,128)(2,1)} %copy-done.12, bf16[272,128]{1,0:T(8,128)(2,1)} %copy-done.13), custom_call_target="tpu_custom_call" | custom-call | flops 800000000 | bytes 2000000 | tf_op jit(solution)/shard_map/stage_x/pallas_call | solution.py:384
  13.6 1.4 %collective-permute-start.3 = (bf16[272,128]{1,0:T(8,128)(2,1)}, bf16[272,128]{1,0:T(8,128)(2,1)S(1)}, u32[]{:S(2)}, u32[]{:S(2)}) collective-permute-start(bf16[272,128]{1,0:T(8,128)(2,1)} %get-tuple-element.25.own_ref), channel_id=1, source_target_pairs={{0,8},{8,16},{16,24},{24,0},{1,9},{9,17},{17,25},{25,1},{2,10},{10... | collective-permute-start | bytes 208904 | tf_op jit(solution)/shard_map/ppermute | solution.py:397
  15.0 2.6 %collective-permute-start.4 = (bf16[272,128]{1,0:T(8,128)(2,1)}, bf16[272,128]{1,0:T(8,128)(2,1)S(1)}, u32[]{:S(2)}, u32[]{:S(2)}) collective-permute-start(bf16[272,128]{1,0:T(8,128)(2,1)} %get-tuple-element.25.own_ref), channel_id=1, source_target_pairs={{0,16},{8,24},{16,0},{24,8},{1,17},{9,25},{17,1},{25,9},{2,18},{10... | collective-permute-start | bytes 208904 | tf_op jit(solution)/shard_map/ppermute | solution.py:397
  17.6 1.1 collective-permute-start.5
  18.7 1.6 %collective-permute-done.4.back2_ref = bf16[272,128]{1,0:T(8,128)(2,1)S(1)} collective-permute-done((bf16[272,128]{1,0:T(8,128)(2,1)}, bf16[272,128]{1,0:T(8,128)(2,1)S(1)}, u32[]{:S(2)}, u32[]{:S(2)}) %collective-permute-start.4) | collective-permute-done | bytes 69664 | tf_op jit(solution)/shard_map/ppermute | solution.py:397
  20.3 1.0 collective-permute-done.5.back3_ref
  21.4 0.6 copy-done.11
  22.0 2.0 %stage_y.1 = (f32[256,128]{1,0:T(8,128)}, f32[256,128]{1,0:T(8,128)}, bf16[272,128]{1,0:T(8,128)(2,1)}) custom-call(s32[1]{0:T(128)} %bitcast.1.place_ref, bf16[272,128]{1,0:T(8,128)(2,1)} %get-tuple-element.25.own_ref, bf16[272,128]{1,0:T(8,128)(2,1)} %copy-done.6, bf16[272,128]{1,0:T(8,128)(2,1)} %copy-done.8, bf16[272,128]{1,0:T(8,128)(2,1)} %copy-done.11), custom_call_target="tpu_custom_call" | custom-call | flops 800000000 | bytes 2000000 | tf_op jit(solution)/shard_map/stage_y/pallas_call | solution.py:384
  24.0 3.5 %collective-permute-start.6 = (bf16[272,128]{1,0:T(8,128)(2,1)}, bf16[272,128]{1,0:T(8,128)(2,1)S(1)}, u32[]{:S(2)}, u32[]{:S(2)}) collective-permute-start(bf16[272,128]{1,0:T(8,128)(2,1)} %get-tuple-element.26), channel_id=1, source_target_pairs={{0,32},{32,64},{64,96},{1,33},{33,65},{65,97},{2,34},{34,66},{66,9... | collective-permute-start | bytes 208904 | tf_op jit(solution)/shard_map/ppermute | solution.py:397
  27.5 5.2 %collective-permute-start.7 = (bf16[272,128]{1,0:T(8,128)(2,1)}, bf16[272,128]{1,0:T(8,128)(2,1)S(1)}, u32[]{:S(2)}, u32[]{:S(2)}) collective-permute-start(bf16[272,128]{1,0:T(8,128)(2,1)} %get-tuple-element.26), channel_id=1, source_target_pairs={{0,64},{32,96},{1,65},{33,97},{2,66},{34,98},{3,67},{35,99},{4,68}... | collective-permute-start | bytes 208904 | tf_op jit(solution)/shard_map/ppermute | solution.py:397
  32.8 1.3 collective-permute-start.8
  34.1 2.8 %within.1 = (f32[256,512]{1,0:T(8,128)}, f32[256,256]{1,0:T(8,128)}) custom-call(bf16[256,256]{1,0:T(8,128)(2,1)} %queries_ref.1, bf16[256,256]{1,0:T(8,128)(2,1)} %keys_ref.3, bf16[256,512]{1,0:T(8,128)(2,1)} %values_ref.3, f32[256,256]{1,0:T(8,128)} %get-tuple-element.31.running_ref, bf16[2,4,128,128]{3,2,1,0:T(8,128)(2,1)} %get-tuple-element.32.states_ref), custom_call_target="tpu_custom_call" | custom-call | flops 800000000 | bytes 2000000 | tf_op jit(solution)/shard_map/within/pallas_call | solution.py:384
  37.5 2.9 %finish.1 = (bf16[128,512]{1,0:T(8,128)(2,1)}, bf16[128,512]{1,0:T(8,128)(2,1)}) custom-call(s32[1]{0:T(128)} %bitcast.place_ref, bf16[272,128]{1,0:T(8,128)(2,1)} %copy-done.5, bf16[272,128]{1,0:T(8,128)(2,1)} %copy-done.7, bf16[272,128]{1,0:T(8,128)(2,1)} %copy-done.10, f32[256,128]{1,0:T(8,128)} %get-tuple-element.27.before_y_ref, ...), custom_call_target="tpu_custom_call" | custom-call | flops 800000000 | bytes 2000000 | tf_op jit(solution)/shard_map/finish/pallas_call | solution.py:384
  40.4 3.8 %collective-permute-start.9 = (bf16[128,512]{1,0:T(8,128)(2,1)}, bf16[128,512]{1,0:T(8,128)(2,1)S(1)}, u32[]{:S(2)}, u32[]{:S(2)}) collective-permute-start(bf16[128,512]{1,0:T(8,128)(2,1)} %get-tuple-element.36), channel_id=1, source_target_pairs={{0,1},{1,0},{2,3},{3,2},{4,5},{5,4},{6,7},{7,6},{8,9},{9,8},{10,11... | collective-permute-start | bytes 393224 | tf_op jit(solution)/shard_map/ppermute | solution.py:464
  44.3 0.7 reshape.32.routes_ref
  45.0 4.0 %routing.1 = (s32[256]{0:T(256)}, s32[384]{0:T(512)}) custom-call(s32[256]{0:T(256)} %reshape.32.routes_ref), custom_call_target="tpu_custom_call" | custom-call | tf_op jit(solution)/shard_map/routing/pallas_call | solution.py:66
  49.1 0.6 copy-done.1
  49.7 5.7 %project.1 = (bf16[128,2048]{1,0:T(8,128)(2,1)}, bf16[384,16,128]{2,1,0:T(8,128)(2,1)}) custom-call(s32[1]{0:T(128)} %bitcast.place_ref, s32[384]{0:T(512)} %get-tuple-element.23.owners_ref, bf16[128,512]{1,0:T(8,128)(2,1)} %get-tuple-element.35.kept_ref, bf16[128,512]{1,0:T(8,128)(2,1)} %copy-done.1, bf16[1024,2048]{1,0:T(8,128)(2,1)} %weight_ref.1, ...), custom_call_target="tpu_custom_call" | custom-call | flops 800000000 | bytes 2000000 | tf_op jit(solution)/shard_map/project/pallas_call | solution.py:384
  55.4 32.9 %all_to_all.10 = bf16[128,48,128]{2,1,0:T(8,128)(2,1)} all-to-all(bf16[128,48,128]{2,1,0:T(8,128)(2,1)} %bitcast.12), channel_id=1, replica_groups=mesh['sp_0'=4,'sp_1'=4,'sp_2'=4,'tp'=2] {'sp_0','sp_1','sp_2','tp'}, dimensions={0} | all-to-all | bytes 3145728 | tf_op jit(solution)/shard_map/all_to_all | solution.py:480
  88.2 8.5 %experts.1 = bf16[384,16,128]{2,1,0:T(8,128)(2,1)} custom-call(bf16[384,16,128]{2,1,0:T(8,128)(2,1)} %bitcast.11, bf16[1,2048,512]{2,1,0:T(8,128)(2,1)} %gate_hbm.1, bf16[1,2048,512]{2,1,0:T(8,128)(2,1)} %up_hbm.1, bf16[1,512,2048]{2,1,0:T(8,128)(2,1)} %down_hbm.1), custom_call_target="tpu_custom_call" | custom-call | tf_op jit(solution)/shard_map/experts/pallas_call | solution.py:118
  96.8 4.4 %all-to-all-start.1 = ((bf16[128,48,128]{2,1,0:T(8,128)(2,1)}), bf16[128,48,128]{2,1,0:T(8,128)(2,1)S(1)}, u32[]{:S(2)}, u32[]{:S(2)}) async-start(bf16[128,48,128]{2,1,0:T(8,128)(2,1)} %bitcast.10), calls=%async_computation.1 | async-start | bytes 3145728 | tf_op jit(solution)/shard_map/all_to_all | solution.py:482
  101.4 0.7 broadcast_divide_fusion.weights_ref
  102.1 24.1 %all-to-all-done.1 = bf16[128,48,128]{2,1,0:T(8,128)(2,1)S(1)} async-done(((bf16[128,48,128]{2,1,0:T(8,128)(2,1)}), bf16[128,48,128]{2,1,0:T(8,128)(2,1)S(1)}, u32[]{:S(2)}, u32[]{:S(2)}) %all-to-all-start.1) | async-done | bytes 1572896 | tf_op jit(solution)/shard_map/all_to_all | solution.py:482
  126.2 1.2 copy-done
  127.4 3.5 %combine.1 = bf16[128,2048]{1,0:T(8,128)(2,1)} custom-call(s32[256]{0:T(256)} %get-tuple-element.22.slots_ref, bf16[384,16,128]{2,1,0:T(8,128)(2,1)} %bitcast.9, bf16[128,2048]{1,0:T(8,128)(2,1)} %get-tuple-element.38.merged_ref, f32[128,2]{1,0:T(8,128)} %broadcast_divide_fusion.weights_ref), custom_call_target="tpu_custom_call" | custom-call | tf_op jit(solution)/shard_map/combine/pallas_call | solution.py:161
  (33 shorter events, 0.9 us)
Async XLA Ops:
  2.6 5.6 %collective-permute-start = (bf16[272,128]{1,0:T(8,128)(2,1)}, bf16[272,128]{1,0:T(8,128)(2,1)S(1)}, u32[]{:S(2)}, u32[]{:S(2)}) collective-permute-start(bf16[272,128]{1,0:T(8,128)(2,1)} %get-tuple-element.24.own_ref), channel_id=1, source_target_pairs={{0,2},{2,4},{4,6},{6,0},{1,3},{3,5},{5,7},{7,1},{8,10},{10,12},{12... | collective-permute-start | bytes 208904 | tf_op jit(solution)/shard_map/ppermute | solution.py:397
  4.7 5.5 %collective-permute-start.1 = (bf16[272,128]{1,0:T(8,128)(2,1)}, bf16[272,128]{1,0:T(8,128)(2,1)S(1)}, u32[]{:S(2)}, u32[]{:S(2)}) collective-permute-start(bf16[272,128]{1,0:T(8,128)(2,1)} %get-tuple-element.24.own_ref), channel_id=1, source_target_pairs={{0,4},{2,6},{4,0},{6,2},{1,5},{3,7},{5,1},{7,3},{8,12},{10,14},{12... | collective-permute-start | bytes 208904 | tf_op jit(solution)/shard_map/ppermute | solution.py:397
  7.1 3.8 %collective-permute-start.2 = (bf16[272,128]{1,0:T(8,128)(2,1)}, bf16[272,128]{1,0:T(8,128)(2,1)S(1)}, u32[]{:S(2)}, u32[]{:S(2)}) collective-permute-start(bf16[272,128]{1,0:T(8,128)(2,1)} %get-tuple-element.24.own_ref), channel_id=1, source_target_pairs={{0,6},{2,0},{4,2},{6,4},{1,7},{3,1},{5,3},{7,5},{8,14},{10,8},{12,... | collective-permute-start | bytes 208904 | tf_op jit(solution)/shard_map/ppermute | solution.py:397
  8.3 2.7 %copy-start.9 = (bf16[272,128]{1,0:T(8,128)(2,1)}, bf16[272,128]{1,0:T(8,128)(2,1)S(1)}, u32[]{:S(2)}) copy-start(bf16[272,128]{1,0:T(8,128)(2,1)S(1)} %collective-permute-done.back1_ref) | copy-start | bytes 208900
  10.1 0.8 copy-start.12
  10.9 0.6 copy-start.13
  13.6 5.1 %collective-permute-start.3 = (bf16[272,128]{1,0:T(8,128)(2,1)}, bf16[272,128]{1,0:T(8,128)(2,1)S(1)}, u32[]{:S(2)}, u32[]{:S(2)}) collective-permute-start(bf16[272,128]{1,0:T(8,128)(2,1)} %get-tuple-element.25.own_ref), channel_id=1, source_target_pairs={{0,8},{8,16},{16,24},{24,0},{1,9},{9,17},{17,25},{25,1},{2,10},{10... | collective-permute-start | bytes 208904 | tf_op jit(solution)/shard_map/ppermute | solution.py:397
  15.0 5.3 %collective-permute-start.4 = (bf16[272,128]{1,0:T(8,128)(2,1)}, bf16[272,128]{1,0:T(8,128)(2,1)S(1)}, u32[]{:S(2)}, u32[]{:S(2)}) collective-permute-start(bf16[272,128]{1,0:T(8,128)(2,1)} %get-tuple-element.25.own_ref), channel_id=1, source_target_pairs={{0,16},{8,24},{16,0},{24,8},{1,17},{9,25},{17,1},{25,9},{2,18},{10... | collective-permute-start | bytes 208904 | tf_op jit(solution)/shard_map/ppermute | solution.py:397
  17.6 3.7 %collective-permute-start.5 = (bf16[272,128]{1,0:T(8,128)(2,1)}, bf16[272,128]{1,0:T(8,128)(2,1)S(1)}, u32[]{:S(2)}, u32[]{:S(2)}) collective-permute-start(bf16[272,128]{1,0:T(8,128)(2,1)} %get-tuple-element.25.own_ref), channel_id=1, source_target_pairs={{0,24},{8,0},{16,8},{24,16},{1,25},{9,1},{17,9},{25,17},{2,26},{10... | collective-permute-start | bytes 208904 | tf_op jit(solution)/shard_map/ppermute | solution.py:397
  18.7 2.6 %copy-start.6 = (bf16[272,128]{1,0:T(8,128)(2,1)}, bf16[272,128]{1,0:T(8,128)(2,1)S(1)}, u32[]{:S(2)}) copy-start(bf16[272,128]{1,0:T(8,128)(2,1)S(1)} %collective-permute-done.3.back1_ref) | copy-start | bytes 208900
  20.3 1.0 copy-start.8
  21.4 0.6 copy-start.11
  24.0 12.8 %collective-permute-start.6 = (bf16[272,128]{1,0:T(8,128)(2,1)}, bf16[272,128]{1,0:T(8,128)(2,1)S(1)}, u32[]{:S(2)}, u32[]{:S(2)}) collective-permute-start(bf16[272,128]{1,0:T(8,128)(2,1)} %get-tuple-element.26), channel_id=1, source_target_pairs={{0,32},{32,64},{64,96},{1,33},{33,65},{65,97},{2,34},{34,66},{66,9... | collective-permute-start | bytes 208904 | tf_op jit(solution)/shard_map/ppermute | solution.py:397
  27.5 9.3 %collective-permute-start.7 = (bf16[272,128]{1,0:T(8,128)(2,1)}, bf16[272,128]{1,0:T(8,128)(2,1)S(1)}, u32[]{:S(2)}, u32[]{:S(2)}) collective-permute-start(bf16[272,128]{1,0:T(8,128)(2,1)} %get-tuple-element.26), channel_id=1, source_target_pairs={{0,64},{32,96},{1,65},{33,97},{2,66},{34,98},{3,67},{35,99},{4,68}... | collective-permute-start | bytes 208904 | tf_op jit(solution)/shard_map/ppermute | solution.py:397
  32.8 4.1 %collective-permute-start.8 = (bf16[272,128]{1,0:T(8,128)(2,1)}, bf16[272,128]{1,0:T(8,128)(2,1)S(1)}, u32[]{:S(2)}, u32[]{:S(2)}) collective-permute-start(bf16[272,128]{1,0:T(8,128)(2,1)} %get-tuple-element.26), channel_id=1, source_target_pairs={{0,96},{1,97},{2,98},{3,99},{4,100},{5,101},{6,102},{7,103},{8,104... | collective-permute-start | bytes 208904 | tf_op jit(solution)/shard_map/ppermute | solution.py:397
  36.8 7.4 %copy-start.2 = (s32[128,2]{0,1:T(2,128)S(1)}, s32[128,2]{0,1:T(2,128)}, u32[]{:S(2)}) copy-start(s32[128,2]{0,1:T(2,128)} %param.24) | copy-start | bytes 3076
  36.9 0.6 copy-start.5
  36.9 0.6 copy-start.7
  36.9 0.7 copy-start.10
  40.4 8.6 %collective-permute-start.9 = (bf16[128,512]{1,0:T(8,128)(2,1)}, bf16[128,512]{1,0:T(8,128)(2,1)S(1)}, u32[]{:S(2)}, u32[]{:S(2)}) collective-permute-start(bf16[128,512]{1,0:T(8,128)(2,1)} %get-tuple-element.36), channel_id=1, source_target_pairs={{0,1},{1,0},{2,3},{3,2},{4,5},{5,4},{6,7},{7,6},{8,9},{9,8},{10,11... | collective-permute-start | bytes 393224 | tf_op jit(solution)/shard_map/ppermute | solution.py:464
  49.1 0.7 copy-start.1
  96.8 4.4 %copy-start.3 = (f32[128,2]{0,1:T(2,128)S(1)}, f32[128,2]{0,1:T(2,128)}, u32[]{:S(2)}) copy-start(f32[128,2]{0,1:T(2,128)} %param.26) | copy-start | bytes 3076
  96.8 4.4 %copy-start.4 = (f32[128]{0:T(128)S(1)}, f32[128]{0:T(128)}, u32[]{:S(2)}) copy-start(f32[128]{0:T(128)} %param.25) | copy-start | bytes 1540
  96.8 29.4 %all-to-all-start.1 = ((bf16[128,48,128]{2,1,0:T(8,128)(2,1)}), bf16[128,48,128]{2,1,0:T(8,128)(2,1)S(1)}, u32[]{:S(2)}, u32[]{:S(2)}) async-start(bf16[128,48,128]{2,1,0:T(8,128)(2,1)} %bitcast.10), calls=%async_computation.1 | async-start | bytes 3145728 | tf_op jit(solution)/shard_map/all_to_all | solution.py:482
  126.2 1.2 copy-start

commit v3 on v2

--- a/solution.py
+++ b/solution.py
@@ -72,17 +72,12 @@
         in_specs=[SMEM_SPEC],
         out_specs=(SMEM_SPEC, SMEM_SPEC),
         scratch_shapes=[pltpu.SMEM((experts_total,), jnp.int32)],
+        compiler_params=limited(1),
         name="routing",
     )(flattened)
 
 
-def experts_kernel(rows_ref, gate_hbm, up_hbm, down_hbm, out_ref, gate, up, down, rows_in, inner, served, sems):
-    copies = [
-        pltpu.make_async_copy(source.at[0], target, sems.at[k])
-        for k, (source, target) in enumerate(((gate_hbm, gate), (up_hbm, up), (down_hbm, down)))
-    ]
-    for copy in copies:
-        copy.start()
+def experts_kernel(rows_ref, gate, up, down, out_ref, rows_in, inner, served):
     swap = swap_matrix()
     count, width = rows_in.shape
     hidden = inner.shape[1]
@@ -91,18 +86,15 @@
         turned = exchange(swap, block).astype(jnp.bfloat16)
         for j in range(width // LANES):
             rows_in[g * SUB : (g + 1) * SUB, j * LANES : (j + 1) * LANES] = turned[j * SUB : (j + 1) * SUB]
-    copies[0].wait()
-    copies[1].wait()
     tile = 256
     for n in range(hidden // tile):
         part = slice(n * tile, (n + 1) * tile)
-        gated = jnp.dot(rows_in[...], gate[:, part], preferred_element_type=jnp.float32)
-        lifted = jnp.dot(rows_in[...], up[:, part], preferred_element_type=jnp.float32)
+        gated = jnp.dot(rows_in[...], gate[0, :, part], preferred_element_type=jnp.float32)
+        lifted = jnp.dot(rows_in[...], up[0, :, part], preferred_element_type=jnp.float32)
         inner[:, part] = (gated / (1.0 + jnp.exp(-gated)) * lifted).astype(jnp.bfloat16)
-    copies[2].wait()
     for n in range(width // tile):
         part = slice(n * tile, (n + 1) * tile)
-        served[:, part] = jnp.dot(inner[...], down[:, part], preferred_element_type=jnp.float32).astype(jnp.bfloat16)
+        served[:, part] = jnp.dot(inner[...], down[0, :, part], preferred_element_type=jnp.float32).astype(jnp.bfloat16)
     for g in range(count // SUB):
         stacked = jnp.concatenate(
             [served[g * SUB : (g + 1) * SUB, j * LANES : (j + 1) * LANES] for j in range(width // LANES)], axis=0
@@ -118,17 +110,14 @@
     return pl.pallas_call(
         experts_kernel,
         out_shape=jax.ShapeDtypeStruct(arrived.shape, jnp.bfloat16),
-        in_specs=[VMEM_SPEC, ANY_SPEC, ANY_SPEC, ANY_SPEC],
+        in_specs=[VMEM_SPEC] * 4,
         out_specs=VMEM_SPEC,
         scratch_shapes=[
-            pltpu.VMEM((width, hidden), jnp.bfloat16),
-            pltpu.VMEM((width, hidden), jnp.bfloat16),
-            pltpu.VMEM((hidden, width), jnp.bfloat16),
             pltpu.VMEM((count, width), jnp.bfloat16),
             pltpu.VMEM((count, hidden), jnp.bfloat16),
             pltpu.VMEM((count, width), jnp.bfloat16),
-            pltpu.SemaphoreType.DMA((3,)),
         ],
+        compiler_params=limited(16),
         name="experts",
     )(arrived, gate_weight, up_weight, down_weight)
 
@@ -164,6 +153,7 @@
         in_specs=[SMEM_SPEC, VMEM_SPEC, VMEM_SPEC, VMEM_SPEC],
         out_specs=VMEM_SPEC,
         scratch_shapes=[pltpu.VMEM((2, rows, SUB, LANES), jnp.bfloat16)],
+        compiler_params=limited(8),
         name="combine",
     )(slots, returned, merged, weights)
 
@@ -380,7 +370,11 @@
     return jax.ShapeDtypeStruct(shape, dtype)
 
 
-def call(kernel, name, outs, operands, scalars=0, scratch=(), cost=2000000):
+def limited(mebibytes):
+    return pltpu.CompilerParams(vmem_limit_bytes=mebibytes << 20)
+
+
+def call(kernel, name, outs, operands, scalars=0, scratch=(), cost=2000000, room=6):
     return pl.pallas_call(
         kernel,
         out_shape=outs,
@@ -388,6 +382,7 @@
         out_specs=jax.tree.map(lambda _: VMEM_SPEC, outs),
         scratch_shapes=list(scratch),
         cost_estimate=pl.CostEstimate(flops=cost * 400, bytes_accessed=cost, transcendentals=0),
+        compiler_params=limited(room),
         name=name,
     )(*operands)
 
@@ -437,7 +432,11 @@
         ),
         (key_rows, value_rows, gate_logits),
     )
+    experts_total = lax.axis_size(SP_TP)
+    capacity = 3 * row_count // experts_total
+    slots, owners = routing(routes, experts_total, capacity)
     behind = from_behind(message, "sp_2", True)
+    slots, owners, *behind = lax.optimization_barrier((slots, owners, *behind))
     before_x, decay_x, message_x = call(
         stage_kernel, "stage_x", (state_shape, state_shape, message_shape), (x, message, *behind), 1
     )
@@ -448,6 +447,7 @@
         (queries, key_rows, value_rows, running, states),
     )
     behind = from_behind(message_x, "sp_1", True)
+    partial, reach, *behind = lax.optimization_barrier((partial, reach, *behind))
     before_y, decay_y, message_y = call(
         stage_kernel, "stage_y", (state_shape, state_shape, message_shape), (y, message_x, *behind), 1
     )
@@ -462,9 +462,6 @@
         [pltpu.VMEM((2, length // 2, values), bf16)],
     )
     taken = lax.ppermute(given, "tp", [(0, 1), (1, 0)])
-    experts_total = lax.axis_size(SP_TP)
-    capacity = 3 * row_count // experts_total
-    slots, owners = routing(routes, experts_total, capacity)
     merged, outgoing = call(
         project_kernel,
         "project",
@@ -475,6 +472,7 @@
         (core, owners, kept, taken, out_weight, residual, norm_gain.reshape(1, -1)),
         2,
         [pltpu.VMEM((row_count, SUB, LANES), bf16)],
+        room=14,
     )
     block = (experts_total, capacity * SUB, LANES)
     arrived = lax.all_to_all(outgoing.reshape(block), SP_TP, split_axis=0, concat_axis=0, tiled=True)

time: 131 us -> 114 us (0.87)
  Pallas kernels: 34.1 us -> 17.4 us
    pallas_call x6, Pallas kernels: 18 us -> 5.55 us  [call(): pl.pallas_call(kernel, out_shape=outs, in_specs=[SMEM_SPEC] * scalars + [...]
    pallas_call x1, Pallas kernels: 8.54 us -> 5.48 us  [experts(): pl.pallas_call(experts_kernel, out_shape=jax.ShapeDtypeStruct(arrived.sha...]
    unnamed x29 -> x35, local copies, waits for them, and re-layouts: 3.88 us -> 5.12 us
  transfers between devices with their start and end apart: 11 -> 11, of which waited for: 5 -> 5; matrix products, arithmetic and copies ran while one was open for 1% -> 0% of each run, Pallas kernels for 5% -> 4%
where the time goes in v3:
time: 114 us
  blocking collectives  32.2 us (28%)
  waiting for transfers between devices  29.9 us (26%)
  starting transfers between devices  28.4 us (25%)
  Pallas kernels  17.4 us (15%)
  local copies, waits for them, and re-layouts  5.37 us (5%)
    all_to_all x1, blocking collectives, local(): lax.all_to_all(outgoing.reshape(block), SP_TP, split_axis=0, concat_axis=...  32.2 us
    all_to_all x1, waiting for transfers between devices, local(): lax.all_to_all(served.reshape(block), SP_TP, split_axis=0, concat_axis=0,...  24.7 us
    ppermute x9, starting transfers between devices, from_behind(): lax.ppermute(message, axis, [(i, (i + k) % RING) for i in range(RING) if...  20.9 us
    pallas_call x6, Pallas kernels, call(): pl.pallas_call(kernel, out_shape=outs, in_specs=[SMEM_SPEC] * scalars + [...  5.55 us
    pallas_call x1, Pallas kernels, experts(): pl.pallas_call(experts_kernel, out_shape=jax.ShapeDtypeStruct(arrived.sha...  5.48 us
    unnamed x35, local copies, waits for them, and re-layouts  5.12 us
    all_to_all x1, starting transfers between devices, local(): lax.all_to_all(served.reshape(block), SP_TP, split_axis=0, concat_axis=0,...  4.53 us
    ppermute x9, waiting for transfers between devices, from_behind(): lax.ppermute(message, axis, [(i, (i + k) % RING) for i in range(RING) if...  4.16 us
  transfers between devices with their start and end apart: 11, of which 5 were waited for; matrix products, arithmetic and copies ran while one was open for 0% of the time, Pallas kernels for 4%

profile of v3, /device:TPU:1, one launch (start us, length us, event | category | flops | bytes accessed | tf_op | source)
XLA Modules:
  0.0 113.5 jit_solution(11048448766139671550)
XLA Ops:
  0.0 0.9 copy-done.6
  1.0 0.9 copy-done.9
  1.9 0.9 copy-done.10
  2.8 0.9 local_state.1
  3.7 2.1 %collective-permute-start = (bf16[272,128]{1,0:T(8,128)(2,1)S(1)}, bf16[272,128]{1,0:T(8,128)(2,1)S(1)}, u32[]{:S(2)}, u32[]{:S(2)}) collective-permute-start(bf16[272,128]{1,0:T(8,128)(2,1)S(1)} %get-tuple-element.34.own_ref), channel_id=1, source_target_pairs={{0,2},{2,4},{4,6},{6,0},{1,3},{3,5},{5,7},{7,1},{8,10},{10,12},{12... | collective-permute-start | bytes 208904 | tf_op jit(solution)/shard_map/ppermute | solution.py:392
  5.8 2.4 %collective-permute-start.1 = (bf16[272,128]{1,0:T(8,128)(2,1)S(1)}, bf16[272,128]{1,0:T(8,128)(2,1)S(1)}, u32[]{:S(2)}, u32[]{:S(2)}) collective-permute-start(bf16[272,128]{1,0:T(8,128)(2,1)S(1)} %get-tuple-element.34.own_ref), channel_id=1, source_target_pairs={{0,4},{2,6},{4,0},{6,2},{1,5},{3,7},{5,1},{7,3},{8,12},{10,14},{12... | collective-permute-start | bytes 208904 | tf_op jit(solution)/shard_map/ppermute | solution.py:392
  8.2 1.2 %collective-permute-start.2 = (bf16[272,128]{1,0:T(8,128)(2,1)S(1)}, bf16[272,128]{1,0:T(8,128)(2,1)S(1)}, u32[]{:S(2)}, u32[]{:S(2)}) collective-permute-start(bf16[272,128]{1,0:T(8,128)(2,1)S(1)} %get-tuple-element.34.own_ref), channel_id=1, source_target_pairs={{0,6},{2,0},{4,2},{6,4},{1,7},{3,1},{5,3},{7,5},{8,14},{10,8},{12,... | collective-permute-start | bytes 208904 | tf_op jit(solution)/shard_map/ppermute | solution.py:392
  9.5 0.1 reshape.32.routes_ref
  9.7 3.9 %routing.1 = (s32[256]{0:T(256)S(1)}, s32[384]{0:T(512)S(1)}) custom-call(s32[256]{0:T(256)S(1)} %reshape.32.routes_ref), custom_call_target="tpu_custom_call" | custom-call | tf_op jit(solution)/shard_map/routing/pallas_call | solution.py:66
  13.6 0.4 stage_x.1
  14.0 1.4 %collective-permute-start.3 = (bf16[272,128]{1,0:T(8,128)(2,1)S(1)}, bf16[272,128]{1,0:T(8,128)(2,1)S(1)}, u32[]{:S(2)}, u32[]{:S(2)}) collective-permute-start(bf16[272,128]{1,0:T(8,128)(2,1)S(1)} %get-tuple-element.40.own_ref), channel_id=1, source_target_pairs={{0,8},{8,16},{16,24},{24,0},{1,9},{9,17},{17,25},{25,1},{2,10},{10... | collective-permute-start | bytes 208904 | tf_op jit(solution)/shard_map/ppermute | solution.py:392
  15.4 2.6 %collective-permute-start.4 = (bf16[272,128]{1,0:T(8,128)(2,1)S(1)}, bf16[272,128]{1,0:T(8,128)(2,1)S(1)}, u32[]{:S(2)}, u32[]{:S(2)}) collective-permute-start(bf16[272,128]{1,0:T(8,128)(2,1)S(1)} %get-tuple-element.40.own_ref), channel_id=1, source_target_pairs={{0,16},{8,24},{16,0},{24,8},{1,17},{9,25},{17,1},{25,9},{2,18},{10... | collective-permute-start | bytes 208904 | tf_op jit(solution)/shard_map/ppermute | solution.py:392
  18.0 1.1 collective-permute-start.5
  19.1 0.8 within.1
  19.9 0.7 collective-permute-done.4.back2_ref
  20.6 1.5 %collective-permute-done.5.back3_ref = bf16[272,128]{1,0:T(8,128)(2,1)S(1)} collective-permute-done((bf16[272,128]{1,0:T(8,128)(2,1)S(1)}, bf16[272,128]{1,0:T(8,128)(2,1)S(1)}, u32[]{:S(2)}, u32[]{:S(2)}) %collective-permute-start.5) | collective-permute-done | bytes 69664 | tf_op jit(solution)/shard_map/ppermute | solution.py:392
  22.1 0.4 stage_y.1
  22.5 3.7 %collective-permute-start.6 = (bf16[272,128]{1,0:T(8,128)(2,1)S(1)}, bf16[272,128]{1,0:T(8,128)(2,1)S(1)}, u32[]{:S(2)}, u32[]{:S(2)}) collective-permute-start(bf16[272,128]{1,0:T(8,128)(2,1)S(1)} %get-tuple-element.48), channel_id=1, source_target_pairs={{0,32},{32,64},{64,96},{1,33},{33,65},{65,97},{2,34},{34,66},{66,9... | collective-permute-start | bytes 208904 | tf_op jit(solution)/shard_map/ppermute | solution.py:392
  26.2 5.2 %collective-permute-start.7 = (bf16[272,128]{1,0:T(8,128)(2,1)S(1)}, bf16[272,128]{1,0:T(8,128)(2,1)S(1)}, u32[]{:S(2)}, u32[]{:S(2)}) collective-permute-start(bf16[272,128]{1,0:T(8,128)(2,1)S(1)} %get-tuple-element.48), channel_id=1, source_target_pairs={{0,64},{32,96},{1,65},{33,97},{2,66},{34,98},{3,67},{35,99},{4,68}... | collective-permute-start | bytes 208904 | tf_op jit(solution)/shard_map/ppermute | solution.py:392
  31.4 1.3 %collective-permute-start.8 = (bf16[272,128]{1,0:T(8,128)(2,1)S(1)}, bf16[272,128]{1,0:T(8,128)(2,1)S(1)}, u32[]{:S(2)}, u32[]{:S(2)}) collective-permute-start(bf16[272,128]{1,0:T(8,128)(2,1)S(1)} %get-tuple-element.48), channel_id=1, source_target_pairs={{0,96},{1,97},{2,98},{3,99},{4,100},{5,101},{6,102},{7,103},{8,104... | collective-permute-start | bytes 208904 | tf_op jit(solution)/shard_map/ppermute | solution.py:392
  32.8 1.9 %collective-permute-done.8.back3_ref = bf16[272,128]{1,0:T(8,128)(2,1)S(1)} collective-permute-done((bf16[272,128]{1,0:T(8,128)(2,1)S(1)}, bf16[272,128]{1,0:T(8,128)(2,1)S(1)}, u32[]{:S(2)}, u32[]{:S(2)}) %collective-permute-start.8) | collective-permute-done | bytes 69664 | tf_op jit(solution)/shard_map/ppermute | solution.py:392
  34.7 0.7 finish.1
  35.4 2.9 %collective-permute-start.9 = (bf16[128,512]{1,0:T(8,128)(2,1)S(1)}, bf16[128,512]{1,0:T(8,128)(2,1)S(1)}, u32[]{:S(2)}, u32[]{:S(2)}) collective-permute-start(bf16[128,512]{1,0:T(8,128)(2,1)S(1)} %get-tuple-element.56), channel_id=1, source_target_pairs={{0,1},{1,0},{2,3},{3,2},{4,5},{5,4},{6,7},{7,6},{8,9},{9,8},{10,11... | collective-permute-start | bytes 393224 | tf_op jit(solution)/shard_map/ppermute | solution.py:464
  38.3 1.0 collective-permute-done.9.taken_ref
  39.3 2.2 %copy-done = bf16[1024,2048]{1,0:T(8,128)(2,1)S(1)} copy-done((bf16[1024,2048]{1,0:T(8,128)(2,1)S(1)}, bf16[1024,2048]{1,0:T(8,128)(2,1)}, u32[]{:S(2)}) %copy-start) | copy-done | bytes 4194328
  41.5 2.4 %project.1 = (bf16[128,2048]{1,0:T(8,128)(2,1)S(1)}, bf16[384,16,128]{2,1,0:T(8,128)(2,1)S(1)}) custom-call(s32[1]{0:T(128)} %bitcast.place_ref, s32[384]{0:T(512)S(1)} %get-tuple-element.36.owners_ref, bf16[128,512]{1,0:T(8,128)(2,1)S(1)} %get-tuple-element.55.kept_ref, bf16[128,512]{1,0:T(8,128)(2,1)S(1)} %collective-permute-done.9.taken_ref, ...), custom_call_target="tpu_custom_call" | custom-call | flops 800000000 | bytes 2000000 | tf_op jit(solution)/shard_map/project/pallas_call | solution.py:378
  43.9 32.2 %all_to_all.10 = bf16[128,48,128]{2,1,0:T(8,128)(2,1)S(1)} all-to-all(bf16[128,48,128]{2,1,0:T(8,128)(2,1)S(1)} %bitcast.11), channel_id=1, replica_groups=mesh['sp_0'=4,'sp_1'=4,'sp_2'=4,'tp'=2] {'sp_0','sp_1','sp_2','tp'}, dimensions={0} | all-to-all | bytes 3145728 | tf_op jit(solution)/shard_map/all_to_all | solution.py:478
  76.1 5.5 %experts.1 = bf16[384,16,128]{2,1,0:T(8,128)(2,1)} custom-call(bf16[384,16,128]{2,1,0:T(8,128)(2,1)S(1)} %bitcast.10, bf16[1,2048,512]{2,1,0:T(8,128)(2,1)S(1)} %copy-done.1, bf16[1,2048,512]{2,1,0:T(8,128)(2,1)S(1)} %copy-done.2, bf16[1,512,2048]{2,1,0:T(8,128)(2,1)S(1)} %copy-done.3), custom_call_target="tpu_custom_call" | custom-call | tf_op jit(solution)/shard_map/experts/pallas_call | solution.py:110
  81.6 4.5 %all-to-all-start.1 = ((bf16[128,48,128]{2,1,0:T(8,128)(2,1)}), bf16[128,48,128]{2,1,0:T(8,128)(2,1)S(1)}, u32[]{:S(2)}, u32[]{:S(2)}) async-start(bf16[128,48,128]{2,1,0:T(8,128)(2,1)} %bitcast.7), calls=%async_computation.1 | async-start | bytes 3145728 | tf_op jit(solution)/shard_map/all_to_all | solution.py:480
  86.2 0.1 copy.22
  86.4 24.7 %all-to-all-done.1 = bf16[128,48,128]{2,1,0:T(8,128)(2,1)S(1)} async-done(((bf16[128,48,128]{2,1,0:T(8,128)(2,1)}), bf16[128,48,128]{2,1,0:T(8,128)(2,1)S(1)}, u32[]{:S(2)}, u32[]{:S(2)}) %all-to-all-start.1) | async-done | bytes 1572896 | tf_op jit(solution)/shard_map/all_to_all | solution.py:480
  111.1 2.4 %combine.1 = bf16[128,2048]{1,0:T(8,128)(2,1)} custom-call(s32[256]{0:T(256)S(1)} %get-tuple-element.35.slots_ref, bf16[384,16,128]{2,1,0:T(8,128)(2,1)S(1)} %bitcast.9, bf16[128,2048]{1,0:T(8,128)(2,1)S(1)} %get-tuple-element.58.merged_ref, f32[128,2]{1,0:T(8,128)S(1)} %broadcast_divide_fusion.weights_ref), custom_call_target="tpu_custom_call" | custom-call | tf_op jit(solution)/shard_map/combine/pallas_call | solution.py:150
  (39 shorter events, 0.3 us)
Async XLA Ops:
  0.0 0.9 copy-start.6
  1.0 0.9 copy-start.9
  1.9 0.9 copy-start.10
  2.8 6.6 %copy-start.14 = (s32[128,2]{0,1:T(2,128)S(1)}, s32[128,2]{0,1:T(2,128)}, u32[]{:S(2)}) copy-start(s32[128,2]{0,1:T(2,128)} %param.24) | copy-start | bytes 3076
  3.7 15.4 %copy-start.7 = (bf16[256,512]{1,0:T(8,128)(2,1)S(1)}, bf16[256,512]{1,0:T(8,128)(2,1)}, u32[]{:S(2)}) copy-start(bf16[256,512]{1,0:T(8,128)(2,1)} %values_ref.3) | copy-start | bytes 786436
  3.7 15.4 %copy-start.11 = (bf16[256,256]{1,0:T(8,128)(2,1)S(1)}, bf16[256,256]{1,0:T(8,128)(2,1)}, u32[]{:S(2)}) copy-start(bf16[256,256]{1,0:T(8,128)(2,1)} %keys_ref.3) | copy-start | bytes 393220
  3.7 15.4 %copy-start.12 = (bf16[256,256]{1,0:T(8,128)(2,1)S(1)}, bf16[256,256]{1,0:T(8,128)(2,1)}, u32[]{:S(2)}) copy-start(bf16[256,256]{1,0:T(8,128)(2,1)} %queries_ref.1) | copy-start | bytes 393220
  3.7 9.9 %collective-permute-start = (bf16[272,128]{1,0:T(8,128)(2,1)S(1)}, bf16[272,128]{1,0:T(8,128)(2,1)S(1)}, u32[]{:S(2)}, u32[]{:S(2)}) collective-permute-start(bf16[272,128]{1,0:T(8,128)(2,1)S(1)} %get-tuple-element.34.own_ref), channel_id=1, source_target_pairs={{0,2},{2,4},{4,6},{6,0},{1,3},{3,5},{5,7},{7,1},{8,10},{10,12},{12... | collective-permute-start | bytes 208904 | tf_op jit(solution)/shard_map/ppermute | solution.py:392
  5.8 7.8 %collective-permute-start.1 = (bf16[272,128]{1,0:T(8,128)(2,1)S(1)}, bf16[272,128]{1,0:T(8,128)(2,1)S(1)}, u32[]{:S(2)}, u32[]{:S(2)}) collective-permute-start(bf16[272,128]{1,0:T(8,128)(2,1)S(1)} %get-tuple-element.34.own_ref), channel_id=1, source_target_pairs={{0,4},{2,6},{4,0},{6,2},{1,5},{3,7},{5,1},{7,3},{8,12},{10,14},{12... | collective-permute-start | bytes 208904 | tf_op jit(solution)/shard_map/ppermute | solution.py:392
  8.2 5.4 %collective-permute-start.2 = (bf16[272,128]{1,0:T(8,128)(2,1)S(1)}, bf16[272,128]{1,0:T(8,128)(2,1)S(1)}, u32[]{:S(2)}, u32[]{:S(2)}) collective-permute-start(bf16[272,128]{1,0:T(8,128)(2,1)S(1)} %get-tuple-element.34.own_ref), channel_id=1, source_target_pairs={{0,6},{2,0},{4,2},{6,4},{1,7},{3,1},{5,3},{7,5},{8,14},{10,8},{12,... | collective-permute-start | bytes 208904 | tf_op jit(solution)/shard_map/ppermute | solution.py:392
  14.0 5.8 %collective-permute-start.3 = (bf16[272,128]{1,0:T(8,128)(2,1)S(1)}, bf16[272,128]{1,0:T(8,128)(2,1)S(1)}, u32[]{:S(2)}, u32[]{:S(2)}) collective-permute-start(bf16[272,128]{1,0:T(8,128)(2,1)S(1)} %get-tuple-element.40.own_ref), channel_id=1, source_target_pairs={{0,8},{8,16},{16,24},{24,0},{1,9},{9,17},{17,25},{25,1},{2,10},{10... | collective-permute-start | bytes 208904 | tf_op jit(solution)/shard_map/ppermute | solution.py:392
  15.4 5.2 %collective-permute-start.4 = (bf16[272,128]{1,0:T(8,128)(2,1)S(1)}, bf16[272,128]{1,0:T(8,128)(2,1)S(1)}, u32[]{:S(2)}, u32[]{:S(2)}) collective-permute-start(bf16[272,128]{1,0:T(8,128)(2,1)S(1)} %get-tuple-element.40.own_ref), channel_id=1, source_target_pairs={{0,16},{8,24},{16,0},{24,8},{1,17},{9,25},{17,1},{25,9},{2,18},{10... | collective-permute-start | bytes 208904 | tf_op jit(solution)/shard_map/ppermute | solution.py:392
  18.0 4.1 %collective-permute-start.5 = (bf16[272,128]{1,0:T(8,128)(2,1)S(1)}, bf16[272,128]{1,0:T(8,128)(2,1)S(1)}, u32[]{:S(2)}, u32[]{:S(2)}) collective-permute-start(bf16[272,128]{1,0:T(8,128)(2,1)S(1)} %get-tuple-element.40.own_ref), channel_id=1, source_target_pairs={{0,24},{8,0},{16,8},{24,16},{1,25},{9,1},{17,9},{25,17},{2,26},{10... | collective-permute-start | bytes 208904 | tf_op jit(solution)/shard_map/ppermute | solution.py:392
  19.8 14.8 %copy-start.8 = (bf16[256,512]{1,0:T(8,128)(2,1)S(1)}, bf16[256,512]{1,0:T(8,128)(2,1)}, u32[]{:S(2)}) copy-start(bf16[256,512]{1,0:T(8,128)(2,1)} %out_gate_ref.1) | copy-start | bytes 786436
  19.9 14.8 %copy-start.13 = (f32[128]{0:T(128)S(1)}, f32[128]{0:T(128)}, u32[]{:S(2)}) copy-start(f32[128]{0:T(128)} %param.21) | copy-start | bytes 1540
  22.5 16.8 %copy-start.4 = (bf16[128,2048]{1,0:T(8,128)(2,1)S(1)}, bf16[128,2048]{1,0:T(8,128)(2,1)}, u32[]{:S(2)}) copy-start(bf16[128,2048]{1,0:T(8,128)(2,1)} %residual_ref.1) | copy-start | bytes 1572868
  22.5 16.8 %copy-start.5 = (f32[2048]{0:T(1024)S(1)}, f32[2048]{0:T(1024)}, u32[]{:S(2)}) copy-start(f32[2048]{0:T(1024)} %param.23) | copy-start | bytes 24580
  22.5 10.2 %collective-permute-start.6 = (bf16[272,128]{1,0:T(8,128)(2,1)S(1)}, bf16[272,128]{1,0:T(8,128)(2,1)S(1)}, u32[]{:S(2)}, u32[]{:S(2)}) collective-permute-start(bf16[272,128]{1,0:T(8,128)(2,1)S(1)} %get-tuple-element.48), channel_id=1, source_target_pairs={{0,32},{32,64},{64,96},{1,33},{33,65},{65,97},{2,34},{34,66},{66,9... | collective-permute-start | bytes 208904 | tf_op jit(solution)/shard_map/ppermute | solution.py:392
  26.2 6.6 %collective-permute-start.7 = (bf16[272,128]{1,0:T(8,128)(2,1)S(1)}, bf16[272,128]{1,0:T(8,128)(2,1)S(1)}, u32[]{:S(2)}, u32[]{:S(2)}) collective-permute-start(bf16[272,128]{1,0:T(8,128)(2,1)S(1)} %get-tuple-element.48), channel_id=1, source_target_pairs={{0,64},{32,96},{1,65},{33,97},{2,66},{34,98},{3,67},{35,99},{4,68}... | collective-permute-start | bytes 208904 | tf_op jit(solution)/shard_map/ppermute | solution.py:392
  31.4 3.3 %collective-permute-start.8 = (bf16[272,128]{1,0:T(8,128)(2,1)S(1)}, bf16[272,128]{1,0:T(8,128)(2,1)S(1)}, u32[]{:S(2)}, u32[]{:S(2)}) collective-permute-start(bf16[272,128]{1,0:T(8,128)(2,1)S(1)} %get-tuple-element.48), channel_id=1, source_target_pairs={{0,96},{1,97},{2,98},{3,99},{4,100},{5,101},{6,102},{7,103},{8,104... | collective-permute-start | bytes 208904 | tf_op jit(solution)/shard_map/ppermute | solution.py:392
  35.4 3.9 %collective-permute-start.9 = (bf16[128,512]{1,0:T(8,128)(2,1)S(1)}, bf16[128,512]{1,0:T(8,128)(2,1)S(1)}, u32[]{:S(2)}, u32[]{:S(2)}) collective-permute-start(bf16[128,512]{1,0:T(8,128)(2,1)S(1)} %get-tuple-element.56), channel_id=1, source_target_pairs={{0,1},{1,0},{2,3},{3,2},{4,5},{5,4},{6,7},{7,6},{8,9},{9,8},{10,11... | collective-permute-start | bytes 393224 | tf_op jit(solution)/shard_map/ppermute | solution.py:464
  39.3 2.2 %copy-start = (bf16[1024,2048]{1,0:T(8,128)(2,1)S(1)}, bf16[1024,2048]{1,0:T(8,128)(2,1)}, u32[]{:S(2)}) copy-start(bf16[1024,2048]{1,0:T(8,128)(2,1)} %weight_ref.1) | copy-start | bytes 12582916
  41.5 34.6 %copy-start.2 = (bf16[1,2048,512]{2,1,0:T(8,128)(2,1)S(1)}, bf16[1,2048,512]{2,1,0:T(8,128)(2,1)}, u32[]{:S(2)}) copy-start(bf16[1,2048,512]{2,1,0:T(8,128)(2,1)} %up.1) | copy-start | bytes 6291460
  41.5 34.6 %copy-start.3 = (bf16[1,512,2048]{2,1,0:T(8,128)(2,1)S(1)}, bf16[1,512,2048]{2,1,0:T(8,128)(2,1)}, u32[]{:S(2)}) copy-start(bf16[1,512,2048]{2,1,0:T(8,128)(2,1)} %down.1) | copy-start | bytes 6291460
  43.9 32.2 %copy-start.1 = (bf16[1,2048,512]{2,1,0:T(8,128)(2,1)S(1)}, bf16[1,2048,512]{2,1,0:T(8,128)(2,1)}, u32[]{:S(2)}) copy-start(bf16[1,2048,512]{2,1,0:T(8,128)(2,1)} %gate.1) | copy-start | bytes 6291460
  81.6 4.5 %copy-start.15 = (f32[128,2]{0,1:T(2,128)S(1)}, f32[128,2]{0,1:T(2,128)}, u32[]{:S(2)}) copy-start(f32[128,2]{0,1:T(2,128)} %param.26) | copy-start | bytes 3076
  81.6 4.5 %copy-start.16 = (f32[128]{0:T(128)S(1)}, f32[128]{0:T(128)}, u32[]{:S(2)}) copy-start(f32[128]{0:T(128)} %param.25) | copy-start | bytes 1540
  81.6 29.5 %all-to-all-start.1 = ((bf16[128,48,128]{2,1,0:T(8,128)(2,1)}), bf16[128,48,128]{2,1,0:T(8,128)(2,1)S(1)}, u32[]{:S(2)}, u32[]{:S(2)}) async-start(bf16[128,48,128]{2,1,0:T(8,128)(2,1)} %bitcast.7), calls=%async_computation.1 | async-start | bytes 3145728 | tf_op jit(solution)/shard_map/all_to_all | solution.py:480

commit v4 on v3

--- a/solution.py
+++ b/solution.py
@@ -16,7 +16,7 @@
 
 VMEM_SPEC = pl.BlockSpec(memory_space=pltpu.VMEM)
 SMEM_SPEC = pl.BlockSpec(memory_space=pltpu.SMEM)
-ANY_SPEC = pl.BlockSpec(memory_space=pl.ANY)
+HBM_SPEC = pl.BlockSpec(memory_space=pl.ANY)
 SUB = 16
 LANES = 128
 SWAP = SUB * SUB
@@ -29,63 +29,74 @@
     return (partner == column).astype(jnp.float32).astype(jnp.bfloat16)
 
 
-def exchange(swap, block):
-    return jnp.dot(swap, block, preferred_element_type=jnp.float32)
-
-
-def routing_kernel(routes_ref, slots_ref, owners_ref, counts):
-    experts_total = counts.shape[0]
-    slot_count = owners_ref.shape[0]
-    route_count = routes_ref.shape[0]
-    capacity = slot_count // experts_total
-
-    def clear_counts(i, carry):
-        counts[i] = 0
-        return carry
-
-    def clear_owners(i, carry):
-        owners_ref[i] = 0
-        return carry
-
-    def place(i, carry):
-        expert = routes_ref[i]
-        used = counts[expert]
-        counts[expert] = used + 1
-        slot = expert * capacity + used
-        slots_ref[i] = slot
-        owners_ref[slot] = i // 2
-        return carry
-
-    lax.fori_loop(0, experts_total, clear_counts, 0, unroll=8)
-    lax.fori_loop(0, slot_count, clear_owners, 0, unroll=8)
-    lax.fori_loop(0, route_count, place, 0, unroll=4)
-
-
-def routing(routes, experts_total, capacity):
-    flattened = routes.reshape(-1)
-    return pl.pallas_call(
+def exchange(swap, blocks):
+    turned = jnp.dot(swap, jnp.concatenate(blocks, axis=1), preferred_element_type=jnp.float32)
+    return [turned[:, k * LANES : (k + 1) * LANES] for k in range(len(blocks))]
+
+
+def stack_chunks(ref, g):
+    width = ref.shape[1]
+    return jnp.concatenate(
+        [ref[g * SUB : (g + 1) * SUB, j * LANES : (j + 1) * LANES] for j in range(width // LANES)], axis=0
+    )
+
+
+def routing_kernel(routes_ref, group_ref, expert_ref, slots_ref, owners_ref, weights_ref):
+    choices, rows = routes_ref.shape
+    capacity = 3
+    bf16 = jnp.bfloat16
+    expert = lax.broadcasted_iota(jnp.int32, (LANES, rows), 0)
+    token = lax.broadcasted_iota(jnp.int32, (LANES, rows), 1)
+    named = [expert == routes_ref[k : k + 1] for k in range(choices)]
+    named = [one.astype(jnp.float32) for one in named]
+    source = lax.broadcasted_iota(jnp.int32, (rows, rows), 0)
+    target = lax.broadcasted_iota(jnp.int32, (rows, rows), 1)
+    before = (source < target).astype(jnp.float32).astype(bf16)
+    used = jnp.dot(sum(named).astype(bf16), before, preferred_element_type=jnp.float32)
+    place = lax.broadcasted_iota(jnp.int32, (8, rows), 0).astype(jnp.float32)
+    name = lax.broadcasted_iota(jnp.int32, (8, rows), 1).astype(jnp.float32)
+    owners = jnp.zeros((8, LANES), jnp.float32)
+    for k in range(choices):
+        rank = jnp.sum(named[k] * used, axis=0, keepdims=True)
+        slots_ref[k : k + 1] = routes_ref[k : k + 1] * capacity + rank.astype(jnp.int32)
+        owned = jnp.where(place == rank, name, 0.0).astype(bf16)
+        owners = owners + lax.dot_general(
+            owned, named[k].astype(bf16), (((1,), (1,)), ((), ())), preferred_element_type=jnp.float32
+        )
+    owners_ref[...] = owners.astype(jnp.int32)
+    score = expert_ref[...]
+    weights = group_ref[...] * score / jnp.sum(score, axis=0, keepdims=True)
+    for k in range(choices):
+        spread = jnp.broadcast_to(weights[k : k + 1], (LANES, rows))
+        weights_ref[k] = spread.T
+
+
+def routing(routes, group_score, expert_score):
+    rows, choices = routes.shape
+    return call(
         routing_kernel,
-        out_shape=(
-            jax.ShapeDtypeStruct(flattened.shape, jnp.int32),
-            jax.ShapeDtypeStruct((experts_total * capacity,), jnp.int32),
+        "routing",
+        (
+            shape_of((choices, rows), jnp.int32),
+            shape_of((8, LANES), jnp.int32),
+            shape_of((choices, rows, LANES), jnp.float32),
         ),
-        in_specs=[SMEM_SPEC],
-        out_specs=(SMEM_SPEC, SMEM_SPEC),
-        scratch_shapes=[pltpu.SMEM((experts_total,), jnp.int32)],
-        compiler_params=limited(1),
-        name="routing",
-    )(flattened)
+        (routes.T, group_score.reshape(1, rows), expert_score.T),
+        room=2,
+    )
 
 
 def experts_kernel(rows_ref, gate, up, down, out_ref, rows_in, inner, served):
     swap = swap_matrix()
     count, width = rows_in.shape
     hidden = inner.shape[1]
-    for g in range(count // SUB):
-        block = rows_ref[g * SUB : (g + 1) * SUB].reshape(SWAP, LANES)
-        turned = exchange(swap, block).astype(jnp.bfloat16)
-        for j in range(width // LANES):
-            rows_in[g * SUB : (g + 1) * SUB, j * LANES : (j + 1) * LANES] = turned[j * SUB : (j + 1) * SUB]
+    groups = count // SUB
+    for g in range(0, groups, 2):
+        blocks = [rows_ref[k * SUB : (k + 1) * SUB].reshape(SWAP, LANES) for k in (g, g + 1)]
+        for k, turned in zip((g, g + 1), exchange(swap, blocks)):
+            turned = turned.astype(jnp.bfloat16)
+            for j in range(width // LANES):
+                rows_in[k * SUB : (k + 1) * SUB, j * LANES : (j + 1) * LANES] = turned[j * SUB : (j + 1) * SUB]
     tile = 256
     for n in range(hidden // tile):
         part = slice(n * tile, (n + 1) * tile)
@@ -95,13 +106,10 @@
     for n in range(width // tile):
         part = slice(n * tile, (n + 1) * tile)
         served[:, part] = jnp.dot(inner[...], down[0, :, part], preferred_element_type=jnp.float32).astype(jnp.bfloat16)
-    for g in range(count // SUB):
-        stacked = jnp.concatenate(
-            [served[g * SUB : (g + 1) * SUB, j * LANES : (j + 1) * LANES] for j in range(width // LANES)], axis=0
-        )
-        out_ref[g * SUB : (g + 1) * SUB] = (
-            exchange(swap, stacked).astype(jnp.bfloat16).reshape(SUB, SUB, LANES)
-        )
+    for g in range(0, groups, 2):
+        blocks = [stack_chunks(served, k) for k in (g, g + 1)]
+        for k, turned in zip((g, g + 1), exchange(swap, blocks)):
+            out_ref[k * SUB : (k + 1) * SUB] = turned.astype(jnp.bfloat16).reshape(SUB, SUB, LANES)
 
 
 def experts(arrived, gate_weight, up_weight, down_weight):
@@ -127,35 +135,32 @@
     rows, width = merged_ref.shape
 
     def copy_row(i, carry):
-        picked[0, i] = returned_ref[slots_ref[2 * i]]
-        picked[1, i] = returned_ref[slots_ref[2 * i + 1]]
+        picked[0, i] = returned_ref[slots_ref[0, i]]
+        picked[1, i] = returned_ref[slots_ref[1, i]]
         return carry
 
     lax.fori_loop(0, rows, copy_row, 0, unroll=8)
     for g in range(rows // SUB):
         group = slice(g * SUB, (g + 1) * SUB)
-        first = exchange(swap, picked[0, group].reshape(SWAP, LANES))
-        second = exchange(swap, picked[1, group].reshape(SWAP, LANES))
-        weight_first = jnp.broadcast_to(weights_ref[group, 0:1], (SUB, LANES))
-        weight_second = jnp.broadcast_to(weights_ref[group, 1:2], (SUB, LANES))
+        first, second = exchange(swap, [picked[k, group].reshape(SWAP, LANES) for k in range(2)])
         for j in range(width // LANES):
             lanes = slice(j * LANES, (j + 1) * LANES)
             part = slice(j * SUB, (j + 1) * SUB)
-            total = weight_first * first[part] + weight_second * second[part]
+            total = weights_ref[0, group] * first[part] + weights_ref[1, group] * second[part]
             out_ref[group, lanes] = (merged_ref[group, lanes].astype(jnp.float32) + total).astype(jnp.bfloat16)
 
 
 def combine(slots, returned, merged, weights):
     rows = merged.shape[0]
-    return pl.pallas_call(
+    return call(
         combine_kernel,
-        out_shape=jax.ShapeDtypeStruct(merged.shape, jnp.bfloat16),
-        in_specs=[SMEM_SPEC, VMEM_SPEC, VMEM_SPEC, VMEM_SPEC],
-        out_specs=VMEM_SPEC,
-        scratch_shapes=[pltpu.VMEM((2, rows, SUB, LANES), jnp.bfloat16)],
-        compiler_params=limited(8),
-        name="combine",
-    )(slots, returned, merged, weights)
+        "combine",
+        shape_of(merged.shape, jnp.bfloat16),
+        (slots, returned, merged, weights),
+        1,
+        [pltpu.VMEM((2, rows, SUB, LANES), jnp.bfloat16)],
+        room=8,
+    )
 
 
 def pieces(value, count):
@@ -173,7 +178,16 @@
     )
 
 
-def state_kernel(keys_ref, values_ref, logits_ref, running_ref, states_ref, message_ref):
+def state_kernel(keys_hbm, values_hbm, logits_hbm, running_ref, states_ref, message_ref, keys_ref, values_ref, logits_ref, sems):
+    copies = [
+        pltpu.make_async_copy(source, target, sems.at[k])
+        for k, (source, target) in enumerate(
+            ((logits_hbm, logits_ref), (keys_hbm, keys_ref), (values_hbm, values_ref))
+        )
+    ]
+    for copy in copies:
+        copy.start()
+    copies[0].wait()
     length, channels = keys_ref.shape
     blocks = length // BLOCK
     pairs = channels // LANES
@@ -191,6 +205,8 @@
     lane = lax.broadcasted_iota(jnp.int32, (length, blocks * LANES), 1)
     member = (token // BLOCK == lane // LANES).astype(jnp.float32).astype(jnp.bfloat16)
     block_decay = jnp.exp(sum(product(part, member, 0, 0) for part in parts))
+    copies[1].wait()
+    copies[2].wait()
     states = [jnp.zeros((LANES, VALUE_DIM), jnp.float32)] * pairs
     total = jnp.zeros((1, channels), jnp.float32)
     for n in range(blocks):
@@ -349,21 +365,28 @@
         square = square + jnp.sum(widened * widened, axis=1, keepdims=True)
     scale = lax.rsqrt(square / width + 1e-06)
     swap = swap_matrix()
-    for g in range(rows // SUB):
-        group = slice(g * SUB, (g + 1) * SUB)
-        stacked = []
-        for j in range(width // LANES):
-            lanes = slice(j * LANES, (j + 1) * LANES)
-            widened = merged_ref[group, lanes].astype(jnp.float32)
-            stacked.append((widened * scale[group] * norm_gain_ref[:, lanes]).astype(jnp.bfloat16))
-        turned = exchange(swap, jnp.concatenate(stacked, axis=0)).astype(jnp.bfloat16)
-        chunked[group] = turned.reshape(SUB, SUB, LANES)
-
-    def copy_row(slot, carry):
-        outgoing_ref[slot] = chunked[owners_ref[slot]]
+    for g in range(0, rows // SUB, 2):
+        blocks = []
+        for k in (g, g + 1):
+            group = slice(k * SUB, (k + 1) * SUB)
+            stacked = []
+            for j in range(width // LANES):
+                lanes = slice(j * LANES, (j + 1) * LANES)
+                widened = merged_ref[group, lanes].astype(jnp.float32)
+                stacked.append((widened * scale[group] * norm_gain_ref[:, lanes]).astype(jnp.bfloat16))
+            blocks.append(jnp.concatenate(stacked, axis=0))
+        for k, turned in zip((g, g + 1), exchange(swap, blocks)):
+            chunked[k * SUB : (k + 1) * SUB] = turned.astype(jnp.bfloat16).reshape(SUB, SUB, LANES)
+
+    experts_total = owners_ref.shape[1]
+    capacity = outgoing_ref.shape[0] // experts_total
+
+    def copy_rows(expert, carry):
+        for place in range(capacity):
+            outgoing_ref[capacity * expert + place] = chunked[owners_ref[place, expert]]
         return carry
 
-    lax.fori_loop(0, outgoing_ref.shape[0], copy_row, 0, unroll=16)
+    lax.fori_loop(0, experts_total, copy_rows, 0, unroll=8)
 
 
 def shape_of(shape, dtype):
@@ -371,14 +394,14 @@
 
 
 def limited(mebibytes):
-    return pltpu.CompilerParams(vmem_limit_bytes=mebibytes << 20)
-
-
-def call(kernel, name, outs, operands, scalars=0, scratch=(), cost=2000000, room=6):
+    return pltpu.CompilerParams(vmem_limit_bytes=int(mebibytes * 1048576))
+
+
+def call(kernel, name, outs, operands, scalars=0, scratch=(), cost=10000000, room=6, far=False):
     return pl.pallas_call(
         kernel,
         out_shape=outs,
-        in_specs=[SMEM_SPEC] * scalars + [VMEM_SPEC] * (len(operands) - scalars),
+        in_specs=[SMEM_SPEC] * scalars + [HBM_SPEC if far else VMEM_SPEC] * (len(operands) - scalars),
         out_specs=jax.tree.map(lambda _: VMEM_SPEC, outs),
         scratch_shapes=list(scratch),
         cost_estimate=pl.CostEstimate(flops=cost * 400, bytes_accessed=cost, transcendentals=0),
@@ -431,12 +454,20 @@
             message_shape,
         ),
         (key_rows, value_rows, gate_logits),
+        scratch=[
+            pltpu.VMEM(key_rows.shape, bf16),
+            pltpu.VMEM(value_rows.shape, bf16),
+            pltpu.VMEM(gate_logits.shape, bf16),
+            pltpu.SemaphoreType.DMA((3,)),
+        ],
+        room=53.8,
+        far=True,
     )
     experts_total = lax.axis_size(SP_TP)
     capacity = 3 * row_count // experts_total
-    slots, owners = routing(routes, experts_total, capacity)
+    slots, owners, weights = routing(routes, group_score, expert_score)
     behind = from_behind(message, "sp_2", True)
-    slots, owners, *behind = lax.optimization_barrier((slots, owners, *behind))
+    slots, owners, weights, *behind = lax.optimization_barrier((slots, owners, weights, *behind))
     before_x, decay_x, message_x = call(
         stage_kernel, "stage_x", (state_shape, state_shape, message_shape), (x, message, *behind), 1
     )
@@ -478,7 +509,6 @@
     arrived = lax.all_to_all(outgoing.reshape(block), SP_TP, split_axis=0, concat_axis=0, tiled=True)
     served = experts(arrived.reshape(outgoing.shape), gate_weight, up_weight, down_weight)
     returned = lax.all_to_all(served.reshape(block), SP_TP, split_axis=0, concat_axis=0, tiled=True)
-    weights = group_score[:, None] * expert_score / jnp.sum(expert_score, axis=1, keepdims=True)
     return combine(slots, returned.reshape(outgoing.shape), merged, weights)
 
 

time: 114 us -> 105 us (0.921)
  blocking collectives: 32.2 us -> 58.6 us
  waiting for transfers between devices: 29.9 us -> 10.3 us
  starting transfers between devices: 28.4 us -> 22.2 us
  local copies, waits for them, and re-layouts: 5.37 us -> 0.07 us
  Pallas kernels: 17.4 us -> 13.7 us
    all_to_all x0 -> x1, blocking collectives: none -> 28.9 us  [local(): lax.all_to_all(served.reshape(block), SP_TP, split_axis=0, concat_axis=0,...]
    all_to_all x1 -> x0, waiting for transfers between devices: 24.7 us -> none  [local(): lax.all_to_all(served.reshape(block), SP_TP, split_axis=0, concat_axis=0,...]
    pallas_call x2 -> x0, Pallas kernels: 6.37 us -> none  [the longest x1 3.93 us: routing(): pl.pallas_call(routing_kernel, out_shape=(jax.ShapeDtypeStruct(flattened....]
    ppermute x9, waiting for transfers between devices: 4.16 us -> 9.28 us  [from_behind(): lax.ppermute(message, axis, [(i, (i + k) % RING) for i in range(RING) if...]
    unnamed x35 -> x32, local copies, waits for them, and re-layouts: 5.12 us -> 0.07 us
    pallas_call x6 -> x8, Pallas kernels: 5.55 us -> 10.2 us  [call(): pl.pallas_call(kernel, out_shape=outs, in_specs=[SMEM_SPEC] * scalars + [...]
    all_to_all x1 -> x0, starting transfers between devices: 4.53 us -> none  [local(): lax.all_to_all(served.reshape(block), SP_TP, split_axis=0, concat_axis=0,...]
    ppermute x9, starting transfers between devices: 20.9 us -> 17.8 us  [from_behind(): lax.ppermute(message, axis, [(i, (i + k) % RING) for i in range(RING) if...]
  transfers between devices with their start and end apart: 11 -> 10, of which waited for: 5 -> 6; matrix products, arithmetic and copies ran while one was open for 0% -> 0% of each run, Pallas kernels for 4% -> 1%
where the time goes in v4:
time: 105 us
  blocking collectives  58.6 us (56%)
  starting transfers between devices  22.2 us (21%)
  Pallas kernels  13.7 us (13%)
  waiting for transfers between devices  10.3 us (10%)
    all_to_all x1, blocking collectives, local(): lax.all_to_all(outgoing.reshape(block), SP_TP, split_axis=0, concat_axis=...  29.7 us
    all_to_all x1, blocking collectives, local(): lax.all_to_all(served.reshape(block), SP_TP, split_axis=0, concat_axis=0,...  28.9 us
    ppermute x9, starting transfers between devices, from_behind(): lax.ppermute(message, axis, [(i, (i + k) % RING) for i in range(RING) if...  17.8 us
    pallas_call x8, Pallas kernels, call(): pl.pallas_call(kernel, out_shape=outs, in_specs=[SMEM_SPEC] * scalars + [...  10.2 us
    ppermute x9, waiting for transfers between devices, from_behind(): lax.ppermute(message, axis, [(i, (i + k) % RING) for i in range(RING) if...  9.28 us
    ppermute x1, starting transfers between devices, local(): taken = lax.ppermute(given, 'tp', [(0, 1), (1, 0)])  4.46 us
    pallas_call x1, Pallas kernels, experts(): pl.pallas_call(experts_kernel, out_shape=jax.ShapeDtypeStruct(arrived.sha...  3.51 us
  transfers between devices with their start and end apart: 10, of which 6 were waited for; matrix products, arithmetic and copies ran while one was open for 0% of the time, Pallas kernels for 1%

profile of v4, /device:TPU:1, one launch (start us, length us, event | category | flops | bytes accessed | tf_op | source)
XLA Modules:
  0.0 105.1 jit_solution(8125725679760338900)
XLA Ops:
  0.0 2.8 %local_state.1 = (f32[256,256]{1,0:T(8,128)}, bf16[2,4,128,128]{3,2,1,0:T(8,128)(2,1)}, bf16[272,128]{1,0:T(8,128)(2,1)S(1)}) custom-call(bf16[256,256]{1,0:T(8,128)(2,1)} %keys_ref.1, bf16[256,512]{1,0:T(8,128)(2,1)} %values_ref.1, bf16[256,256]{1,0:T(8,128)(2,1)} %logits_hbm.1), custom_call_target="tpu_custom_call" | custom-call | flops 4000000000 | bytes 10000000 | tf_op jit(solution)/shard_map/local_state/pallas_call | solution.py:401
  2.8 3.4 %collective-permute-start.2 = (bf16[272,128]{1,0:T(8,128)(2,1)S(1)}, bf16[272,128]{1,0:T(8,128)(2,1)S(1)}, u32[]{:S(2)}, u32[]{:S(2)}) collective-permute-start(bf16[272,128]{1,0:T(8,128)(2,1)S(1)} %get-tuple-element.37.own_ref), channel_id=1, source_target_pairs={{0,6},{2,0},{4,2},{6,4},{1,7},{3,1},{5,3},{7,5},{8,14},{10,8},{12,... | collective-permute-start | bytes 208904 | tf_op jit(solution)/shard_map/ppermute | solution.py:415
  6.2 0.5 collective-permute-start.1
  6.7 0.6 collective-permute-start
  7.3 0.3 routing.1
  7.6 3.3 %collective-permute-done.1.back2_ref = bf16[272,128]{1,0:T(8,128)(2,1)S(1)} collective-permute-done((bf16[272,128]{1,0:T(8,128)(2,1)S(1)}, bf16[272,128]{1,0:T(8,128)(2,1)S(1)}, u32[]{:S(2)}, u32[]{:S(2)}) %collective-permute-start.1) | collective-permute-done | bytes 69664 | tf_op jit(solution)/shard_map/ppermute | solution.py:415
  10.9 1.1 %collective-permute-done.back1_ref = bf16[272,128]{1,0:T(8,128)(2,1)S(1)} collective-permute-done((bf16[272,128]{1,0:T(8,128)(2,1)S(1)}, bf16[272,128]{1,0:T(8,128)(2,1)S(1)}, u32[]{:S(2)}, u32[]{:S(2)}) %collective-permute-start) | collective-permute-done | bytes 69664 | tf_op jit(solution)/shard_map/ppermute | solution.py:415
  12.0 0.4 stage_x.1
  12.4 2.8 %collective-permute-start.5 = (bf16[272,128]{1,0:T(8,128)(2,1)S(1)}, bf16[272,128]{1,0:T(8,128)(2,1)S(1)}, u32[]{:S(2)}, u32[]{:S(2)}) collective-permute-start(bf16[272,128]{1,0:T(8,128)(2,1)S(1)} %get-tuple-element.43.own_ref), channel_id=1, source_target_pairs={{0,24},{8,0},{16,8},{24,16},{1,25},{9,1},{17,9},{25,17},{2,26},{10... | collective-permute-start | bytes 208904 | tf_op jit(solution)/shard_map/ppermute | solution.py:415
  15.2 0.3 collective-permute-start.4
  15.5 0.7 collective-permute-start.3
  16.3 0.8 within.1
  17.0 0.0 collective-permute-done.5.back3_ref
  17.0 2.9 %collective-permute-done.4.back2_ref = bf16[272,128]{1,0:T(8,128)(2,1)S(1)} collective-permute-done((bf16[272,128]{1,0:T(8,128)(2,1)S(1)}, bf16[272,128]{1,0:T(8,128)(2,1)S(1)}, u32[]{:S(2)}, u32[]{:S(2)}) %collective-permute-start.4) | collective-permute-done | bytes 69664 | tf_op jit(solution)/shard_map/ppermute | solution.py:415
  19.9 0.7 collective-permute-done.3.back1_ref
  20.6 0.4 stage_y.1
  21.0 5.7 %collective-permute-start.8 = (bf16[272,128]{1,0:T(8,128)(2,1)S(1)}, bf16[272,128]{1,0:T(8,128)(2,1)S(1)}, u32[]{:S(2)}, u32[]{:S(2)}) collective-permute-start(bf16[272,128]{1,0:T(8,128)(2,1)S(1)} %get-tuple-element.51), channel_id=1, source_target_pairs={{0,96},{1,97},{2,98},{3,99},{4,100},{5,101},{6,102},{7,103},{8,104... | collective-permute-start | bytes 208904 | tf_op jit(solution)/shard_map/ppermute | solution.py:415
  26.7 1.3 %collective-permute-start.7 = (bf16[272,128]{1,0:T(8,128)(2,1)S(1)}, bf16[272,128]{1,0:T(8,128)(2,1)S(1)}, u32[]{:S(2)}, u32[]{:S(2)}) collective-permute-start(bf16[272,128]{1,0:T(8,128)(2,1)S(1)} %get-tuple-element.51), channel_id=1, source_target_pairs={{0,64},{32,96},{1,65},{33,97},{2,66},{34,98},{3,67},{35,99},{4,68}... | collective-permute-start | bytes 208904 | tf_op jit(solution)/shard_map/ppermute | solution.py:415
  28.0 2.5 %collective-permute-start.6 = (bf16[272,128]{1,0:T(8,128)(2,1)S(1)}, bf16[272,128]{1,0:T(8,128)(2,1)S(1)}, u32[]{:S(2)}, u32[]{:S(2)}) collective-permute-start(bf16[272,128]{1,0:T(8,128)(2,1)S(1)} %get-tuple-element.51), channel_id=1, source_target_pairs={{0,32},{32,64},{64,96},{1,33},{33,65},{65,97},{2,34},{34,66},{66,9... | collective-permute-start | bytes 208904 | tf_op jit(solution)/shard_map/ppermute | solution.py:415
  30.5 0.0 collective-permute-done.8.back3_ref
  30.5 1.3 %collective-permute-done.6.back1_ref = bf16[272,128]{1,0:T(8,128)(2,1)S(1)} collective-permute-done((bf16[272,128]{1,0:T(8,128)(2,1)S(1)}, bf16[272,128]{1,0:T(8,128)(2,1)S(1)}, u32[]{:S(2)}, u32[]{:S(2)}) %collective-permute-start.6) | collective-permute-done | bytes 69664 | tf_op jit(solution)/shard_map/ppermute | solution.py:415
  31.8 0.0 copy-start.9
  31.8 0.7 finish.1
  32.6 4.5 %collective-permute-start.9 = (bf16[128,512]{1,0:T(8,128)(2,1)S(1)}, bf16[128,512]{1,0:T(8,128)(2,1)S(1)}, u32[]{:S(2)}, u32[]{:S(2)}) collective-permute-start(bf16[128,512]{1,0:T(8,128)(2,1)S(1)} %get-tuple-element.59), channel_id=1, source_target_pairs={{0,1},{1,0},{2,3},{3,2},{4,5},{5,4},{6,7},{7,6},{8,9},{9,8},{10,11... | collective-permute-start | bytes 393224 | tf_op jit(solution)/shard_map/ppermute | solution.py:495
  37.0 1.0 collective-permute-done.9.taken_ref
  38.0 0.0 copy-start.2
  38.0 2.5 %project.1 = (bf16[128,2048]{1,0:T(8,128)(2,1)S(1)}, bf16[384,16,128]{2,1,0:T(8,128)(2,1)S(1)}) custom-call(s32[1]{0:T(128)} %bitcast.3.place_ref, s32[8,128]{1,0:T(8,128)S(1)} %get-tuple-element.39.owners_ref, bf16[128,512]{1,0:T(8,128)(2,1)S(1)} %get-tuple-element.58.kept_ref, bf16[128,512]{1,0:T(8,128)(2,1)S(1)} %collective-permute-done.9.taken_ref, ...), custom_call_target="tpu_custom_call" | custom-call | flops 4000000000 | bytes 10000000 | tf_op jit(solution)/shard_map/project/pallas_call | solution.py:401
  40.6 0.0 copy-start
  40.6 29.7 %all_to_all.10 = bf16[128,48,128]{2,1,0:T(8,128)(2,1)S(1)} all-to-all(bf16[128,48,128]{2,1,0:T(8,128)(2,1)S(1)} %bitcast.14), channel_id=1, replica_groups=mesh['sp_0'=4,'sp_1'=4,'sp_2'=4,'tp'=2] {'sp_0','sp_1','sp_2','tp'}, dimensions={0} | all-to-all | bytes 3145728 | tf_op jit(solution)/shard_map/all_to_all | solution.py:509
  70.3 3.5 %experts.1 = bf16[384,16,128]{2,1,0:T(8,128)(2,1)S(1)} custom-call(bf16[384,16,128]{2,1,0:T(8,128)(2,1)S(1)} %bitcast.12, bf16[1,2048,512]{2,1,0:T(8,128)(2,1)S(1)} %copy-done, bf16[1,2048,512]{2,1,0:T(8,128)(2,1)S(1)} %copy-done.1, bf16[1,512,2048]{2,1,0:T(8,128)(2,1)S(1)} %copy-done.2), custom_call_target="tpu_custom_call" | custom-call | tf_op jit(solution)/shard_map/experts/pallas_call | solution.py:118
  73.8 28.9 %all_to_all.11 = bf16[128,48,128]{2,1,0:T(8,128)(2,1)S(1)} all-to-all(bf16[128,48,128]{2,1,0:T(8,128)(2,1)S(1)} %bitcast.13), channel_id=1, replica_groups=mesh['sp_0'=4,'sp_1'=4,'sp_2'=4,'tp'=2] {'sp_0','sp_1','sp_2','tp'}, dimensions={0} | all-to-all | bytes 3145728 | tf_op jit(solution)/shard_map/all_to_all | solution.py:511
  102.7 2.3 %combine.1 = bf16[128,2048]{1,0:T(8,128)(2,1)} custom-call(s32[2,128]{1,0:T(2,128)S(1)} %get-tuple-element.38.slots_ref, bf16[384,16,128]{2,1,0:T(8,128)(2,1)S(1)} %bitcast.15, bf16[128,2048]{1,0:T(8,128)(2,1)S(1)} %get-tuple-element.61.merged_ref, f32[2,128,128]{2,1,0:T(8,128)S(1)} %get-tuple-element.62.weights_ref), custom_call_target="tpu_custom_call" | custom-call | flops 4000000000 | bytes 10000000 | tf_op jit(solution)/shard_map/combine/pallas_call | solution.py:401
  (31 shorter events, 0.1 us)
Async XLA Ops:
  0.0 7.3 %copy-start.11 = (f32[128,2]{0,1:T(2,128)S(1)}, f32[128,2]{0,1:T(2,128)}, u32[]{:S(2)}) copy-start(f32[128,2]{0,1:T(2,128)} %param.26) | copy-start | bytes 3076
  0.0 7.3 %copy-start.12 = (f32[128]{0:T(128)S(1)}, f32[128]{0:T(128)}, u32[]{:S(2)}) copy-start(f32[128]{0:T(128)} %param.25) | copy-start | bytes 1540
  0.0 7.3 %copy-start.10 = (s32[128,2]{0,1:T(2,128)S(1)}, s32[128,2]{0,1:T(2,128)}, u32[]{:S(2)}) copy-start(s32[128,2]{0,1:T(2,128)} %param.24) | copy-start | bytes 3076
  2.8 4.8 %collective-permute-start.2 = (bf16[272,128]{1,0:T(8,128)(2,1)S(1)}, bf16[272,128]{1,0:T(8,128)(2,1)S(1)}, u32[]{:S(2)}, u32[]{:S(2)}) collective-permute-start(bf16[272,128]{1,0:T(8,128)(2,1)S(1)} %get-tuple-element.37.own_ref), channel_id=1, source_target_pairs={{0,6},{2,0},{4,2},{6,4},{1,7},{3,1},{5,3},{7,5},{8,14},{10,8},{12,... | collective-permute-start | bytes 208904 | tf_op jit(solution)/shard_map/ppermute | solution.py:415
  6.2 4.7 %collective-permute-start.1 = (bf16[272,128]{1,0:T(8,128)(2,1)S(1)}, bf16[272,128]{1,0:T(8,128)(2,1)S(1)}, u32[]{:S(2)}, u32[]{:S(2)}) collective-permute-start(bf16[272,128]{1,0:T(8,128)(2,1)S(1)} %get-tuple-element.37.own_ref), channel_id=1, source_target_pairs={{0,4},{2,6},{4,0},{6,2},{1,5},{3,7},{5,1},{7,3},{8,12},{10,14},{12... | collective-permute-start | bytes 208904 | tf_op jit(solution)/shard_map/ppermute | solution.py:415
  6.7 5.3 %collective-permute-start = (bf16[272,128]{1,0:T(8,128)(2,1)S(1)}, bf16[272,128]{1,0:T(8,128)(2,1)S(1)}, u32[]{:S(2)}, u32[]{:S(2)}) collective-permute-start(bf16[272,128]{1,0:T(8,128)(2,1)S(1)} %get-tuple-element.37.own_ref), channel_id=1, source_target_pairs={{0,2},{2,4},{4,6},{6,0},{1,3},{3,5},{5,7},{7,1},{8,10},{10,12},{12... | collective-permute-start | bytes 208904 | tf_op jit(solution)/shard_map/ppermute | solution.py:415
  12.0 4.3 %copy-start.5 = (bf16[256,512]{1,0:T(8,128)(2,1)S(1)}, bf16[256,512]{1,0:T(8,128)(2,1)}, u32[]{:S(2)}) copy-start(bf16[256,512]{1,0:T(8,128)(2,1)} %values_ref.1) | copy-start | bytes 786436
  12.0 4.3 %copy-start.7 = (bf16[256,256]{1,0:T(8,128)(2,1)S(1)}, bf16[256,256]{1,0:T(8,128)(2,1)}, u32[]{:S(2)}) copy-start(bf16[256,256]{1,0:T(8,128)(2,1)} %keys_ref.1) | copy-start | bytes 393220
  12.0 4.3 %copy-start.8 = (bf16[256,256]{1,0:T(8,128)(2,1)S(1)}, bf16[256,256]{1,0:T(8,128)(2,1)}, u32[]{:S(2)}) copy-start(bf16[256,256]{1,0:T(8,128)(2,1)} %queries_ref.1) | copy-start | bytes 393220
  12.0 4.3 %copy-start.14 = (f32[256,256]{1,0:T(8,128)S(1)}, f32[256,256]{1,0:T(8,128)}, u32[]{:S(2)}) copy-start(f32[256,256]{1,0:T(8,128)} %get-tuple-element.44.running_ref) | copy-start | bytes 786436
  12.0 4.3 %copy-start.15 = (bf16[2,4,128,128]{3,2,1,0:T(8,128)(2,1)S(1)}, bf16[2,4,128,128]{3,2,1,0:T(8,128)(2,1)}, u32[]{:S(2)}) copy-start(bf16[2,4,128,128]{3,2,1,0:T(8,128)(2,1)} %get-tuple-element.45.states_ref) | copy-start | bytes 786436
  12.4 4.6 %collective-permute-start.5 = (bf16[272,128]{1,0:T(8,128)(2,1)S(1)}, bf16[272,128]{1,0:T(8,128)(2,1)S(1)}, u32[]{:S(2)}, u32[]{:S(2)}) collective-permute-start(bf16[272,128]{1,0:T(8,128)(2,1)S(1)} %get-tuple-element.43.own_ref), channel_id=1, source_target_pairs={{0,24},{8,0},{16,8},{24,16},{1,25},{9,1},{17,9},{25,17},{2,26},{10... | collective-permute-start | bytes 208904 | tf_op jit(solution)/shard_map/ppermute | solution.py:415
  15.2 4.7 %collective-permute-start.4 = (bf16[272,128]{1,0:T(8,128)(2,1)S(1)}, bf16[272,128]{1,0:T(8,128)(2,1)S(1)}, u32[]{:S(2)}, u32[]{:S(2)}) collective-permute-start(bf16[272,128]{1,0:T(8,128)(2,1)S(1)} %get-tuple-element.43.own_ref), channel_id=1, source_target_pairs={{0,16},{8,24},{16,0},{24,8},{1,17},{9,25},{17,1},{25,9},{2,18},{10... | collective-permute-start | bytes 208904 | tf_op jit(solution)/shard_map/ppermute | solution.py:415
  15.5 5.1 %collective-permute-start.3 = (bf16[272,128]{1,0:T(8,128)(2,1)S(1)}, bf16[272,128]{1,0:T(8,128)(2,1)S(1)}, u32[]{:S(2)}, u32[]{:S(2)}) collective-permute-start(bf16[272,128]{1,0:T(8,128)(2,1)S(1)} %get-tuple-element.43.own_ref), channel_id=1, source_target_pairs={{0,8},{8,16},{16,24},{24,0},{1,9},{9,17},{17,25},{25,1},{2,10},{10... | collective-permute-start | bytes 208904 | tf_op jit(solution)/shard_map/ppermute | solution.py:415
  20.6 11.2 %copy-start.6 = (bf16[256,512]{1,0:T(8,128)(2,1)S(1)}, bf16[256,512]{1,0:T(8,128)(2,1)}, u32[]{:S(2)}) copy-start(bf16[256,512]{1,0:T(8,128)(2,1)} %out_gate_ref.1) | copy-start | bytes 786436
  20.6 11.2 %copy-start.13 = (f32[128]{0:T(128)S(1)}, f32[128]{0:T(128)}, u32[]{:S(2)}) copy-start(f32[128]{0:T(128)} %param.21) | copy-start | bytes 1540
  21.0 9.5 %collective-permute-start.8 = (bf16[272,128]{1,0:T(8,128)(2,1)S(1)}, bf16[272,128]{1,0:T(8,128)(2,1)S(1)}, u32[]{:S(2)}, u32[]{:S(2)}) collective-permute-start(bf16[272,128]{1,0:T(8,128)(2,1)S(1)} %get-tuple-element.51), channel_id=1, source_target_pairs={{0,96},{1,97},{2,98},{3,99},{4,100},{5,101},{6,102},{7,103},{8,104... | collective-permute-start | bytes 208904 | tf_op jit(solution)/shard_map/ppermute | solution.py:415
  26.7 3.8 %collective-permute-start.7 = (bf16[272,128]{1,0:T(8,128)(2,1)S(1)}, bf16[272,128]{1,0:T(8,128)(2,1)S(1)}, u32[]{:S(2)}, u32[]{:S(2)}) collective-permute-start(bf16[272,128]{1,0:T(8,128)(2,1)S(1)} %get-tuple-element.51), channel_id=1, source_target_pairs={{0,64},{32,96},{1,65},{33,97},{2,66},{34,98},{3,67},{35,99},{4,68}... | collective-permute-start | bytes 208904 | tf_op jit(solution)/shard_map/ppermute | solution.py:415
  28.0 3.8 %collective-permute-start.6 = (bf16[272,128]{1,0:T(8,128)(2,1)S(1)}, bf16[272,128]{1,0:T(8,128)(2,1)S(1)}, u32[]{:S(2)}, u32[]{:S(2)}) collective-permute-start(bf16[272,128]{1,0:T(8,128)(2,1)S(1)} %get-tuple-element.51), channel_id=1, source_target_pairs={{0,32},{32,64},{64,96},{1,33},{33,65},{65,97},{2,34},{34,66},{66,9... | collective-permute-start | bytes 208904 | tf_op jit(solution)/shard_map/ppermute | solution.py:415
  31.8 6.2 %copy-start.3 = (bf16[1024,2048]{1,0:T(8,128)(2,1)S(1)}, bf16[1024,2048]{1,0:T(8,128)(2,1)}, u32[]{:S(2)}) copy-start(bf16[1024,2048]{1,0:T(8,128)(2,1)} %weight_ref.1) | copy-start | bytes 12582916
  31.8 6.2 %copy-start.4 = (bf16[128,2048]{1,0:T(8,128)(2,1)S(1)}, bf16[128,2048]{1,0:T(8,128)(2,1)}, u32[]{:S(2)}) copy-start(bf16[128,2048]{1,0:T(8,128)(2,1)} %residual_ref.1) | copy-start | bytes 1572868
  31.8 6.2 %copy-start.9 = (f32[2048]{0:T(1024)S(1)}, f32[2048]{0:T(1024)}, u32[]{:S(2)}) copy-start(f32[2048]{0:T(1024)} %param.23) | copy-start | bytes 24580
  32.6 5.4 %collective-permute-start.9 = (bf16[128,512]{1,0:T(8,128)(2,1)S(1)}, bf16[128,512]{1,0:T(8,128)(2,1)S(1)}, u32[]{:S(2)}, u32[]{:S(2)}) collective-permute-start(bf16[128,512]{1,0:T(8,128)(2,1)S(1)} %get-tuple-element.59), channel_id=1, source_target_pairs={{0,1},{1,0},{2,3},{3,2},{4,5},{5,4},{6,7},{7,6},{8,9},{9,8},{10,11... | collective-permute-start | bytes 393224 | tf_op jit(solution)/shard_map/ppermute | solution.py:495
  38.0 32.3 %copy-start.1 = (bf16[1,2048,512]{2,1,0:T(8,128)(2,1)S(1)}, bf16[1,2048,512]{2,1,0:T(8,128)(2,1)}, u32[]{:S(2)}) copy-start(bf16[1,2048,512]{2,1,0:T(8,128)(2,1)} %up.1) | copy-start | bytes 6291460
  38.0 32.3 %copy-start.2 = (bf16[1,512,2048]{2,1,0:T(8,128)(2,1)S(1)}, bf16[1,512,2048]{2,1,0:T(8,128)(2,1)}, u32[]{:S(2)}) copy-start(bf16[1,512,2048]{2,1,0:T(8,128)(2,1)} %down.1) | copy-start | bytes 6291460
  40.6 29.8 %copy-start = (bf16[1,2048,512]{2,1,0:T(8,128)(2,1)S(1)}, bf16[1,2048,512]{2,1,0:T(8,128)(2,1)}, u32[]{:S(2)}) copy-start(bf16[1,2048,512]{2,1,0:T(8,128)(2,1)} %gate.1) | copy-start | bytes 6291460

commit v5 on v4

--- a/solution.py
+++ b/solution.py
@@ -75,7 +75,6 @@
     rows, choices = routes.shape
     return call(
         routing_kernel,
-        "routing",
         (
             shape_of((choices, rows), jnp.int32),
             shape_of((8, LANES), jnp.int32),
@@ -154,7 +153,6 @@
     rows = merged.shape[0]
     return call(
         combine_kernel,
-        "combine",
         shape_of(merged.shape, jnp.bfloat16),
         (slots, returned, merged, weights),
         1,
@@ -178,7 +176,39 @@
     )
 
 
-def state_kernel(keys_hbm, values_hbm, logits_hbm, running_ref, states_ref, message_ref, keys_ref, values_ref, logits_ref, sems):
+def running_sums(logits):
+    length = logits.shape[0]
+    blocks = length // BLOCK
+    decay_log = (jnp.minimum(logits, 0.0) - jnp.log1p(jnp.exp(-jnp.abs(logits)))) / 16.0
+    parts = pieces(decay_log, 3)
+    row = lax.broadcasted_iota(jnp.int32, (length, length), 0)
+    column = lax.broadcasted_iota(jnp.int32, (length, length), 1)
+    earlier = (row >= column) & (row // BLOCK == column // BLOCK)
+    earlier = earlier.astype(jnp.float32).astype(jnp.bfloat16)
+    running = sum(product(earlier, part) for part in parts)
+    token = lax.broadcasted_iota(jnp.int32, (length, blocks * LANES), 0)
+    lane = lax.broadcasted_iota(jnp.int32, (length, blocks * LANES), 1)
+    member = (token // BLOCK == lane // LANES).astype(jnp.float32).astype(jnp.bfloat16)
+    block_decay = jnp.exp(sum(product(part, member, 0, 0) for part in parts))
+    return running, block_decay
+
+
+def grow(states, n, running, block_decay, keys_ref, values_ref):
+    wide = 2 * VALUE_DIM
+    rows = slice(n * BLOCK, (n + 1) * BLOCK)
+    closing = running[(n + 1) * BLOCK - 1 : (n + 1) * BLOCK]
+    key_closing = keys_ref[rows].astype(jnp.float32) * jnp.exp(closing - running[rows])
+    key_closing = key_closing.astype(jnp.bfloat16)
+    after = []
+    for p, state in enumerate(states):
+        lanes = slice(p * LANES, (p + 1) * LANES)
+        grown = product(key_closing[:, lanes], values_ref[rows, p * wide : (p + 1) * wide], 0, 0)
+        grown = jnp.concatenate([grown[:KEY_DIM, :VALUE_DIM], grown[KEY_DIM:, VALUE_DIM:]], axis=0)
+        after.append(block_decay[lanes, n * LANES : (n + 1) * LANES] * state + grown)
+    return after
+
+
+def state_kernel(keys_hbm, values_hbm, logits_hbm, message_ref, keys_ref, values_ref, logits_ref, sems):
     copies = [
         pltpu.make_async_copy(source, target, sems.at[k])
         for k, (source, target) in enumerate(
@@ -191,38 +221,14 @@
     length, channels = keys_ref.shape
     blocks = length // BLOCK
     pairs = channels // LANES
-    wide = 2 * VALUE_DIM
-    logits = logits_ref[...].astype(jnp.float32)
-    decay_log = (jnp.minimum(logits, 0.0) - jnp.log1p(jnp.exp(-jnp.abs(logits)))) / 16.0
-    parts = pieces(decay_log, 3)
-    row = lax.broadcasted_iota(jnp.int32, (length, length), 0)
-    column = lax.broadcasted_iota(jnp.int32, (length, length), 1)
-    earlier = (row >= column) & (row // BLOCK == column // BLOCK)
-    earlier = earlier.astype(jnp.float32).astype(jnp.bfloat16)
-    running = sum(product(earlier, part) for part in parts)
-    running_ref[...] = running
-    token = lax.broadcasted_iota(jnp.int32, (length, blocks * LANES), 0)
-    lane = lax.broadcasted_iota(jnp.int32, (length, blocks * LANES), 1)
-    member = (token // BLOCK == lane // LANES).astype(jnp.float32).astype(jnp.bfloat16)
-    block_decay = jnp.exp(sum(product(part, member, 0, 0) for part in parts))
+    running, block_decay = running_sums(logits_ref[...].astype(jnp.float32))
     copies[1].wait()
     copies[2].wait()
     states = [jnp.zeros((LANES, VALUE_DIM), jnp.float32)] * pairs
     total = jnp.zeros((1, channels), jnp.float32)
     for n in range(blocks):
-        rows = slice(n * BLOCK, (n + 1) * BLOCK)
-        closing = running[(n + 1) * BLOCK - 1 : (n + 1) * BLOCK]
-        total = total + closing
-        key_closing = keys_ref[rows].astype(jnp.float32) * jnp.exp(closing - running[rows])
-        key_closing = key_closing.astype(jnp.bfloat16)
-        for p in range(pairs):
-            states_ref[p, n] = states[p].astype(jnp.bfloat16)
-            grown = product(
-                key_closing[:, p * LANES : (p + 1) * LANES], values_ref[rows, p * wide : (p + 1) * wide], 0, 0
-            )
-            grown = jnp.concatenate([grown[:KEY_DIM, :VALUE_DIM], grown[KEY_DIM:, VALUE_DIM:]], axis=0)
-            decay = block_decay[p * LANES : (p + 1) * LANES, n * LANES : (n + 1) * LANES]
-            states[p] = decay * states[p] + grown
+        total = total + running[(n + 1) * BLOCK - 1 : (n + 1) * BLOCK]
+        states = grow(states, n, running, block_decay, keys_ref, values_ref)
     for p in range(pairs):
         message_ref[p * LANES : (p + 1) * LANES] = states[p].astype(jnp.bfloat16)
     message_ref[channels:] = pack_decay(jnp.exp(total))
@@ -290,17 +296,19 @@
     ).astype(jnp.bfloat16)
 
 
-def within_kernel(queries_ref, keys_ref, values_ref, running_ref, states_ref, partial_ref, reach_ref):
+def within_kernel(queries_ref, keys_ref, values_ref, logits_ref, partial_ref, reach_ref):
     length, channels = keys_ref.shape
     blocks = length // BLOCK
     pairs = channels // LANES
+    running_all, block_decay = running_sums(logits_ref[...].astype(jnp.float32))
+    states = [jnp.zeros((LANES, VALUE_DIM), jnp.float32)] * pairs
     lead = jnp.zeros((1, channels), jnp.float32)
     row = lax.broadcasted_iota(jnp.int32, (2 * BLOCK, BLOCK), 0)
     column = lax.broadcasted_iota(jnp.int32, (2 * BLOCK, BLOCK), 1)
     causal = (row & (BLOCK - 1)) >= column
     for n in range(blocks):
         rows = slice(n * BLOCK, (n + 1) * BLOCK)
-        running = running_ref[rows]
+        running = running_all[rows]
         query_scaled = queries_ref[rows].astype(jnp.float32) * KEY_DIM ** (-0.5) * jnp.exp(running)
         key_inverse = (keys_ref[rows].astype(jnp.float32) * jnp.exp(-running)).astype(jnp.bfloat16)
         reach_ref[rows] = query_scaled * jnp.exp(lead)
@@ -309,23 +317,26 @@
             lanes = slice(p * LANES, (p + 1) * LANES)
             masked = masked_heads(query_scaled[:, lanes])
             scores = jnp.where(causal, product(masked, key_inverse[:, lanes], 1, 1), 0.0).astype(jnp.bfloat16)
-            carried = product(masked, states_ref[p, n])
+            carried = product(masked, states[p].astype(jnp.bfloat16))
             for h in range(2):
                 place = slice((2 * p + h) * VALUE_DIM, (2 * p + h + 1) * VALUE_DIM)
                 part = slice(h * BLOCK, (h + 1) * BLOCK)
                 partial_ref[rows, place] = product(scores[part], values_ref[rows, place]) + carried[part]
+        if n + 1 < blocks:
+            states = grow(states, n, running_all, block_decay, keys_ref, values_ref)
 
 
 def finish_kernel(
     place_ref, back1_ref, back2_ref, back3_ref, before_y_ref, decay_y_ref, before_x_ref, decay_x_ref,
     partial_ref, reach_ref, head_gain_ref, out_gate_ref, kept_ref, given_ref, whole,
 ):
-    core = place_ref[0]
+    core, plane = place_ref[0], place_ref[1]
     length, channels = reach_ref.shape
     pairs = channels // LANES
     state = jnp.zeros((channels, VALUE_DIM), jnp.float32)
-    for ref in (back3_ref, back2_ref, back1_ref):
-        state = unpack_decay(ref)[1] * state + ref[:channels].astype(jnp.float32)
+    for k, ref in ((3, back3_ref), (2, back2_ref), (1, back1_ref)):
+        passed = unpack_decay(ref)[1] * state + ref[:channels].astype(jnp.float32)
+        state = jnp.where(plane >= k, passed, state)
     state = before_y_ref[...] + decay_y_ref[...] * state
     state = (before_x_ref[...] + decay_x_ref[...] * state).astype(jnp.bfloat16)
     half = length // 2
@@ -397,7 +408,7 @@
     return pltpu.CompilerParams(vmem_limit_bytes=int(mebibytes * 1048576))
 
 
-def call(kernel, name, outs, operands, scalars=0, scratch=(), cost=10000000, room=6, far=False):
+def call(kernel, outs, operands, scalars=0, scratch=(), cost=10000000, room=6, far=False):
     return pl.pallas_call(
         kernel,
         out_shape=outs,
@@ -406,17 +417,14 @@
         scratch_shapes=list(scratch),
         cost_estimate=pl.CostEstimate(flops=cost * 400, bytes_accessed=cost, transcendentals=0),
         compiler_params=limited(room),
-        name=name,
     )(*operands)
 
 
-def from_behind(message, axis, wrap):
-    return [
-        lax.ppermute(
-            message, axis, [(i, (i + k) % RING) for i in range(RING) if wrap or i + k < RING]
-        )
-        for k in range(1, RING)
-    ]
+def from_behind(message, axis):
+    moved = []
+    for k in range(1, RING):
+        moved.append(lax.ppermute(message, axis, [(i, (i + k) % RING) for i in range(RING)]))
+    return moved
 
 
 def local(
@@ -439,20 +447,13 @@
     row_count, model_width = residual.shape
     length, channels = queries.shape
     values = value_rows.shape[1]
-    blocks = length // BLOCK
-    pairs = channels // LANES
     f32, bf16 = jnp.float32, jnp.bfloat16
     z, y, x, core = (lax.axis_index(axis).astype(jnp.int32).reshape(1) for axis in SP_TP)
     message_shape = shape_of((channels + SUB, VALUE_DIM), bf16)
     state_shape = shape_of((channels, VALUE_DIM), f32)
-    running, states, message = call(
+    message = call(
         state_kernel,
-        "local_state",
-        (
-            shape_of((length, channels), f32),
-            shape_of((pairs, blocks, LANES, VALUE_DIM), bf16),
-            message_shape,
-        ),
+        message_shape,
         (key_rows, value_rows, gate_logits),
         scratch=[
             pltpu.VMEM(key_rows.shape, bf16),
@@ -466,36 +467,33 @@
     experts_total = lax.axis_size(SP_TP)
     capacity = 3 * row_count // experts_total
     slots, owners, weights = routing(routes, group_score, expert_score)
-    behind = from_behind(message, "sp_2", True)
+    behind = from_behind(message, "sp_2")
     slots, owners, weights, *behind = lax.optimization_barrier((slots, owners, weights, *behind))
     before_x, decay_x, message_x = call(
-        stage_kernel, "stage_x", (state_shape, state_shape, message_shape), (x, message, *behind), 1
+        stage_kernel, (state_shape, state_shape, message_shape), (x, message, *behind), 1
     )
     partial, reach = call(
         within_kernel,
-        "within",
         (shape_of((length, values), f32), shape_of((length, channels), f32)),
-        (queries, key_rows, value_rows, running, states),
-    )
-    behind = from_behind(message_x, "sp_1", True)
+        (queries, key_rows, value_rows, gate_logits),
+    )
+    behind = from_behind(message_x, "sp_1")
     partial, reach, *behind = lax.optimization_barrier((partial, reach, *behind))
     before_y, decay_y, message_y = call(
-        stage_kernel, "stage_y", (state_shape, state_shape, message_shape), (y, message_x, *behind), 1
-    )
-    behind = from_behind(message_y, "sp_0", False)
+        stage_kernel, (state_shape, state_shape, message_shape), (y, message_x, *behind), 1
+    )
+    behind = from_behind(message_y, "sp_0")
     half = shape_of((length // 2, values), bf16)
     kept, given = call(
         finish_kernel,
-        "finish",
         (half, half),
-        (core, *behind, before_y, decay_y, before_x, decay_x, partial, reach, head_gain.reshape(1, -1), out_gate),
+        (jnp.concatenate([core, z]), *behind, before_y, decay_y, before_x, decay_x, partial, reach, head_gain.reshape(1, -1), out_gate),
         1,
         [pltpu.VMEM((2, length // 2, values), bf16)],
     )
     taken = lax.ppermute(given, "tp", [(0, 1), (1, 0)])
     merged, outgoing = call(
         project_kernel,
-        "project",
         (
             shape_of((row_count, model_width), bf16),
             shape_of((experts_total * capacity, SUB, LANES), bf16),

time: 105 us -> 103 us (0.981)
  starting transfers between devices: 22.2 us -> 17.6 us
  waiting for transfers between devices: 10.3 us -> 12.5 us
    ppermute x9, starting transfers between devices: 17.8 us -> 12.9 us  [from_behind(): lax.ppermute(message, axis, [(i, (i + k) % RING) for i in range(RING)])]
    ppermute x9, waiting for transfers between devices: 9.28 us -> 11.5 us  [from_behind(): lax.ppermute(message, axis, [(i, (i + k) % RING) for i in range(RING)])]
  transfers between devices with their start and end apart: 10 -> 10, of which waited for: 6 -> 8; matrix products, arithmetic and copies ran while one was open for 0% -> 0% of each run, Pallas kernels for 1% -> 2%
where the time goes in v5:
time: 103 us; the launch traced here: 102 us
  blocking collectives  57.7 us (56%)
  starting transfers between devices  17.6 us (17%)
  Pallas kernels  14.4 us (14%)
  waiting for transfers between devices  12.5 us (12%)
    all_to_all x1, blocking collectives, local(): lax.all_to_all(served.reshape(block), SP_TP, split_axis=0, concat_axis=0,...  28.9 us
    all_to_all x1, blocking collectives, local(): lax.all_to_all(outgoing.reshape(block), SP_TP, split_axis=0, concat_axis=...  28.8 us
    ppermute x9, starting transfers between devices, from_behind(): lax.ppermute(message, axis, [(i, (i + k) % RING) for i in range(RING)])  12.9 us
    ppermute x9, waiting for transfers between devices, from_behind(): lax.ppermute(message, axis, [(i, (i + k) % RING) for i in range(RING)])  11.5 us
    pallas_call x8, Pallas kernels, call(): pl.pallas_call(kernel, out_shape=outs, in_specs=[SMEM_SPEC] * scalars + [...  10.9 us
    ppermute x1, starting transfers between devices, local(): taken = lax.ppermute(given, 'tp', [(0, 1), (1, 0)])  4.75 us
    pallas_call x1, Pallas kernels, experts(): pl.pallas_call(experts_kernel, out_shape=jax.ShapeDtypeStruct(arrived.sha...  3.51 us
  transfers between devices with their start and end apart: 10, of which 8 were waited for; matrix products, arithmetic and copies ran while one was open for 0% of the time, Pallas kernels for 2%

profile of v5, /device:TPU:1, one launch (start us, length us, event | category | flops | bytes accessed | tf_op | source)
XLA Modules:
  0.0 102.4 jit_solution(13816779556242851182)
XLA Ops:
  0.0 2.1 %shard_map.146.own_ref = bf16[272,128]{1,0:T(8,128)(2,1)S(1)} custom-call(bf16[256,256]{1,0:T(8,128)(2,1)} %keys_ref.1, bf16[256,512]{1,0:T(8,128)(2,1)} %values_ref.1, bf16[256,256]{1,0:T(8,128)(2,1)} %logits_ref.1), custom_call_target="tpu_custom_call" | custom-call | flops 4000000000 | bytes 10000000 | tf_op jit(solution)/shard_map/pallas_call | solution.py:412
  2.2 3.4 %collective-permute-start.2 = (bf16[272,128]{1,0:T(8,128)(2,1)S(1)}, bf16[272,128]{1,0:T(8,128)(2,1)S(1)}, u32[]{:S(2)}, u32[]{:S(2)}) collective-permute-start(bf16[272,128]{1,0:T(8,128)(2,1)S(1)} %shard_map.146.own_ref), channel_id=1, source_target_pairs={{0,6},{2,0},{4,2},{6,4},{1,7},{3,1},{5,3},{7,5},{8,14},{10,8},{12,... | collective-permute-start | bytes 208904 | tf_op jit(solution)/shard_map/ppermute | solution.py:426
  5.5 0.5 collective-permute-start.1
  6.0 0.6 collective-permute-start
  6.7 0.3 shard_map.145
  6.9 3.3 %collective-permute-done.1.back2_ref = bf16[272,128]{1,0:T(8,128)(2,1)S(1)} collective-permute-done((bf16[272,128]{1,0:T(8,128)(2,1)S(1)}, bf16[272,128]{1,0:T(8,128)(2,1)S(1)}, u32[]{:S(2)}, u32[]{:S(2)}) %collective-permute-start.1) | collective-permute-done | bytes 69664 | tf_op jit(solution)/shard_map/ppermute | solution.py:426
  10.2 1.1 %collective-permute-done.back1_ref = bf16[272,128]{1,0:T(8,128)(2,1)S(1)} collective-permute-done((bf16[272,128]{1,0:T(8,128)(2,1)S(1)}, bf16[272,128]{1,0:T(8,128)(2,1)S(1)}, u32[]{:S(2)}, u32[]{:S(2)}) %collective-permute-start) | collective-permute-done | bytes 69664 | tf_op jit(solution)/shard_map/ppermute | solution.py:426
  11.3 0.4 shard_map.147
  11.7 2.8 %collective-permute-start.5 = (bf16[272,128]{1,0:T(8,128)(2,1)S(1)}, bf16[272,128]{1,0:T(8,128)(2,1)S(1)}, u32[]{:S(2)}, u32[]{:S(2)}) collective-permute-start(bf16[272,128]{1,0:T(8,128)(2,1)S(1)} %get-tuple-element.39.own_ref), channel_id=1, source_target_pairs={{0,24},{8,0},{16,8},{24,16},{1,25},{9,1},{17,9},{25,17},{2,26},{10... | collective-permute-start | bytes 208904 | tf_op jit(solution)/shard_map/ppermute | solution.py:426
  14.5 0.4 collective-permute-start.4
  14.9 0.7 collective-permute-start.3
  15.6 1.6 %shard_map.148 = (f32[256,512]{1,0:T(8,128)S(1)}, f32[256,256]{1,0:T(8,128)S(1)}) custom-call(bf16[256,256]{1,0:T(8,128)(2,1)S(1)} %copy-done.9, bf16[256,256]{1,0:T(8,128)(2,1)S(1)} %copy-done.7, bf16[256,512]{1,0:T(8,128)(2,1)S(1)} %copy-done.5, bf16[256,256]{1,0:T(8,128)(2,1)S(1)} %copy-done.8), custom_call_target="tpu_custom_call" | custom-call | flops 4000000000 | bytes 10000000 | tf_op jit(solution)/shard_map/pallas_call | solution.py:412
  17.1 2.1 %collective-permute-done.4.back2_ref = bf16[272,128]{1,0:T(8,128)(2,1)S(1)} collective-permute-done((bf16[272,128]{1,0:T(8,128)(2,1)S(1)}, bf16[272,128]{1,0:T(8,128)(2,1)S(1)}, u32[]{:S(2)}, u32[]{:S(2)}) %collective-permute-start.4) | collective-permute-done | bytes 69664 | tf_op jit(solution)/shard_map/ppermute | solution.py:426
  19.2 0.7 collective-permute-done.3.back1_ref
  19.9 0.4 shard_map.149
  20.3 3.8 %collective-permute-start.8 = (bf16[272,128]{1,0:T(8,128)(2,1)S(1)}, bf16[272,128]{1,0:T(8,128)(2,1)S(1)}, u32[]{:S(2)}, u32[]{:S(2)}) collective-permute-start(bf16[272,128]{1,0:T(8,128)(2,1)S(1)} %get-tuple-element.45), channel_id=1, source_target_pairs={{0,96},{32,0},{64,32},{96,64},{1,97},{33,1},{65,33},{97,65},{2,98}... | collective-permute-start | bytes 208904 | tf_op jit(solution)/shard_map/ppermute | solution.py:426
  24.1 0.7 collective-permute-start.6
  24.8 0.1 pad_add_fusion.place_ref
  24.9 1.2 %collective-permute-done.8.back3_ref = bf16[272,128]{1,0:T(8,128)(2,1)S(1)} collective-permute-done((bf16[272,128]{1,0:T(8,128)(2,1)S(1)}, bf16[272,128]{1,0:T(8,128)(2,1)S(1)}, u32[]{:S(2)}, u32[]{:S(2)}) %collective-permute-start.8) | collective-permute-done | bytes 69664 | tf_op jit(solution)/shard_map/ppermute | solution.py:426
  26.1 2.8 %collective-permute-done.7.back2_ref = bf16[272,128]{1,0:T(8,128)(2,1)S(1)} collective-permute-done((bf16[272,128]{1,0:T(8,128)(2,1)S(1)}, bf16[272,128]{1,0:T(8,128)(2,1)S(1)}, u32[]{:S(2)}, u32[]{:S(2)}) %collective-permute-start.7) | collective-permute-done | bytes 69664 | tf_op jit(solution)/shard_map/ppermute | solution.py:426
  28.9 0.4 collective-permute-done.6.back1_ref
  29.3 0.0 copy-start.10
  29.3 1.3 %shard_map.150 = (bf16[128,512]{1,0:T(8,128)(2,1)S(1)}, bf16[128,512]{1,0:T(8,128)(2,1)S(1)}) custom-call(s32[2]{0:T(128)S(1)} %pad_add_fusion.place_ref, bf16[272,128]{1,0:T(8,128)(2,1)S(1)} %collective-permute-done.6.back1_ref, bf16[272,128]{1,0:T(8,128)(2,1)S(1)} %collective-permute-done.7.back2_ref, ...), custom_call_target="tpu_custom_call" | custom-call | flops 4000000000 | bytes 10000000 | tf_op jit(solution)/shard_map/pallas_call | solution.py:412
  30.6 4.8 %collective-permute-start.9 = (bf16[128,512]{1,0:T(8,128)(2,1)S(1)}, bf16[128,512]{1,0:T(8,128)(2,1)S(1)}, u32[]{:S(2)}, u32[]{:S(2)}) collective-permute-start(bf16[128,512]{1,0:T(8,128)(2,1)S(1)} %get-tuple-element.53), channel_id=1, source_target_pairs={{0,1},{1,0},{2,3},{3,2},{4,5},{5,4},{6,7},{7,6},{8,9},{9,8},{10,11... | collective-permute-start | bytes 393224 | tf_op jit(solution)/shard_map/ppermute | solution.py:494
  35.3 1.0 collective-permute-done.9.taken_ref
  36.3 0.0 copy-start.2
  36.3 2.5 %shard_map.151 = (bf16[128,2048]{1,0:T(8,128)(2,1)S(1)}, bf16[384,16,128]{2,1,0:T(8,128)(2,1)S(1)}) custom-call(s32[1]{0:T(128)} %bitcast.3.place_ref, s32[8,128]{1,0:T(8,128)S(1)} %get-tuple-element.35.owners_ref, bf16[128,512]{1,0:T(8,128)(2,1)S(1)} %get-tuple-element.52.kept_ref, bf16[128,512]{1,0:T(8,128)(2,1)S(1)} %collective-permute-done.9.taken_ref, ...), custom_call_target="tpu_custom_call" | custom-call | flops 4000000000 | bytes 10000000 | tf_op jit(solution)/shard_map/pallas_call | solution.py:412
  38.9 0.0 copy-start
  38.9 28.8 %all_to_all.10 = bf16[128,48,128]{2,1,0:T(8,128)(2,1)S(1)} all-to-all(bf16[128,48,128]{2,1,0:T(8,128)(2,1)S(1)} %bitcast.15), channel_id=1, replica_groups=mesh['sp_0'=4,'sp_1'=4,'sp_2'=4,'tp'=2] {'sp_0','sp_1','sp_2','tp'}, dimensions={0} | all-to-all | bytes 3145728 | tf_op jit(solution)/shard_map/all_to_all | solution.py:507
  67.7 3.5 %experts.1 = bf16[384,16,128]{2,1,0:T(8,128)(2,1)S(1)} custom-call(bf16[384,16,128]{2,1,0:T(8,128)(2,1)S(1)} %bitcast.13, bf16[1,2048,512]{2,1,0:T(8,128)(2,1)S(1)} %copy-done, bf16[1,2048,512]{2,1,0:T(8,128)(2,1)S(1)} %copy-done.1, bf16[1,512,2048]{2,1,0:T(8,128)(2,1)S(1)} %copy-done.2), custom_call_target="tpu_custom_call" | custom-call | tf_op jit(solution)/shard_map/experts/pallas_call | solution.py:117
  71.2 28.9 %all_to_all.11 = bf16[128,48,128]{2,1,0:T(8,128)(2,1)S(1)} all-to-all(bf16[128,48,128]{2,1,0:T(8,128)(2,1)S(1)} %bitcast.14), channel_id=1, replica_groups=mesh['sp_0'=4,'sp_1'=4,'sp_2'=4,'tp'=2] {'sp_0','sp_1','sp_2','tp'}, dimensions={0} | all-to-all | bytes 3145728 | tf_op jit(solution)/shard_map/all_to_all | solution.py:509
  100.1 2.3 %shard_map.152 = bf16[128,2048]{1,0:T(8,128)(2,1)} custom-call(s32[2,128]{1,0:T(2,128)S(1)} %get-tuple-element.34.slots_ref, bf16[384,16,128]{2,1,0:T(8,128)(2,1)S(1)} %bitcast.16, bf16[128,2048]{1,0:T(8,128)(2,1)S(1)} %get-tuple-element.55.merged_ref, f32[2,128,128]{2,1,0:T(8,128)S(1)} %get-tuple-element.56.weights_ref), custom_call_target="tpu_custom_call" | custom-call | flops 4000000000 | bytes 10000000 | tf_op jit(solution)/shard_map/pallas_call | solution.py:412
  (30 shorter events, 0.1 us)
Async XLA Ops:
  0.0 6.6 %copy-start.12 = (f32[128,2]{0,1:T(2,128)S(1)}, f32[128,2]{0,1:T(2,128)}, u32[]{:S(2)}) copy-start(f32[128,2]{0,1:T(2,128)} %param.26) | copy-start | bytes 3076
  0.0 6.6 %copy-start.13 = (f32[128]{0:T(128)S(1)}, f32[128]{0:T(128)}, u32[]{:S(2)}) copy-start(f32[128]{0:T(128)} %param.25) | copy-start | bytes 1540
  0.0 6.6 %copy-start.11 = (s32[128,2]{0,1:T(2,128)S(1)}, s32[128,2]{0,1:T(2,128)}, u32[]{:S(2)}) copy-start(s32[128,2]{0,1:T(2,128)} %param.24) | copy-start | bytes 3076
  2.2 4.8 %collective-permute-start.2 = (bf16[272,128]{1,0:T(8,128)(2,1)S(1)}, bf16[272,128]{1,0:T(8,128)(2,1)S(1)}, u32[]{:S(2)}, u32[]{:S(2)}) collective-permute-start(bf16[272,128]{1,0:T(8,128)(2,1)S(1)} %shard_map.146.own_ref), channel_id=1, source_target_pairs={{0,6},{2,0},{4,2},{6,4},{1,7},{3,1},{5,3},{7,5},{8,14},{10,8},{12,... | collective-permute-start | bytes 208904 | tf_op jit(solution)/shard_map/ppermute | solution.py:426
  5.5 4.7 %collective-permute-start.1 = (bf16[272,128]{1,0:T(8,128)(2,1)S(1)}, bf16[272,128]{1,0:T(8,128)(2,1)S(1)}, u32[]{:S(2)}, u32[]{:S(2)}) collective-permute-start(bf16[272,128]{1,0:T(8,128)(2,1)S(1)} %shard_map.146.own_ref), channel_id=1, source_target_pairs={{0,4},{2,6},{4,0},{6,2},{1,5},{3,7},{5,1},{7,3},{8,12},{10,14},{12... | collective-permute-start | bytes 208904 | tf_op jit(solution)/shard_map/ppermute | solution.py:426
  6.0 5.3 %collective-permute-start = (bf16[272,128]{1,0:T(8,128)(2,1)S(1)}, bf16[272,128]{1,0:T(8,128)(2,1)S(1)}, u32[]{:S(2)}, u32[]{:S(2)}) collective-permute-start(bf16[272,128]{1,0:T(8,128)(2,1)S(1)} %shard_map.146.own_ref), channel_id=1, source_target_pairs={{0,2},{2,4},{4,6},{6,0},{1,3},{3,5},{5,7},{7,1},{8,10},{10,12},{12... | collective-permute-start | bytes 208904 | tf_op jit(solution)/shard_map/ppermute | solution.py:426
  11.3 4.3 %copy-start.5 = (bf16[256,512]{1,0:T(8,128)(2,1)S(1)}, bf16[256,512]{1,0:T(8,128)(2,1)}, u32[]{:S(2)}) copy-start(bf16[256,512]{1,0:T(8,128)(2,1)} %values_ref.1) | copy-start | bytes 786436
  11.3 4.3 %copy-start.7 = (bf16[256,256]{1,0:T(8,128)(2,1)S(1)}, bf16[256,256]{1,0:T(8,128)(2,1)}, u32[]{:S(2)}) copy-start(bf16[256,256]{1,0:T(8,128)(2,1)} %keys_ref.1) | copy-start | bytes 393220
  11.3 4.3 %copy-start.8 = (bf16[256,256]{1,0:T(8,128)(2,1)S(1)}, bf16[256,256]{1,0:T(8,128)(2,1)}, u32[]{:S(2)}) copy-start(bf16[256,256]{1,0:T(8,128)(2,1)} %logits_ref.1) | copy-start | bytes 393220
  11.3 4.3 %copy-start.9 = (bf16[256,256]{1,0:T(8,128)(2,1)S(1)}, bf16[256,256]{1,0:T(8,128)(2,1)}, u32[]{:S(2)}) copy-start(bf16[256,256]{1,0:T(8,128)(2,1)} %queries_ref.1) | copy-start | bytes 393220
  11.7 5.4 %collective-permute-start.5 = (bf16[272,128]{1,0:T(8,128)(2,1)S(1)}, bf16[272,128]{1,0:T(8,128)(2,1)S(1)}, u32[]{:S(2)}, u32[]{:S(2)}) collective-permute-start(bf16[272,128]{1,0:T(8,128)(2,1)S(1)} %get-tuple-element.39.own_ref), channel_id=1, source_target_pairs={{0,24},{8,0},{16,8},{24,16},{1,25},{9,1},{17,9},{25,17},{2,26},{10... | collective-permute-start | bytes 208904 | tf_op jit(solution)/shard_map/ppermute | solution.py:426
  14.5 4.7 %collective-permute-start.4 = (bf16[272,128]{1,0:T(8,128)(2,1)S(1)}, bf16[272,128]{1,0:T(8,128)(2,1)S(1)}, u32[]{:S(2)}, u32[]{:S(2)}) collective-permute-start(bf16[272,128]{1,0:T(8,128)(2,1)S(1)} %get-tuple-element.39.own_ref), channel_id=1, source_target_pairs={{0,16},{8,24},{16,0},{24,8},{1,17},{9,25},{17,1},{25,9},{2,18},{10... | collective-permute-start | bytes 208904 | tf_op jit(solution)/shard_map/ppermute | solution.py:426
  14.9 5.1 %collective-permute-start.3 = (bf16[272,128]{1,0:T(8,128)(2,1)S(1)}, bf16[272,128]{1,0:T(8,128)(2,1)S(1)}, u32[]{:S(2)}, u32[]{:S(2)}) collective-permute-start(bf16[272,128]{1,0:T(8,128)(2,1)S(1)} %get-tuple-element.39.own_ref), channel_id=1, source_target_pairs={{0,8},{8,16},{16,24},{24,0},{1,9},{9,17},{17,25},{25,1},{2,10},{10... | collective-permute-start | bytes 208904 | tf_op jit(solution)/shard_map/ppermute | solution.py:426
  19.9 9.3 %copy-start.6 = (bf16[256,512]{1,0:T(8,128)(2,1)S(1)}, bf16[256,512]{1,0:T(8,128)(2,1)}, u32[]{:S(2)}) copy-start(bf16[256,512]{1,0:T(8,128)(2,1)} %out_gate_ref.1) | copy-start | bytes 786436
  19.9 9.3 %copy-start.14 = (f32[128]{0:T(128)S(1)}, f32[128]{0:T(128)}, u32[]{:S(2)}) copy-start(f32[128]{0:T(128)} %param.21) | copy-start | bytes 1540
  20.3 5.8 %collective-permute-start.8 = (bf16[272,128]{1,0:T(8,128)(2,1)S(1)}, bf16[272,128]{1,0:T(8,128)(2,1)S(1)}, u32[]{:S(2)}, u32[]{:S(2)}) collective-permute-start(bf16[272,128]{1,0:T(8,128)(2,1)S(1)} %get-tuple-element.45), channel_id=1, source_target_pairs={{0,96},{32,0},{64,32},{96,64},{1,97},{33,1},{65,33},{97,65},{2,98}... | collective-permute-start | bytes 208904 | tf_op jit(solution)/shard_map/ppermute | solution.py:426
  24.1 4.8 %collective-permute-start.7 = (bf16[272,128]{1,0:T(8,128)(2,1)S(1)}, bf16[272,128]{1,0:T(8,128)(2,1)S(1)}, u32[]{:S(2)}, u32[]{:S(2)}) collective-permute-start(bf16[272,128]{1,0:T(8,128)(2,1)S(1)} %get-tuple-element.45), channel_id=1, source_target_pairs={{0,64},{32,96},{64,0},{96,32},{1,65},{33,97},{65,1},{97,33},{2,66}... | collective-permute-start | bytes 208904 | tf_op jit(solution)/shard_map/ppermute | solution.py:426
  24.1 5.1 %collective-permute-start.6 = (bf16[272,128]{1,0:T(8,128)(2,1)S(1)}, bf16[272,128]{1,0:T(8,128)(2,1)S(1)}, u32[]{:S(2)}, u32[]{:S(2)}) collective-permute-start(bf16[272,128]{1,0:T(8,128)(2,1)S(1)} %get-tuple-element.45), channel_id=1, source_target_pairs={{0,32},{32,64},{64,96},{96,0},{1,33},{33,65},{65,97},{97,1},{2,34}... | collective-permute-start | bytes 208904 | tf_op jit(solution)/shard_map/ppermute | solution.py:426
  29.3 7.0 %copy-start.3 = (bf16[1024,2048]{1,0:T(8,128)(2,1)S(1)}, bf16[1024,2048]{1,0:T(8,128)(2,1)}, u32[]{:S(2)}) copy-start(bf16[1024,2048]{1,0:T(8,128)(2,1)} %weight_ref.1) | copy-start | bytes 12582916
  29.3 7.0 %copy-start.4 = (bf16[128,2048]{1,0:T(8,128)(2,1)S(1)}, bf16[128,2048]{1,0:T(8,128)(2,1)}, u32[]{:S(2)}) copy-start(bf16[128,2048]{1,0:T(8,128)(2,1)} %residual_ref.1) | copy-start | bytes 1572868
  29.3 7.0 %copy-start.10 = (f32[2048]{0:T(1024)S(1)}, f32[2048]{0:T(1024)}, u32[]{:S(2)}) copy-start(f32[2048]{0:T(1024)} %param.23) | copy-start | bytes 24580
  30.6 5.7 %collective-permute-start.9 = (bf16[128,512]{1,0:T(8,128)(2,1)S(1)}, bf16[128,512]{1,0:T(8,128)(2,1)S(1)}, u32[]{:S(2)}, u32[]{:S(2)}) collective-permute-start(bf16[128,512]{1,0:T(8,128)(2,1)S(1)} %get-tuple-element.53), channel_id=1, source_target_pairs={{0,1},{1,0},{2,3},{3,2},{4,5},{5,4},{6,7},{7,6},{8,9},{9,8},{10,11... | collective-permute-start | bytes 393224 | tf_op jit(solution)/shard_map/ppermute | solution.py:494
  36.3 31.4 %copy-start.1 = (bf16[1,2048,512]{2,1,0:T(8,128)(2,1)S(1)}, bf16[1,2048,512]{2,1,0:T(8,128)(2,1)}, u32[]{:S(2)}) copy-start(bf16[1,2048,512]{2,1,0:T(8,128)(2,1)} %up.1) | copy-start | bytes 6291460
  36.3 31.4 %copy-start.2 = (bf16[1,512,2048]{2,1,0:T(8,128)(2,1)S(1)}, bf16[1,512,2048]{2,1,0:T(8,128)(2,1)}, u32[]{:S(2)}) copy-start(bf16[1,512,2048]{2,1,0:T(8,128)(2,1)} %down.1) | copy-start | bytes 6291460
  38.9 28.8 %copy-start = (bf16[1,2048,512]{2,1,0:T(8,128)(2,1)S(1)}, bf16[1,2048,512]{2,1,0:T(8,128)(2,1)}, u32[]{:S(2)}) copy-start(bf16[1,2048,512]{2,1,0:T(8,128)(2,1)} %gate.1) | copy-start | bytes 6291460

commit v6 on v5

--- a/solution.py
+++ b/solution.py
@@ -327,10 +327,10 @@
 
 
 def finish_kernel(
-    place_ref, back1_ref, back2_ref, back3_ref, before_y_ref, decay_y_ref, before_x_ref, decay_x_ref,
+    place_ref, plane_ref, back1_ref, back2_ref, back3_ref, before_y_ref, decay_y_ref, before_x_ref, decay_x_ref,
     partial_ref, reach_ref, head_gain_ref, out_gate_ref, kept_ref, given_ref, whole,
 ):
-    core, plane = place_ref[0], place_ref[1]
+    core, plane = place_ref[0], plane_ref[0]
     length, channels = reach_ref.shape
     pairs = channels // LANES
     state = jnp.zeros((channels, VALUE_DIM), jnp.float32)
@@ -487,8 +487,8 @@
     kept, given = call(
         finish_kernel,
         (half, half),
-        (jnp.concatenate([core, z]), *behind, before_y, decay_y, before_x, decay_x, partial, reach, head_gain.reshape(1, -1), out_gate),
-        1,
+        (core, z, *behind, before_y, decay_y, before_x, decay_x, partial, reach, head_gain.reshape(1, -1), out_gate),
+        2,
         [pltpu.VMEM((2, length // 2, values), bf16)],
     )
     taken = lax.ppermute(given, "tp", [(0, 1), (1, 0)])

time: 103 us -> 102 us (level)
  no operation moved by 1% of the time
where the time goes in v6:
time: 102 us
  blocking collectives  57.8 us (57%)
  starting transfers between devices  17.6 us (17%)
  Pallas kernels  13.8 us (14%)
  waiting for transfers between devices  12.5 us (12%)
    all_to_all x1, blocking collectives, local(): lax.all_to_all(outgoing.reshape(block), SP_TP, split_axis=0, concat_axis=...  28.9 us
    all_to_all x1, blocking collectives, local(): lax.all_to_all(served.reshape(block), SP_TP, split_axis=0, concat_axis=0,...  28.9 us
    ppermute x9, starting transfers between devices, from_behind(): lax.ppermute(message, axis, [(i, (i + k) % RING) for i in range(RING)])  12.9 us
    ppermute x9, waiting for transfers between devices, from_behind(): lax.ppermute(message, axis, [(i, (i + k) % RING) for i in range(RING)])  11.6 us
    pallas_call x8, Pallas kernels, call(): pl.pallas_call(kernel, out_shape=outs, in_specs=[SMEM_SPEC] * scalars + [...  10.3 us
    ppermute x1, starting transfers between devices, local(): taken = lax.ppermute(given, 'tp', [(0, 1), (1, 0)])  4.74 us
    pallas_call x1, Pallas kernels, experts(): pl.pallas_call(experts_kernel, out_shape=jax.ShapeDtypeStruct(arrived.sha...  3.51 us
  transfers between devices with their start and end apart: 10, of which 8 were waited for; matrix products, arithmetic and copies ran while one was open for 0% of the time, Pallas kernels for 2%

profile of v6, /device:TPU:1, one launch (start us, length us, event | category | flops | bytes accessed | tf_op | source)
XLA Modules:
  0.0 101.9 jit_solution(4960924482966751870)
XLA Ops:
  0.0 2.1 %shard_map.146.own_ref = bf16[272,128]{1,0:T(8,128)(2,1)S(1)} custom-call(bf16[256,256]{1,0:T(8,128)(2,1)} %keys_ref.1, bf16[256,512]{1,0:T(8,128)(2,1)} %values_ref.1, bf16[256,256]{1,0:T(8,128)(2,1)} %logits_ref.1), custom_call_target="tpu_custom_call" | custom-call | flops 4000000000 | bytes 10000000 | tf_op jit(solution)/shard_map/pallas_call | solution.py:412
  2.2 3.4 %collective-permute-start.2 = (bf16[272,128]{1,0:T(8,128)(2,1)S(1)}, bf16[272,128]{1,0:T(8,128)(2,1)S(1)}, u32[]{:S(2)}, u32[]{:S(2)}) collective-permute-start(bf16[272,128]{1,0:T(8,128)(2,1)S(1)} %shard_map.146.own_ref), channel_id=1, source_target_pairs={{0,6},{2,0},{4,2},{6,4},{1,7},{3,1},{5,3},{7,5},{8,14},{10,8},{12,... | collective-permute-start | bytes 208904 | tf_op jit(solution)/shard_map/ppermute | solution.py:426
  5.5 0.5 collective-permute-start.1
  6.0 0.6 collective-permute-start
  6.7 0.3 shard_map.145
  6.9 0.0 collective-permute-done.2.back3_ref
  6.9 3.3 %collective-permute-done.1.back2_ref = bf16[272,128]{1,0:T(8,128)(2,1)S(1)} collective-permute-done((bf16[272,128]{1,0:T(8,128)(2,1)S(1)}, bf16[272,128]{1,0:T(8,128)(2,1)S(1)}, u32[]{:S(2)}, u32[]{:S(2)}) %collective-permute-start.1) | collective-permute-done | bytes 69664 | tf_op jit(solution)/shard_map/ppermute | solution.py:426
  10.2 1.1 %collective-permute-done.back1_ref = bf16[272,128]{1,0:T(8,128)(2,1)S(1)} collective-permute-done((bf16[272,128]{1,0:T(8,128)(2,1)S(1)}, bf16[272,128]{1,0:T(8,128)(2,1)S(1)}, u32[]{:S(2)}, u32[]{:S(2)}) %collective-permute-start) | collective-permute-done | bytes 69664 | tf_op jit(solution)/shard_map/ppermute | solution.py:426
  11.3 0.4 shard_map.147
  11.7 2.8 %collective-permute-start.5 = (bf16[272,128]{1,0:T(8,128)(2,1)S(1)}, bf16[272,128]{1,0:T(8,128)(2,1)S(1)}, u32[]{:S(2)}, u32[]{:S(2)}) collective-permute-start(bf16[272,128]{1,0:T(8,128)(2,1)S(1)} %get-tuple-element.39.own_ref), channel_id=1, source_target_pairs={{0,24},{8,0},{16,8},{24,16},{1,25},{9,1},{17,9},{25,17},{2,26},{10... | collective-permute-start | bytes 208904 | tf_op jit(solution)/shard_map/ppermute | solution.py:426
  14.5 0.4 collective-permute-start.4
  14.9 0.7 collective-permute-start.3
  15.6 1.6 %shard_map.148 = (f32[256,512]{1,0:T(8,128)S(1)}, f32[256,256]{1,0:T(8,128)S(1)}) custom-call(bf16[256,256]{1,0:T(8,128)(2,1)S(1)} %copy-done.9, bf16[256,256]{1,0:T(8,128)(2,1)S(1)} %copy-done.7, bf16[256,512]{1,0:T(8,128)(2,1)S(1)} %copy-done.5, bf16[256,256]{1,0:T(8,128)(2,1)S(1)} %copy-done.8), custom_call_target="tpu_custom_call" | custom-call | flops 4000000000 | bytes 10000000 | tf_op jit(solution)/shard_map/pallas_call | solution.py:412
  17.1 2.1 %collective-permute-done.4.back2_ref = bf16[272,128]{1,0:T(8,128)(2,1)S(1)} collective-permute-done((bf16[272,128]{1,0:T(8,128)(2,1)S(1)}, bf16[272,128]{1,0:T(8,128)(2,1)S(1)}, u32[]{:S(2)}, u32[]{:S(2)}) %collective-permute-start.4) | collective-permute-done | bytes 69664 | tf_op jit(solution)/shard_map/ppermute | solution.py:426
  19.2 0.7 collective-permute-done.3.back1_ref
  19.9 0.4 shard_map.149
  20.3 3.8 %collective-permute-start.8 = (bf16[272,128]{1,0:T(8,128)(2,1)S(1)}, bf16[272,128]{1,0:T(8,128)(2,1)S(1)}, u32[]{:S(2)}, u32[]{:S(2)}) collective-permute-start(bf16[272,128]{1,0:T(8,128)(2,1)S(1)} %get-tuple-element.45), channel_id=1, source_target_pairs={{0,96},{32,0},{64,32},{96,64},{1,97},{33,1},{65,33},{97,65},{2,98}... | collective-permute-start | bytes 208904 | tf_op jit(solution)/shard_map/ppermute | solution.py:426
  24.1 0.7 collective-permute-start.6
  24.9 1.3 %collective-permute-done.8.back3_ref = bf16[272,128]{1,0:T(8,128)(2,1)S(1)} collective-permute-done((bf16[272,128]{1,0:T(8,128)(2,1)S(1)}, bf16[272,128]{1,0:T(8,128)(2,1)S(1)}, u32[]{:S(2)}, u32[]{:S(2)}) %collective-permute-start.8) | collective-permute-done | bytes 69664 | tf_op jit(solution)/shard_map/ppermute | solution.py:426
  26.1 2.8 %collective-permute-done.7.back2_ref = bf16[272,128]{1,0:T(8,128)(2,1)S(1)} collective-permute-done((bf16[272,128]{1,0:T(8,128)(2,1)S(1)}, bf16[272,128]{1,0:T(8,128)(2,1)S(1)}, u32[]{:S(2)}, u32[]{:S(2)}) %collective-permute-start.7) | collective-permute-done | bytes 69664 | tf_op jit(solution)/shard_map/ppermute | solution.py:426
  28.9 0.4 collective-permute-done.6.back1_ref
  29.3 0.0 copy-start.10
  29.3 0.7 shard_map.150
  30.0 4.7 %collective-permute-start.9 = (bf16[128,512]{1,0:T(8,128)(2,1)S(1)}, bf16[128,512]{1,0:T(8,128)(2,1)S(1)}, u32[]{:S(2)}, u32[]{:S(2)}) collective-permute-start(bf16[128,512]{1,0:T(8,128)(2,1)S(1)} %get-tuple-element.53), channel_id=1, source_target_pairs={{0,1},{1,0},{2,3},{3,2},{4,5},{5,4},{6,7},{7,6},{8,9},{9,8},{10,11... | collective-permute-start | bytes 393224 | tf_op jit(solution)/shard_map/ppermute | solution.py:494
  34.8 1.0 collective-permute-done.9.taken_ref
  35.8 0.0 copy-start.2
  35.8 2.5 %shard_map.151 = (bf16[128,2048]{1,0:T(8,128)(2,1)S(1)}, bf16[384,16,128]{2,1,0:T(8,128)(2,1)S(1)}) custom-call(s32[1]{0:T(128)} %bitcast.3.place_ref, s32[8,128]{1,0:T(8,128)S(1)} %get-tuple-element.35.owners_ref, bf16[128,512]{1,0:T(8,128)(2,1)S(1)} %get-tuple-element.52.kept_ref, bf16[128,512]{1,0:T(8,128)(2,1)S(1)} %collective-permute-done.9.taken_ref, ...), custom_call_target="tpu_custom_call" | custom-call | flops 4000000000 | bytes 10000000 | tf_op jit(solution)/shard_map/pallas_call | solution.py:412
  38.3 0.0 copy-start
  38.3 28.9 %all_to_all.10 = bf16[128,48,128]{2,1,0:T(8,128)(2,1)S(1)} all-to-all(bf16[128,48,128]{2,1,0:T(8,128)(2,1)S(1)} %bitcast.15), channel_id=1, replica_groups=mesh['sp_0'=4,'sp_1'=4,'sp_2'=4,'tp'=2] {'sp_0','sp_1','sp_2','tp'}, dimensions={0} | all-to-all | bytes 3145728 | tf_op jit(solution)/shard_map/all_to_all | solution.py:507
  67.2 3.5 %experts.1 = bf16[384,16,128]{2,1,0:T(8,128)(2,1)S(1)} custom-call(bf16[384,16,128]{2,1,0:T(8,128)(2,1)S(1)} %bitcast.13, bf16[1,2048,512]{2,1,0:T(8,128)(2,1)S(1)} %copy-done, bf16[1,2048,512]{2,1,0:T(8,128)(2,1)S(1)} %copy-done.1, bf16[1,512,2048]{2,1,0:T(8,128)(2,1)S(1)} %copy-done.2), custom_call_target="tpu_custom_call" | custom-call | tf_op jit(solution)/shard_map/experts/pallas_call | solution.py:117
  70.7 28.9 %all_to_all.11 = bf16[128,48,128]{2,1,0:T(8,128)(2,1)S(1)} all-to-all(bf16[128,48,128]{2,1,0:T(8,128)(2,1)S(1)} %bitcast.14), channel_id=1, replica_groups=mesh['sp_0'=4,'sp_1'=4,'sp_2'=4,'tp'=2] {'sp_0','sp_1','sp_2','tp'}, dimensions={0} | all-to-all | bytes 3145728 | tf_op jit(solution)/shard_map/all_to_all | solution.py:509
  99.6 2.3 %shard_map.152 = bf16[128,2048]{1,0:T(8,128)(2,1)} custom-call(s32[2,128]{1,0:T(2,128)S(1)} %get-tuple-element.34.slots_ref, bf16[384,16,128]{2,1,0:T(8,128)(2,1)S(1)} %bitcast.16, bf16[128,2048]{1,0:T(8,128)(2,1)S(1)} %get-tuple-element.55.merged_ref, f32[2,128,128]{2,1,0:T(8,128)S(1)} %get-tuple-element.56.weights_ref), custom_call_target="tpu_custom_call" | custom-call | flops 4000000000 | bytes 10000000 | tf_op jit(solution)/shard_map/pallas_call | solution.py:412
  (29 shorter events, 0.1 us)
Async XLA Ops:
  0.0 6.6 %copy-start.12 = (f32[128,2]{0,1:T(2,128)S(1)}, f32[128,2]{0,1:T(2,128)}, u32[]{:S(2)}) copy-start(f32[128,2]{0,1:T(2,128)} %param.26) | copy-start | bytes 3076
  0.0 6.6 %copy-start.13 = (f32[128]{0:T(128)S(1)}, f32[128]{0:T(128)}, u32[]{:S(2)}) copy-start(f32[128]{0:T(128)} %param.25) | copy-start | bytes 1540
  0.0 6.6 %copy-start.11 = (s32[128,2]{0,1:T(2,128)S(1)}, s32[128,2]{0,1:T(2,128)}, u32[]{:S(2)}) copy-start(s32[128,2]{0,1:T(2,128)} %param.24) | copy-start | bytes 3076
  2.2 4.8 %collective-permute-start.2 = (bf16[272,128]{1,0:T(8,128)(2,1)S(1)}, bf16[272,128]{1,0:T(8,128)(2,1)S(1)}, u32[]{:S(2)}, u32[]{:S(2)}) collective-permute-start(bf16[272,128]{1,0:T(8,128)(2,1)S(1)} %shard_map.146.own_ref), channel_id=1, source_target_pairs={{0,6},{2,0},{4,2},{6,4},{1,7},{3,1},{5,3},{7,5},{8,14},{10,8},{12,... | collective-permute-start | bytes 208904 | tf_op jit(solution)/shard_map/ppermute | solution.py:426
  5.5 4.7 %collective-permute-start.1 = (bf16[272,128]{1,0:T(8,128)(2,1)S(1)}, bf16[272,128]{1,0:T(8,128)(2,1)S(1)}, u32[]{:S(2)}, u32[]{:S(2)}) collective-permute-start(bf16[272,128]{1,0:T(8,128)(2,1)S(1)} %shard_map.146.own_ref), channel_id=1, source_target_pairs={{0,4},{2,6},{4,0},{6,2},{1,5},{3,7},{5,1},{7,3},{8,12},{10,14},{12... | collective-permute-start | bytes 208904 | tf_op jit(solution)/shard_map/ppermute | solution.py:426
  6.0 5.3 %collective-permute-start = (bf16[272,128]{1,0:T(8,128)(2,1)S(1)}, bf16[272,128]{1,0:T(8,128)(2,1)S(1)}, u32[]{:S(2)}, u32[]{:S(2)}) collective-permute-start(bf16[272,128]{1,0:T(8,128)(2,1)S(1)} %shard_map.146.own_ref), channel_id=1, source_target_pairs={{0,2},{2,4},{4,6},{6,0},{1,3},{3,5},{5,7},{7,1},{8,10},{10,12},{12... | collective-permute-start | bytes 208904 | tf_op jit(solution)/shard_map/ppermute | solution.py:426
  11.3 4.3 %copy-start.5 = (bf16[256,512]{1,0:T(8,128)(2,1)S(1)}, bf16[256,512]{1,0:T(8,128)(2,1)}, u32[]{:S(2)}) copy-start(bf16[256,512]{1,0:T(8,128)(2,1)} %values_ref.1) | copy-start | bytes 786436
  11.3 4.3 %copy-start.7 = (bf16[256,256]{1,0:T(8,128)(2,1)S(1)}, bf16[256,256]{1,0:T(8,128)(2,1)}, u32[]{:S(2)}) copy-start(bf16[256,256]{1,0:T(8,128)(2,1)} %keys_ref.1) | copy-start | bytes 393220
  11.3 4.3 %copy-start.8 = (bf16[256,256]{1,0:T(8,128)(2,1)S(1)}, bf16[256,256]{1,0:T(8,128)(2,1)}, u32[]{:S(2)}) copy-start(bf16[256,256]{1,0:T(8,128)(2,1)} %logits_ref.1) | copy-start | bytes 393220
  11.3 4.3 %copy-start.9 = (bf16[256,256]{1,0:T(8,128)(2,1)S(1)}, bf16[256,256]{1,0:T(8,128)(2,1)}, u32[]{:S(2)}) copy-start(bf16[256,256]{1,0:T(8,128)(2,1)} %queries_ref.1) | copy-start | bytes 393220
  11.7 5.4 %collective-permute-start.5 = (bf16[272,128]{1,0:T(8,128)(2,1)S(1)}, bf16[272,128]{1,0:T(8,128)(2,1)S(1)}, u32[]{:S(2)}, u32[]{:S(2)}) collective-permute-start(bf16[272,128]{1,0:T(8,128)(2,1)S(1)} %get-tuple-element.39.own_ref), channel_id=1, source_target_pairs={{0,24},{8,0},{16,8},{24,16},{1,25},{9,1},{17,9},{25,17},{2,26},{10... | collective-permute-start | bytes 208904 | tf_op jit(solution)/shard_map/ppermute | solution.py:426
  14.5 4.7 %collective-permute-start.4 = (bf16[272,128]{1,0:T(8,128)(2,1)S(1)}, bf16[272,128]{1,0:T(8,128)(2,1)S(1)}, u32[]{:S(2)}, u32[]{:S(2)}) collective-permute-start(bf16[272,128]{1,0:T(8,128)(2,1)S(1)} %get-tuple-element.39.own_ref), channel_id=1, source_target_pairs={{0,16},{8,24},{16,0},{24,8},{1,17},{9,25},{17,1},{25,9},{2,18},{10... | collective-permute-start | bytes 208904 | tf_op jit(solution)/shard_map/ppermute | solution.py:426
  14.9 5.1 %collective-permute-start.3 = (bf16[272,128]{1,0:T(8,128)(2,1)S(1)}, bf16[272,128]{1,0:T(8,128)(2,1)S(1)}, u32[]{:S(2)}, u32[]{:S(2)}) collective-permute-start(bf16[272,128]{1,0:T(8,128)(2,1)S(1)} %get-tuple-element.39.own_ref), channel_id=1, source_target_pairs={{0,8},{8,16},{16,24},{24,0},{1,9},{9,17},{17,25},{25,1},{2,10},{10... | collective-permute-start | bytes 208904 | tf_op jit(solution)/shard_map/ppermute | solution.py:426
  19.9 9.3 %copy-start.6 = (bf16[256,512]{1,0:T(8,128)(2,1)S(1)}, bf16[256,512]{1,0:T(8,128)(2,1)}, u32[]{:S(2)}) copy-start(bf16[256,512]{1,0:T(8,128)(2,1)} %out_gate_ref.1) | copy-start | bytes 786436
  19.9 9.4 %copy-start.14 = (f32[128]{0:T(128)S(1)}, f32[128]{0:T(128)}, u32[]{:S(2)}) copy-start(f32[128]{0:T(128)} %param.21) | copy-start | bytes 1540
  20.3 5.8 %collective-permute-start.8 = (bf16[272,128]{1,0:T(8,128)(2,1)S(1)}, bf16[272,128]{1,0:T(8,128)(2,1)S(1)}, u32[]{:S(2)}, u32[]{:S(2)}) collective-permute-start(bf16[272,128]{1,0:T(8,128)(2,1)S(1)} %get-tuple-element.45), channel_id=1, source_target_pairs={{0,96},{32,0},{64,32},{96,64},{1,97},{33,1},{65,33},{97,65},{2,98}... | collective-permute-start | bytes 208904 | tf_op jit(solution)/shard_map/ppermute | solution.py:426
  24.1 4.8 %collective-permute-start.7 = (bf16[272,128]{1,0:T(8,128)(2,1)S(1)}, bf16[272,128]{1,0:T(8,128)(2,1)S(1)}, u32[]{:S(2)}, u32[]{:S(2)}) collective-permute-start(bf16[272,128]{1,0:T(8,128)(2,1)S(1)} %get-tuple-element.45), channel_id=1, source_target_pairs={{0,64},{32,96},{64,0},{96,32},{1,65},{33,97},{65,1},{97,33},{2,66}... | collective-permute-start | bytes 208904 | tf_op jit(solution)/shard_map/ppermute | solution.py:426
  24.1 5.1 %collective-permute-start.6 = (bf16[272,128]{1,0:T(8,128)(2,1)S(1)}, bf16[272,128]{1,0:T(8,128)(2,1)S(1)}, u32[]{:S(2)}, u32[]{:S(2)}) collective-permute-start(bf16[272,128]{1,0:T(8,128)(2,1)S(1)} %get-tuple-element.45), channel_id=1, source_target_pairs={{0,32},{32,64},{64,96},{96,0},{1,33},{33,65},{65,97},{97,1},{2,34}... | collective-permute-start | bytes 208904 | tf_op jit(solution)/shard_map/ppermute | solution.py:426
  29.3 6.5 %copy-start.3 = (bf16[1024,2048]{1,0:T(8,128)(2,1)S(1)}, bf16[1024,2048]{1,0:T(8,128)(2,1)}, u32[]{:S(2)}) copy-start(bf16[1024,2048]{1,0:T(8,128)(2,1)} %weight_ref.1) | copy-start | bytes 12582916
  29.3 6.5 %copy-start.4 = (bf16[128,2048]{1,0:T(8,128)(2,1)S(1)}, bf16[128,2048]{1,0:T(8,128)(2,1)}, u32[]{:S(2)}) copy-start(bf16[128,2048]{1,0:T(8,128)(2,1)} %residual_ref.1) | copy-start | bytes 1572868
  29.3 6.5 %copy-start.10 = (f32[2048]{0:T(1024)S(1)}, f32[2048]{0:T(1024)}, u32[]{:S(2)}) copy-start(f32[2048]{0:T(1024)} %param.23) | copy-start | bytes 24580
  30.0 5.7 %collective-permute-start.9 = (bf16[128,512]{1,0:T(8,128)(2,1)S(1)}, bf16[128,512]{1,0:T(8,128)(2,1)S(1)}, u32[]{:S(2)}, u32[]{:S(2)}) collective-permute-start(bf16[128,512]{1,0:T(8,128)(2,1)S(1)} %get-tuple-element.53), channel_id=1, source_target_pairs={{0,1},{1,0},{2,3},{3,2},{4,5},{5,4},{6,7},{7,6},{8,9},{9,8},{10,11... | collective-permute-start | bytes 393224 | tf_op jit(solution)/shard_map/ppermute | solution.py:494
  35.8 31.5 %copy-start.1 = (bf16[1,2048,512]{2,1,0:T(8,128)(2,1)S(1)}, bf16[1,2048,512]{2,1,0:T(8,128)(2,1)}, u32[]{:S(2)}) copy-start(bf16[1,2048,512]{2,1,0:T(8,128)(2,1)} %up.1) | copy-start | bytes 6291460
  35.8 31.4 %copy-start.2 = (bf16[1,512,2048]{2,1,0:T(8,128)(2,1)S(1)}, bf16[1,512,2048]{2,1,0:T(8,128)(2,1)}, u32[]{:S(2)}) copy-start(bf16[1,512,2048]{2,1,0:T(8,128)(2,1)} %down.1) | copy-start | bytes 6291460
  38.3 28.9 %copy-start = (bf16[1,2048,512]{2,1,0:T(8,128)(2,1)S(1)}, bf16[1,2048,512]{2,1,0:T(8,128)(2,1)}, u32[]{:S(2)}) copy-start(bf16[1,2048,512]{2,1,0:T(8,128)(2,1)} %gate.1) | copy-start | bytes 6291460

commit v7 on v6

--- a/solution.py
+++ b/solution.py
@@ -16,7 +16,7 @@
 
 VMEM_SPEC = pl.BlockSpec(memory_space=pltpu.VMEM)
 SMEM_SPEC = pl.BlockSpec(memory_space=pltpu.SMEM)
-HBM_SPEC = pl.BlockSpec(memory_space=pl.ANY)
+ANY_SPEC = pl.BlockSpec(memory_space=pl.ANY)
 SUB = 16
 LANES = 128
 SWAP = SUB * SUB
@@ -129,36 +129,48 @@
     )(arrived, gate_weight, up_weight, down_weight)
 
 
-def combine_kernel(slots_ref, returned_ref, merged_ref, weights_ref, out_ref, picked):
+def combine_kernel(slots_vmem, returned_ref, merged_ref, weights_ref, out_hbm, out_ref, slots_ref, sem, sems):
+    indices = pltpu.make_async_copy(slots_vmem, slots_ref, sem.at[0])
+    indices.start()
     swap = swap_matrix()
     rows, width = merged_ref.shape
-
-    def copy_row(i, carry):
-        picked[0, i] = returned_ref[slots_ref[0, i]]
-        picked[1, i] = returned_ref[slots_ref[1, i]]
-        return carry
-
-    lax.fori_loop(0, rows, copy_row, 0, unroll=8)
+    indices.wait()
+    copies = []
     for g in range(rows // SUB):
         group = slice(g * SUB, (g + 1) * SUB)
-        first, second = exchange(swap, [picked[k, group].reshape(SWAP, LANES) for k in range(2)])
+        picked = [
+            jnp.concatenate([returned_ref[slots_ref[k, g * SUB + i]] for i in range(SUB)], axis=0) for k in range(2)
+        ]
+        first, second = exchange(swap, picked)
         for j in range(width // LANES):
             lanes = slice(j * LANES, (j + 1) * LANES)
             part = slice(j * SUB, (j + 1) * SUB)
             total = weights_ref[0, group] * first[part] + weights_ref[1, group] * second[part]
             out_ref[group, lanes] = (merged_ref[group, lanes].astype(jnp.float32) + total).astype(jnp.bfloat16)
+        if g % 2 == 1:
+            both = pl.ds((g - 1) * SUB, 2 * SUB)
+            copies.append(pltpu.make_async_copy(out_ref.at[both], out_hbm.at[both], sems.at[g // 2]))
+            copies[-1].start()
+    for copy in copies:
+        copy.wait()
 
 
 def combine(slots, returned, merged, weights):
     rows = merged.shape[0]
-    return call(
+    return pl.pallas_call(
         combine_kernel,
-        shape_of(merged.shape, jnp.bfloat16),
-        (slots, returned, merged, weights),
-        1,
-        [pltpu.VMEM((2, rows, SUB, LANES), jnp.bfloat16)],
-        room=8,
-    )
+        out_shape=shape_of(merged.shape, jnp.bfloat16),
+        in_specs=[VMEM_SPEC] * 4,
+        out_specs=ANY_SPEC,
+        scratch_shapes=[
+            pltpu.VMEM(merged.shape, jnp.bfloat16),
+            pltpu.SMEM(slots.shape, jnp.int32),
+            pltpu.SemaphoreType.DMA((1,)),
+            pltpu.SemaphoreType.DMA((rows // SUB // 2,)),
+        ],
+        compiler_params=limited(8),
+        name="combine",
+    )(slots, returned, merged, weights)
 
 
 def pieces(value, count):
@@ -178,33 +190,29 @@
 
 def running_sums(logits):
     length = logits.shape[0]
-    blocks = length // BLOCK
     decay_log = (jnp.minimum(logits, 0.0) - jnp.log1p(jnp.exp(-jnp.abs(logits)))) / 16.0
     parts = pieces(decay_log, 3)
     row = lax.broadcasted_iota(jnp.int32, (length, length), 0)
     column = lax.broadcasted_iota(jnp.int32, (length, length), 1)
     earlier = (row >= column) & (row // BLOCK == column // BLOCK)
     earlier = earlier.astype(jnp.float32).astype(jnp.bfloat16)
-    running = sum(product(earlier, part) for part in parts)
-    token = lax.broadcasted_iota(jnp.int32, (length, blocks * LANES), 0)
-    lane = lax.broadcasted_iota(jnp.int32, (length, blocks * LANES), 1)
-    member = (token // BLOCK == lane // LANES).astype(jnp.float32).astype(jnp.bfloat16)
-    block_decay = jnp.exp(sum(product(part, member, 0, 0) for part in parts))
-    return running, block_decay
-
-
-def grow(states, n, running, block_decay, keys_ref, values_ref):
+    return sum(product(earlier, part) for part in parts)
+
+
+def grow(states, n, running, keys_ref, values_ref):
     wide = 2 * VALUE_DIM
     rows = slice(n * BLOCK, (n + 1) * BLOCK)
     closing = running[(n + 1) * BLOCK - 1 : (n + 1) * BLOCK]
     key_closing = keys_ref[rows].astype(jnp.float32) * jnp.exp(closing - running[rows])
     key_closing = key_closing.astype(jnp.bfloat16)
+    decay = jnp.exp(closing)
+    lane = lax.broadcasted_iota(jnp.int32, (VALUE_DIM, LANES), 1)
     after = []
     for p, state in enumerate(states):
         lanes = slice(p * LANES, (p + 1) * LANES)
-        grown = product(key_closing[:, lanes], values_ref[rows, p * wide : (p + 1) * wide], 0, 0)
-        grown = jnp.concatenate([grown[:KEY_DIM, :VALUE_DIM], grown[KEY_DIM:, VALUE_DIM:]], axis=0)
-        after.append(block_decay[lanes, n * LANES : (n + 1) * LANES] * state + grown)
+        grown = product(values_ref[rows, p * wide : (p + 1) * wide], key_closing[:, lanes], 0, 0)
+        grown = jnp.where(lane < KEY_DIM, grown[:VALUE_DIM], grown[VALUE_DIM:])
+        after.append(decay[:, lanes] * state + grown)
     return after
 
 
@@ -221,17 +229,17 @@
     length, channels = keys_ref.shape
     blocks = length // BLOCK
     pairs = channels // LANES
-    running, block_decay = running_sums(logits_ref[...].astype(jnp.float32))
+    running = running_sums(logits_ref[...].astype(jnp.float32))
     copies[1].wait()
     copies[2].wait()
-    states = [jnp.zeros((LANES, VALUE_DIM), jnp.float32)] * pairs
+    states = [jnp.zeros((VALUE_DIM, LANES), jnp.float32)] * pairs
     total = jnp.zeros((1, channels), jnp.float32)
     for n in range(blocks):
         total = total + running[(n + 1) * BLOCK - 1 : (n + 1) * BLOCK]
-        states = grow(states, n, running, block_decay, keys_ref, values_ref)
+        states = grow(states, n, running, keys_ref, values_ref)
     for p in range(pairs):
-        message_ref[p * LANES : (p + 1) * LANES] = states[p].astype(jnp.bfloat16)
-    message_ref[channels:] = pack_decay(jnp.exp(total))
+        message_ref[p * VALUE_DIM : (p + 1) * VALUE_DIM] = states[p].astype(jnp.bfloat16)
+    message_ref[pairs * VALUE_DIM :] = pack_decay(jnp.exp(total))
 
 
 def pack_decay(decay):
@@ -246,47 +254,39 @@
     return packed.astype(jnp.bfloat16)
 
 
-def unpack_decay(message_ref):
-    channels = message_ref.shape[0] - SUB
-    pairs = channels // LANES
-    packed = message_ref[channels:].astype(jnp.float32)
-    diagonal = lax.broadcasted_iota(jnp.int32, (LANES, LANES), 0) == lax.broadcasted_iota(
-        jnp.int32, (LANES, LANES), 1
-    )
-    ones = jnp.ones((LANES, VALUE_DIM), jnp.bfloat16)
-    spread = []
-    for p in range(pairs):
-        both = [jnp.where(diagonal, packed[k : k + 1], 0.0).astype(jnp.bfloat16) for k in (p, pairs + p)]
-        spread.append(product(both[0], ones) + product(both[1], ones))
-    line = jnp.concatenate([packed[p : p + 1] + packed[pairs + p : pairs + p + 1] for p in range(pairs)], axis=1)
-    return line, jnp.concatenate(spread, axis=0)
+def unpack(message_ref):
+    states = message_ref.shape[0] - SUB
+    pairs = states // VALUE_DIM
+    packed = message_ref[states:].astype(jnp.float32)
+    decays = [packed[p : p + 1] + packed[pairs + p : pairs + p + 1] for p in range(pairs)]
+    return decays, [message_ref[p * VALUE_DIM : (p + 1) * VALUE_DIM].astype(jnp.float32) for p in range(pairs)]
 
 
 def stage_kernel(place_ref, own_ref, back1_ref, back2_ref, back3_ref, before_ref, decay_ref, message_ref):
     place = place_ref[0]
-    channels = own_ref.shape[0] - SUB
-    received = []
-    for ref in (back1_ref, back2_ref, back3_ref):
-        line, spread = unpack_decay(ref)
-        received.append((line, spread, ref[:channels].astype(jnp.float32)))
-    own_line, own_spread = unpack_decay(own_ref)
-    before = jnp.zeros((channels, VALUE_DIM), jnp.float32)
-    decay = jnp.ones((channels, VALUE_DIM), jnp.float32)
-    for k in (3, 2, 1):
-        valid = place >= k
-        _, spread, state = received[k - 1]
-        before = jnp.where(valid, spread * before + state, before)
-        decay = jnp.where(valid, spread * decay, decay)
-    before_ref[...] = before
-    decay_ref[...] = decay
-    total = own_spread * before + own_ref[:channels].astype(jnp.float32)
-    for k in (3, 2, 1):
-        later = place < k
-        _, spread, state = received[k - 1]
-        total = jnp.where(later, spread * total + state, total)
-    message_ref[:channels] = total.astype(jnp.bfloat16)
-    line = own_line * received[0][0] * received[1][0] * received[2][0]
-    message_ref[channels:] = pack_decay(line)
+    own_decays, own_states = unpack(own_ref)
+    pairs = len(own_decays)
+    received = [unpack(ref) for ref in (back1_ref, back2_ref, back3_ref)]
+    whole = []
+    for p in range(pairs):
+        rows = slice(p * VALUE_DIM, (p + 1) * VALUE_DIM)
+        before = jnp.zeros((VALUE_DIM, LANES), jnp.float32)
+        decay = jnp.ones((1, LANES), jnp.float32)
+        for k in (3, 2, 1):
+            valid = place >= k
+            passed, state = received[k - 1][0][p], received[k - 1][1][p]
+            before = jnp.where(valid, passed * before + state, before)
+            decay = jnp.where(valid, passed * decay, decay)
+        before_ref[rows] = before
+        decay_ref[p * 8 : (p + 1) * 8] = jnp.broadcast_to(decay, (8, LANES))
+        total = own_decays[p] * before + own_states[p]
+        for k in (3, 2, 1):
+            later = place < k
+            passed, state = received[k - 1][0][p], received[k - 1][1][p]
+            total = jnp.where(later, passed * total + state, total)
+        message_ref[rows] = total.astype(jnp.bfloat16)
+        whole.append(own_decays[p] * received[0][0][p] * received[1][0][p] * received[2][0][p])
+    message_ref[pairs * VALUE_DIM :] = pack_decay(jnp.concatenate(whole, axis=1))
 
 
 def masked_heads(rows):
@@ -296,12 +296,18 @@
     ).astype(jnp.bfloat16)
 
 
-def within_kernel(queries_ref, keys_ref, values_ref, logits_ref, partial_ref, reach_ref):
+def within_kernel(
+    queries_ref, keys_ref, values_ref, logits_ref, head_gain_ref, out_gate_ref, partial_ref, reach_ref, gating_ref
+):
+    for h in range(out_gate_ref.shape[1] // VALUE_DIM):
+        place = slice(h * VALUE_DIM, (h + 1) * VALUE_DIM)
+        gate = out_gate_ref[:, place].astype(jnp.float32)
+        gating_ref[:, place] = head_gain_ref[...] * (gate / (1.0 + jnp.exp(-gate)))
     length, channels = keys_ref.shape
     blocks = length // BLOCK
     pairs = channels // LANES
-    running_all, block_decay = running_sums(logits_ref[...].astype(jnp.float32))
-    states = [jnp.zeros((LANES, VALUE_DIM), jnp.float32)] * pairs
+    running_all = running_sums(logits_ref[...].astype(jnp.float32))
+    states = [jnp.zeros((VALUE_DIM, LANES), jnp.float32)] * pairs
     lead = jnp.zeros((1, channels), jnp.float32)
     row = lax.broadcasted_iota(jnp.int32, (2 * BLOCK, BLOCK), 0)
     column = lax.broadcasted_iota(jnp.int32, (2 * BLOCK, BLOCK), 1)
@@ -317,39 +323,39 @@
             lanes = slice(p * LANES, (p + 1) * LANES)
             masked = masked_heads(query_scaled[:, lanes])
             scores = jnp.where(causal, product(masked, key_inverse[:, lanes], 1, 1), 0.0).astype(jnp.bfloat16)
-            carried = product(masked, states[p].astype(jnp.bfloat16))
+            carried = product(masked, states[p].astype(jnp.bfloat16), 1, 1)
             for h in range(2):
                 place = slice((2 * p + h) * VALUE_DIM, (2 * p + h + 1) * VALUE_DIM)
                 part = slice(h * BLOCK, (h + 1) * BLOCK)
                 partial_ref[rows, place] = product(scores[part], values_ref[rows, place]) + carried[part]
         if n + 1 < blocks:
-            states = grow(states, n, running_all, block_decay, keys_ref, values_ref)
+            states = grow(states, n, running_all, keys_ref, values_ref)
 
 
 def finish_kernel(
     place_ref, plane_ref, back1_ref, back2_ref, back3_ref, before_y_ref, decay_y_ref, before_x_ref, decay_x_ref,
-    partial_ref, reach_ref, head_gain_ref, out_gate_ref, kept_ref, given_ref, whole,
+    partial_ref, reach_ref, gating_ref, kept_ref, given_ref, whole,
 ):
     core, plane = place_ref[0], plane_ref[0]
     length, channels = reach_ref.shape
     pairs = channels // LANES
-    state = jnp.zeros((channels, VALUE_DIM), jnp.float32)
-    for k, ref in ((3, back3_ref), (2, back2_ref), (1, back1_ref)):
-        passed = unpack_decay(ref)[1] * state + ref[:channels].astype(jnp.float32)
-        state = jnp.where(plane >= k, passed, state)
-    state = before_y_ref[...] + decay_y_ref[...] * state
-    state = (before_x_ref[...] + decay_x_ref[...] * state).astype(jnp.bfloat16)
+    received = [unpack(ref) for ref in (back1_ref, back2_ref, back3_ref)]
     half = length // 2
     for p in range(pairs):
         lanes = slice(p * LANES, (p + 1) * LANES)
-        carried = product(masked_heads(reach_ref[:, lanes]), state[lanes])
+        rows = slice(p * VALUE_DIM, (p + 1) * VALUE_DIM)
+        state = jnp.zeros((VALUE_DIM, LANES), jnp.float32)
+        for k in (3, 2, 1):
+            decay, grown = received[k - 1][0][p], received[k - 1][1][p]
+            state = jnp.where(plane >= k, decay * state + grown, state)
+        state = before_y_ref[rows] + decay_y_ref[p * 8 : p * 8 + 1] * state
+        state = before_x_ref[rows] + decay_x_ref[p * 8 : p * 8 + 1] * state
+        carried = product(masked_heads(reach_ref[:, lanes]), state.astype(jnp.bfloat16), 1, 1)
         for h in range(2):
             place = slice((2 * p + h) * VALUE_DIM, (2 * p + h + 1) * VALUE_DIM)
             attended = partial_ref[:, place] + carried[h * length : (h + 1) * length]
             scale = lax.rsqrt(jnp.mean(attended * attended, axis=1, keepdims=True) + 1e-06)
-            gate = out_gate_ref[:, place].astype(jnp.float32)
-            result = attended * scale * head_gain_ref[...] * (gate / (1.0 + jnp.exp(-gate)))
-            result = result.astype(jnp.bfloat16)
+            result = (attended * scale * gating_ref[:, place]).astype(jnp.bfloat16)
             whole[0, :, place] = result[:half]
             whole[1, :, place] = result[half:]
     kept_ref[...] = whole[core]
@@ -357,9 +363,11 @@
 
 
 def project_kernel(
-    place_ref, owners_ref, kept_ref, taken_ref, weight_ref, residual_ref, norm_gain_ref, merged_ref, outgoing_ref,
-    chunked,
+    place_ref, owners_vmem, kept_ref, taken_ref, weight_ref, residual_ref, norm_gain_ref, merged_ref, outgoing_ref,
+    chunked, owners_ref, sem,
 ):
+    indices = pltpu.make_async_copy(owners_vmem, owners_ref, sem.at[0])
+    indices.start()
     core = place_ref[0]
     rows, width = residual_ref.shape
     depth = kept_ref.shape[1]
@@ -392,12 +400,17 @@
     experts_total = owners_ref.shape[1]
     capacity = outgoing_ref.shape[0] // experts_total
 
-    def copy_rows(expert, carry):
-        for place in range(capacity):
-            outgoing_ref[capacity * expert + place] = chunked[owners_ref[place, expert]]
+    batch = 8
+    indices.wait()
+
+    def copy_rows(step, carry):
+        first = step * batch
+        rows = [chunked[owners_ref[place, first + k]] for k in range(batch) for place in range(capacity)]
+        for k, row in enumerate(rows):
+            outgoing_ref[capacity * first + k] = row
         return carry
 
-    lax.fori_loop(0, experts_total, copy_rows, 0, unroll=8)
+    lax.fori_loop(0, experts_total // batch, copy_rows, 0, unroll=2)
 
 
 def shape_of(shape, dtype):
@@ -412,7 +425,7 @@
     return pl.pallas_call(
         kernel,
         out_shape=outs,
-        in_specs=[SMEM_SPEC] * scalars + [HBM_SPEC if far else VMEM_SPEC] * (len(operands) - scalars),
+        in_specs=[SMEM_SPEC] * scalars + [ANY_SPEC if far else VMEM_SPEC] * (len(operands) - scalars),
         out_specs=jax.tree.map(lambda _: VMEM_SPEC, outs),
         scratch_shapes=list(scratch),
         cost_estimate=pl.CostEstimate(flops=cost * 400, bytes_accessed=cost, transcendentals=0),
@@ -449,8 +462,10 @@
     values = value_rows.shape[1]
     f32, bf16 = jnp.float32, jnp.bfloat16
     z, y, x, core = (lax.axis_index(axis).astype(jnp.int32).reshape(1) for axis in SP_TP)
-    message_shape = shape_of((channels + SUB, VALUE_DIM), bf16)
-    state_shape = shape_of((channels, VALUE_DIM), f32)
+    pairs = channels // LANES
+    message_shape = shape_of((pairs * VALUE_DIM + SUB, LANES), bf16)
+    state_shape = shape_of((pairs * VALUE_DIM, LANES), f32)
+    decay_shape = shape_of((pairs * 8, LANES), f32)
     message = call(
         state_kernel,
         message_shape,
@@ -470,24 +485,24 @@
     behind = from_behind(message, "sp_2")
     slots, owners, weights, *behind = lax.optimization_barrier((slots, owners, weights, *behind))
     before_x, decay_x, message_x = call(
-        stage_kernel, (state_shape, state_shape, message_shape), (x, message, *behind), 1
-    )
-    partial, reach = call(
+        stage_kernel, (state_shape, decay_shape, message_shape), (x, message, *behind), 1
+    )
+    partial, reach, gating = call(
         within_kernel,
-        (shape_of((length, values), f32), shape_of((length, channels), f32)),
-        (queries, key_rows, value_rows, gate_logits),
+        (shape_of((length, values), f32), shape_of((length, channels), f32), shape_of((length, values), f32)),
+        (queries, key_rows, value_rows, gate_logits, head_gain.reshape(1, -1), out_gate),
     )
     behind = from_behind(message_x, "sp_1")
-    partial, reach, *behind = lax.optimization_barrier((partial, reach, *behind))
+    partial, reach, gating, *behind = lax.optimization_barrier((partial, reach, gating, *behind))
     before_y, decay_y, message_y = call(
-        stage_kernel, (state_shape, state_shape, message_shape), (y, message_x, *behind), 1
+        stage_kernel, (state_shape, decay_shape, message_shape), (y, message_x, *behind), 1
     )
     behind = from_behind(message_y, "sp_0")
     half = shape_of((length // 2, values), bf16)
     kept, given = call(
         finish_kernel,
         (half, half),
-        (core, z, *behind, before_y, decay_y, before_x, decay_x, partial, reach, head_gain.reshape(1, -1), out_gate),
+        (core, z, *behind, before_y, decay_y, before_x, decay_x, partial, reach, gating),
         2,
         [pltpu.VMEM((2, length // 2, values), bf16)],
     )
@@ -499,8 +514,12 @@
             shape_of((experts_total * capacity, SUB, LANES), bf16),
         ),
         (core, owners, kept, taken, out_weight, residual, norm_gain.reshape(1, -1)),
-        2,
-        [pltpu.VMEM((row_count, SUB, LANES), bf16)],
+        1,
+        [
+            pltpu.VMEM((row_count, SUB, LANES), bf16),
+            pltpu.SMEM(owners.shape, jnp.int32),
+            pltpu.SemaphoreType.DMA((1,)),
+        ],
         room=14,
     )
     block = (experts_total, capacity * SUB, LANES)

time: 102 us -> 100 us (0.980)
  Pallas kernels: 13.8 us -> 11.8 us
    pallas_call x8 -> x7, Pallas kernels: 10.3 us -> 6.54 us  [call(): pl.pallas_call(kernel, out_shape=outs, in_specs=[SMEM_SPEC] * scalars + [...]
    pallas_call x0 -> x1, Pallas kernels: none -> 1.71 us  [combine(): pl.pallas_call(combine_kernel, out_shape=shape_of(merged.shape, jnp.bfloa...]
where the time goes in v7:
time: 100 us
  blocking collectives  58.1 us (58%)
  starting transfers between devices  17.6 us (18%)
  waiting for transfers between devices  12.4 us (12%)
  Pallas kernels  11.8 us (12%)
    all_to_all x1, blocking collectives, local(): lax.all_to_all(outgoing.reshape(block), SP_TP, split_axis=0, concat_axis=...  29.2 us
    all_to_all x1, blocking collectives, local(): lax.all_to_all(served.reshape(block), SP_TP, split_axis=0, concat_axis=0,...  28.9 us
    ppermute x9, starting transfers between devices, from_behind(): lax.ppermute(message, axis, [(i, (i + k) % RING) for i in range(RING)])  12.9 us
    ppermute x9, waiting for transfers between devices, from_behind(): lax.ppermute(message, axis, [(i, (i + k) % RING) for i in range(RING)])  11.4 us
    pallas_call x7, Pallas kernels, call(): pl.pallas_call(kernel, out_shape=outs, in_specs=[SMEM_SPEC] * scalars + [...  6.54 us
    ppermute x1, starting transfers between devices, local(): taken = lax.ppermute(given, 'tp', [(0, 1), (1, 0)])  4.75 us
    pallas_call x1, Pallas kernels, experts(): pl.pallas_call(experts_kernel, out_shape=jax.ShapeDtypeStruct(arrived.sha...  3.51 us
  transfers between devices with their start and end apart: 10, of which 8 were waited for; matrix products, arithmetic and copies ran while one was open for 0% of the time, Pallas kernels for 2%

profile of v7, /device:TPU:1, one launch (start us, length us, event | category | flops | bytes accessed | tf_op | source)
XLA Modules:
  0.0 100.0 jit_solution(438319847990921656)
XLA Ops:
  0.0 1.9 %shard_map.146.own_ref = bf16[272,128]{1,0:T(8,128)(2,1)S(1)} custom-call(bf16[256,256]{1,0:T(8,128)(2,1)} %keys_ref.1, bf16[256,512]{1,0:T(8,128)(2,1)} %values_ref.1, bf16[256,256]{1,0:T(8,128)(2,1)} %logits_ref.1), custom_call_target="tpu_custom_call" | custom-call | flops 4000000000 | bytes 10000000 | tf_op jit(solution)/shard_map/pallas_call | solution.py:425
  1.9 3.4 %collective-permute-start.2 = (bf16[272,128]{1,0:T(8,128)(2,1)S(1)}, bf16[272,128]{1,0:T(8,128)(2,1)S(1)}, u32[]{:S(2)}, u32[]{:S(2)}) collective-permute-start(bf16[272,128]{1,0:T(8,128)(2,1)S(1)} %shard_map.146.own_ref), channel_id=1, source_target_pairs={{0,6},{2,0},{4,2},{6,4},{1,7},{3,1},{5,3},{7,5},{8,14},{10,8},{12,... | collective-permute-start | bytes 208904 | tf_op jit(solution)/shard_map/ppermute | solution.py:439
  5.3 0.5 collective-permute-start.1
  5.8 0.6 collective-permute-start
  6.4 0.3 shard_map.145
  6.7 3.3 %collective-permute-done.1.back2_ref = bf16[272,128]{1,0:T(8,128)(2,1)S(1)} collective-permute-done((bf16[272,128]{1,0:T(8,128)(2,1)S(1)}, bf16[272,128]{1,0:T(8,128)(2,1)S(1)}, u32[]{:S(2)}, u32[]{:S(2)}) %collective-permute-start.1) | collective-permute-done | bytes 69664 | tf_op jit(solution)/shard_map/ppermute | solution.py:439
  10.0 1.1 %collective-permute-done.back1_ref = bf16[272,128]{1,0:T(8,128)(2,1)S(1)} collective-permute-done((bf16[272,128]{1,0:T(8,128)(2,1)S(1)}, bf16[272,128]{1,0:T(8,128)(2,1)S(1)}, u32[]{:S(2)}, u32[]{:S(2)}) %collective-permute-start) | collective-permute-done | bytes 69664 | tf_op jit(solution)/shard_map/ppermute | solution.py:439
  11.1 0.0 copy-start.9
  11.1 0.0 copy-start.14
  11.1 0.1 shard_map.147
  11.3 2.8 %collective-permute-start.5 = (bf16[272,128]{1,0:T(8,128)(2,1)S(1)}, bf16[272,128]{1,0:T(8,128)(2,1)S(1)}, u32[]{:S(2)}, u32[]{:S(2)}) collective-permute-start(bf16[272,128]{1,0:T(8,128)(2,1)S(1)} %get-tuple-element.41.own_ref), channel_id=1, source_target_pairs={{0,24},{8,0},{16,8},{24,16},{1,25},{9,1},{17,9},{25,17},{2,26},{10... | collective-permute-start | bytes 208904 | tf_op jit(solution)/shard_map/ppermute | solution.py:439
  14.1 0.3 collective-permute-start.4
  14.4 0.7 collective-permute-start.3
  15.1 1.7 %shard_map.148 = (f32[256,512]{1,0:T(8,128)S(1)}, f32[256,256]{1,0:T(8,128)S(1)}, f32[256,512]{1,0:T(8,128)S(1)}) custom-call(bf16[256,256]{1,0:T(8,128)(2,1)S(1)} %copy-done.9, bf16[256,256]{1,0:T(8,128)(2,1)S(1)} %copy-done.7, bf16[256,512]{1,0:T(8,128)(2,1)S(1)} %copy-done.5, bf16[256,256]{1,0:T(8,128)(2,1)S(1)} %copy-done.8, f32[1,128]{1,0:T(1,128)S(1)} %bitcast.21, ...), custom_call_target="tpu_custom_call" | custom-call | flops 4000000000 | bytes 10000000 | tf_op jit(solution)/shard_map/pallas_call | solution.py:425
  16.9 1.9 %collective-permute-done.4.back2_ref = bf16[272,128]{1,0:T(8,128)(2,1)S(1)} collective-permute-done((bf16[272,128]{1,0:T(8,128)(2,1)S(1)}, bf16[272,128]{1,0:T(8,128)(2,1)S(1)}, u32[]{:S(2)}, u32[]{:S(2)}) %collective-permute-start.4) | collective-permute-done | bytes 69664 | tf_op jit(solution)/shard_map/ppermute | solution.py:439
  18.8 0.7 collective-permute-done.3.back1_ref
  19.5 0.1 shard_map.149
  19.6 3.8 %collective-permute-start.8 = (bf16[272,128]{1,0:T(8,128)(2,1)S(1)}, bf16[272,128]{1,0:T(8,128)(2,1)S(1)}, u32[]{:S(2)}, u32[]{:S(2)}) collective-permute-start(bf16[272,128]{1,0:T(8,128)(2,1)S(1)} %get-tuple-element.48), channel_id=1, source_target_pairs={{0,96},{32,0},{64,32},{96,64},{1,97},{33,1},{65,33},{97,65},{2,98}... | collective-permute-start | bytes 208904 | tf_op jit(solution)/shard_map/ppermute | solution.py:439
  23.4 0.7 collective-permute-start.6
  24.1 1.3 %collective-permute-done.8.back3_ref = bf16[272,128]{1,0:T(8,128)(2,1)S(1)} collective-permute-done((bf16[272,128]{1,0:T(8,128)(2,1)S(1)}, bf16[272,128]{1,0:T(8,128)(2,1)S(1)}, u32[]{:S(2)}, u32[]{:S(2)}) %collective-permute-start.8) | collective-permute-done | bytes 69664 | tf_op jit(solution)/shard_map/ppermute | solution.py:439
  25.4 2.8 %collective-permute-done.7.back2_ref = bf16[272,128]{1,0:T(8,128)(2,1)S(1)} collective-permute-done((bf16[272,128]{1,0:T(8,128)(2,1)S(1)}, bf16[272,128]{1,0:T(8,128)(2,1)S(1)}, u32[]{:S(2)}, u32[]{:S(2)}) %collective-permute-start.7) | collective-permute-done | bytes 69664 | tf_op jit(solution)/shard_map/ppermute | solution.py:439
  28.2 0.4 collective-permute-done.6.back1_ref
  28.6 0.5 shard_map.150
  29.0 4.7 %collective-permute-start.9 = (bf16[128,512]{1,0:T(8,128)(2,1)S(1)}, bf16[128,512]{1,0:T(8,128)(2,1)S(1)}, u32[]{:S(2)}, u32[]{:S(2)}) collective-permute-start(bf16[128,512]{1,0:T(8,128)(2,1)S(1)} %get-tuple-element.57), channel_id=1, source_target_pairs={{0,1},{1,0},{2,3},{3,2},{4,5},{5,4},{6,7},{7,6},{8,9},{9,8},{10,11... | collective-permute-start | bytes 393224 | tf_op jit(solution)/shard_map/ppermute | solution.py:509
  33.8 1.0 collective-permute-done.9.taken_ref
  34.8 0.0 copy-start.2
  34.8 1.9 %shard_map.151 = (bf16[128,2048]{1,0:T(8,128)(2,1)S(1)}, bf16[384,16,128]{2,1,0:T(8,128)(2,1)S(1)}) custom-call(s32[1]{0:T(128)} %bitcast.3.place_ref, s32[8,128]{1,0:T(8,128)S(1)} %get-tuple-element.37.owners_vmem, bf16[128,512]{1,0:T(8,128)(2,1)S(1)} %get-tuple-element.56.kept_ref, bf16[128,512]{1,0:T(8,128)(2,1)S(1)} %collective-permute-done.9.taken_ref, ...), custom_call_target="tpu_custom_call" | custom-call | flops 4000000000 | bytes 10000000 | tf_op jit(solution)/shard_map/pallas_call | solution.py:425
  36.7 0.0 copy-start
  36.7 29.2 %all_to_all.10 = bf16[128,48,128]{2,1,0:T(8,128)(2,1)S(1)} all-to-all(bf16[128,48,128]{2,1,0:T(8,128)(2,1)S(1)} %bitcast.16), channel_id=1, replica_groups=mesh['sp_0'=4,'sp_1'=4,'sp_2'=4,'tp'=2] {'sp_0','sp_1','sp_2','tp'}, dimensions={0} | all-to-all | bytes 3145728 | tf_op jit(solution)/shard_map/all_to_all | solution.py:526
  65.9 3.5 %experts.1 = bf16[384,16,128]{2,1,0:T(8,128)(2,1)S(1)} custom-call(bf16[384,16,128]{2,1,0:T(8,128)(2,1)S(1)} %bitcast.14, bf16[1,2048,512]{2,1,0:T(8,128)(2,1)S(1)} %copy-done, bf16[1,2048,512]{2,1,0:T(8,128)(2,1)S(1)} %copy-done.1, bf16[1,512,2048]{2,1,0:T(8,128)(2,1)S(1)} %copy-done.2), custom_call_target="tpu_custom_call" | custom-call | tf_op jit(solution)/shard_map/experts/pallas_call | solution.py:117
  69.4 28.9 %all_to_all.11 = bf16[128,48,128]{2,1,0:T(8,128)(2,1)S(1)} all-to-all(bf16[128,48,128]{2,1,0:T(8,128)(2,1)S(1)} %bitcast.15), channel_id=1, replica_groups=mesh['sp_0'=4,'sp_1'=4,'sp_2'=4,'tp'=2] {'sp_0','sp_1','sp_2','tp'}, dimensions={0} | all-to-all | bytes 3145728 | tf_op jit(solution)/shard_map/all_to_all | solution.py:528
  98.3 1.7 %combine.1 = bf16[128,2048]{1,0:T(8,128)(2,1)} custom-call(s32[2,128]{1,0:T(2,128)S(1)} %get-tuple-element.36.slots_vmem, bf16[384,16,128]{2,1,0:T(8,128)(2,1)S(1)} %bitcast.13, bf16[128,2048]{1,0:T(8,128)(2,1)S(1)} %get-tuple-element.59.merged_ref, f32[2,128,128]{2,1,0:T(8,128)S(1)} %get-tuple-element.60.weights_ref), custom_call_target="tpu_custom_call" | custom-call | tf_op jit(solution)/shard_map/combine/pallas_call | solution.py:160
  (29 shorter events, 0.1 us)
Async XLA Ops:
  0.0 6.4 %copy-start.12 = (f32[128,2]{0,1:T(2,128)S(1)}, f32[128,2]{0,1:T(2,128)}, u32[]{:S(2)}) copy-start(f32[128,2]{0,1:T(2,128)} %param.26) | copy-start | bytes 3076
  0.0 6.4 %copy-start.13 = (f32[128]{0:T(128)S(1)}, f32[128]{0:T(128)}, u32[]{:S(2)}) copy-start(f32[128]{0:T(128)} %param.25) | copy-start | bytes 1540
  0.0 6.4 %copy-start.11 = (s32[128,2]{0,1:T(2,128)S(1)}, s32[128,2]{0,1:T(2,128)}, u32[]{:S(2)}) copy-start(s32[128,2]{0,1:T(2,128)} %param.24) | copy-start | bytes 3076
  1.9 4.8 %collective-permute-start.2 = (bf16[272,128]{1,0:T(8,128)(2,1)S(1)}, bf16[272,128]{1,0:T(8,128)(2,1)S(1)}, u32[]{:S(2)}, u32[]{:S(2)}) collective-permute-start(bf16[272,128]{1,0:T(8,128)(2,1)S(1)} %shard_map.146.own_ref), channel_id=1, source_target_pairs={{0,6},{2,0},{4,2},{6,4},{1,7},{3,1},{5,3},{7,5},{8,14},{10,8},{12,... | collective-permute-start | bytes 208904 | tf_op jit(solution)/shard_map/ppermute | solution.py:439
  5.3 4.7 %collective-permute-start.1 = (bf16[272,128]{1,0:T(8,128)(2,1)S(1)}, bf16[272,128]{1,0:T(8,128)(2,1)S(1)}, u32[]{:S(2)}, u32[]{:S(2)}) collective-permute-start(bf16[272,128]{1,0:T(8,128)(2,1)S(1)} %shard_map.146.own_ref), channel_id=1, source_target_pairs={{0,4},{2,6},{4,0},{6,2},{1,5},{3,7},{5,1},{7,3},{8,12},{10,14},{12... | collective-permute-start | bytes 208904 | tf_op jit(solution)/shard_map/ppermute | solution.py:439
  5.8 5.3 %collective-permute-start = (bf16[272,128]{1,0:T(8,128)(2,1)S(1)}, bf16[272,128]{1,0:T(8,128)(2,1)S(1)}, u32[]{:S(2)}, u32[]{:S(2)}) collective-permute-start(bf16[272,128]{1,0:T(8,128)(2,1)S(1)} %shard_map.146.own_ref), channel_id=1, source_target_pairs={{0,2},{2,4},{4,6},{6,0},{1,3},{3,5},{5,7},{7,1},{8,10},{10,12},{12... | collective-permute-start | bytes 208904 | tf_op jit(solution)/shard_map/ppermute | solution.py:439
  11.1 4.0 %copy-start.5 = (bf16[256,512]{1,0:T(8,128)(2,1)S(1)}, bf16[256,512]{1,0:T(8,128)(2,1)}, u32[]{:S(2)}) copy-start(bf16[256,512]{1,0:T(8,128)(2,1)} %values_ref.1) | copy-start | bytes 786436
  11.1 4.0 %copy-start.6 = (bf16[256,512]{1,0:T(8,128)(2,1)S(1)}, bf16[256,512]{1,0:T(8,128)(2,1)}, u32[]{:S(2)}) copy-start(bf16[256,512]{1,0:T(8,128)(2,1)} %out_gate_ref.1) | copy-start | bytes 786436
  11.1 4.0 %copy-start.7 = (bf16[256,256]{1,0:T(8,128)(2,1)S(1)}, bf16[256,256]{1,0:T(8,128)(2,1)}, u32[]{:S(2)}) copy-start(bf16[256,256]{1,0:T(8,128)(2,1)} %keys_ref.1) | copy-start | bytes 393220
  11.1 4.0 %copy-start.8 = (bf16[256,256]{1,0:T(8,128)(2,1)S(1)}, bf16[256,256]{1,0:T(8,128)(2,1)}, u32[]{:S(2)}) copy-start(bf16[256,256]{1,0:T(8,128)(2,1)} %logits_ref.1) | copy-start | bytes 393220
  11.1 4.0 %copy-start.9 = (bf16[256,256]{1,0:T(8,128)(2,1)S(1)}, bf16[256,256]{1,0:T(8,128)(2,1)}, u32[]{:S(2)}) copy-start(bf16[256,256]{1,0:T(8,128)(2,1)} %queries_ref.1) | copy-start | bytes 393220
  11.1 4.0 %copy-start.14 = (f32[128]{0:T(128)S(1)}, f32[128]{0:T(128)}, u32[]{:S(2)}) copy-start(f32[128]{0:T(128)} %param.21) | copy-start | bytes 1540
  11.3 5.6 %collective-permute-start.5 = (bf16[272,128]{1,0:T(8,128)(2,1)S(1)}, bf16[272,128]{1,0:T(8,128)(2,1)S(1)}, u32[]{:S(2)}, u32[]{:S(2)}) collective-permute-start(bf16[272,128]{1,0:T(8,128)(2,1)S(1)} %get-tuple-element.41.own_ref), channel_id=1, source_target_pairs={{0,24},{8,0},{16,8},{24,16},{1,25},{9,1},{17,9},{25,17},{2,26},{10... | collective-permute-start | bytes 208904 | tf_op jit(solution)/shard_map/ppermute | solution.py:439
  14.1 4.7 %collective-permute-start.4 = (bf16[272,128]{1,0:T(8,128)(2,1)S(1)}, bf16[272,128]{1,0:T(8,128)(2,1)S(1)}, u32[]{:S(2)}, u32[]{:S(2)}) collective-permute-start(bf16[272,128]{1,0:T(8,128)(2,1)S(1)} %get-tuple-element.41.own_ref), channel_id=1, source_target_pairs={{0,16},{8,24},{16,0},{24,8},{1,17},{9,25},{17,1},{25,9},{2,18},{10... | collective-permute-start | bytes 208904 | tf_op jit(solution)/shard_map/ppermute | solution.py:439
  14.4 5.1 %collective-permute-start.3 = (bf16[272,128]{1,0:T(8,128)(2,1)S(1)}, bf16[272,128]{1,0:T(8,128)(2,1)S(1)}, u32[]{:S(2)}, u32[]{:S(2)}) collective-permute-start(bf16[272,128]{1,0:T(8,128)(2,1)S(1)} %get-tuple-element.41.own_ref), channel_id=1, source_target_pairs={{0,8},{8,16},{16,24},{24,0},{1,9},{9,17},{17,25},{25,1},{2,10},{10... | collective-permute-start | bytes 208904 | tf_op jit(solution)/shard_map/ppermute | solution.py:439
  19.6 5.8 %collective-permute-start.8 = (bf16[272,128]{1,0:T(8,128)(2,1)S(1)}, bf16[272,128]{1,0:T(8,128)(2,1)S(1)}, u32[]{:S(2)}, u32[]{:S(2)}) collective-permute-start(bf16[272,128]{1,0:T(8,128)(2,1)S(1)} %get-tuple-element.48), channel_id=1, source_target_pairs={{0,96},{32,0},{64,32},{96,64},{1,97},{33,1},{65,33},{97,65},{2,98}... | collective-permute-start | bytes 208904 | tf_op jit(solution)/shard_map/ppermute | solution.py:439
  23.4 4.8 %collective-permute-start.7 = (bf16[272,128]{1,0:T(8,128)(2,1)S(1)}, bf16[272,128]{1,0:T(8,128)(2,1)S(1)}, u32[]{:S(2)}, u32[]{:S(2)}) collective-permute-start(bf16[272,128]{1,0:T(8,128)(2,1)S(1)} %get-tuple-element.48), channel_id=1, source_target_pairs={{0,64},{32,96},{64,0},{96,32},{1,65},{33,97},{65,1},{97,33},{2,66}... | collective-permute-start | bytes 208904 | tf_op jit(solution)/shard_map/ppermute | solution.py:439
  23.4 5.1 %collective-permute-start.6 = (bf16[272,128]{1,0:T(8,128)(2,1)S(1)}, bf16[272,128]{1,0:T(8,128)(2,1)S(1)}, u32[]{:S(2)}, u32[]{:S(2)}) collective-permute-start(bf16[272,128]{1,0:T(8,128)(2,1)S(1)} %get-tuple-element.48), channel_id=1, source_target_pairs={{0,32},{32,64},{64,96},{96,0},{1,33},{33,65},{65,97},{97,1},{2,34}... | collective-permute-start | bytes 208904 | tf_op jit(solution)/shard_map/ppermute | solution.py:439
  28.6 6.2 %copy-start.3 = (bf16[1024,2048]{1,0:T(8,128)(2,1)S(1)}, bf16[1024,2048]{1,0:T(8,128)(2,1)}, u32[]{:S(2)}) copy-start(bf16[1024,2048]{1,0:T(8,128)(2,1)} %weight_ref.1) | copy-start | bytes 12582916
  28.6 6.2 %copy-start.4 = (bf16[128,2048]{1,0:T(8,128)(2,1)S(1)}, bf16[128,2048]{1,0:T(8,128)(2,1)}, u32[]{:S(2)}) copy-start(bf16[128,2048]{1,0:T(8,128)(2,1)} %residual_ref.1) | copy-start | bytes 1572868
  28.6 6.2 %copy-start.10 = (f32[2048]{0:T(1024)S(1)}, f32[2048]{0:T(1024)}, u32[]{:S(2)}) copy-start(f32[2048]{0:T(1024)} %param.23) | copy-start | bytes 24580
  29.0 5.7 %collective-permute-start.9 = (bf16[128,512]{1,0:T(8,128)(2,1)S(1)}, bf16[128,512]{1,0:T(8,128)(2,1)S(1)}, u32[]{:S(2)}, u32[]{:S(2)}) collective-permute-start(bf16[128,512]{1,0:T(8,128)(2,1)S(1)} %get-tuple-element.57), channel_id=1, source_target_pairs={{0,1},{1,0},{2,3},{3,2},{4,5},{5,4},{6,7},{7,6},{8,9},{9,8},{10,11... | collective-permute-start | bytes 393224 | tf_op jit(solution)/shard_map/ppermute | solution.py:509
  34.8 31.1 %copy-start.1 = (bf16[1,2048,512]{2,1,0:T(8,128)(2,1)S(1)}, bf16[1,2048,512]{2,1,0:T(8,128)(2,1)}, u32[]{:S(2)}) copy-start(bf16[1,2048,512]{2,1,0:T(8,128)(2,1)} %up.1) | copy-start | bytes 6291460
  34.8 31.1 %copy-start.2 = (bf16[1,512,2048]{2,1,0:T(8,128)(2,1)S(1)}, bf16[1,512,2048]{2,1,0:T(8,128)(2,1)}, u32[]{:S(2)}) copy-start(bf16[1,512,2048]{2,1,0:T(8,128)(2,1)} %down.1) | copy-start | bytes 6291460
  36.7 29.2 %copy-start = (bf16[1,2048,512]{2,1,0:T(8,128)(2,1)S(1)}, bf16[1,2048,512]{2,1,0:T(8,128)(2,1)}, u32[]{:S(2)}) copy-start(bf16[1,2048,512]{2,1,0:T(8,128)(2,1)} %gate.1) | copy-start | bytes 6291460

commit v8 on v7

--- a/solution.py
+++ b/solution.py
@@ -362,23 +362,31 @@
     given_ref[...] = whole[1 - core]
 
 
+def own_kernel(place_ref, kept_ref, weight_ref, residual_ref, partial_ref):
+    core = place_ref[0]
+    depth = kept_ref.shape[1]
+    tile = 256
+    own = pl.ds(pl.multiple_of(core * depth, depth), depth)
+    for n in range(residual_ref.shape[1] // tile):
+        part = slice(n * tile, (n + 1) * tile)
+        partial_ref[:, part] = residual_ref[:, part].astype(jnp.float32) + product(kept_ref[...], weight_ref[own, part])
+
+
 def project_kernel(
-    place_ref, owners_vmem, kept_ref, taken_ref, weight_ref, residual_ref, norm_gain_ref, merged_ref, outgoing_ref,
+    place_ref, owners_vmem, taken_ref, weight_ref, partial_ref, norm_gain_ref, merged_ref, outgoing_ref,
     chunked, owners_ref, sem,
 ):
     indices = pltpu.make_async_copy(owners_vmem, owners_ref, sem.at[0])
     indices.start()
     core = place_ref[0]
-    rows, width = residual_ref.shape
-    depth = kept_ref.shape[1]
+    rows, width = partial_ref.shape
+    depth = taken_ref.shape[1]
     tile = 256
-    own = pl.ds(pl.multiple_of(core * depth, depth), depth)
     other = pl.ds(pl.multiple_of((1 - core) * depth, depth), depth)
     square = jnp.zeros((rows, 1), jnp.float32)
     for n in range(width // tile):
         part = slice(n * tile, (n + 1) * tile)
-        projected = product(kept_ref[...], weight_ref[own, part]) + product(taken_ref[...], weight_ref[other, part])
-        merged = (residual_ref[:, part].astype(jnp.float32) + projected).astype(jnp.bfloat16)
+        merged = (partial_ref[:, part] + product(taken_ref[...], weight_ref[other, part])).astype(jnp.bfloat16)
         merged_ref[:, part] = merged
         widened = merged.astype(jnp.float32)
         square = square + jnp.sum(widened * widened, axis=1, keepdims=True)
@@ -400,17 +408,12 @@
     experts_total = owners_ref.shape[1]
     capacity = outgoing_ref.shape[0] // experts_total
 
+    indices.wait()
     batch = 8
-    indices.wait()
-
-    def copy_rows(step, carry):
-        first = step * batch
+    for first in range(0, experts_total, batch):
         rows = [chunked[owners_ref[place, first + k]] for k in range(batch) for place in range(capacity)]
         for k, row in enumerate(rows):
             outgoing_ref[capacity * first + k] = row
-        return carry
-
-    lax.fori_loop(0, experts_total // batch, copy_rows, 0, unroll=2)
 
 
 def shape_of(shape, dtype):
@@ -487,17 +490,18 @@
     before_x, decay_x, message_x = call(
         stage_kernel, (state_shape, decay_shape, message_shape), (x, message, *behind), 1
     )
+    behind = from_behind(message_x, "sp_1")
+    before_y, decay_y, message_y = call(
+        stage_kernel, (state_shape, decay_shape, message_shape), (y, message_x, *behind), 1
+    )
+    behind = from_behind(message_y, "sp_0")
+    message_y, queries, key_rows = lax.optimization_barrier((message_y, queries, key_rows))
     partial, reach, gating = call(
         within_kernel,
         (shape_of((length, values), f32), shape_of((length, channels), f32), shape_of((length, values), f32)),
         (queries, key_rows, value_rows, gate_logits, head_gain.reshape(1, -1), out_gate),
     )
-    behind = from_behind(message_x, "sp_1")
     partial, reach, gating, *behind = lax.optimization_barrier((partial, reach, gating, *behind))
-    before_y, decay_y, message_y = call(
-        stage_kernel, (state_shape, decay_shape, message_shape), (y, message_x, *behind), 1
-    )
-    behind = from_behind(message_y, "sp_0")
     half = shape_of((length // 2, values), bf16)
     kept, given = call(
         finish_kernel,
@@ -505,15 +509,18 @@
         (core, z, *behind, before_y, decay_y, before_x, decay_x, partial, reach, gating),
         2,
         [pltpu.VMEM((2, length // 2, values), bf16)],
+        cost=300000,
     )
     taken = lax.ppermute(given, "tp", [(0, 1), (1, 0)])
+    projected = call(own_kernel, shape_of((row_count, model_width), f32), (core, kept, out_weight, residual), 1, room=8)
+    projected, taken = lax.optimization_barrier((projected, taken))
     merged, outgoing = call(
         project_kernel,
         (
             shape_of((row_count, model_width), bf16),
             shape_of((experts_total * capacity, SUB, LANES), bf16),
         ),
-        (core, owners, kept, taken, out_weight, residual, norm_gain.reshape(1, -1)),
+        (core, owners, taken, out_weight, projected, norm_gain.reshape(1, -1)),
         1,
         [
             pltpu.VMEM((row_count, SUB, LANES), bf16),

time: 100 us -> 99.1 us (level)
    pallas_call x7 -> x8, Pallas kernels: 6.54 us -> 6.38 us  [call(): pl.pallas_call(kernel, out_shape=outs, in_specs=[SMEM_SPEC] * scalars + [...]
  transfers between devices with their start and end apart: 10 -> 10, of which waited for: 8 -> 8; matrix products, arithmetic and copies ran while one was open for 0% -> 0% of each run, Pallas kernels for 2% -> 3%
where the time goes in v8:
time: 99.1 us; the launch traced here: 99 us
  blocking collectives  57.7 us (58%)
  starting transfers between devices  17.6 us (18%)
  waiting for transfers between devices  11.9 us (12%)
  Pallas kernels  11.6 us (12%)
    all_to_all x1, blocking collectives, local(): lax.all_to_all(served.reshape(block), SP_TP, split_axis=0, concat_axis=0,...  28.9 us
    all_to_all x1, blocking collectives, local(): lax.all_to_all(outgoing.reshape(block), SP_TP, split_axis=0, concat_axis=...  28.8 us
    ppermute x9, starting transfers between devices, from_behind(): lax.ppermute(message, axis, [(i, (i + k) % RING) for i in range(RING)])  12.9 us
    ppermute x9, waiting for transfers between devices, from_behind(): lax.ppermute(message, axis, [(i, (i + k) % RING) for i in range(RING)])  11.4 us
    pallas_call x8, Pallas kernels, call(): pl.pallas_call(kernel, out_shape=outs, in_specs=[SMEM_SPEC] * scalars + [...  6.38 us
    ppermute x1, starting transfers between devices, local(): taken = lax.ppermute(given, 'tp', [(0, 1), (1, 0)])  4.75 us
    pallas_call x1, Pallas kernels, experts(): pl.pallas_call(experts_kernel, out_shape=jax.ShapeDtypeStruct(arrived.sha...  3.51 us
  transfers between devices with their start and end apart: 10, of which 8 were waited for; matrix products, arithmetic and copies ran while one was open for 0% of the time, Pallas kernels for 3%

profile of v8, /device:TPU:1, one launch (start us, length us, event | category | flops | bytes accessed | tf_op | source)
XLA Modules:
  0.0 99.0 jit_solution(12194926202524193079)
XLA Ops:
  0.0 1.9 %shard_map.146.own_ref = bf16[272,128]{1,0:T(8,128)(2,1)S(1)} custom-call(bf16[256,256]{1,0:T(8,128)(2,1)} %keys_ref, bf16[256,512]{1,0:T(8,128)(2,1)} %values_ref.1, bf16[256,256]{1,0:T(8,128)(2,1)} %logits_ref.1), custom_call_target="tpu_custom_call" | custom-call | flops 4000000000 | bytes 10000000 | tf_op jit(solution)/shard_map/pallas_call | solution.py:428
  1.9 3.4 %collective-permute-start.2 = (bf16[272,128]{1,0:T(8,128)(2,1)S(1)}, bf16[272,128]{1,0:T(8,128)(2,1)S(1)}, u32[]{:S(2)}, u32[]{:S(2)}) collective-permute-start(bf16[272,128]{1,0:T(8,128)(2,1)S(1)} %shard_map.146.own_ref), channel_id=1, source_target_pairs={{0,6},{2,0},{4,2},{6,4},{1,7},{3,1},{5,3},{7,5},{8,14},{10,8},{12,... | collective-permute-start | bytes 208904 | tf_op jit(solution)/shard_map/ppermute | solution.py:442
  5.3 0.5 collective-permute-start.1
  5.8 0.6 collective-permute-start
  6.4 0.3 shard_map.145
  6.7 3.3 %collective-permute-done.1.back2_ref = bf16[272,128]{1,0:T(8,128)(2,1)S(1)} collective-permute-done((bf16[272,128]{1,0:T(8,128)(2,1)S(1)}, bf16[272,128]{1,0:T(8,128)(2,1)S(1)}, u32[]{:S(2)}, u32[]{:S(2)}) %collective-permute-start.1) | collective-permute-done | bytes 69664 | tf_op jit(solution)/shard_map/ppermute | solution.py:442
  10.0 1.1 %collective-permute-done.back1_ref = bf16[272,128]{1,0:T(8,128)(2,1)S(1)} collective-permute-done((bf16[272,128]{1,0:T(8,128)(2,1)S(1)}, bf16[272,128]{1,0:T(8,128)(2,1)S(1)}, u32[]{:S(2)}, u32[]{:S(2)}) %collective-permute-start) | collective-permute-done | bytes 69664 | tf_op jit(solution)/shard_map/ppermute | solution.py:442
  11.1 0.1 shard_map.147
  11.2 2.8 %collective-permute-start.5 = (bf16[272,128]{1,0:T(8,128)(2,1)S(1)}, bf16[272,128]{1,0:T(8,128)(2,1)S(1)}, u32[]{:S(2)}, u32[]{:S(2)}) collective-permute-start(bf16[272,128]{1,0:T(8,128)(2,1)S(1)} %get-tuple-element.45.own_ref), channel_id=1, source_target_pairs={{0,24},{8,0},{16,8},{24,16},{1,25},{9,1},{17,9},{25,17},{2,26},{10... | collective-permute-start | bytes 208904 | tf_op jit(solution)/shard_map/ppermute | solution.py:442
  14.0 0.3 collective-permute-start.4
  14.4 0.7 collective-permute-start.3
  15.1 0.3 collective-permute-done.5.back3_ref
  15.4 3.4 %collective-permute-done.4.back2_ref = bf16[272,128]{1,0:T(8,128)(2,1)S(1)} collective-permute-done((bf16[272,128]{1,0:T(8,128)(2,1)S(1)}, bf16[272,128]{1,0:T(8,128)(2,1)S(1)}, u32[]{:S(2)}, u32[]{:S(2)}) %collective-permute-start.4) | collective-permute-done | bytes 69664 | tf_op jit(solution)/shard_map/ppermute | solution.py:442
  18.8 0.7 collective-permute-done.3.back1_ref
  19.4 0.0 copy-start.9
  19.5 0.0 copy-start.14
  19.5 0.1 shard_map.148
  19.6 3.8 %collective-permute-start.8 = (bf16[272,128]{1,0:T(8,128)(2,1)S(1)}, bf16[272,128]{1,0:T(8,128)(2,1)S(1)}, u32[]{:S(2)}, u32[]{:S(2)}) collective-permute-start(bf16[272,128]{1,0:T(8,128)(2,1)S(1)} %get-tuple-element.46), channel_id=1, source_target_pairs={{0,96},{32,0},{64,32},{96,64},{1,97},{33,1},{65,33},{97,65},{2,98}... | collective-permute-start | bytes 208904 | tf_op jit(solution)/shard_map/ppermute | solution.py:442
  23.4 0.7 collective-permute-start.6
  24.2 0.0 copy-start.4
  24.2 1.7 %shard_map.149 = (f32[256,512]{1,0:T(8,128)S(1)}, f32[256,256]{1,0:T(8,128)S(1)}, f32[256,512]{1,0:T(8,128)S(1)}) custom-call(bf16[256,256]{1,0:T(8,128)(2,1)S(1)} %copy-done.9, bf16[256,256]{1,0:T(8,128)(2,1)S(1)} %copy-done.7, bf16[256,512]{1,0:T(8,128)(2,1)S(1)} %copy-done.5, bf16[256,256]{1,0:T(8,128)(2,1)S(1)} %copy-done.8, f32[1,128]{1,0:T(1,128)S(1)} %bitcast.21, ...), custom_call_target="tpu_custom_call" | custom-call | flops 4000000000 | bytes 10000000 | tf_op jit(solution)/shard_map/pallas_call | solution.py:428
  25.9 2.3 %collective-permute-done.7.back2_ref = bf16[272,128]{1,0:T(8,128)(2,1)S(1)} collective-permute-done((bf16[272,128]{1,0:T(8,128)(2,1)S(1)}, bf16[272,128]{1,0:T(8,128)(2,1)S(1)}, u32[]{:S(2)}, u32[]{:S(2)}) %collective-permute-start.7) | collective-permute-done | bytes 69664 | tf_op jit(solution)/shard_map/ppermute | solution.py:442
  28.2 0.4 collective-permute-done.6.back1_ref
  28.6 0.5 shard_map.150
  29.0 4.7 %collective-permute-start.9 = (bf16[128,512]{1,0:T(8,128)(2,1)S(1)}, bf16[128,512]{1,0:T(8,128)(2,1)S(1)}, u32[]{:S(2)}, u32[]{:S(2)}) collective-permute-start(bf16[128,512]{1,0:T(8,128)(2,1)S(1)} %get-tuple-element.63), channel_id=1, source_target_pairs={{0,1},{1,0},{2,3},{3,2},{4,5},{5,4},{6,7},{7,6},{8,9},{9,8},{10,11... | collective-permute-start | bytes 393224 | tf_op jit(solution)/shard_map/ppermute | solution.py:514
  33.8 0.5 shard_map.151.partial_ref
  34.3 0.5 collective-permute-done.9.taken_ref
  34.8 1.3 %shard_map.152 = (bf16[128,2048]{1,0:T(8,128)(2,1)S(1)}, bf16[384,16,128]{2,1,0:T(8,128)(2,1)S(1)}) custom-call(s32[1]{0:T(128)} %bitcast.3.place_ref, s32[8,128]{1,0:T(8,128)S(1)} %get-tuple-element.41.owners_vmem, bf16[128,512]{1,0:T(8,128)(2,1)S(1)} %collective-permute-done.9.taken_ref, bf16[1024,2048]{1,0:T(8,128)(2,1)S(1)} %copy-done.3, ...), custom_call_target="tpu_custom_call" | custom-call | flops 4000000000 | bytes 10000000 | tf_op jit(solution)/shard_map/pallas_call | solution.py:428
  36.0 28.8 %all_to_all.10 = bf16[128,48,128]{2,1,0:T(8,128)(2,1)S(1)} all-to-all(bf16[128,48,128]{2,1,0:T(8,128)(2,1)S(1)} %bitcast.16), channel_id=1, replica_groups=mesh['sp_0'=4,'sp_1'=4,'sp_2'=4,'tp'=2] {'sp_0','sp_1','sp_2','tp'}, dimensions={0} | all-to-all | bytes 3145728 | tf_op jit(solution)/shard_map/all_to_all | solution.py:533
  64.9 3.5 %experts.1 = bf16[384,16,128]{2,1,0:T(8,128)(2,1)S(1)} custom-call(bf16[384,16,128]{2,1,0:T(8,128)(2,1)S(1)} %bitcast.14, bf16[1,2048,512]{2,1,0:T(8,128)(2,1)S(1)} %copy-done, bf16[1,2048,512]{2,1,0:T(8,128)(2,1)S(1)} %copy-done.1, bf16[1,512,2048]{2,1,0:T(8,128)(2,1)S(1)} %copy-done.2), custom_call_target="tpu_custom_call" | custom-call | tf_op jit(solution)/shard_map/experts/pallas_call | solution.py:117
  68.4 28.9 %all_to_all.11 = bf16[128,48,128]{2,1,0:T(8,128)(2,1)S(1)} all-to-all(bf16[128,48,128]{2,1,0:T(8,128)(2,1)S(1)} %bitcast.15), channel_id=1, replica_groups=mesh['sp_0'=4,'sp_1'=4,'sp_2'=4,'tp'=2] {'sp_0','sp_1','sp_2','tp'}, dimensions={0} | all-to-all | bytes 3145728 | tf_op jit(solution)/shard_map/all_to_all | solution.py:535
  97.3 1.7 %combine.1 = bf16[128,2048]{1,0:T(8,128)(2,1)} custom-call(s32[2,128]{1,0:T(2,128)S(1)} %get-tuple-element.40.slots_vmem, bf16[384,16,128]{2,1,0:T(8,128)(2,1)S(1)} %bitcast.13, bf16[128,2048]{1,0:T(8,128)(2,1)S(1)} %get-tuple-element.67.merged_ref, f32[2,128,128]{2,1,0:T(8,128)S(1)} %get-tuple-element.68.weights_ref), custom_call_target="tpu_custom_call" | custom-call | tf_op jit(solution)/shard_map/combine/pallas_call | solution.py:160
  (30 shorter events, 0.1 us)
Async XLA Ops:
  0.0 6.4 %copy-start.12 = (f32[128,2]{0,1:T(2,128)S(1)}, f32[128,2]{0,1:T(2,128)}, u32[]{:S(2)}) copy-start(f32[128,2]{0,1:T(2,128)} %param.26) | copy-start | bytes 3076
  0.0 6.4 %copy-start.13 = (f32[128]{0:T(128)S(1)}, f32[128]{0:T(128)}, u32[]{:S(2)}) copy-start(f32[128]{0:T(128)} %param.25) | copy-start | bytes 1540
  0.0 6.4 %copy-start.11 = (s32[128,2]{0,1:T(2,128)S(1)}, s32[128,2]{0,1:T(2,128)}, u32[]{:S(2)}) copy-start(s32[128,2]{0,1:T(2,128)} %param.24) | copy-start | bytes 3076
  1.9 4.8 %collective-permute-start.2 = (bf16[272,128]{1,0:T(8,128)(2,1)S(1)}, bf16[272,128]{1,0:T(8,128)(2,1)S(1)}, u32[]{:S(2)}, u32[]{:S(2)}) collective-permute-start(bf16[272,128]{1,0:T(8,128)(2,1)S(1)} %shard_map.146.own_ref), channel_id=1, source_target_pairs={{0,6},{2,0},{4,2},{6,4},{1,7},{3,1},{5,3},{7,5},{8,14},{10,8},{12,... | collective-permute-start | bytes 208904 | tf_op jit(solution)/shard_map/ppermute | solution.py:442
  5.3 4.7 %collective-permute-start.1 = (bf16[272,128]{1,0:T(8,128)(2,1)S(1)}, bf16[272,128]{1,0:T(8,128)(2,1)S(1)}, u32[]{:S(2)}, u32[]{:S(2)}) collective-permute-start(bf16[272,128]{1,0:T(8,128)(2,1)S(1)} %shard_map.146.own_ref), channel_id=1, source_target_pairs={{0,4},{2,6},{4,0},{6,2},{1,5},{3,7},{5,1},{7,3},{8,12},{10,14},{12... | collective-permute-start | bytes 208904 | tf_op jit(solution)/shard_map/ppermute | solution.py:442
  5.8 5.3 %collective-permute-start = (bf16[272,128]{1,0:T(8,128)(2,1)S(1)}, bf16[272,128]{1,0:T(8,128)(2,1)S(1)}, u32[]{:S(2)}, u32[]{:S(2)}) collective-permute-start(bf16[272,128]{1,0:T(8,128)(2,1)S(1)} %shard_map.146.own_ref), channel_id=1, source_target_pairs={{0,2},{2,4},{4,6},{6,0},{1,3},{3,5},{5,7},{7,1},{8,10},{10,12},{12... | collective-permute-start | bytes 208904 | tf_op jit(solution)/shard_map/ppermute | solution.py:442
  11.2 4.2 %collective-permute-start.5 = (bf16[272,128]{1,0:T(8,128)(2,1)S(1)}, bf16[272,128]{1,0:T(8,128)(2,1)S(1)}, u32[]{:S(2)}, u32[]{:S(2)}) collective-permute-start(bf16[272,128]{1,0:T(8,128)(2,1)S(1)} %get-tuple-element.45.own_ref), channel_id=1, source_target_pairs={{0,24},{8,0},{16,8},{24,16},{1,25},{9,1},{17,9},{25,17},{2,26},{10... | collective-permute-start | bytes 208904 | tf_op jit(solution)/shard_map/ppermute | solution.py:442
  14.0 4.7 %collective-permute-start.4 = (bf16[272,128]{1,0:T(8,128)(2,1)S(1)}, bf16[272,128]{1,0:T(8,128)(2,1)S(1)}, u32[]{:S(2)}, u32[]{:S(2)}) collective-permute-start(bf16[272,128]{1,0:T(8,128)(2,1)S(1)} %get-tuple-element.45.own_ref), channel_id=1, source_target_pairs={{0,16},{8,24},{16,0},{24,8},{1,17},{9,25},{17,1},{25,9},{2,18},{10... | collective-permute-start | bytes 208904 | tf_op jit(solution)/shard_map/ppermute | solution.py:442
  14.4 5.1 %collective-permute-start.3 = (bf16[272,128]{1,0:T(8,128)(2,1)S(1)}, bf16[272,128]{1,0:T(8,128)(2,1)S(1)}, u32[]{:S(2)}, u32[]{:S(2)}) collective-permute-start(bf16[272,128]{1,0:T(8,128)(2,1)S(1)} %get-tuple-element.45.own_ref), channel_id=1, source_target_pairs={{0,8},{8,16},{16,24},{24,0},{1,9},{9,17},{17,25},{25,1},{2,10},{10... | collective-permute-start | bytes 208904 | tf_op jit(solution)/shard_map/ppermute | solution.py:442
  19.4 4.7 %copy-start.5 = (bf16[256,512]{1,0:T(8,128)(2,1)S(1)}, bf16[256,512]{1,0:T(8,128)(2,1)}, u32[]{:S(2)}) copy-start(bf16[256,512]{1,0:T(8,128)(2,1)} %values_ref.1) | copy-start | bytes 786436
  19.4 4.7 %copy-start.6 = (bf16[256,512]{1,0:T(8,128)(2,1)S(1)}, bf16[256,512]{1,0:T(8,128)(2,1)}, u32[]{:S(2)}) copy-start(bf16[256,512]{1,0:T(8,128)(2,1)} %out_gate_ref.1) | copy-start | bytes 786436
  19.4 4.7 %copy-start.7 = (bf16[256,256]{1,0:T(8,128)(2,1)S(1)}, bf16[256,256]{1,0:T(8,128)(2,1)}, u32[]{:S(2)}) copy-start(bf16[256,256]{1,0:T(8,128)(2,1)} %keys_ref) | copy-start | bytes 393220
  19.4 4.7 %copy-start.8 = (bf16[256,256]{1,0:T(8,128)(2,1)S(1)}, bf16[256,256]{1,0:T(8,128)(2,1)}, u32[]{:S(2)}) copy-start(bf16[256,256]{1,0:T(8,128)(2,1)} %logits_ref.1) | copy-start | bytes 393220
  19.4 4.7 %copy-start.9 = (bf16[256,256]{1,0:T(8,128)(2,1)S(1)}, bf16[256,256]{1,0:T(8,128)(2,1)}, u32[]{:S(2)}) copy-start(bf16[256,256]{1,0:T(8,128)(2,1)} %queries_ref) | copy-start | bytes 393220
  19.5 4.7 %copy-start.14 = (f32[128]{0:T(128)S(1)}, f32[128]{0:T(128)}, u32[]{:S(2)}) copy-start(f32[128]{0:T(128)} %param.21) | copy-start | bytes 1540
  19.6 6.3 %collective-permute-start.8 = (bf16[272,128]{1,0:T(8,128)(2,1)S(1)}, bf16[272,128]{1,0:T(8,128)(2,1)S(1)}, u32[]{:S(2)}, u32[]{:S(2)}) collective-permute-start(bf16[272,128]{1,0:T(8,128)(2,1)S(1)} %get-tuple-element.46), channel_id=1, source_target_pairs={{0,96},{32,0},{64,32},{96,64},{1,97},{33,1},{65,33},{97,65},{2,98}... | collective-permute-start | bytes 208904 | tf_op jit(solution)/shard_map/ppermute | solution.py:442
  23.4 4.8 %collective-permute-start.7 = (bf16[272,128]{1,0:T(8,128)(2,1)S(1)}, bf16[272,128]{1,0:T(8,128)(2,1)S(1)}, u32[]{:S(2)}, u32[]{:S(2)}) collective-permute-start(bf16[272,128]{1,0:T(8,128)(2,1)S(1)} %get-tuple-element.46), channel_id=1, source_target_pairs={{0,64},{32,96},{64,0},{96,32},{1,65},{33,97},{65,1},{97,33},{2,66}... | collective-permute-start | bytes 208904 | tf_op jit(solution)/shard_map/ppermute | solution.py:442
  23.4 5.1 %collective-permute-start.6 = (bf16[272,128]{1,0:T(8,128)(2,1)S(1)}, bf16[272,128]{1,0:T(8,128)(2,1)S(1)}, u32[]{:S(2)}, u32[]{:S(2)}) collective-permute-start(bf16[272,128]{1,0:T(8,128)(2,1)S(1)} %get-tuple-element.46), channel_id=1, source_target_pairs={{0,32},{32,64},{64,96},{96,0},{1,33},{33,65},{65,97},{97,1},{2,34}... | collective-permute-start | bytes 208904 | tf_op jit(solution)/shard_map/ppermute | solution.py:442
  24.2 9.6 %copy-start.3 = (bf16[1024,2048]{1,0:T(8,128)(2,1)S(1)}, bf16[1024,2048]{1,0:T(8,128)(2,1)}, u32[]{:S(2)}) copy-start(bf16[1024,2048]{1,0:T(8,128)(2,1)} %weight_ref.3) | copy-start | bytes 12582916
  24.2 9.6 %copy-start.4 = (bf16[128,2048]{1,0:T(8,128)(2,1)S(1)}, bf16[128,2048]{1,0:T(8,128)(2,1)}, u32[]{:S(2)}) copy-start(bf16[128,2048]{1,0:T(8,128)(2,1)} %residual_ref.1) | copy-start | bytes 1572868
  29.0 5.7 %collective-permute-start.9 = (bf16[128,512]{1,0:T(8,128)(2,1)S(1)}, bf16[128,512]{1,0:T(8,128)(2,1)S(1)}, u32[]{:S(2)}, u32[]{:S(2)}) collective-permute-start(bf16[128,512]{1,0:T(8,128)(2,1)S(1)} %get-tuple-element.63), channel_id=1, source_target_pairs={{0,1},{1,0},{2,3},{3,2},{4,5},{5,4},{6,7},{7,6},{8,9},{9,8},{10,11... | collective-permute-start | bytes 393224 | tf_op jit(solution)/shard_map/ppermute | solution.py:514
  33.8 1.0 copy-start.10
  34.8 30.1 %copy-start.1 = (bf16[1,2048,512]{2,1,0:T(8,128)(2,1)S(1)}, bf16[1,2048,512]{2,1,0:T(8,128)(2,1)}, u32[]{:S(2)}) copy-start(bf16[1,2048,512]{2,1,0:T(8,128)(2,1)} %up.1) | copy-start | bytes 6291460
  34.8 30.1 %copy-start.2 = (bf16[1,512,2048]{2,1,0:T(8,128)(2,1)S(1)}, bf16[1,512,2048]{2,1,0:T(8,128)(2,1)}, u32[]{:S(2)}) copy-start(bf16[1,512,2048]{2,1,0:T(8,128)(2,1)} %down.1) | copy-start | bytes 6291460
  36.0 28.8 %copy-start = (bf16[1,2048,512]{2,1,0:T(8,128)(2,1)S(1)}, bf16[1,2048,512]{2,1,0:T(8,128)(2,1)}, u32[]{:S(2)}) copy-start(bf16[1,2048,512]{2,1,0:T(8,128)(2,1)} %gate.1) | copy-start | bytes 6291460

commit v9 on v8

--- a/solution.py
+++ b/solution.py
@@ -32,6 +32,14 @@
 def exchange(swap, blocks):
     turned = jnp.dot(swap, jnp.concatenate(blocks, axis=1), preferred_element_type=jnp.float32)
     return [turned[:, k * LANES : (k + 1) * LANES] for k in range(len(blocks))]
+
+
+def turn(block):
+    return jnp.transpose(block.reshape(SUB, SUB, LANES), (1, 0, 2)).reshape(SWAP, LANES)
+
+
+def swap_groups(swap, blocks, by_matmul):
+    return exchange(swap, blocks) if by_matmul else [turn(block) for block in blocks]
 
 
 def stack_chunks(ref, g):
@@ -92,7 +100,7 @@
     groups = count // SUB
     for g in range(0, groups, 2):
         blocks = [rows_ref[k * SUB : (k + 1) * SUB].reshape(SWAP, LANES) for k in (g, g + 1)]
-        for k, turned in zip((g, g + 1), exchange(swap, blocks)):
+        for k, turned in zip((g, g + 1), swap_groups(swap, blocks, False)):
             turned = turned.astype(jnp.bfloat16)
             for j in range(width // LANES):
                 rows_in[k * SUB : (k + 1) * SUB, j * LANES : (j + 1) * LANES] = turned[j * SUB : (j + 1) * SUB]
@@ -107,7 +115,7 @@
         served[:, part] = jnp.dot(inner[...], down[0, :, part], preferred_element_type=jnp.float32).astype(jnp.bfloat16)
     for g in range(0, groups, 2):
         blocks = [stack_chunks(served, k) for k in (g, g + 1)]
-        for k, turned in zip((g, g + 1), exchange(swap, blocks)):
+        for k, turned in zip((g, g + 1), swap_groups(swap, blocks, False)):
             out_ref[k * SUB : (k + 1) * SUB] = turned.astype(jnp.bfloat16).reshape(SUB, SUB, LANES)
 
 
@@ -402,7 +410,7 @@
                 widened = merged_ref[group, lanes].astype(jnp.float32)
                 stacked.append((widened * scale[group] * norm_gain_ref[:, lanes]).astype(jnp.bfloat16))
             blocks.append(jnp.concatenate(stacked, axis=0))
-        for k, turned in zip((g, g + 1), exchange(swap, blocks)):
+        for k, turned in zip((g, g + 1), swap_groups(swap, blocks, False)):
             chunked[k * SUB : (k + 1) * SUB] = turned.astype(jnp.bfloat16).reshape(SUB, SUB, LANES)
 
     experts_total = owners_ref.shape[1]

time: 99.1 us -> 98.5 us (level)
  no operation moved by 1% of the time
where the time goes in v9:
time: 98.5 us; the launch traced here: 98.4 us
  blocking collectives  57.7 us (59%)
  starting transfers between devices  17.6 us (18%)
  waiting for transfers between devices  11.9 us (12%)
  Pallas kernels  11 us (11%)
    all_to_all x1, blocking collectives, local(): lax.all_to_all(served.reshape(block), SP_TP, split_axis=0, concat_axis=0,...  28.9 us
    all_to_all x1, blocking collectives, local(): lax.all_to_all(outgoing.reshape(block), SP_TP, split_axis=0, concat_axis=...  28.8 us
    ppermute x9, starting transfers between devices, from_behind(): lax.ppermute(message, axis, [(i, (i + k) % RING) for i in range(RING)])  12.9 us
    ppermute x9, waiting for transfers between devices, from_behind(): lax.ppermute(message, axis, [(i, (i + k) % RING) for i in range(RING)])  11.4 us
    pallas_call x8, Pallas kernels, call(): pl.pallas_call(kernel, out_shape=outs, in_specs=[SMEM_SPEC] * scalars + [...  6.25 us
    ppermute x1, starting transfers between devices, local(): taken = lax.ppermute(given, 'tp', [(0, 1), (1, 0)])  4.75 us
    pallas_call x1, Pallas kernels, experts(): pl.pallas_call(experts_kernel, out_shape=jax.ShapeDtypeStruct(arrived.sha...  3.05 us
  transfers between devices with their start and end apart: 10, of which 8 were waited for; matrix products, arithmetic and copies ran while one was open for 0% of the time, Pallas kernels for 3%

profile of v9, /device:TPU:1, one launch (start us, length us, event | category | flops | bytes accessed | tf_op | source)
XLA Modules:
  0.0 98.4 jit_solution(5818144158422588203)
XLA Ops:
  0.0 1.9 %shard_map.146.own_ref = bf16[272,128]{1,0:T(8,128)(2,1)S(1)} custom-call(bf16[256,256]{1,0:T(8,128)(2,1)} %keys_ref, bf16[256,512]{1,0:T(8,128)(2,1)} %values_ref.1, bf16[256,256]{1,0:T(8,128)(2,1)} %logits_ref.1), custom_call_target="tpu_custom_call" | custom-call | flops 4000000000 | bytes 10000000 | tf_op jit(solution)/shard_map/pallas_call | solution.py:436
  1.9 3.4 %collective-permute-start.2 = (bf16[272,128]{1,0:T(8,128)(2,1)S(1)}, bf16[272,128]{1,0:T(8,128)(2,1)S(1)}, u32[]{:S(2)}, u32[]{:S(2)}) collective-permute-start(bf16[272,128]{1,0:T(8,128)(2,1)S(1)} %shard_map.146.own_ref), channel_id=1, source_target_pairs={{0,6},{2,0},{4,2},{6,4},{1,7},{3,1},{5,3},{7,5},{8,14},{10,8},{12,... | collective-permute-start | bytes 208904 | tf_op jit(solution)/shard_map/ppermute | solution.py:450
  5.3 0.5 collective-permute-start.1
  5.8 0.6 collective-permute-start
  6.4 0.3 shard_map.145
  6.7 3.3 %collective-permute-done.1.back2_ref = bf16[272,128]{1,0:T(8,128)(2,1)S(1)} collective-permute-done((bf16[272,128]{1,0:T(8,128)(2,1)S(1)}, bf16[272,128]{1,0:T(8,128)(2,1)S(1)}, u32[]{:S(2)}, u32[]{:S(2)}) %collective-permute-start.1) | collective-permute-done | bytes 69664 | tf_op jit(solution)/shard_map/ppermute | solution.py:450
  10.0 1.1 %collective-permute-done.back1_ref = bf16[272,128]{1,0:T(8,128)(2,1)S(1)} collective-permute-done((bf16[272,128]{1,0:T(8,128)(2,1)S(1)}, bf16[272,128]{1,0:T(8,128)(2,1)S(1)}, u32[]{:S(2)}, u32[]{:S(2)}) %collective-permute-start) | collective-permute-done | bytes 69664 | tf_op jit(solution)/shard_map/ppermute | solution.py:450
  11.1 0.1 shard_map.147
  11.2 2.8 %collective-permute-start.5 = (bf16[272,128]{1,0:T(8,128)(2,1)S(1)}, bf16[272,128]{1,0:T(8,128)(2,1)S(1)}, u32[]{:S(2)}, u32[]{:S(2)}) collective-permute-start(bf16[272,128]{1,0:T(8,128)(2,1)S(1)} %get-tuple-element.45.own_ref), channel_id=1, source_target_pairs={{0,24},{8,0},{16,8},{24,16},{1,25},{9,1},{17,9},{25,17},{2,26},{10... | collective-permute-start | bytes 208904 | tf_op jit(solution)/shard_map/ppermute | solution.py:450
  14.0 0.3 collective-permute-start.4
  14.4 0.7 collective-permute-start.3
  15.1 0.3 collective-permute-done.5.back3_ref
  15.4 3.4 %collective-permute-done.4.back2_ref = bf16[272,128]{1,0:T(8,128)(2,1)S(1)} collective-permute-done((bf16[272,128]{1,0:T(8,128)(2,1)S(1)}, bf16[272,128]{1,0:T(8,128)(2,1)S(1)}, u32[]{:S(2)}, u32[]{:S(2)}) %collective-permute-start.4) | collective-permute-done | bytes 69664 | tf_op jit(solution)/shard_map/ppermute | solution.py:450
  18.8 0.7 collective-permute-done.3.back1_ref
  19.4 0.0 copy-start.9
  19.5 0.0 copy-start.14
  19.5 0.1 shard_map.148
  19.6 3.8 %collective-permute-start.8 = (bf16[272,128]{1,0:T(8,128)(2,1)S(1)}, bf16[272,128]{1,0:T(8,128)(2,1)S(1)}, u32[]{:S(2)}, u32[]{:S(2)}) collective-permute-start(bf16[272,128]{1,0:T(8,128)(2,1)S(1)} %get-tuple-element.46), channel_id=1, source_target_pairs={{0,96},{32,0},{64,32},{96,64},{1,97},{33,1},{65,33},{97,65},{2,98}... | collective-permute-start | bytes 208904 | tf_op jit(solution)/shard_map/ppermute | solution.py:450
  23.4 0.7 collective-permute-start.6
  24.2 0.0 copy-start.4
  24.2 1.7 %shard_map.149 = (f32[256,512]{1,0:T(8,128)S(1)}, f32[256,256]{1,0:T(8,128)S(1)}, f32[256,512]{1,0:T(8,128)S(1)}) custom-call(bf16[256,256]{1,0:T(8,128)(2,1)S(1)} %copy-done.9, bf16[256,256]{1,0:T(8,128)(2,1)S(1)} %copy-done.7, bf16[256,512]{1,0:T(8,128)(2,1)S(1)} %copy-done.5, bf16[256,256]{1,0:T(8,128)(2,1)S(1)} %copy-done.8, f32[1,128]{1,0:T(1,128)S(1)} %bitcast.21, ...), custom_call_target="tpu_custom_call" | custom-call | flops 4000000000 | bytes 10000000 | tf_op jit(solution)/shard_map/pallas_call | solution.py:436
  25.9 2.3 %collective-permute-done.7.back2_ref = bf16[272,128]{1,0:T(8,128)(2,1)S(1)} collective-permute-done((bf16[272,128]{1,0:T(8,128)(2,1)S(1)}, bf16[272,128]{1,0:T(8,128)(2,1)S(1)}, u32[]{:S(2)}, u32[]{:S(2)}) %collective-permute-start.7) | collective-permute-done | bytes 69664 | tf_op jit(solution)/shard_map/ppermute | solution.py:450
  28.2 0.4 collective-permute-done.6.back1_ref
  28.6 0.5 shard_map.150
  29.0 4.7 %collective-permute-start.9 = (bf16[128,512]{1,0:T(8,128)(2,1)S(1)}, bf16[128,512]{1,0:T(8,128)(2,1)S(1)}, u32[]{:S(2)}, u32[]{:S(2)}) collective-permute-start(bf16[128,512]{1,0:T(8,128)(2,1)S(1)} %get-tuple-element.63), channel_id=1, source_target_pairs={{0,1},{1,0},{2,3},{3,2},{4,5},{5,4},{6,7},{7,6},{8,9},{9,8},{10,11... | collective-permute-start | bytes 393224 | tf_op jit(solution)/shard_map/ppermute | solution.py:522
  33.8 0.5 shard_map.151.partial_ref
  34.3 0.5 collective-permute-done.9.taken_ref
  34.8 1.1 %shard_map.152 = (bf16[128,2048]{1,0:T(8,128)(2,1)S(1)}, bf16[384,16,128]{2,1,0:T(8,128)(2,1)S(1)}) custom-call(s32[1]{0:T(128)} %bitcast.3.place_ref, s32[8,128]{1,0:T(8,128)S(1)} %get-tuple-element.41.owners_vmem, bf16[128,512]{1,0:T(8,128)(2,1)S(1)} %collective-permute-done.9.taken_ref, bf16[1024,2048]{1,0:T(8,128)(2,1)S(1)} %copy-done.3, ...), custom_call_target="tpu_custom_call" | custom-call | flops 4000000000 | bytes 10000000 | tf_op jit(solution)/shard_map/pallas_call | solution.py:436
  35.9 28.8 %all_to_all.10 = bf16[128,48,128]{2,1,0:T(8,128)(2,1)S(1)} all-to-all(bf16[128,48,128]{2,1,0:T(8,128)(2,1)S(1)} %bitcast.16), channel_id=1, replica_groups=mesh['sp_0'=4,'sp_1'=4,'sp_2'=4,'tp'=2] {'sp_0','sp_1','sp_2','tp'}, dimensions={0} | all-to-all | bytes 3145728 | tf_op jit(solution)/shard_map/all_to_all | solution.py:541
  64.7 3.0 %experts.1 = bf16[384,16,128]{2,1,0:T(8,128)(2,1)S(1)} custom-call(bf16[384,16,128]{2,1,0:T(8,128)(2,1)S(1)} %bitcast.14, bf16[1,2048,512]{2,1,0:T(8,128)(2,1)S(1)} %copy-done, bf16[1,2048,512]{2,1,0:T(8,128)(2,1)S(1)} %copy-done.1, bf16[1,512,2048]{2,1,0:T(8,128)(2,1)S(1)} %copy-done.2), custom_call_target="tpu_custom_call" | custom-call | tf_op jit(solution)/shard_map/experts/pallas_call | solution.py:125
  67.8 28.9 %all_to_all.11 = bf16[128,48,128]{2,1,0:T(8,128)(2,1)S(1)} all-to-all(bf16[128,48,128]{2,1,0:T(8,128)(2,1)S(1)} %bitcast.15), channel_id=1, replica_groups=mesh['sp_0'=4,'sp_1'=4,'sp_2'=4,'tp'=2] {'sp_0','sp_1','sp_2','tp'}, dimensions={0} | all-to-all | bytes 3145728 | tf_op jit(solution)/shard_map/all_to_all | solution.py:543
  96.7 1.7 %combine.1 = bf16[128,2048]{1,0:T(8,128)(2,1)} custom-call(s32[2,128]{1,0:T(2,128)S(1)} %get-tuple-element.40.slots_vmem, bf16[384,16,128]{2,1,0:T(8,128)(2,1)S(1)} %bitcast.13, bf16[128,2048]{1,0:T(8,128)(2,1)S(1)} %get-tuple-element.67.merged_ref, f32[2,128,128]{2,1,0:T(8,128)S(1)} %get-tuple-element.68.weights_ref), custom_call_target="tpu_custom_call" | custom-call | tf_op jit(solution)/shard_map/combine/pallas_call | solution.py:168
  (30 shorter events, 0.1 us)
Async XLA Ops:
  0.0 6.4 %copy-start.12 = (f32[128,2]{0,1:T(2,128)S(1)}, f32[128,2]{0,1:T(2,128)}, u32[]{:S(2)}) copy-start(f32[128,2]{0,1:T(2,128)} %param.26) | copy-start | bytes 3076
  0.0 6.4 %copy-start.13 = (f32[128]{0:T(128)S(1)}, f32[128]{0:T(128)}, u32[]{:S(2)}) copy-start(f32[128]{0:T(128)} %param.25) | copy-start | bytes 1540
  0.0 6.4 %copy-start.11 = (s32[128,2]{0,1:T(2,128)S(1)}, s32[128,2]{0,1:T(2,128)}, u32[]{:S(2)}) copy-start(s32[128,2]{0,1:T(2,128)} %param.24) | copy-start | bytes 3076
  1.9 4.8 %collective-permute-start.2 = (bf16[272,128]{1,0:T(8,128)(2,1)S(1)}, bf16[272,128]{1,0:T(8,128)(2,1)S(1)}, u32[]{:S(2)}, u32[]{:S(2)}) collective-permute-start(bf16[272,128]{1,0:T(8,128)(2,1)S(1)} %shard_map.146.own_ref), channel_id=1, source_target_pairs={{0,6},{2,0},{4,2},{6,4},{1,7},{3,1},{5,3},{7,5},{8,14},{10,8},{12,... | collective-permute-start | bytes 208904 | tf_op jit(solution)/shard_map/ppermute | solution.py:450
  5.3 4.7 %collective-permute-start.1 = (bf16[272,128]{1,0:T(8,128)(2,1)S(1)}, bf16[272,128]{1,0:T(8,128)(2,1)S(1)}, u32[]{:S(2)}, u32[]{:S(2)}) collective-permute-start(bf16[272,128]{1,0:T(8,128)(2,1)S(1)} %shard_map.146.own_ref), channel_id=1, source_target_pairs={{0,4},{2,6},{4,0},{6,2},{1,5},{3,7},{5,1},{7,3},{8,12},{10,14},{12... | collective-permute-start | bytes 208904 | tf_op jit(solution)/shard_map/ppermute | solution.py:450
  5.8 5.3 %collective-permute-start = (bf16[272,128]{1,0:T(8,128)(2,1)S(1)}, bf16[272,128]{1,0:T(8,128)(2,1)S(1)}, u32[]{:S(2)}, u32[]{:S(2)}) collective-permute-start(bf16[272,128]{1,0:T(8,128)(2,1)S(1)} %shard_map.146.own_ref), channel_id=1, source_target_pairs={{0,2},{2,4},{4,6},{6,0},{1,3},{3,5},{5,7},{7,1},{8,10},{10,12},{12... | collective-permute-start | bytes 208904 | tf_op jit(solution)/shard_map/ppermute | solution.py:450
  11.2 4.2 %collective-permute-start.5 = (bf16[272,128]{1,0:T(8,128)(2,1)S(1)}, bf16[272,128]{1,0:T(8,128)(2,1)S(1)}, u32[]{:S(2)}, u32[]{:S(2)}) collective-permute-start(bf16[272,128]{1,0:T(8,128)(2,1)S(1)} %get-tuple-element.45.own_ref), channel_id=1, source_target_pairs={{0,24},{8,0},{16,8},{24,16},{1,25},{9,1},{17,9},{25,17},{2,26},{10... | collective-permute-start | bytes 208904 | tf_op jit(solution)/shard_map/ppermute | solution.py:450
  14.0 4.7 %collective-permute-start.4 = (bf16[272,128]{1,0:T(8,128)(2,1)S(1)}, bf16[272,128]{1,0:T(8,128)(2,1)S(1)}, u32[]{:S(2)}, u32[]{:S(2)}) collective-permute-start(bf16[272,128]{1,0:T(8,128)(2,1)S(1)} %get-tuple-element.45.own_ref), channel_id=1, source_target_pairs={{0,16},{8,24},{16,0},{24,8},{1,17},{9,25},{17,1},{25,9},{2,18},{10... | collective-permute-start | bytes 208904 | tf_op jit(solution)/shard_map/ppermute | solution.py:450
  14.4 5.1 %collective-permute-start.3 = (bf16[272,128]{1,0:T(8,128)(2,1)S(1)}, bf16[272,128]{1,0:T(8,128)(2,1)S(1)}, u32[]{:S(2)}, u32[]{:S(2)}) collective-permute-start(bf16[272,128]{1,0:T(8,128)(2,1)S(1)} %get-tuple-element.45.own_ref), channel_id=1, source_target_pairs={{0,8},{8,16},{16,24},{24,0},{1,9},{9,17},{17,25},{25,1},{2,10},{10... | collective-permute-start | bytes 208904 | tf_op jit(solution)/shard_map/ppermute | solution.py:450
  19.4 4.7 %copy-start.5 = (bf16[256,512]{1,0:T(8,128)(2,1)S(1)}, bf16[256,512]{1,0:T(8,128)(2,1)}, u32[]{:S(2)}) copy-start(bf16[256,512]{1,0:T(8,128)(2,1)} %values_ref.1) | copy-start | bytes 786436
  19.4 4.7 %copy-start.6 = (bf16[256,512]{1,0:T(8,128)(2,1)S(1)}, bf16[256,512]{1,0:T(8,128)(2,1)}, u32[]{:S(2)}) copy-start(bf16[256,512]{1,0:T(8,128)(2,1)} %out_gate_ref.1) | copy-start | bytes 786436
  19.4 4.7 %copy-start.7 = (bf16[256,256]{1,0:T(8,128)(2,1)S(1)}, bf16[256,256]{1,0:T(8,128)(2,1)}, u32[]{:S(2)}) copy-start(bf16[256,256]{1,0:T(8,128)(2,1)} %keys_ref) | copy-start | bytes 393220
  19.4 4.7 %copy-start.8 = (bf16[256,256]{1,0:T(8,128)(2,1)S(1)}, bf16[256,256]{1,0:T(8,128)(2,1)}, u32[]{:S(2)}) copy-start(bf16[256,256]{1,0:T(8,128)(2,1)} %logits_ref.1) | copy-start | bytes 393220
  19.4 4.7 %copy-start.9 = (bf16[256,256]{1,0:T(8,128)(2,1)S(1)}, bf16[256,256]{1,0:T(8,128)(2,1)}, u32[]{:S(2)}) copy-start(bf16[256,256]{1,0:T(8,128)(2,1)} %queries_ref) | copy-start | bytes 393220
  19.5 4.7 %copy-start.14 = (f32[128]{0:T(128)S(1)}, f32[128]{0:T(128)}, u32[]{:S(2)}) copy-start(f32[128]{0:T(128)} %param.21) | copy-start | bytes 1540
  19.6 6.3 %collective-permute-start.8 = (bf16[272,128]{1,0:T(8,128)(2,1)S(1)}, bf16[272,128]{1,0:T(8,128)(2,1)S(1)}, u32[]{:S(2)}, u32[]{:S(2)}) collective-permute-start(bf16[272,128]{1,0:T(8,128)(2,1)S(1)} %get-tuple-element.46), channel_id=1, source_target_pairs={{0,96},{32,0},{64,32},{96,64},{1,97},{33,1},{65,33},{97,65},{2,98}... | collective-permute-start | bytes 208904 | tf_op jit(solution)/shard_map/ppermute | solution.py:450
  23.4 4.8 %collective-permute-start.7 = (bf16[272,128]{1,0:T(8,128)(2,1)S(1)}, bf16[272,128]{1,0:T(8,128)(2,1)S(1)}, u32[]{:S(2)}, u32[]{:S(2)}) collective-permute-start(bf16[272,128]{1,0:T(8,128)(2,1)S(1)} %get-tuple-element.46), channel_id=1, source_target_pairs={{0,64},{32,96},{64,0},{96,32},{1,65},{33,97},{65,1},{97,33},{2,66}... | collective-permute-start | bytes 208904 | tf_op jit(solution)/shard_map/ppermute | solution.py:450
  23.4 5.1 %collective-permute-start.6 = (bf16[272,128]{1,0:T(8,128)(2,1)S(1)}, bf16[272,128]{1,0:T(8,128)(2,1)S(1)}, u32[]{:S(2)}, u32[]{:S(2)}) collective-permute-start(bf16[272,128]{1,0:T(8,128)(2,1)S(1)} %get-tuple-element.46), channel_id=1, source_target_pairs={{0,32},{32,64},{64,96},{96,0},{1,33},{33,65},{65,97},{97,1},{2,34}... | collective-permute-start | bytes 208904 | tf_op jit(solution)/shard_map/ppermute | solution.py:450
  24.2 9.6 %copy-start.3 = (bf16[1024,2048]{1,0:T(8,128)(2,1)S(1)}, bf16[1024,2048]{1,0:T(8,128)(2,1)}, u32[]{:S(2)}) copy-start(bf16[1024,2048]{1,0:T(8,128)(2,1)} %weight_ref.3) | copy-start | bytes 12582916
  24.2 9.6 %copy-start.4 = (bf16[128,2048]{1,0:T(8,128)(2,1)S(1)}, bf16[128,2048]{1,0:T(8,128)(2,1)}, u32[]{:S(2)}) copy-start(bf16[128,2048]{1,0:T(8,128)(2,1)} %residual_ref.1) | copy-start | bytes 1572868
  29.0 5.7 %collective-permute-start.9 = (bf16[128,512]{1,0:T(8,128)(2,1)S(1)}, bf16[128,512]{1,0:T(8,128)(2,1)S(1)}, u32[]{:S(2)}, u32[]{:S(2)}) collective-permute-start(bf16[128,512]{1,0:T(8,128)(2,1)S(1)} %get-tuple-element.63), channel_id=1, source_target_pairs={{0,1},{1,0},{2,3},{3,2},{4,5},{5,4},{6,7},{7,6},{8,9},{9,8},{10,11... | collective-permute-start | bytes 393224 | tf_op jit(solution)/shard_map/ppermute | solution.py:522
  33.8 1.0 copy-start.10
  34.8 30.0 %copy-start.1 = (bf16[1,2048,512]{2,1,0:T(8,128)(2,1)S(1)}, bf16[1,2048,512]{2,1,0:T(8,128)(2,1)}, u32[]{:S(2)}) copy-start(bf16[1,2048,512]{2,1,0:T(8,128)(2,1)} %up.1) | copy-start | bytes 6291460
  34.8 30.0 %copy-start.2 = (bf16[1,512,2048]{2,1,0:T(8,128)(2,1)S(1)}, bf16[1,512,2048]{2,1,0:T(8,128)(2,1)}, u32[]{:S(2)}) copy-start(bf16[1,512,2048]{2,1,0:T(8,128)(2,1)} %down.1) | copy-start | bytes 6291460
  35.9 28.8 %copy-start = (bf16[1,2048,512]{2,1,0:T(8,128)(2,1)S(1)}, bf16[1,2048,512]{2,1,0:T(8,128)(2,1)}, u32[]{:S(2)}) copy-start(bf16[1,2048,512]{2,1,0:T(8,128)(2,1)} %gate.1) | copy-start | bytes 6291460

commit v10 on v9

--- a/solution.py
+++ b/solution.py
@@ -196,12 +196,20 @@
     )
 
 
-def running_sums(logits):
-    length = logits.shape[0]
+def decay_parts(logits):
     decay_log = (jnp.minimum(logits, 0.0) - jnp.log1p(jnp.exp(-jnp.abs(logits)))) / 16.0
-    parts = pieces(decay_log, 3)
+    return decay_log, pieces(decay_log, 3)
+
+
+def ordered(length):
     row = lax.broadcasted_iota(jnp.int32, (length, length), 0)
     column = lax.broadcasted_iota(jnp.int32, (length, length), 1)
+    return row, column
+
+
+def running_sums(logits):
+    _, parts = decay_parts(logits)
+    row, column = ordered(logits.shape[0])
     earlier = (row >= column) & (row // BLOCK == column // BLOCK)
     earlier = earlier.astype(jnp.float32).astype(jnp.bfloat16)
     return sum(product(earlier, part) for part in parts)
@@ -212,13 +220,14 @@
     rows = slice(n * BLOCK, (n + 1) * BLOCK)
     closing = running[(n + 1) * BLOCK - 1 : (n + 1) * BLOCK]
     key_closing = keys_ref[rows].astype(jnp.float32) * jnp.exp(closing - running[rows])
-    key_closing = key_closing.astype(jnp.bfloat16)
+    key_closing = pieces(key_closing, 2)
     decay = jnp.exp(closing)
     lane = lax.broadcasted_iota(jnp.int32, (VALUE_DIM, LANES), 1)
     after = []
     for p, state in enumerate(states):
         lanes = slice(p * LANES, (p + 1) * LANES)
-        grown = product(values_ref[rows, p * wide : (p + 1) * wide], key_closing[:, lanes], 0, 0)
+        value = values_ref[rows, p * wide : (p + 1) * wide]
+        grown = product(value, key_closing[0][:, lanes], 0, 0) + product(value, key_closing[1][:, lanes], 0, 0)
         grown = jnp.where(lane < KEY_DIM, grown[:VALUE_DIM], grown[VALUE_DIM:])
         after.append(decay[:, lanes] * state + grown)
     return after
@@ -235,18 +244,22 @@
         copy.start()
     copies[0].wait()
     length, channels = keys_ref.shape
-    blocks = length // BLOCK
     pairs = channels // LANES
-    running = running_sums(logits_ref[...].astype(jnp.float32))
+    wide = 2 * VALUE_DIM
+    decay_log, parts = decay_parts(logits_ref[...].astype(jnp.float32))
+    row, column = ordered(length)
+    later = (row < column).astype(jnp.float32).astype(jnp.bfloat16)
+    ahead = sum(product(later, part) for part in parts)
+    factor = jnp.exp(ahead)
+    total = ahead[0:1] + decay_log[0:1]
     copies[1].wait()
+    key_end = (keys_ref[...].astype(jnp.float32) * factor).astype(jnp.bfloat16)
     copies[2].wait()
-    states = [jnp.zeros((VALUE_DIM, LANES), jnp.float32)] * pairs
-    total = jnp.zeros((1, channels), jnp.float32)
-    for n in range(blocks):
-        total = total + running[(n + 1) * BLOCK - 1 : (n + 1) * BLOCK]
-        states = grow(states, n, running, keys_ref, values_ref)
+    lane = lax.broadcasted_iota(jnp.int32, (VALUE_DIM, LANES), 1)
     for p in range(pairs):
-        message_ref[p * VALUE_DIM : (p + 1) * VALUE_DIM] = states[p].astype(jnp.bfloat16)
+        grown = product(values_ref[:, p * wide : (p + 1) * wide], key_end[:, p * LANES : (p + 1) * LANES], 0, 0)
+        state = jnp.where(lane < KEY_DIM, grown[:VALUE_DIM], grown[VALUE_DIM:])
+        message_ref[p * VALUE_DIM : (p + 1) * VALUE_DIM] = state.astype(jnp.bfloat16)
     message_ref[pairs * VALUE_DIM :] = pack_decay(jnp.exp(total))
 
 
@@ -324,18 +337,22 @@
         rows = slice(n * BLOCK, (n + 1) * BLOCK)
         running = running_all[rows]
         query_scaled = queries_ref[rows].astype(jnp.float32) * KEY_DIM ** (-0.5) * jnp.exp(running)
-        key_inverse = (keys_ref[rows].astype(jnp.float32) * jnp.exp(-running)).astype(jnp.bfloat16)
+        key_inverse = pieces(keys_ref[rows].astype(jnp.float32) * jnp.exp(-running), 2)
         reach_ref[rows] = query_scaled * jnp.exp(lead)
         lead = lead + running[BLOCK - 1 : BLOCK]
         for p in range(pairs):
             lanes = slice(p * LANES, (p + 1) * LANES)
-            masked = masked_heads(query_scaled[:, lanes])
-            scores = jnp.where(causal, product(masked, key_inverse[:, lanes], 1, 1), 0.0).astype(jnp.bfloat16)
-            carried = product(masked, states[p].astype(jnp.bfloat16), 1, 1)
+            high, low = (masked_heads(part.astype(jnp.float32)) for part in pieces(query_scaled[:, lanes], 2))
+            scores = product(high, key_inverse[0][:, lanes], 1, 1)
+            scores = scores + product(high, key_inverse[1][:, lanes], 1, 1) + product(low, key_inverse[0][:, lanes], 1, 1)
+            scores = pieces(jnp.where(causal, scores, 0.0), 2)
+            before = pieces(states[p], 2)
+            carried = product(high, before[0], 1, 1) + product(high, before[1], 1, 1) + product(low, before[0], 1, 1)
             for h in range(2):
                 place = slice((2 * p + h) * VALUE_DIM, (2 * p + h + 1) * VALUE_DIM)
                 part = slice(h * BLOCK, (h + 1) * BLOCK)
-                partial_ref[rows, place] = product(scores[part], values_ref[rows, place]) + carried[part]
+                value = values_ref[rows, place]
+                partial_ref[rows, place] = product(scores[0][part], value) + product(scores[1][part], value) + carried[part]
         if n + 1 < blocks:
             states = grow(states, n, running_all, keys_ref, values_ref)
 

time: 98.5 us -> 98.4 us (level)
  no operation moved by 1% of the time
where the time goes in v10:
time: 98.4 us; the launch traced here: 98.3 us
  blocking collectives  57.7 us (59%)
  starting transfers between devices  17.6 us (18%)
  Pallas kernels  11.5 us (12%)
  waiting for transfers between devices  11.3 us (11%)
    all_to_all x1, blocking collectives, local(): lax.all_to_all(served.reshape(block), SP_TP, split_axis=0, concat_axis=0,...  28.9 us
    all_to_all x1, blocking collectives, local(): lax.all_to_all(outgoing.reshape(block), SP_TP, split_axis=0, concat_axis=...  28.8 us
    ppermute x9, starting transfers between devices, from_behind(): lax.ppermute(message, axis, [(i, (i + k) % RING) for i in range(RING)])  12.9 us
    ppermute x9, waiting for transfers between devices, from_behind(): lax.ppermute(message, axis, [(i, (i + k) % RING) for i in range(RING)])  10.8 us
    pallas_call x8, Pallas kernels, call(): pl.pallas_call(kernel, out_shape=outs, in_specs=[SMEM_SPEC] * scalars + [...  6.69 us
    ppermute x1, starting transfers between devices, local(): taken = lax.ppermute(given, 'tp', [(0, 1), (1, 0)])  4.75 us
    pallas_call x1, Pallas kernels, experts(): pl.pallas_call(experts_kernel, out_shape=jax.ShapeDtypeStruct(arrived.sha...  3.05 us
  transfers between devices with their start and end apart: 10, of which 8 were waited for; matrix products, arithmetic and copies ran while one was open for 0% of the time, Pallas kernels for 3%

profile of v10, /device:TPU:1, one launch (start us, length us, event | category | flops | bytes accessed | tf_op | source)
XLA Modules:
  0.0 98.3 jit_solution(9072899213926610088)
XLA Ops:
  0.0 1.8 %shard_map.146.own_ref = bf16[272,128]{1,0:T(8,128)(2,1)S(1)} custom-call(bf16[256,256]{1,0:T(8,128)(2,1)} %keys_ref, bf16[256,512]{1,0:T(8,128)(2,1)} %values_ref.1, bf16[256,256]{1,0:T(8,128)(2,1)} %logits_ref.1), custom_call_target="tpu_custom_call" | custom-call | flops 4000000000 | bytes 10000000 | tf_op jit(solution)/shard_map/pallas_call | solution.py:453
  1.8 3.4 %collective-permute-start.2 = (bf16[272,128]{1,0:T(8,128)(2,1)S(1)}, bf16[272,128]{1,0:T(8,128)(2,1)S(1)}, u32[]{:S(2)}, u32[]{:S(2)}) collective-permute-start(bf16[272,128]{1,0:T(8,128)(2,1)S(1)} %shard_map.146.own_ref), channel_id=1, source_target_pairs={{0,6},{2,0},{4,2},{6,4},{1,7},{3,1},{5,3},{7,5},{8,14},{10,8},{12,... | collective-permute-start | bytes 208904 | tf_op jit(solution)/shard_map/ppermute | solution.py:467
  5.2 0.5 collective-permute-start.1
  5.7 0.6 collective-permute-start
  6.3 0.3 shard_map.145
  6.6 3.3 %collective-permute-done.1.back2_ref = bf16[272,128]{1,0:T(8,128)(2,1)S(1)} collective-permute-done((bf16[272,128]{1,0:T(8,128)(2,1)S(1)}, bf16[272,128]{1,0:T(8,128)(2,1)S(1)}, u32[]{:S(2)}, u32[]{:S(2)}) %collective-permute-start.1) | collective-permute-done | bytes 69664 | tf_op jit(solution)/shard_map/ppermute | solution.py:467
  9.9 1.1 %collective-permute-done.back1_ref = bf16[272,128]{1,0:T(8,128)(2,1)S(1)} collective-permute-done((bf16[272,128]{1,0:T(8,128)(2,1)S(1)}, bf16[272,128]{1,0:T(8,128)(2,1)S(1)}, u32[]{:S(2)}, u32[]{:S(2)}) %collective-permute-start) | collective-permute-done | bytes 69664 | tf_op jit(solution)/shard_map/ppermute | solution.py:467
  11.0 0.1 shard_map.147
  11.1 2.8 %collective-permute-start.5 = (bf16[272,128]{1,0:T(8,128)(2,1)S(1)}, bf16[272,128]{1,0:T(8,128)(2,1)S(1)}, u32[]{:S(2)}, u32[]{:S(2)}) collective-permute-start(bf16[272,128]{1,0:T(8,128)(2,1)S(1)} %get-tuple-element.45.own_ref), channel_id=1, source_target_pairs={{0,24},{8,0},{16,8},{24,16},{1,25},{9,1},{17,9},{25,17},{2,26},{10... | collective-permute-start | bytes 208904 | tf_op jit(solution)/shard_map/ppermute | solution.py:467
  13.9 0.3 collective-permute-start.4
  14.3 0.7 collective-permute-start.3
  14.9 0.3 collective-permute-done.5.back3_ref
  15.3 3.4 %collective-permute-done.4.back2_ref = bf16[272,128]{1,0:T(8,128)(2,1)S(1)} collective-permute-done((bf16[272,128]{1,0:T(8,128)(2,1)S(1)}, bf16[272,128]{1,0:T(8,128)(2,1)S(1)}, u32[]{:S(2)}, u32[]{:S(2)}) %collective-permute-start.4) | collective-permute-done | bytes 69664 | tf_op jit(solution)/shard_map/ppermute | solution.py:467
  18.6 0.7 collective-permute-done.3.back1_ref
  19.3 0.0 copy-start.9
  19.3 0.0 copy-start.14
  19.4 0.1 shard_map.148
  19.5 3.8 %collective-permute-start.8 = (bf16[272,128]{1,0:T(8,128)(2,1)S(1)}, bf16[272,128]{1,0:T(8,128)(2,1)S(1)}, u32[]{:S(2)}, u32[]{:S(2)}) collective-permute-start(bf16[272,128]{1,0:T(8,128)(2,1)S(1)} %get-tuple-element.46), channel_id=1, source_target_pairs={{0,96},{32,0},{64,32},{96,64},{1,97},{33,1},{65,33},{97,65},{2,98}... | collective-permute-start | bytes 208904 | tf_op jit(solution)/shard_map/ppermute | solution.py:467
  23.3 0.7 collective-permute-start.6
  24.1 0.0 copy-start.3
  24.1 2.3 %shard_map.149 = (f32[256,512]{1,0:T(8,128)S(1)}, f32[256,256]{1,0:T(8,128)S(1)}, f32[256,512]{1,0:T(8,128)S(1)}) custom-call(bf16[256,256]{1,0:T(8,128)(2,1)S(1)} %copy-done.9, bf16[256,256]{1,0:T(8,128)(2,1)S(1)} %copy-done.7, bf16[256,512]{1,0:T(8,128)(2,1)S(1)} %copy-done.5, bf16[256,256]{1,0:T(8,128)(2,1)S(1)} %copy-done.8, f32[1,128]{1,0:T(1,128)S(1)} %bitcast.21, ...), custom_call_target="tpu_custom_call" | custom-call | flops 4000000000 | bytes 10000000 | tf_op jit(solution)/shard_map/pallas_call | solution.py:453
  26.4 1.7 %collective-permute-done.7.back2_ref = bf16[272,128]{1,0:T(8,128)(2,1)S(1)} collective-permute-done((bf16[272,128]{1,0:T(8,128)(2,1)S(1)}, bf16[272,128]{1,0:T(8,128)(2,1)S(1)}, u32[]{:S(2)}, u32[]{:S(2)}) %collective-permute-start.7) | collective-permute-done | bytes 69664 | tf_op jit(solution)/shard_map/ppermute | solution.py:467
  28.1 0.4 collective-permute-done.6.back1_ref
  28.4 0.5 shard_map.150
  28.9 4.7 %collective-permute-start.9 = (bf16[128,512]{1,0:T(8,128)(2,1)S(1)}, bf16[128,512]{1,0:T(8,128)(2,1)S(1)}, u32[]{:S(2)}, u32[]{:S(2)}) collective-permute-start(bf16[128,512]{1,0:T(8,128)(2,1)S(1)} %get-tuple-element.63), channel_id=1, source_target_pairs={{0,1},{1,0},{2,3},{3,2},{4,5},{5,4},{6,7},{7,6},{8,9},{9,8},{10,11... | collective-permute-start | bytes 393224 | tf_op jit(solution)/shard_map/ppermute | solution.py:539
  33.7 0.5 shard_map.151.partial_ref
  34.1 0.5 collective-permute-done.9.taken_ref
  34.6 1.1 %shard_map.152 = (bf16[128,2048]{1,0:T(8,128)(2,1)S(1)}, bf16[384,16,128]{2,1,0:T(8,128)(2,1)S(1)}) custom-call(s32[1]{0:T(128)} %bitcast.3.place_ref, s32[8,128]{1,0:T(8,128)S(1)} %get-tuple-element.41.owners_vmem, bf16[128,512]{1,0:T(8,128)(2,1)S(1)} %collective-permute-done.9.taken_ref, bf16[1024,2048]{1,0:T(8,128)(2,1)S(1)} %copy-done.3, ...), custom_call_target="tpu_custom_call" | custom-call | flops 4000000000 | bytes 10000000 | tf_op jit(solution)/shard_map/pallas_call | solution.py:453
  35.8 28.8 %all_to_all.10 = bf16[128,48,128]{2,1,0:T(8,128)(2,1)S(1)} all-to-all(bf16[128,48,128]{2,1,0:T(8,128)(2,1)S(1)} %bitcast.16), channel_id=1, replica_groups=mesh['sp_0'=4,'sp_1'=4,'sp_2'=4,'tp'=2] {'sp_0','sp_1','sp_2','tp'}, dimensions={0} | all-to-all | bytes 3145728 | tf_op jit(solution)/shard_map/all_to_all | solution.py:558
  64.6 3.0 %experts.1 = bf16[384,16,128]{2,1,0:T(8,128)(2,1)S(1)} custom-call(bf16[384,16,128]{2,1,0:T(8,128)(2,1)S(1)} %bitcast.14, bf16[1,2048,512]{2,1,0:T(8,128)(2,1)S(1)} %copy-done, bf16[1,2048,512]{2,1,0:T(8,128)(2,1)S(1)} %copy-done.1, bf16[1,512,2048]{2,1,0:T(8,128)(2,1)S(1)} %copy-done.2), custom_call_target="tpu_custom_call" | custom-call | tf_op jit(solution)/shard_map/experts/pallas_call | solution.py:125
  67.7 28.9 %all_to_all.11 = bf16[128,48,128]{2,1,0:T(8,128)(2,1)S(1)} all-to-all(bf16[128,48,128]{2,1,0:T(8,128)(2,1)S(1)} %bitcast.15), channel_id=1, replica_groups=mesh['sp_0'=4,'sp_1'=4,'sp_2'=4,'tp'=2] {'sp_0','sp_1','sp_2','tp'}, dimensions={0} | all-to-all | bytes 3145728 | tf_op jit(solution)/shard_map/all_to_all | solution.py:560
  96.6 1.7 %combine.1 = bf16[128,2048]{1,0:T(8,128)(2,1)} custom-call(s32[2,128]{1,0:T(2,128)S(1)} %get-tuple-element.40.slots_vmem, bf16[384,16,128]{2,1,0:T(8,128)(2,1)S(1)} %bitcast.13, bf16[128,2048]{1,0:T(8,128)(2,1)S(1)} %get-tuple-element.67.merged_ref, f32[2,128,128]{2,1,0:T(8,128)S(1)} %get-tuple-element.68.weights_ref), custom_call_target="tpu_custom_call" | custom-call | tf_op jit(solution)/shard_map/combine/pallas_call | solution.py:168
  (30 shorter events, 0.1 us)
Async XLA Ops:
  0.0 6.3 %copy-start.12 = (f32[128,2]{0,1:T(2,128)S(1)}, f32[128,2]{0,1:T(2,128)}, u32[]{:S(2)}) copy-start(f32[128,2]{0,1:T(2,128)} %param.26) | copy-start | bytes 3076
  0.0 6.3 %copy-start.13 = (f32[128]{0:T(128)S(1)}, f32[128]{0:T(128)}, u32[]{:S(2)}) copy-start(f32[128]{0:T(128)} %param.25) | copy-start | bytes 1540
  0.0 6.3 %copy-start.11 = (s32[128,2]{0,1:T(2,128)S(1)}, s32[128,2]{0,1:T(2,128)}, u32[]{:S(2)}) copy-start(s32[128,2]{0,1:T(2,128)} %param.24) | copy-start | bytes 3076
  1.8 4.8 %collective-permute-start.2 = (bf16[272,128]{1,0:T(8,128)(2,1)S(1)}, bf16[272,128]{1,0:T(8,128)(2,1)S(1)}, u32[]{:S(2)}, u32[]{:S(2)}) collective-permute-start(bf16[272,128]{1,0:T(8,128)(2,1)S(1)} %shard_map.146.own_ref), channel_id=1, source_target_pairs={{0,6},{2,0},{4,2},{6,4},{1,7},{3,1},{5,3},{7,5},{8,14},{10,8},{12,... | collective-permute-start | bytes 208904 | tf_op jit(solution)/shard_map/ppermute | solution.py:467
  5.2 4.7 %collective-permute-start.1 = (bf16[272,128]{1,0:T(8,128)(2,1)S(1)}, bf16[272,128]{1,0:T(8,128)(2,1)S(1)}, u32[]{:S(2)}, u32[]{:S(2)}) collective-permute-start(bf16[272,128]{1,0:T(8,128)(2,1)S(1)} %shard_map.146.own_ref), channel_id=1, source_target_pairs={{0,4},{2,6},{4,0},{6,2},{1,5},{3,7},{5,1},{7,3},{8,12},{10,14},{12... | collective-permute-start | bytes 208904 | tf_op jit(solution)/shard_map/ppermute | solution.py:467
  5.7 5.3 %collective-permute-start = (bf16[272,128]{1,0:T(8,128)(2,1)S(1)}, bf16[272,128]{1,0:T(8,128)(2,1)S(1)}, u32[]{:S(2)}, u32[]{:S(2)}) collective-permute-start(bf16[272,128]{1,0:T(8,128)(2,1)S(1)} %shard_map.146.own_ref), channel_id=1, source_target_pairs={{0,2},{2,4},{4,6},{6,0},{1,3},{3,5},{5,7},{7,1},{8,10},{10,12},{12... | collective-permute-start | bytes 208904 | tf_op jit(solution)/shard_map/ppermute | solution.py:467
  11.1 4.2 %collective-permute-start.5 = (bf16[272,128]{1,0:T(8,128)(2,1)S(1)}, bf16[272,128]{1,0:T(8,128)(2,1)S(1)}, u32[]{:S(2)}, u32[]{:S(2)}) collective-permute-start(bf16[272,128]{1,0:T(8,128)(2,1)S(1)} %get-tuple-element.45.own_ref), channel_id=1, source_target_pairs={{0,24},{8,0},{16,8},{24,16},{1,25},{9,1},{17,9},{25,17},{2,26},{10... | collective-permute-start | bytes 208904 | tf_op jit(solution)/shard_map/ppermute | solution.py:467
  13.9 4.7 %collective-permute-start.4 = (bf16[272,128]{1,0:T(8,128)(2,1)S(1)}, bf16[272,128]{1,0:T(8,128)(2,1)S(1)}, u32[]{:S(2)}, u32[]{:S(2)}) collective-permute-start(bf16[272,128]{1,0:T(8,128)(2,1)S(1)} %get-tuple-element.45.own_ref), channel_id=1, source_target_pairs={{0,16},{8,24},{16,0},{24,8},{1,17},{9,25},{17,1},{25,9},{2,18},{10... | collective-permute-start | bytes 208904 | tf_op jit(solution)/shard_map/ppermute | solution.py:467
  14.3 5.1 %collective-permute-start.3 = (bf16[272,128]{1,0:T(8,128)(2,1)S(1)}, bf16[272,128]{1,0:T(8,128)(2,1)S(1)}, u32[]{:S(2)}, u32[]{:S(2)}) collective-permute-start(bf16[272,128]{1,0:T(8,128)(2,1)S(1)} %get-tuple-element.45.own_ref), channel_id=1, source_target_pairs={{0,8},{8,16},{16,24},{24,0},{1,9},{9,17},{17,25},{25,1},{2,10},{10... | collective-permute-start | bytes 208904 | tf_op jit(solution)/shard_map/ppermute | solution.py:467
  19.3 4.7 %copy-start.5 = (bf16[256,512]{1,0:T(8,128)(2,1)S(1)}, bf16[256,512]{1,0:T(8,128)(2,1)}, u32[]{:S(2)}) copy-start(bf16[256,512]{1,0:T(8,128)(2,1)} %values_ref.1) | copy-start | bytes 786436
  19.3 4.7 %copy-start.6 = (bf16[256,512]{1,0:T(8,128)(2,1)S(1)}, bf16[256,512]{1,0:T(8,128)(2,1)}, u32[]{:S(2)}) copy-start(bf16[256,512]{1,0:T(8,128)(2,1)} %out_gate_ref.1) | copy-start | bytes 786436
  19.3 4.7 %copy-start.7 = (bf16[256,256]{1,0:T(8,128)(2,1)S(1)}, bf16[256,256]{1,0:T(8,128)(2,1)}, u32[]{:S(2)}) copy-start(bf16[256,256]{1,0:T(8,128)(2,1)} %keys_ref) | copy-start | bytes 393220
  19.3 4.7 %copy-start.8 = (bf16[256,256]{1,0:T(8,128)(2,1)S(1)}, bf16[256,256]{1,0:T(8,128)(2,1)}, u32[]{:S(2)}) copy-start(bf16[256,256]{1,0:T(8,128)(2,1)} %logits_ref.1) | copy-start | bytes 393220
  19.3 4.7 %copy-start.9 = (bf16[256,256]{1,0:T(8,128)(2,1)S(1)}, bf16[256,256]{1,0:T(8,128)(2,1)}, u32[]{:S(2)}) copy-start(bf16[256,256]{1,0:T(8,128)(2,1)} %queries_ref) | copy-start | bytes 393220
  19.3 4.7 %copy-start.14 = (f32[128]{0:T(128)S(1)}, f32[128]{0:T(128)}, u32[]{:S(2)}) copy-start(f32[128]{0:T(128)} %param.21) | copy-start | bytes 1540
  19.5 6.9 %collective-permute-start.8 = (bf16[272,128]{1,0:T(8,128)(2,1)S(1)}, bf16[272,128]{1,0:T(8,128)(2,1)S(1)}, u32[]{:S(2)}, u32[]{:S(2)}) collective-permute-start(bf16[272,128]{1,0:T(8,128)(2,1)S(1)} %get-tuple-element.46), channel_id=1, source_target_pairs={{0,96},{32,0},{64,32},{96,64},{1,97},{33,1},{65,33},{97,65},{2,98}... | collective-permute-start | bytes 208904 | tf_op jit(solution)/shard_map/ppermute | solution.py:467
  23.3 4.8 %collective-permute-start.7 = (bf16[272,128]{1,0:T(8,128)(2,1)S(1)}, bf16[272,128]{1,0:T(8,128)(2,1)S(1)}, u32[]{:S(2)}, u32[]{:S(2)}) collective-permute-start(bf16[272,128]{1,0:T(8,128)(2,1)S(1)} %get-tuple-element.46), channel_id=1, source_target_pairs={{0,64},{32,96},{64,0},{96,32},{1,65},{33,97},{65,1},{97,33},{2,66}... | collective-permute-start | bytes 208904 | tf_op jit(solution)/shard_map/ppermute | solution.py:467
  23.3 5.1 %collective-permute-start.6 = (bf16[272,128]{1,0:T(8,128)(2,1)S(1)}, bf16[272,128]{1,0:T(8,128)(2,1)S(1)}, u32[]{:S(2)}, u32[]{:S(2)}) collective-permute-start(bf16[272,128]{1,0:T(8,128)(2,1)S(1)} %get-tuple-element.46), channel_id=1, source_target_pairs={{0,32},{32,64},{64,96},{96,0},{1,33},{33,65},{65,97},{97,1},{2,34}... | collective-permute-start | bytes 208904 | tf_op jit(solution)/shard_map/ppermute | solution.py:467
  24.1 9.6 %copy-start.3 = (bf16[1024,2048]{1,0:T(8,128)(2,1)S(1)}, bf16[1024,2048]{1,0:T(8,128)(2,1)}, u32[]{:S(2)}) copy-start(bf16[1024,2048]{1,0:T(8,128)(2,1)} %weight_ref.3) | copy-start | bytes 12582916
  24.1 9.6 %copy-start.4 = (bf16[128,2048]{1,0:T(8,128)(2,1)S(1)}, bf16[128,2048]{1,0:T(8,128)(2,1)}, u32[]{:S(2)}) copy-start(bf16[128,2048]{1,0:T(8,128)(2,1)} %residual_ref.1) | copy-start | bytes 1572868
  28.9 5.7 %collective-permute-start.9 = (bf16[128,512]{1,0:T(8,128)(2,1)S(1)}, bf16[128,512]{1,0:T(8,128)(2,1)S(1)}, u32[]{:S(2)}, u32[]{:S(2)}) collective-permute-start(bf16[128,512]{1,0:T(8,128)(2,1)S(1)} %get-tuple-element.63), channel_id=1, source_target_pairs={{0,1},{1,0},{2,3},{3,2},{4,5},{5,4},{6,7},{7,6},{8,9},{9,8},{10,11... | collective-permute-start | bytes 393224 | tf_op jit(solution)/shard_map/ppermute | solution.py:539
  33.7 1.0 %copy-start.10 = (f32[2048]{0:T(1024)S(1)}, f32[2048]{0:T(1024)}, u32[]{:S(2)}) copy-start(f32[2048]{0:T(1024)} %param.23) | copy-start | bytes 24580
  34.6 30.0 %copy-start.1 = (bf16[1,2048,512]{2,1,0:T(8,128)(2,1)S(1)}, bf16[1,2048,512]{2,1,0:T(8,128)(2,1)}, u32[]{:S(2)}) copy-start(bf16[1,2048,512]{2,1,0:T(8,128)(2,1)} %up.1) | copy-start | bytes 6291460
  34.6 30.0 %copy-start.2 = (bf16[1,512,2048]{2,1,0:T(8,128)(2,1)S(1)}, bf16[1,512,2048]{2,1,0:T(8,128)(2,1)}, u32[]{:S(2)}) copy-start(bf16[1,512,2048]{2,1,0:T(8,128)(2,1)} %down.1) | copy-start | bytes 6291460
  35.8 28.8 %copy-start = (bf16[1,2048,512]{2,1,0:T(8,128)(2,1)S(1)}, bf16[1,2048,512]{2,1,0:T(8,128)(2,1)}, u32[]{:S(2)}) copy-start(bf16[1,2048,512]{2,1,0:T(8,128)(2,1)} %gate.1) | copy-start | bytes 6291460

commit v11 on v10

--- a/solution.py
+++ b/solution.py
@@ -357,17 +357,27 @@
             states = grow(states, n, running_all, keys_ref, values_ref)
 
 
-def finish_kernel(
+def finish_half(core, reach_ref, partial_ref, gating_ref, state_of, result_ref):
+    half = result_ref.shape[0]
+    tokens = pl.ds(pl.multiple_of(core * half, half), half)
+    for p in range(reach_ref.shape[1] // LANES):
+        lanes = slice(p * LANES, (p + 1) * LANES)
+        carried = product(masked_heads(reach_ref[tokens, lanes]), state_of(p), 1, 1)
+        for h in range(2):
+            place = slice((2 * p + h) * VALUE_DIM, (2 * p + h + 1) * VALUE_DIM)
+            attended = partial_ref[tokens, place] + carried[h * half : (h + 1) * half]
+            scale = lax.rsqrt(jnp.mean(attended * attended, axis=1, keepdims=True) + 1e-06)
+            result_ref[:, place] = (attended * scale * gating_ref[tokens, place]).astype(jnp.bfloat16)
+
+
+def given_kernel(
     place_ref, plane_ref, back1_ref, back2_ref, back3_ref, before_y_ref, decay_y_ref, before_x_ref, decay_x_ref,
-    partial_ref, reach_ref, gating_ref, kept_ref, given_ref, whole,
+    partial_ref, reach_ref, gating_ref, given_ref, state_ref,
 ):
-    core, plane = place_ref[0], plane_ref[0]
-    length, channels = reach_ref.shape
-    pairs = channels // LANES
+    plane = plane_ref[0]
     received = [unpack(ref) for ref in (back1_ref, back2_ref, back3_ref)]
-    half = length // 2
-    for p in range(pairs):
-        lanes = slice(p * LANES, (p + 1) * LANES)
+
+    def state_of(p):
         rows = slice(p * VALUE_DIM, (p + 1) * VALUE_DIM)
         state = jnp.zeros((VALUE_DIM, LANES), jnp.float32)
         for k in (3, 2, 1):
@@ -375,16 +385,17 @@
             state = jnp.where(plane >= k, decay * state + grown, state)
         state = before_y_ref[rows] + decay_y_ref[p * 8 : p * 8 + 1] * state
         state = before_x_ref[rows] + decay_x_ref[p * 8 : p * 8 + 1] * state
-        carried = product(masked_heads(reach_ref[:, lanes]), state.astype(jnp.bfloat16), 1, 1)
-        for h in range(2):
-            place = slice((2 * p + h) * VALUE_DIM, (2 * p + h + 1) * VALUE_DIM)
-            attended = partial_ref[:, place] + carried[h * length : (h + 1) * length]
-            scale = lax.rsqrt(jnp.mean(attended * attended, axis=1, keepdims=True) + 1e-06)
-            result = (attended * scale * gating_ref[:, place]).astype(jnp.bfloat16)
-            whole[0, :, place] = result[:half]
-            whole[1, :, place] = result[half:]
-    kept_ref[...] = whole[core]
-    given_ref[...] = whole[1 - core]
+        state_ref[rows] = state.astype(jnp.bfloat16)
+        return state.astype(jnp.bfloat16)
+
+    finish_half(1 - place_ref[0], reach_ref, partial_ref, gating_ref, state_of, given_ref)
+
+
+def kept_kernel(place_ref, state_ref, partial_ref, reach_ref, gating_ref, kept_ref):
+    def state_of(p):
+        return state_ref[p * VALUE_DIM : (p + 1) * VALUE_DIM]
+
+    finish_half(place_ref[0], reach_ref, partial_ref, gating_ref, state_of, kept_ref)
 
 
 def own_kernel(place_ref, kept_ref, weight_ref, residual_ref, partial_ref):
@@ -528,14 +539,14 @@
     )
     partial, reach, gating, *behind = lax.optimization_barrier((partial, reach, gating, *behind))
     half = shape_of((length // 2, values), bf16)
-    kept, given = call(
-        finish_kernel,
-        (half, half),
+    given, entering = call(
+        given_kernel,
+        (half, shape_of((pairs * VALUE_DIM, LANES), bf16)),
         (core, z, *behind, before_y, decay_y, before_x, decay_x, partial, reach, gating),
         2,
-        [pltpu.VMEM((2, length // 2, values), bf16)],
         cost=300000,
     )
+    kept = call(kept_kernel, half, (core, entering, partial, reach, gating), 1, cost=300000)
     taken = lax.ppermute(given, "tp", [(0, 1), (1, 0)])
     projected = call(own_kernel, shape_of((row_count, model_width), f32), (core, kept, out_weight, residual), 1, room=8)
     projected, taken = lax.optimization_barrier((projected, taken))

time: 98.4 us -> 98.7 us (level)
    pallas_call x8 -> x9, Pallas kernels: 6.69 us -> 6.9 us  [call(): pl.pallas_call(kernel, out_shape=outs, in_specs=[SMEM_SPEC] * scalars + [...]
where the time goes in v11:
time: 98.7 us; the launch traced here: 98.5 us
  blocking collectives  57.7 us (58%)
  starting transfers between devices  17.6 us (18%)
  Pallas kernels  11.7 us (12%)
  waiting for transfers between devices  11.3 us (11%)
    all_to_all x1, blocking collectives, local(): lax.all_to_all(served.reshape(block), SP_TP, split_axis=0, concat_axis=0,...  28.9 us
    all_to_all x1, blocking collectives, local(): lax.all_to_all(outgoing.reshape(block), SP_TP, split_axis=0, concat_axis=...  28.8 us
    ppermute x9, starting transfers between devices, from_behind(): lax.ppermute(message, axis, [(i, (i + k) % RING) for i in range(RING)])  12.9 us
    ppermute x9, waiting for transfers between devices, from_behind(): lax.ppermute(message, axis, [(i, (i + k) % RING) for i in range(RING)])  10.8 us
    pallas_call x9, Pallas kernels, call(): pl.pallas_call(kernel, out_shape=outs, in_specs=[SMEM_SPEC] * scalars + [...  6.9 us
    ppermute x1, starting transfers between devices, local(): taken = lax.ppermute(given, 'tp', [(0, 1), (1, 0)])  4.75 us
    pallas_call x1, Pallas kernels, experts(): pl.pallas_call(experts_kernel, out_shape=jax.ShapeDtypeStruct(arrived.sha...  3.05 us
  transfers between devices with their start and end apart: 10, of which 8 were waited for; matrix products, arithmetic and copies ran while one was open for 0% of the time, Pallas kernels for 3%

profile of v11, /device:TPU:1, one launch (start us, length us, event | category | flops | bytes accessed | tf_op | source)
XLA Modules:
  0.0 98.5 jit_solution(15403839784147294215)
XLA Ops:
  0.0 1.8 %shard_map.146.own_ref = bf16[272,128]{1,0:T(8,128)(2,1)S(1)} custom-call(bf16[256,256]{1,0:T(8,128)(2,1)} %keys_ref, bf16[256,512]{1,0:T(8,128)(2,1)} %values_ref.1, bf16[256,256]{1,0:T(8,128)(2,1)} %logits_ref.1), custom_call_target="tpu_custom_call" | custom-call | flops 4000000000 | bytes 10000000 | tf_op jit(solution)/shard_map/pallas_call | solution.py:464
  1.8 3.4 %collective-permute-start.2 = (bf16[272,128]{1,0:T(8,128)(2,1)S(1)}, bf16[272,128]{1,0:T(8,128)(2,1)S(1)}, u32[]{:S(2)}, u32[]{:S(2)}) collective-permute-start(bf16[272,128]{1,0:T(8,128)(2,1)S(1)} %shard_map.146.own_ref), channel_id=1, source_target_pairs={{0,6},{2,0},{4,2},{6,4},{1,7},{3,1},{5,3},{7,5},{8,14},{10,8},{12,... | collective-permute-start | bytes 208904 | tf_op jit(solution)/shard_map/ppermute | solution.py:478
  5.2 0.5 collective-permute-start.1
  5.7 0.6 collective-permute-start
  6.3 0.3 shard_map.145
  6.6 3.3 %collective-permute-done.1.back2_ref = bf16[272,128]{1,0:T(8,128)(2,1)S(1)} collective-permute-done((bf16[272,128]{1,0:T(8,128)(2,1)S(1)}, bf16[272,128]{1,0:T(8,128)(2,1)S(1)}, u32[]{:S(2)}, u32[]{:S(2)}) %collective-permute-start.1) | collective-permute-done | bytes 69664 | tf_op jit(solution)/shard_map/ppermute | solution.py:478
  9.9 1.1 %collective-permute-done.back1_ref = bf16[272,128]{1,0:T(8,128)(2,1)S(1)} collective-permute-done((bf16[272,128]{1,0:T(8,128)(2,1)S(1)}, bf16[272,128]{1,0:T(8,128)(2,1)S(1)}, u32[]{:S(2)}, u32[]{:S(2)}) %collective-permute-start) | collective-permute-done | bytes 69664 | tf_op jit(solution)/shard_map/ppermute | solution.py:478
  11.0 0.1 shard_map.147
  11.1 2.8 %collective-permute-start.5 = (bf16[272,128]{1,0:T(8,128)(2,1)S(1)}, bf16[272,128]{1,0:T(8,128)(2,1)S(1)}, u32[]{:S(2)}, u32[]{:S(2)}) collective-permute-start(bf16[272,128]{1,0:T(8,128)(2,1)S(1)} %get-tuple-element.45.own_ref), channel_id=1, source_target_pairs={{0,24},{8,0},{16,8},{24,16},{1,25},{9,1},{17,9},{25,17},{2,26},{10... | collective-permute-start | bytes 208904 | tf_op jit(solution)/shard_map/ppermute | solution.py:478
  13.9 0.3 collective-permute-start.4
  14.3 0.7 collective-permute-start.3
  14.9 0.3 collective-permute-done.5.back3_ref
  15.3 3.4 %collective-permute-done.4.back2_ref = bf16[272,128]{1,0:T(8,128)(2,1)S(1)} collective-permute-done((bf16[272,128]{1,0:T(8,128)(2,1)S(1)}, bf16[272,128]{1,0:T(8,128)(2,1)S(1)}, u32[]{:S(2)}, u32[]{:S(2)}) %collective-permute-start.4) | collective-permute-done | bytes 69664 | tf_op jit(solution)/shard_map/ppermute | solution.py:478
  18.6 0.7 collective-permute-done.3.back1_ref
  19.3 0.0 copy-start.9
  19.3 0.0 copy-start.14
  19.4 0.1 shard_map.148
  19.5 3.8 %collective-permute-start.8 = (bf16[272,128]{1,0:T(8,128)(2,1)S(1)}, bf16[272,128]{1,0:T(8,128)(2,1)S(1)}, u32[]{:S(2)}, u32[]{:S(2)}) collective-permute-start(bf16[272,128]{1,0:T(8,128)(2,1)S(1)} %get-tuple-element.46), channel_id=1, source_target_pairs={{0,96},{32,0},{64,32},{96,64},{1,97},{33,1},{65,33},{97,65},{2,98}... | collective-permute-start | bytes 208904 | tf_op jit(solution)/shard_map/ppermute | solution.py:478
  23.3 0.7 collective-permute-start.6
  24.1 2.3 %shard_map.149 = (f32[256,512]{1,0:T(8,128)S(1)}, f32[256,256]{1,0:T(8,128)S(1)}, f32[256,512]{1,0:T(8,128)S(1)}) custom-call(bf16[256,256]{1,0:T(8,128)(2,1)S(1)} %copy-done.9, bf16[256,256]{1,0:T(8,128)(2,1)S(1)} %copy-done.7, bf16[256,512]{1,0:T(8,128)(2,1)S(1)} %copy-done.5, bf16[256,256]{1,0:T(8,128)(2,1)S(1)} %copy-done.8, f32[1,128]{1,0:T(1,128)S(1)} %bitcast.21, ...), custom_call_target="tpu_custom_call" | custom-call | flops 4000000000 | bytes 10000000 | tf_op jit(solution)/shard_map/pallas_call | solution.py:464
  26.4 1.7 %collective-permute-done.7.back2_ref = bf16[272,128]{1,0:T(8,128)(2,1)S(1)} collective-permute-done((bf16[272,128]{1,0:T(8,128)(2,1)S(1)}, bf16[272,128]{1,0:T(8,128)(2,1)S(1)}, u32[]{:S(2)}, u32[]{:S(2)}) %collective-permute-start.7) | collective-permute-done | bytes 69664 | tf_op jit(solution)/shard_map/ppermute | solution.py:478
  28.1 0.4 collective-permute-done.6.back1_ref
  28.4 0.4 shard_map.150
  28.8 0.3 shard_map.151.kept_ref
  29.1 4.7 %collective-permute-start.9 = (bf16[128,512]{1,0:T(8,128)(2,1)S(1)}, bf16[128,512]{1,0:T(8,128)(2,1)S(1)}, u32[]{:S(2)}, u32[]{:S(2)}) collective-permute-start(bf16[128,512]{1,0:T(8,128)(2,1)S(1)} %get-tuple-element.63), channel_id=1, source_target_pairs={{0,1},{1,0},{2,3},{3,2},{4,5},{5,4},{6,7},{7,6},{8,9},{9,8},{10,11... | collective-permute-start | bytes 393224 | tf_op jit(solution)/shard_map/ppermute | solution.py:550
  33.9 0.5 shard_map.152.partial_ref
  34.4 0.5 collective-permute-done.9.taken_ref
  34.9 1.1 %shard_map.153 = (bf16[128,2048]{1,0:T(8,128)(2,1)S(1)}, bf16[384,16,128]{2,1,0:T(8,128)(2,1)S(1)}) custom-call(s32[1]{0:T(128)} %bitcast.3.place_ref, s32[8,128]{1,0:T(8,128)S(1)} %get-tuple-element.41.owners_vmem, bf16[128,512]{1,0:T(8,128)(2,1)S(1)} %collective-permute-done.9.taken_ref, bf16[1024,2048]{1,0:T(8,128)(2,1)S(1)} %copy-done.3, ...), custom_call_target="tpu_custom_call" | custom-call | flops 4000000000 | bytes 10000000 | tf_op jit(solution)/shard_map/pallas_call | solution.py:464
  36.0 28.8 %all_to_all.10 = bf16[128,48,128]{2,1,0:T(8,128)(2,1)S(1)} all-to-all(bf16[128,48,128]{2,1,0:T(8,128)(2,1)S(1)} %bitcast.16), channel_id=1, replica_groups=mesh['sp_0'=4,'sp_1'=4,'sp_2'=4,'tp'=2] {'sp_0','sp_1','sp_2','tp'}, dimensions={0} | all-to-all | bytes 3145728 | tf_op jit(solution)/shard_map/all_to_all | solution.py:569
  64.8 3.0 %experts.1 = bf16[384,16,128]{2,1,0:T(8,128)(2,1)S(1)} custom-call(bf16[384,16,128]{2,1,0:T(8,128)(2,1)S(1)} %bitcast.14, bf16[1,2048,512]{2,1,0:T(8,128)(2,1)S(1)} %copy-done, bf16[1,2048,512]{2,1,0:T(8,128)(2,1)S(1)} %copy-done.1, bf16[1,512,2048]{2,1,0:T(8,128)(2,1)S(1)} %copy-done.2), custom_call_target="tpu_custom_call" | custom-call | tf_op jit(solution)/shard_map/experts/pallas_call | solution.py:125
  67.9 28.9 %all_to_all.11 = bf16[128,48,128]{2,1,0:T(8,128)(2,1)S(1)} all-to-all(bf16[128,48,128]{2,1,0:T(8,128)(2,1)S(1)} %bitcast.15), channel_id=1, replica_groups=mesh['sp_0'=4,'sp_1'=4,'sp_2'=4,'tp'=2] {'sp_0','sp_1','sp_2','tp'}, dimensions={0} | all-to-all | bytes 3145728 | tf_op jit(solution)/shard_map/all_to_all | solution.py:571
  96.8 1.7 %combine.1 = bf16[128,2048]{1,0:T(8,128)(2,1)} custom-call(s32[2,128]{1,0:T(2,128)S(1)} %get-tuple-element.40.slots_vmem, bf16[384,16,128]{2,1,0:T(8,128)(2,1)S(1)} %bitcast.13, bf16[128,2048]{1,0:T(8,128)(2,1)S(1)} %get-tuple-element.67.merged_ref, f32[2,128,128]{2,1,0:T(8,128)S(1)} %get-tuple-element.68.weights_ref), custom_call_target="tpu_custom_call" | custom-call | tf_op jit(solution)/shard_map/combine/pallas_call | solution.py:168
  (31 shorter events, 0.1 us)
Async XLA Ops:
  0.0 6.3 %copy-start.12 = (f32[128,2]{0,1:T(2,128)S(1)}, f32[128,2]{0,1:T(2,128)}, u32[]{:S(2)}) copy-start(f32[128,2]{0,1:T(2,128)} %param.26) | copy-start | bytes 3076
  0.0 6.3 %copy-start.13 = (f32[128]{0:T(128)S(1)}, f32[128]{0:T(128)}, u32[]{:S(2)}) copy-start(f32[128]{0:T(128)} %param.25) | copy-start | bytes 1540
  0.0 6.3 %copy-start.11 = (s32[128,2]{0,1:T(2,128)S(1)}, s32[128,2]{0,1:T(2,128)}, u32[]{:S(2)}) copy-start(s32[128,2]{0,1:T(2,128)} %param.24) | copy-start | bytes 3076
  1.8 4.8 %collective-permute-start.2 = (bf16[272,128]{1,0:T(8,128)(2,1)S(1)}, bf16[272,128]{1,0:T(8,128)(2,1)S(1)}, u32[]{:S(2)}, u32[]{:S(2)}) collective-permute-start(bf16[272,128]{1,0:T(8,128)(2,1)S(1)} %shard_map.146.own_ref), channel_id=1, source_target_pairs={{0,6},{2,0},{4,2},{6,4},{1,7},{3,1},{5,3},{7,5},{8,14},{10,8},{12,... | collective-permute-start | bytes 208904 | tf_op jit(solution)/shard_map/ppermute | solution.py:478
  5.2 4.7 %collective-permute-start.1 = (bf16[272,128]{1,0:T(8,128)(2,1)S(1)}, bf16[272,128]{1,0:T(8,128)(2,1)S(1)}, u32[]{:S(2)}, u32[]{:S(2)}) collective-permute-start(bf16[272,128]{1,0:T(8,128)(2,1)S(1)} %shard_map.146.own_ref), channel_id=1, source_target_pairs={{0,4},{2,6},{4,0},{6,2},{1,5},{3,7},{5,1},{7,3},{8,12},{10,14},{12... | collective-permute-start | bytes 208904 | tf_op jit(solution)/shard_map/ppermute | solution.py:478
  5.7 5.3 %collective-permute-start = (bf16[272,128]{1,0:T(8,128)(2,1)S(1)}, bf16[272,128]{1,0:T(8,128)(2,1)S(1)}, u32[]{:S(2)}, u32[]{:S(2)}) collective-permute-start(bf16[272,128]{1,0:T(8,128)(2,1)S(1)} %shard_map.146.own_ref), channel_id=1, source_target_pairs={{0,2},{2,4},{4,6},{6,0},{1,3},{3,5},{5,7},{7,1},{8,10},{10,12},{12... | collective-permute-start | bytes 208904 | tf_op jit(solution)/shard_map/ppermute | solution.py:478
  11.1 4.2 %collective-permute-start.5 = (bf16[272,128]{1,0:T(8,128)(2,1)S(1)}, bf16[272,128]{1,0:T(8,128)(2,1)S(1)}, u32[]{:S(2)}, u32[]{:S(2)}) collective-permute-start(bf16[272,128]{1,0:T(8,128)(2,1)S(1)} %get-tuple-element.45.own_ref), channel_id=1, source_target_pairs={{0,24},{8,0},{16,8},{24,16},{1,25},{9,1},{17,9},{25,17},{2,26},{10... | collective-permute-start | bytes 208904 | tf_op jit(solution)/shard_map/ppermute | solution.py:478
  13.9 4.7 %collective-permute-start.4 = (bf16[272,128]{1,0:T(8,128)(2,1)S(1)}, bf16[272,128]{1,0:T(8,128)(2,1)S(1)}, u32[]{:S(2)}, u32[]{:S(2)}) collective-permute-start(bf16[272,128]{1,0:T(8,128)(2,1)S(1)} %get-tuple-element.45.own_ref), channel_id=1, source_target_pairs={{0,16},{8,24},{16,0},{24,8},{1,17},{9,25},{17,1},{25,9},{2,18},{10... | collective-permute-start | bytes 208904 | tf_op jit(solution)/shard_map/ppermute | solution.py:478
  14.3 5.1 %collective-permute-start.3 = (bf16[272,128]{1,0:T(8,128)(2,1)S(1)}, bf16[272,128]{1,0:T(8,128)(2,1)S(1)}, u32[]{:S(2)}, u32[]{:S(2)}) collective-permute-start(bf16[272,128]{1,0:T(8,128)(2,1)S(1)} %get-tuple-element.45.own_ref), channel_id=1, source_target_pairs={{0,8},{8,16},{16,24},{24,0},{1,9},{9,17},{17,25},{25,1},{2,10},{10... | collective-permute-start | bytes 208904 | tf_op jit(solution)/shard_map/ppermute | solution.py:478
  19.3 4.7 %copy-start.5 = (bf16[256,512]{1,0:T(8,128)(2,1)S(1)}, bf16[256,512]{1,0:T(8,128)(2,1)}, u32[]{:S(2)}) copy-start(bf16[256,512]{1,0:T(8,128)(2,1)} %values_ref.1) | copy-start | bytes 786436
  19.3 4.7 %copy-start.6 = (bf16[256,512]{1,0:T(8,128)(2,1)S(1)}, bf16[256,512]{1,0:T(8,128)(2,1)}, u32[]{:S(2)}) copy-start(bf16[256,512]{1,0:T(8,128)(2,1)} %out_gate_ref.1) | copy-start | bytes 786436
  19.3 4.7 %copy-start.7 = (bf16[256,256]{1,0:T(8,128)(2,1)S(1)}, bf16[256,256]{1,0:T(8,128)(2,1)}, u32[]{:S(2)}) copy-start(bf16[256,256]{1,0:T(8,128)(2,1)} %keys_ref) | copy-start | bytes 393220
  19.3 4.7 %copy-start.8 = (bf16[256,256]{1,0:T(8,128)(2,1)S(1)}, bf16[256,256]{1,0:T(8,128)(2,1)}, u32[]{:S(2)}) copy-start(bf16[256,256]{1,0:T(8,128)(2,1)} %logits_ref.1) | copy-start | bytes 393220
  19.3 4.7 %copy-start.9 = (bf16[256,256]{1,0:T(8,128)(2,1)S(1)}, bf16[256,256]{1,0:T(8,128)(2,1)}, u32[]{:S(2)}) copy-start(bf16[256,256]{1,0:T(8,128)(2,1)} %queries_ref) | copy-start | bytes 393220
  19.3 4.7 %copy-start.14 = (f32[128]{0:T(128)S(1)}, f32[128]{0:T(128)}, u32[]{:S(2)}) copy-start(f32[128]{0:T(128)} %param.21) | copy-start | bytes 1540
  19.5 6.9 %collective-permute-start.8 = (bf16[272,128]{1,0:T(8,128)(2,1)S(1)}, bf16[272,128]{1,0:T(8,128)(2,1)S(1)}, u32[]{:S(2)}, u32[]{:S(2)}) collective-permute-start(bf16[272,128]{1,0:T(8,128)(2,1)S(1)} %get-tuple-element.46), channel_id=1, source_target_pairs={{0,96},{32,0},{64,32},{96,64},{1,97},{33,1},{65,33},{97,65},{2,98}... | collective-permute-start | bytes 208904 | tf_op jit(solution)/shard_map/ppermute | solution.py:478
  23.3 4.8 %collective-permute-start.7 = (bf16[272,128]{1,0:T(8,128)(2,1)S(1)}, bf16[272,128]{1,0:T(8,128)(2,1)S(1)}, u32[]{:S(2)}, u32[]{:S(2)}) collective-permute-start(bf16[272,128]{1,0:T(8,128)(2,1)S(1)} %get-tuple-element.46), channel_id=1, source_target_pairs={{0,64},{32,96},{64,0},{96,32},{1,65},{33,97},{65,1},{97,33},{2,66}... | collective-permute-start | bytes 208904 | tf_op jit(solution)/shard_map/ppermute | solution.py:478
  23.3 5.1 %collective-permute-start.6 = (bf16[272,128]{1,0:T(8,128)(2,1)S(1)}, bf16[272,128]{1,0:T(8,128)(2,1)S(1)}, u32[]{:S(2)}, u32[]{:S(2)}) collective-permute-start(bf16[272,128]{1,0:T(8,128)(2,1)S(1)} %get-tuple-element.46), channel_id=1, source_target_pairs={{0,32},{32,64},{64,96},{96,0},{1,33},{33,65},{65,97},{97,1},{2,34}... | collective-permute-start | bytes 208904 | tf_op jit(solution)/shard_map/ppermute | solution.py:478
  24.1 9.8 %copy-start.3 = (bf16[1024,2048]{1,0:T(8,128)(2,1)S(1)}, bf16[1024,2048]{1,0:T(8,128)(2,1)}, u32[]{:S(2)}) copy-start(bf16[1024,2048]{1,0:T(8,128)(2,1)} %weight_ref.3) | copy-start | bytes 12582916
  26.3 7.5 %copy-start.4 = (bf16[128,2048]{1,0:T(8,128)(2,1)S(1)}, bf16[128,2048]{1,0:T(8,128)(2,1)}, u32[]{:S(2)}) copy-start(bf16[128,2048]{1,0:T(8,128)(2,1)} %residual_ref.1) | copy-start | bytes 1572868
  29.1 5.7 %copy-start.10 = (f32[2048]{0:T(1024)S(1)}, f32[2048]{0:T(1024)}, u32[]{:S(2)}) copy-start(f32[2048]{0:T(1024)} %param.23) | copy-start | bytes 24580
  29.1 5.7 %collective-permute-start.9 = (bf16[128,512]{1,0:T(8,128)(2,1)S(1)}, bf16[128,512]{1,0:T(8,128)(2,1)S(1)}, u32[]{:S(2)}, u32[]{:S(2)}) collective-permute-start(bf16[128,512]{1,0:T(8,128)(2,1)S(1)} %get-tuple-element.63), channel_id=1, source_target_pairs={{0,1},{1,0},{2,3},{3,2},{4,5},{5,4},{6,7},{7,6},{8,9},{9,8},{10,11... | collective-permute-start | bytes 393224 | tf_op jit(solution)/shard_map/ppermute | solution.py:550
  34.9 30.0 %copy-start.1 = (bf16[1,2048,512]{2,1,0:T(8,128)(2,1)S(1)}, bf16[1,2048,512]{2,1,0:T(8,128)(2,1)}, u32[]{:S(2)}) copy-start(bf16[1,2048,512]{2,1,0:T(8,128)(2,1)} %up.1) | copy-start | bytes 6291460
  34.9 30.0 %copy-start.2 = (bf16[1,512,2048]{2,1,0:T(8,128)(2,1)S(1)}, bf16[1,512,2048]{2,1,0:T(8,128)(2,1)}, u32[]{:S(2)}) copy-start(bf16[1,512,2048]{2,1,0:T(8,128)(2,1)} %down.1) | copy-start | bytes 6291460
  36.0 28.8 %copy-start = (bf16[1,2048,512]{2,1,0:T(8,128)(2,1)S(1)}, bf16[1,2048,512]{2,1,0:T(8,128)(2,1)}, u32[]{:S(2)}) copy-start(bf16[1,2048,512]{2,1,0:T(8,128)(2,1)} %gate.1) | copy-start | bytes 6291460
